TPU v7x, 256 devices: a whole 4x4x8 slice. The times are simulated.
256 devices in a mesh: sp: 64 (over z, x, core), tp: 4 (over y).
Axes of the slice: x: 4, y: 4, z: 8, core: 2. Of those that a mesh axis runs over, the one named last changes fastest.
Arguments:
- residual: bfloat16 [16384, 2048], P(('sp', 'tp')), may hold values from -6 to 6
- first_query: bfloat16 [16384, 512], P('sp', 'tp'), may hold values from -6 to 6
- second_query: bfloat16 [16384, 512], P('sp', 'tp'), may hold values from -6 to 6
- first_key: bfloat16 [16384, 512], P('sp', 'tp'), may hold values from -6 to 6
- second_key: bfloat16 [16384, 512], P('sp', 'tp'), may hold values from -6 to 6
- values: bfloat16 [16384, 1024], P('sp', 'tp'), may hold values from -6 to 6
- lambdas: float32 [8], P('tp'), may hold values from 0.3 to 0.8
- head_gain: float32 [128], replicated, may hold values from 0.1 to 1.9
- out_weight: bfloat16 [1024, 2048], P('tp'), may hold values from -0.1875 to 0.1875
- norm_gain: float32 [2048], replicated, may hold values from 0.1 to 1.9
- up_weight: bfloat16 [2048, 4096], P('sp', 'tp'), may hold values from -0.125 to 0.125
- down_weight: bfloat16 [4096, 2048], P('tp', 'sp'), may hold values from -0.09375 to 0.09375
Outputs:
- mixed: bfloat16 [16384, 2048], P(('sp', 'tp'))
All inputs are finite; a program needn't handle non-finite values.
Results may differ from a plain program's by a relative error of at most 0.019.
Values may be sent and summed in bfloat16 or wider, within the bound.
No kernel may reach another device: no remote copies, remote signals or barrier semaphores. Data moves between devices by JAX's collectives and lax.ppermute only.
A program may use at most 128 MiB of HBM per device.

v0:
```python
import jax
import jax.numpy as jnp
from jax import lax
from jax.sharding import PartitionSpec as P


def side_by_side(arrays, axis, dim, along):
    ends, at = ([], 0)
    for a in arrays[:-1]:
        at += a.shape[along]
        ends.append(at)
    both = jnp.concatenate(arrays, axis=along)
    return tuple(jnp.split(lax.all_gather(both, axis, axis=dim, tiled=True), ends, axis=along))


def in_blocks(shard, dim, count):
    before, after = (shard.shape[:dim], shard.shape[dim + 1 :])
    return jnp.moveaxis(shard.reshape(*before, count, -1, *after), dim, 0)


def sent_and_summed(shard, axis, dim):
    parts = in_blocks(shard, dim, lax.axis_size(axis))
    arrived = lax.all_to_all(parts, axis, split_axis=0, concat_axis=0, tiled=True)
    return arrived.astype(jnp.float32).sum(axis=0)


def sent_to_all(shard, axis):
    copies = jnp.broadcast_to(shard, (lax.axis_size(axis), *shard.shape))
    return lax.all_to_all(copies, axis, split_axis=0, concat_axis=0, tiled=True)


def in_order(parts, dim):
    dims = list(parts.shape[1:])
    dims[dim] *= parts.shape[0]
    return jnp.moveaxis(parts, 0, dim).reshape(dims)


def gathered_copies(shard, axis, dim):
    parts = sent_to_all(shard, axis)
    return in_order(parts, dim)


def rotate(blocked, positions):
    half = blocked.shape[-1] // 2
    inverse = 10000.0 ** (-jnp.arange(0, half, dtype=jnp.float32) * 2.0 / blocked.shape[-1])
    angle = positions[:, None] * inverse[None, :]
    cosine = jnp.cos(angle)[:, None, :]
    sine = jnp.sin(angle)[:, None, :]
    first, second = (blocked[..., :half], blocked[..., half:])
    return jnp.concatenate(
        [first * cosine - second * sine, second * cosine + first * sine], axis=-1
    )


def absorb(state, queries, keys, vals, factor):
    top, total, summed = state
    scores = jnp.einsum("qhe,khe->qhk", queries, keys, preferred_element_type=jnp.float32) * factor
    peak = jnp.maximum(top, jnp.max(scores, axis=-1))
    shrink = jnp.exp(top - peak)
    weights = jnp.exp(scores - peak[..., None])
    total = total * shrink + jnp.sum(weights, axis=-1)
    summed = summed * shrink[..., None] + jnp.einsum(
        "qhk,khe->qhe", weights.astype(jnp.bfloat16), vals, preferred_element_type=jnp.float32
    )
    return (peak, total, summed)


def layer_norm(stream, gain):
    center = stream - jnp.mean(stream, axis=-1, keepdims=True)
    spread = jnp.mean(center * center, axis=-1, keepdims=True)
    return center * lax.rsqrt(spread + 1e-05) * gain


def local(
    residual,
    first_query,
    second_query,
    first_key,
    second_key,
    values,
    lambdas,
    head_gain,
    out_weight,
    norm_gain,
    up_weight,
    down_weight,
):
    local_rows = first_query.shape[0]
    head_count = lambdas.shape[0]
    head_width = first_query.shape[1] // head_count
    value_width = values.shape[1] // head_count
    factor = head_width ** (-0.5)
    up_full, down_full = (
        lax.all_gather(up_weight, "sp", axis=0, tiled=True),
        lax.all_gather(down_weight, "sp", axis=1, tiled=True),
    )
    positions = (lax.axis_index("sp") * local_rows + jnp.arange(local_rows)).astype(jnp.float32)

    def prepare(source):
        turned = rotate(
            source.astype(jnp.float32).reshape(local_rows, head_count, head_width), positions
        )
        return turned.astype(jnp.bfloat16)

    query_a, query_b = (prepare(first_query), prepare(second_query))
    key_a = prepare(first_key).reshape(local_rows, head_count * head_width)
    key_b = prepare(second_key).reshape(local_rows, head_count * head_width)
    start_state = (
        jnp.full((local_rows, head_count), -1e30, jnp.float32),
        jnp.zeros((local_rows, head_count), jnp.float32),
        jnp.zeros((local_rows, head_count, value_width), jnp.float32),
    )
    piece_a, piece_b, piece_v = side_by_side((key_a, key_b, values), "sp", 0, 1)
    count = piece_a.shape[0]
    block = 512
    blocks = count // block

    def advance(state, item):
        block_a, block_b, block_v = item
        return (
            (
                absorb(state[0], query_a, block_a, block_v, factor),
                absorb(state[1], query_b, block_b, block_v, factor),
            ),
            None,
        )

    items = (
        piece_a.reshape(blocks, block, head_count, head_width),
        piece_b.reshape(blocks, block, head_count, head_width),
        piece_v.reshape(blocks, block, head_count, value_width),
    )
    state_a, state_b = lax.scan(advance, (start_state, start_state), items)[0]
    diff = state_a[2] / state_a[1][..., None] - lambdas[None, :, None] * (
        state_b[2] / state_b[1][..., None]
    )
    scale = lax.rsqrt(jnp.mean(diff * diff, axis=-1, keepdims=True) + 1e-05)
    flat = (
        (diff * scale * head_gain * 0.8)
        .astype(jnp.bfloat16)
        .reshape(local_rows, head_count * value_width)
    )
    projected = sent_and_summed(
        jnp.dot(flat, out_weight, preferred_element_type=jnp.float32).astype(jnp.bfloat16), "tp", 0
    )
    own_normed = layer_norm(residual.astype(jnp.float32) + projected, norm_gain).astype(
        jnp.bfloat16
    )
    whole = gathered_copies(own_normed, "tp", 0)
    lifted = jnp.dot(whole, up_full, preferred_element_type=jnp.float32)
    hidden = jnp.square(jax.nn.relu(lifted)).astype(jnp.bfloat16)
    lowered = sent_and_summed(
        jnp.dot(hidden, down_full, preferred_element_type=jnp.float32).astype(jnp.bfloat16), "tp", 0
    )
    return (own_normed.astype(jnp.float32) + lowered).astype(jnp.bfloat16)


def solution(mesh):
    in_specs = (
        P(("sp", "tp"), None),
        P("sp", "tp"),
        P("sp", "tp"),
        P("sp", "tp"),
        P("sp", "tp"),
        P("sp", "tp"),
        P("tp"),
        P(),
        P("tp", None),
        P(),
        P("sp", "tp"),
        P("tp", "sp"),
    )
    out_specs = P(("sp", "tp"), None)
    return jax.shard_map(local, mesh=mesh, in_specs=in_specs, out_specs=out_specs, check_vma=False)
```

profile of v0, /device:TPU:2, one launch (start us, length us, event | category | flops | bytes accessed | tf_op | source)
XLA Modules:
  0.0 631.3 jit_solution(8063370554751849443)
XLA Ops:
  14.2 99.5 %all-gather.4.cloned.1.call-done = bf16[16384,512]{1,0:T(8,128)(2,1)} async-done(((bf16[256,512]{1,0:T(8,128)(2,1)}), bf16[16384,512]{1,0:T(8,128)(2,1)}) %all-gather.4.cloned.1.call-update) | async-done | bytes 16777232 | tf_op jit(solution)/shard_map/all_gather | solution.py:13
  113.7 5.8 fusion.31
  119.5 14.7 %reshape.161 = bf16[32,512,2,64]{3,2,1,0:T(2,128)(2,1)} reshape(bf16[16384,128]{1,0:T(8,128)(2,1)} %get-tuple-element.162) | data formatting | bytes 8388608 | tf_op jit(solution)/shard_map/reshape | solution.py:129
  134.2 18.3 %copy.32 = bf16[32,512,2,64]{1,3,2,0:T(8,128)(2,1)} copy(bf16[32,512,2,64]{3,2,1,0:T(2,128)(2,1)} %reshape.161) | data formatting | bytes 8388608
  152.5 14.7 %reshape.163 = bf16[32,512,2,64]{3,2,1,0:T(2,128)(2,1)} reshape(bf16[16384,128]{1,0:T(8,128)(2,1)} %get-tuple-element.161) | data formatting | bytes 8388608 | tf_op jit(solution)/shard_map/reshape | solution.py:130
  167.2 18.4 %copy.34 = bf16[32,512,2,64]{1,3,2,0:T(8,128)(2,1)} copy(bf16[32,512,2,64]{3,2,1,0:T(2,128)(2,1)} %reshape.163) | data formatting | bytes 8388608
  185.6 7.1 %split.13 = bf16[16384,256]{1,0:T(8,128)(2,1)} slice(bf16[16384,512]{1,0:T(8,128)(2,1)} %all-gather.4.cloned.1.call-done), slice={[0:16384], [256:512]} | slice | bytes 16777216 | tf_op jit(solution)/shard_map/split | solution.py:13
  192.7 12.5 %reshape.162 = bf16[32,512,2,128]{3,2,1,0:T(2,128)(2,1)} reshape(bf16[16384,256]{1,0:T(8,128)(2,1)} %split.13) | data formatting | bytes 16777216 | tf_op jit(solution)/shard_map/reshape | solution.py:131
  205.3 354.2 %while.21 = (s32[]{:T(128)}, f32[256,2]{0,1:T(2,128)S(1)}, f32[256,2]{0,1:T(2,128)}, f32[256,2,128]{0,2,1:T(8,128)}, f32[256,2]{0,1:T(2,128)S(1)}, /*index=5*/f3...) while((s32[]{:T(128)}, f32[256,2]{0,1:T(2,128)S(1)}, ...), condition=%wide.region_5.6_spmd.clone, body=%wide.region_0.5_spmd.clone.sunk | while | flops 204870656 | bytes 9372823 | solution.py:133
  222.3 2.0 fusion.68
  233.4 2.0 fusion.68
  244.5 2.0 fusion.68
  246.5 2.0 fusion.67
  255.6 2.0 fusion.68
  257.6 2.0 fusion.67
  266.7 2.0 fusion.68
  277.8 2.0 fusion.68
  279.8 2.0 fusion.67
  288.9 2.0 fusion.68
  300.1 2.0 fusion.68
  311.2 2.0 fusion.68
  322.3 2.0 fusion.68
  333.4 2.0 fusion.68
  344.5 2.0 fusion.68
  355.6 2.0 fusion.68
  366.7 2.0 fusion.68
  377.8 2.0 fusion.68
  388.9 2.0 fusion.68
  400.0 2.0 fusion.68
  411.1 2.0 fusion.68
  422.2 2.0 fusion.68
  433.3 2.0 fusion.68
  444.5 2.0 fusion.68
  455.6 2.0 fusion.68
  466.7 2.0 fusion.68
  477.8 2.0 fusion.68
  488.9 2.0 fusion.68
  500.0 2.0 fusion.68
  511.1 2.0 fusion.68
  522.2 2.0 fusion.68
  533.3 2.0 fusion.68
  544.4 2.0 fusion.68
  555.5 2.0 fusion.68
  561.9 19.7 %all_to_all.15 = bf16[4,64,2048]{2,1,0:T(8,128)(2,1)S(1)} all-to-all(bf16[4,64,2048]{2,1,0:T(8,128)(2,1)S(1)} %bitcast.60), channel_id=1, replica_groups=mesh['sp'=64,'tp'=4] {'tp'}, dimensions={0} | all-to-all | bytes 2097152 | tf_op jit(solution)/shard_map/all_to_all | solution.py:23
  583.5 3.5 all-to-all-start.1
  587.0 14.7 %all-to-all-done.1 = bf16[4,64,2048]{2,1,0:T(8,128)(2,1)S(1)} async-done(((bf16[4,64,2048]{2,1,0:T(8,128)(2,1)}), bf16[4,64,2048]{2,1,0:T(8,128)(2,1)S(1)}, u32[]{:S(2)}, u32[]{:S(2)}) %all-to-all-start.1) | async-done | bytes 1048608 | tf_op jit(solution)/shard_map/all_to_all | solution.py:29
  601.7 5.8 convolution_convert_fusion
  607.5 16.3 %all_to_all.16 = bf16[4,64,2048]{2,1,0:T(8,128)(2,1)S(1)} all-to-all(bf16[4,64,2048]{2,1,0:T(8,128)(2,1)S(1)} %bitcast.62), channel_id=1, replica_groups=mesh['sp'=64,'tp'=4] {'tp'}, dimensions={0} | all-to-all | bytes 2097152 | tf_op jit(solution)/shard_map/all_to_all | solution.py:23
  (428 shorter events, 298.1 us)
Async XLA Ops:
  6.5 554.9 %copy-start = (bf16[256,2048]{1,0:T(8,128)(2,1)S(1)}, bf16[256,2048]{1,0:T(8,128)(2,1)}, u32[]{:S(2)}) copy-start(bf16[256,2048]{1,0:T(8,128)(2,1)} %param.22) | copy-start | bytes 3145732
  6.5 107.1 %all-gather.4.cloned.1.call-start = ((), (), s32[]{:S(2)}) async-start(), calls=%async_computation.3 | async-start | bytes 17039360 | tf_op jit(solution)/shard_map/all_gather | solution.py:13
  12.6 574.4 %all-gather.6.cloned.1.call-start = ((), (), s32[]{:S(2)}) async-start(), calls=%async_computation.4 | async-start | bytes 4259840 | tf_op jit(solution)/shard_map/all_gather | solution.py:94
  13.4 573.6 %all-gather.8.cloned.1.call-start = ((), (), s32[]{:S(2)}) async-start(), calls=%async_computation.5 | async-start | bytes 4259840 | tf_op jit(solution)/shard_map/all_gather | solution.py:95
  559.5 22.3 %copy-start.1 = (bf16[64,2048]{1,0:T(8,128)(2,1)S(1)}, bf16[64,2048]{1,0:T(8,128)(2,1)}, u32[]{:S(2)}) copy-start(bf16[64,2048]{1,0:T(8,128)(2,1)} %param.14) | copy-start | bytes 786436
  559.5 22.7 %copy-start.2 = (f32[2048]{0:T(1024)S(1)}, f32[2048]{0:T(1024)}, u32[]{:S(2)}) copy-start(f32[2048]{0:T(1024)} %param.23) | copy-start | bytes 24580
  583.5 18.2 %all-to-all-start.1 = ((bf16[4,64,2048]{2,1,0:T(8,128)(2,1)}), bf16[4,64,2048]{2,1,0:T(8,128)(2,1)S(1)}, u32[]{:S(2)}, u32[]{:S(2)}) async-start(bf16[4,64,2048]{2,1,0:T(8,128)(2,1)} %broadcast_in_dim.11), calls=%async_computation.1 | async-start | bytes 2097152 | tf_op jit(solution)/shard_map/all_to_all | solution.py:29
Sparse Core Ops, SparseCore 0:
  12.7 100.8 all-gather.3
  116.4 76.0 all-gather.5
  195.3 76.1 all-gather.7
where the time goes:
time: 639 us; the launch traced here: 631 us
  matrix products  214 us (33%)
  local copies, waits for them, and re-layouts  191 us (30%)
  waiting for transfers between devices  116 us (18%)
  other arithmetic  56.9 us (9%)
  blocking collectives  36 us (6%)
  between operations  13.3 us (2%)
    dot_general x64, matrix products, absorb(): jnp.einsum('qhk,khe->qhe', weights.astype(jnp.bfloat16), vals, preferred_...  126 us
    all_gather x1, waiting for transfers between devices, side_by_side(): lax.all_gather(both, axis, axis=dim, tiled=True)  99.5 us
    dynamic_slice x64, local copies, waits for them, and re-layouts, local(): state_a, state_b = lax.scan(advance, (start_state, start_state), items)[0]  94.4 us
    dot_general x64, matrix products, absorb(): jnp.einsum('qhe,khe->qhk', queries, keys, preferred_element_type=jnp.floa...  80.9 us
    add x32, other arithmetic, absorb(): total = total * shrink + jnp.sum(weights, axis=-1)  40.6 us
    unnamed x8, local copies, waits for them, and re-layouts  36.7 us
    all_to_all x2, blocking collectives, sent_and_summed(): lax.all_to_all(parts, axis, split_axis=0, concat_axis=0, tiled=True)  36 us
    reshape x1, local copies, waits for them, and re-layouts, local(): piece_b.reshape(blocks, block, head_count, head_width)  14.7 us
  transfers between devices with their start and end apart: 4, of which 2 were waited for; matrix products, arithmetic and copies ran while one was open for 71% of the time, Pallas kernels for 0%

commit v1 on v0

v1 whole, which is shorter than its diff:
```python
import jax
import jax.numpy as jnp
from jax import lax
from jax.experimental import pallas as pl
from jax.experimental.pallas import tpu as pltpu
from jax.sharding import Mesh, PartitionSpec as P

F32 = jnp.float32
BF16 = jnp.bfloat16
TOK = 256
HEAD = 64
VD = 128
LOG2E = 1.4426950408889634
NT = (((1,), (1,)), ((), ()))
NN = (((1,), (0,)), ((), ()))
ANY = pl.BlockSpec(memory_space=pl.ANY)
SMEM = pl.BlockSpec(memory_space=pltpu.SMEM)
VMEM = pl.BlockSpec(memory_space=pltpu.VMEM)
WIDE = 5 * VD


def prep_kernel(cos_ref, sin_ref, qa_ref, qb_ref, ka_ref, kb_ref, v_ref, q_out, kv_out):
    cos = cos_ref[...]
    sin = sin_ref[...]
    lane = lax.broadcasted_iota(jnp.int32, cos.shape, 1)
    front = (lane % HEAD) < HEAD // 2

    def turn(ref):
        x = ref[...].astype(F32)
        other = jnp.where(front, pltpu.roll(x, 128 - 32, 1), pltpu.roll(x, 32, 1))
        return (x * cos + other * sin).astype(BF16)

    q_out[:, 0:128] = turn(qa_ref)
    q_out[:, 128:256] = turn(qb_ref)
    kv_out[0:TOK, 0:128] = turn(ka_ref)
    kv_out[0:TOK, 128:256] = turn(kb_ref)
    kv_out[TOK : 2 * TOK, :] = v_ref[...].astype(F32).T.astype(BF16)


def prepare(first_query, second_query, first_key, second_key, values, start):
    positions = (start + jnp.arange(TOK)).astype(F32)
    half = HEAD // 2
    inverse = 10000.0 ** (-jnp.arange(0, half, dtype=F32) * 2.0 / HEAD)
    angle = positions[:, None] * inverse[None, :]
    cos, sin = jnp.cos(angle), jnp.sin(angle)
    cos4 = jnp.concatenate([cos] * 4, axis=1)
    sin4 = jnp.concatenate([-sin, sin, -sin, sin], axis=1)
    return pl.pallas_call(
        prep_kernel,
        out_shape=(
            jax.ShapeDtypeStruct((TOK, 2 * VD), BF16),
            jax.ShapeDtypeStruct((2 * TOK, 2 * VD), BF16),
        ),
        in_specs=[VMEM] * 7,
        out_specs=(VMEM, VMEM),
        name="prep",
    )(cos4, sin4, first_query, second_query, first_key, second_key, values)


def three_parts(value):
    hi = value.astype(BF16).astype(F32)
    rest = value - hi
    mid = rest.astype(BF16).astype(F32)
    return hi, mid, rest - mid


GROUP = 4


def attend_kernel(x_ref, lam_ref, q0, q1, q2, q3, kv_ref, out_ref, qs, sc, acc, top, tot, stat):
    lane = lax.broadcasted_iota(jnp.int32, (TOK, 128), 1)
    for o, q in enumerate((q0, q1, q2, q3)):
        for m in range(2):
            scaled = q[:, m * 128 : (m + 1) * 128].astype(F32) * (LOG2E * HEAD**-0.5)
            hi = scaled.astype(BF16).astype(F32)
            lo = scaled - hi
            for h in range(2):
                mine = (lane < HEAD) if h == 0 else (lane >= HEAD)
                qs[o, 2 * h + m, :, 0:128] = jnp.where(mine, hi, 0.0).astype(BF16)
                qs[o, 2 * h + m, :, 128:256] = jnp.where(mine, lo, 0.0).astype(BF16)
    top[...] = jnp.full_like(top, -1e30)
    tot[...] = jnp.zeros_like(tot)
    acc[...] = jnp.zeros_like(acc)

    def scores(slot, group, o, hm):
        m = hm % 2
        keys = kv_ref[pl.ds(group * GROUP, GROUP), 0:TOK, m * 128 : (m + 1) * 128]
        keys = keys.reshape(GROUP * TOK, 128)
        both = jnp.concatenate([keys, keys], axis=1)
        sc[slot] = lax.dot_general(both, qs[o, hm], NT, preferred_element_type=F32)

    groups = kv_ref.shape[0] // GROUP
    scores(0, 0, 0, 0)

    def step(i, carry):
        group, o = i // 4, i % 4
        after = jnp.minimum(i + 1, groups * 4 - 1)
        for hm in range(4):
            if hm < 3:
                scores((hm + 1) % 2, group, o, hm + 1)
            else:
                scores(0, after // 4, after % 4, 0)
            h = hm // 2
            s = sc[hm % 2]
            old = top[o, hm]
            new = jnp.maximum(old, jnp.max(s, axis=0, keepdims=True))
            shrink = jnp.exp2(old - new)
            p = jnp.exp2(s - new)
            top[o, hm] = new
            tot[o, hm] = tot[o, hm] * shrink + jnp.sum(p, axis=0, keepdims=True)
            vals = jnp.concatenate(
                [kv_ref[group * GROUP + g, TOK + h * VD : TOK + (h + 1) * VD, :] for g in range(GROUP)],
                axis=1,
            )
            acc[o, hm] = acc[o, hm] * shrink + lax.dot_general(
                vals, p.astype(BF16), NN, preferred_element_type=F32
            )
        return carry

    lax.fori_loop(0, groups * 4, step, 0)
    stat[...] = jnp.zeros_like(stat)
    for h in range(2):
        for i, part in enumerate(three_parts(jnp.full((1, TOK), lam_ref[h], F32))):
            stat[12 + 3 * h + i : 13 + 3 * h + i, :] = part
    for o in range(4):
        home = (x_ref[0] + 4 - o) % 4
        for hm in range(4):
            total = tot[o, hm]
            out_ref[home, :, hm * VD : (hm + 1) * VD] = (acc[o, hm] / total).T.astype(BF16)
            for i, part in enumerate(three_parts(top[o, hm] + jnp.log2(total))):
                stat[3 * hm + i : 3 * hm + i + 1, :] = part
        out_ref[home, :, 4 * VD :] = stat[...].T.astype(BF16)


def attend(x, lambdas, queries, kv):
    return pl.pallas_call(
        attend_kernel,
        out_shape=jax.ShapeDtypeStruct((4, TOK, WIDE), BF16),
        in_specs=[SMEM, SMEM] + [VMEM] * 5,
        out_specs=VMEM,
        scratch_shapes=[
            pltpu.VMEM((4, 4, TOK, 256), BF16),
            pltpu.VMEM((2, GROUP * TOK, TOK), F32),
            pltpu.VMEM((4, 4, VD, TOK), F32),
            pltpu.VMEM((4, 4, 1, TOK), F32),
            pltpu.VMEM((4, 4, 1, TOK), F32),
            pltpu.VMEM((VD, TOK), F32),
        ],
        compiler_params=pltpu.CompilerParams(vmem_limit_bytes=40 * 2**20),
        name="attend",
    )(x, lambdas, *queries, kv)


def merge_kernel(y_ref, part_ref, gain_ref, res_ref, norm_ref, w0, w1, w2, w3, out_ref, wbuf, sem):
    copies = [
        pltpu.make_async_copy(w, wbuf.at[o], sem.at[o]) for o, w in enumerate((w0, w1, w2, w3))
    ]
    for copy in copies:
        copy.start()
    stream = res_ref[...].astype(F32)
    for o in range(4):
        y = (y_ref[0] + 4 - o) % 4
        parts = [part_ref[4 * k + y] for k in range(4)]
        stats = [p[:, 4 * VD :].astype(F32) for p in parts]
        heads = []
        for h in range(2):
            maps = []
            for m in range(2):
                hm = 2 * h + m
                at = 3 * hm
                lse = [s[:, at : at + 1] + s[:, at + 1 : at + 2] + s[:, at + 2 : at + 3] for s in stats]
                peak = jnp.maximum(jnp.maximum(lse[0], lse[1]), jnp.maximum(lse[2], lse[3]))
                share = [jnp.exp2(e - peak) for e in lse]
                inv = 1.0 / (share[0] + share[1] + share[2] + share[3])
                maps.append(
                    sum(
                        p[:, hm * VD : (hm + 1) * VD].astype(F32) * (w * inv)
                        for p, w in zip(parts, share)
                    )
                )
            at = 12 + 3 * h
            lam = stats[0][:, at : at + 1] + stats[0][:, at + 1 : at + 2] + stats[0][:, at + 2 : at + 3]
            diff = maps[0] - lam * maps[1]
            scale = lax.rsqrt(jnp.mean(diff * diff, axis=-1, keepdims=True) + 1e-05)
            heads.append((diff * scale * gain_ref[...] * 0.8).astype(BF16))
        flat = jnp.concatenate(heads, axis=1)
        copies[o].wait()
        stream = stream + lax.dot_general(flat, wbuf[o], NN, preferred_element_type=F32)
    center = stream - jnp.mean(stream, axis=-1, keepdims=True)
    spread = jnp.mean(center * center, axis=-1, keepdims=True)
    out_ref[...] = (center * lax.rsqrt(spread + 1e-05) * norm_ref[...]).astype(BF16)


def merge(y, part, head_gain, residual, norm_gain, weights):
    rows, width = residual.shape
    return pl.pallas_call(
        merge_kernel,
        out_shape=jax.ShapeDtypeStruct((rows, width), BF16),
        in_specs=[SMEM] + [VMEM] * 4 + [ANY] * 4,
        out_specs=VMEM,
        scratch_shapes=[pltpu.VMEM((4, 2 * VD, width), BF16), pltpu.SemaphoreType.DMA((4,))],
        compiler_params=pltpu.CompilerParams(vmem_limit_bytes=24 * 2**20),
        name="merge",
    )(y, part, head_gain.reshape(1, VD), residual, norm_gain.reshape(1, width), *weights)


def mixer_kernel(n0, n1, n2, n3, w_ref, o0, o1, o2, o3, up, down, sem):
    cuts = 4
    per = up.shape[0] // cuts
    copies = []
    for side, buf in enumerate((up, down)):
        for i in range(cuts):
            at = pl.ds(i * per, per)
            copies.append(pltpu.make_async_copy(w_ref.at[at, side], buf.at[at], sem.at[side * cuts + i]))
            copies[-1].start()
    hidden_width = up.shape[2]
    step = per * up.shape[1]
    x = jnp.concatenate([n[...] for n in (n0, n1, n2, n3)], axis=0)
    lifted = jnp.zeros((x.shape[0], hidden_width), F32)
    for i in range(cuts):
        copies[i].wait()
        block = up[i * per : (i + 1) * per].reshape(step, hidden_width)
        lifted = lifted + lax.dot_general(
            x[:, i * step : (i + 1) * step], block, NN, preferred_element_type=F32
        )
    pos = jnp.maximum(lifted, 0.0)
    hidden = (pos * pos).astype(BF16)
    rows = n0.shape[0]
    for i in range(cuts):
        copies[cuts + i].wait()
        block = down[i * per : (i + 1) * per].reshape(step, hidden_width)
        low = lax.dot_general(hidden, block, NT, preferred_element_type=F32)
        for k, o in enumerate((o0, o1, o2, o3)):
            o[:, i * step : (i + 1) * step] = low[k * rows : (k + 1) * rows].astype(o.dtype)


def mixer(pieces, weights):
    rows, width = pieces[0].shape
    return pl.pallas_call(
        mixer_kernel,
        out_shape=[jax.ShapeDtypeStruct((rows, width), F32 if k == 0 else BF16) for k in range(4)],
        in_specs=[VMEM] * 4 + [ANY],
        out_specs=[VMEM] * 4,
        scratch_shapes=[
            pltpu.VMEM((weights.shape[0],) + weights.shape[2:], BF16),
            pltpu.VMEM((weights.shape[0],) + weights.shape[2:], BF16),
            pltpu.SemaphoreType.DMA((8,)),
        ],
        compiler_params=pltpu.CompilerParams(vmem_limit_bytes=32 * 2**20),
        name="mixer",
    )(*pieces, weights)


def shifted(value, axis, by):
    size = lax.axis_size(axis)
    return lax.ppermute(value, axis, [(i, (i + by) % size) for i in range(size)])


def local(
    residual,
    first_query,
    second_query,
    first_key,
    second_key,
    values,
    lambdas,
    head_gain,
    out_weight,
    norm_gain,
    up_weight,
    down_weight,
):
    sp = lax.axis_index(("z", "x", "c"))
    x = lax.axis_index("x").astype(jnp.int32).reshape(1)
    y = lax.axis_index("tp").astype(jnp.int32).reshape(1)
    query, kv = prepare(first_query, second_query, first_key, second_key, values, sp * TOK)
    kv_all = lax.all_gather(kv, ("z", "c"))
    both = jnp.stack([up_weight, down_weight.T])
    queries = [query] + [shifted(query, "x", o) for o in (1, 2, 3)]
    out_weights = [out_weight] + [shifted(out_weight, "tp", o) for o in (1, 2, 3)]
    mix_weights = lax.all_gather(both, ("z", "x", "c"))
    part = attend(x, lambdas, queries, kv_all)
    part = part.reshape(16, 64, WIDE)
    part = lax.all_to_all(part, ("x", "tp"), split_axis=0, concat_axis=0, tiled=True)
    normed = merge(y, part, head_gain, residual, norm_gain, out_weights)
    pieces = [normed] + [shifted(normed, "tp", o) for o in (1, 2, 3)]
    lows = mixer(pieces, mix_weights)
    total = normed.astype(F32) + lows[0]
    for o in (1, 2, 3):
        total = total + shifted(lows[o], "tp", -o).astype(F32)
    return total.astype(BF16)


def solution(mesh):
    fine = Mesh(mesh.devices.reshape(8, 4, 2, 4), ("z", "x", "c", "tp"))
    sp = ("z", "x", "c")
    in_specs = (
        P(sp + ("tp",), None),
        P(sp, "tp"),
        P(sp, "tp"),
        P(sp, "tp"),
        P(sp, "tp"),
        P(sp, "tp"),
        P("tp"),
        P(),
        P("tp", None),
        P(),
        P(sp, "tp"),
        P("tp", sp),
    )
    out_specs = P(sp + ("tp",), None)
    return jax.shard_map(local, mesh=fine, in_specs=in_specs, out_specs=out_specs, check_vma=False)
```

time: 639 us -> 206 us (0.32); the launches traced: 631 us -> 205 us
  matrix products: 214 us -> 0 us
  local copies, waits for them, and re-layouts: 191 us -> 7.14 us
  other arithmetic: 56.9 us -> 3.92 us
  Pallas kernels: 0 us -> 36.5 us
  blocking collectives: 36 us -> 0 us
  starting transfers between devices: 3.6 us -> 26.2 us
    dot_general x130 -> x0, matrix products: 214 us -> none  [the longest x64 126 us: absorb(): jnp.einsum('qhk,khe->qhe', weights.astype(jnp.bfloat16), vals, preferred_...]
    dynamic_slice x64 -> x0, local copies, waits for them, and re-layouts: 94.4 us -> none  [local(): state_a, state_b = lax.scan(advance, (start_state, start_state), items)[0]]
    ppermute x0 -> x12, waiting for transfers between devices: none -> 84.5 us  [shifted(): lax.ppermute(value, axis, [(i, (i + by) % size) for i in range(size)])]
    all_gather x3 -> x2, waiting for transfers between devices: 99.5 us -> 33.1 us  [the longest x1 33.1 us: local(): kv_all = lax.all_gather(kv, ('z', 'c'))]
    reshape x7 -> x0, local copies, waits for them, and re-layouts: 45.8 us -> none  [the longest x1 14.7 us: local(): piece_b.reshape(blocks, block, head_count, head_width)]
    add x32 -> x0, other arithmetic: 40.6 us -> none  [absorb(): total = total * shrink + jnp.sum(weights, axis=-1)]
    pallas_call x0 -> x4, Pallas kernels: none -> 36.5 us  [the longest x1 27.4 us: attend(): pl.pallas_call(attend_kernel, out_shape=jax.ShapeDtypeStruct((4, TOK, WID...]
    all_to_all x2 -> x0, blocking collectives: 36 us -> none  [sent_and_summed(): lax.all_to_all(parts, axis, split_axis=0, concat_axis=0, tiled=True)]
  transfers between devices with their start and end apart: 4 -> 15, of which waited for: 2 -> 11; matrix products, arithmetic and copies ran while one was open for 71% -> 1% of each run, Pallas kernels for 0% -> 15%
where the time goes in v1:
time: 206 us; the launch traced here: 205 us
  waiting for transfers between devices  118 us (57%)
  Pallas kernels  36.5 us (18%)
  starting transfers between devices  26.2 us (13%)
  between operations  13.5 us (7%)
  local copies, waits for them, and re-layouts  7.14 us (3%)
  other arithmetic  3.92 us (2%)
    ppermute x12, waiting for transfers between devices, shifted(): lax.ppermute(value, axis, [(i, (i + by) % size) for i in range(size)])  84.5 us
    all_gather x1, waiting for transfers between devices, local(): kv_all = lax.all_gather(kv, ('z', 'c'))  33.1 us
    pallas_call x1, Pallas kernels, attend(): pl.pallas_call(attend_kernel, out_shape=jax.ShapeDtypeStruct((4, TOK, WID...  27.4 us
    ppermute x12, starting transfers between devices, shifted(): lax.ppermute(value, axis, [(i, (i + by) % size) for i in range(size)])  18.8 us
    all_to_all x1, starting transfers between devices, local(): lax.all_to_all(part, ('x', 'tp'), split_axis=0, concat_axis=0, tiled=True)  7.28 us
    unnamed x16, local copies, waits for them, and re-layouts  7.14 us
  transfers between devices with their start and end apart: 15, of which 11 were waited for; matrix products, arithmetic and copies ran while one was open for 1% of the time, Pallas kernels for 15%

profile of v1, /device:TPU:2, one launch (start us, length us, event | category | flops | bytes accessed | tf_op | source)
XLA Modules:
  0.0 204.8 jit_solution(18249218367862465205)
XLA Ops:
  6.5 0.0 all-gather.5.cloned.1.call-start
  6.6 0.5 fusion
  7.1 1.0 pad_maximum_fusion
  8.1 2.2 %prep.1 = (bf16[256,256]{1,0:T(8,128)(2,1)}, bf16[512,256]{1,0:T(8,128)(2,1)}) custom-call(f32[256,128]{1,0:T(8,128)} %get-tuple-element.20.cos_ref, f32[256,128]{1,0:T(8,128)} %get-tuple-element.21.sin_ref, bf16[256,128]{1,0:T(8,128)(2,1)} %qa_ref.1, bf16[256,128]{1,0:T(8,128)(2,1)} %qb_ref.1, bf16[256,128]{1,0:T(8,128)(2,1)} %ka_ref.1, ...), custom_call_target="tpu_custom_call" | custom-call | tf_op jit(solution)/shard_map/prep/pallas_call | solution.py:48
  10.2 0.0 all-gather.5.cloned.1.call-update
  10.3 0.0 all-gather.7.cloned.1.call-start
  10.3 1.5 pad_maximum_fusion.2
  11.9 0.0 all-gather.7.cloned.1.call-update
  11.9 1.6 collective-permute-start
  13.4 2.8 %collective-permute-start.1 = (bf16[256,256]{1,0:T(8,128)(2,1)}, bf16[256,256]{1,0:T(8,128)(2,1)S(1)}, u32[]{:S(2)}, u32[]{:S(2)}) collective-permute-start(bf16[256,256]{1,0:T(8,128)(2,1)} %get-tuple-element.11.q0), channel_id=1, source_target_pairs={{0,16},{8,24},{16,0},{24,8},{1,17},{9,25},{17,1},{25,9},{2,18},{10... | collective-permute-start | bytes 393224 | tf_op jit(solution)/shard_map/ppermute | solution.py:256
  16.3 0.4 collective-permute-start.2
  16.7 1.0 collective-permute-done.q1
  17.8 3.8 %collective-permute-done.1.q2 = bf16[256,256]{1,0:T(8,128)(2,1)S(1)} collective-permute-done((bf16[256,256]{1,0:T(8,128)(2,1)}, bf16[256,256]{1,0:T(8,128)(2,1)S(1)}, u32[]{:S(2)}, u32[]{:S(2)}) %collective-permute-start.1) | collective-permute-done | bytes 131104 | tf_op jit(solution)/shard_map/ppermute | solution.py:256
  21.5 0.7 collective-permute-done.2.q3
  22.2 33.1 %all-gather.5.cloned.1.call-done = bf16[8192,256]{1,0:T(8,128)(2,1)} async-done(((bf16[512,256]{1,0:T(8,128)(2,1)}), bf16[8192,256]{1,0:T(8,128)(2,1)}) %all-gather.5.cloned.1.call-update) | async-done | bytes 4194320 | tf_op jit(solution)/shard_map/all_gather | solution.py:277
  55.3 0.0 copy-start.1
  55.3 2.2 %copy-done.1 = bf16[8192,256]{1,0:T(8,128)(2,1)S(1)} copy-done((bf16[8192,256]{1,0:T(8,128)(2,1)S(1)}, bf16[8192,256]{1,0:T(8,128)(2,1)}, u32[]{:S(2)}) %copy-start.1) | copy-done | bytes 4194328
  57.4 0.9 copy-done.4
  58.3 0.7 copy-done.6
  59.0 27.4 %attend.1 = bf16[4,256,640]{2,1,0:T(8,128)(2,1)} custom-call(s32[1]{0:T(128)} %bitcast.1.x_ref, f32[2]{0:T(128)S(1)} %copy-done.6, bf16[256,256]{1,0:T(8,128)(2,1)S(1)} %copy-done.4, bf16[256,256]{1,0:T(8,128)(2,1)S(1)} %collective-permute-done.q1, bf16[256,256]{1,0:T(8,128)(2,1)S(1)} %collective-permute-done.1.q2, ...), custom_call_target="tpu_custom_call" | custom-call | tf_op jit(solution)/shard_map/attend/pallas_call | solution.py:136
  86.4 7.3 %all-to-all-start = ((bf16[16,64,640]{2,1,0:T(8,128)(2,1)}), bf16[16,64,640]{2,1,0:T(8,128)(2,1)S(1)}, u32[]{:S(2)}, u32[]{:S(2)}) async-start(bf16[16,64,640]{2,1,0:T(8,128)(2,1)} %bitcast.3), calls=%async_computation | async-start | bytes 2621440 | tf_op jit(solution)/shard_map/all_to_all | solution.py:284
  93.6 0.0 copy-done.2
  93.7 1.5 collective-permute-start.3
  95.2 2.7 %collective-permute-start.4 = (bf16[256,2048]{1,0:T(8,128)(2,1)S(1)}, bf16[256,2048]{1,0:T(8,128)(2,1)}, u32[]{:S(2)}, u32[]{:S(2)}) collective-permute-start(bf16[256,2048]{1,0:T(8,128)(2,1)S(1)} %copy-done.2), channel_id=1, source_target_pairs={{0,2},{1,3},{2,0},{3,1},{4,6},{5,7},{6,4},{7,5},{8,10},{9,11},{10,... | collective-permute-start | bytes 3145736 | tf_op jit(solution)/shard_map/ppermute | solution.py:256
  97.9 1.5 collective-permute-start.5
  99.3 35.0 %collective-permute-done.3.w1 = bf16[256,2048]{1,0:T(8,128)(2,1)} collective-permute-done((bf16[256,2048]{1,0:T(8,128)(2,1)S(1)}, bf16[256,2048]{1,0:T(8,128)(2,1)}, u32[]{:S(2)}, u32[]{:S(2)}) %collective-permute-start.3) | collective-permute-done | bytes 1048608 | tf_op jit(solution)/shard_map/ppermute | solution.py:256
  134.4 22.1 %collective-permute-done.4.w2 = bf16[256,2048]{1,0:T(8,128)(2,1)} collective-permute-done((bf16[256,2048]{1,0:T(8,128)(2,1)S(1)}, bf16[256,2048]{1,0:T(8,128)(2,1)}, u32[]{:S(2)}, u32[]{:S(2)}) %collective-permute-start.4) | collective-permute-done | bytes 1048608 | tf_op jit(solution)/shard_map/ppermute | solution.py:256
  156.4 0.0 collective-permute-done.5.w3
  156.4 0.0 all-to-all-done.part_ref
  156.4 0.0 copy-done.3
  156.4 0.0 copy-done.5
  156.4 0.0 copy-done.7
  156.5 2.9 %merge.1.n0 = bf16[64,2048]{1,0:T(8,128)(2,1)S(1)} custom-call(s32[1]{0:T(128)} %bitcast.y_ref, bf16[16,64,640]{2,1,0:T(8,128)(2,1)S(1)} %all-to-all-done.part_ref, f32[1,128]{1,0:T(1,128)S(1)} %bitcast.14, bf16[64,2048]{1,0:T(8,128)(2,1)S(1)} %copy-done.3, f32[1,2048]{1,0:T(1,128)S(1)} %bitcast.13, bf16[256,2048]{1,0:T(8,128)(2,1)S(1)} %copy-done.2, ...), custom_call_target="tpu_custom_call" | custom-call | tf_op jit(solution)/shard_map/merge/pallas_call | solution.py:196
  159.4 0.1 collective-permute-start.6
  159.5 2.1 %collective-permute-start.7 = (bf16[64,2048]{1,0:T(8,128)(2,1)S(1)}, bf16[64,2048]{1,0:T(8,128)(2,1)S(1)}, u32[]{:S(2)}, u32[]{:S(2)}) collective-permute-start(bf16[64,2048]{1,0:T(8,128)(2,1)S(1)} %merge.1.n0), channel_id=1, source_target_pairs={{0,2},{1,3},{2,0},{3,1},{4,6},{5,7},{6,4},{7,5},{8,10},{9,11},{10,... | collective-permute-start | bytes 786440 | tf_op jit(solution)/shard_map/ppermute | solution.py:256
  161.6 1.7 collective-permute-start.8
  163.3 10.4 %collective-permute-done.6.n1 = bf16[64,2048]{1,0:T(8,128)(2,1)S(1)} collective-permute-done((bf16[64,2048]{1,0:T(8,128)(2,1)S(1)}, bf16[64,2048]{1,0:T(8,128)(2,1)S(1)}, u32[]{:S(2)}, u32[]{:S(2)}) %collective-permute-start.6) | collective-permute-done | bytes 262176 | tf_op jit(solution)/shard_map/ppermute | solution.py:256
  173.6 0.0 collective-permute-done.7.n2
  173.6 0.6 collective-permute-done.8.n3
  174.3 3.4 %copy-done = bf16[128,32,1024]{2,1,0:T(8,128)(2,1)S(1)} copy-done((bf16[128,32,1024]{2,1,0:T(8,128)(2,1)S(1)}, bf16[128,32,1024]{2,1,0:T(8,128)(2,1)}, u32[]{:S(2)}) %copy-start) | copy-done | bytes 8388632
  177.6 4.0 %mixer.1 = (f32[64,2048]{1,0:T(8,128)S(1)}, bf16[64,2048]{1,0:T(8,128)(2,1)S(1)}, bf16[64,2048]{1,0:T(8,128)(2,1)S(1)}, bf16[64,2048]{1,0:T(8,128)(2,1)S(1)}) custom-call(bf16[64,2048]{1,0:T(8,128)(2,1)S(1)} %merge.1.n0, bf16[64,2048]{1,0:T(8,128)(2,1)S(1)} %collective-permute-done.6.n1, bf16[64,2048]{1,0:T(8,128)(2,1)S(1)} %collective-permute-done.7.n2, ...), custom_call_target="tpu_custom_call" | custom-call | tf_op jit(solution)/shard_map/mixer/pallas_call | solution.py:239
  181.7 1.2 collective-permute-start.10
  182.9 2.3 %collective-permute-start.11 = (bf16[64,2048]{1,0:T(8,128)(2,1)S(1)}, bf16[64,2048]{1,0:T(8,128)(2,1)S(1)}, u32[]{:S(2)}, u32[]{:S(2)}) collective-permute-start(bf16[64,2048]{1,0:T(8,128)(2,1)S(1)} %get-tuple-element.16), channel_id=1, source_target_pairs={{0,1},{1,2},{2,3},{3,0},{4,5},{5,6},{6,7},{7,4},{8,9},{9,10},{10,1... | collective-permute-start | bytes 786440 | tf_op jit(solution)/shard_map/ppermute | solution.py:256
  185.2 0.9 collective-permute-start.9
  186.2 6.3 %collective-permute-done.10 = bf16[64,2048]{1,0:T(8,128)(2,1)S(1)} collective-permute-done((bf16[64,2048]{1,0:T(8,128)(2,1)S(1)}, bf16[64,2048]{1,0:T(8,128)(2,1)S(1)}, u32[]{:S(2)}, u32[]{:S(2)}) %collective-permute-start.10) | collective-permute-done | bytes 262176 | tf_op jit(solution)/shard_map/ppermute | solution.py:256
  192.5 3.5 %collective-permute-done.11 = bf16[64,2048]{1,0:T(8,128)(2,1)S(1)} collective-permute-done((bf16[64,2048]{1,0:T(8,128)(2,1)S(1)}, bf16[64,2048]{1,0:T(8,128)(2,1)S(1)}, u32[]{:S(2)}, u32[]{:S(2)}) %collective-permute-start.11) | collective-permute-done | bytes 262176 | tf_op jit(solution)/shard_map/ppermute | solution.py:256
  196.0 1.1 collective-permute-done.9
  197.1 0.9 add_convert_fusion
  (10 shorter events, 0.0 us)
Async XLA Ops:
  6.5 48.7 %all-gather.5.cloned.1.call-start = ((), (), s32[]{:S(2)}) async-start(), calls=%async_computation.1 | async-start | bytes 4456448 | tf_op jit(solution)/shard_map/all_gather | solution.py:277
  10.3 164.0 %all-gather.7.cloned.1.call-start = ((), (), s32[]{:S(2)}) async-start(), calls=%async_computation.2 | async-start | bytes 8519680 | tf_op jit(solution)/shard_map/all_gather | solution.py:281
  11.9 5.9 %collective-permute-start = (bf16[256,256]{1,0:T(8,128)(2,1)}, bf16[256,256]{1,0:T(8,128)(2,1)S(1)}, u32[]{:S(2)}, u32[]{:S(2)}) collective-permute-start(bf16[256,256]{1,0:T(8,128)(2,1)} %get-tuple-element.11.q0), channel_id=1, source_target_pairs={{0,8},{8,16},{16,24},{24,0},{1,9},{9,17},{17,25},{25,1},{2,10},{10... | collective-permute-start | bytes 393224 | tf_op jit(solution)/shard_map/ppermute | solution.py:256
  13.4 8.1 %collective-permute-start.1 = (bf16[256,256]{1,0:T(8,128)(2,1)}, bf16[256,256]{1,0:T(8,128)(2,1)S(1)}, u32[]{:S(2)}, u32[]{:S(2)}) collective-permute-start(bf16[256,256]{1,0:T(8,128)(2,1)} %get-tuple-element.11.q0), channel_id=1, source_target_pairs={{0,16},{8,24},{16,0},{24,8},{1,17},{9,25},{17,1},{25,9},{2,18},{10... | collective-permute-start | bytes 393224 | tf_op jit(solution)/shard_map/ppermute | solution.py:256
  16.3 5.9 %collective-permute-start.2 = (bf16[256,256]{1,0:T(8,128)(2,1)}, bf16[256,256]{1,0:T(8,128)(2,1)S(1)}, u32[]{:S(2)}, u32[]{:S(2)}) collective-permute-start(bf16[256,256]{1,0:T(8,128)(2,1)} %get-tuple-element.11.q0), channel_id=1, source_target_pairs={{0,24},{8,0},{16,8},{24,16},{1,25},{9,1},{17,9},{25,17},{2,26},{10... | collective-permute-start | bytes 393224 | tf_op jit(solution)/shard_map/ppermute | solution.py:256
  55.3 2.2 %copy-start.1 = (bf16[8192,256]{1,0:T(8,128)(2,1)S(1)}, bf16[8192,256]{1,0:T(8,128)(2,1)}, u32[]{:S(2)}) copy-start(bf16[8192,256]{1,0:T(8,128)(2,1)} %all-gather.5.cloned.1.call-done) | copy-start | bytes 12582916
  57.4 0.9 copy-start.4
  58.3 0.7 copy-start.6
  59.0 34.7 %copy-start.2 = (bf16[256,2048]{1,0:T(8,128)(2,1)S(1)}, bf16[256,2048]{1,0:T(8,128)(2,1)}, u32[]{:S(2)}) copy-start(bf16[256,2048]{1,0:T(8,128)(2,1)} %w0.1) | copy-start | bytes 3145732
  59.0 97.4 %copy-start.3 = (bf16[64,2048]{1,0:T(8,128)(2,1)S(1)}, bf16[64,2048]{1,0:T(8,128)(2,1)}, u32[]{:S(2)}) copy-start(bf16[64,2048]{1,0:T(8,128)(2,1)} %res_ref.1) | copy-start | bytes 786436
  59.0 97.4 %copy-start.5 = (f32[2048]{0:T(1024)S(1)}, f32[2048]{0:T(1024)}, u32[]{:S(2)}) copy-start(f32[2048]{0:T(1024)} %param.21) | copy-start | bytes 24580
  59.0 97.4 %copy-start.7 = (f32[128]{0:T(128)S(1)}, f32[128]{0:T(128)}, u32[]{:S(2)}) copy-start(f32[128]{0:T(128)} %param.19) | copy-start | bytes 1540
  86.4 70.1 %all-to-all-start = ((bf16[16,64,640]{2,1,0:T(8,128)(2,1)}), bf16[16,64,640]{2,1,0:T(8,128)(2,1)S(1)}, u32[]{:S(2)}, u32[]{:S(2)}) async-start(bf16[16,64,640]{2,1,0:T(8,128)(2,1)} %bitcast.3), calls=%async_computation | async-start | bytes 2621440 | tf_op jit(solution)/shard_map/all_to_all | solution.py:284
  93.7 40.7 %collective-permute-start.3 = (bf16[256,2048]{1,0:T(8,128)(2,1)S(1)}, bf16[256,2048]{1,0:T(8,128)(2,1)}, u32[]{:S(2)}, u32[]{:S(2)}) collective-permute-start(bf16[256,2048]{1,0:T(8,128)(2,1)S(1)} %copy-done.2), channel_id=1, source_target_pairs={{0,1},{1,2},{2,3},{3,0},{4,5},{5,6},{6,7},{7,4},{8,9},{9,10},{10,1... | collective-permute-start | bytes 3145736 | tf_op jit(solution)/shard_map/ppermute | solution.py:256
  95.2 61.2 %collective-permute-start.4 = (bf16[256,2048]{1,0:T(8,128)(2,1)S(1)}, bf16[256,2048]{1,0:T(8,128)(2,1)}, u32[]{:S(2)}, u32[]{:S(2)}) collective-permute-start(bf16[256,2048]{1,0:T(8,128)(2,1)S(1)} %copy-done.2), channel_id=1, source_target_pairs={{0,2},{1,3},{2,0},{3,1},{4,6},{5,7},{6,4},{7,5},{8,10},{9,11},{10,... | collective-permute-start | bytes 3145736 | tf_op jit(solution)/shard_map/ppermute | solution.py:256
  97.9 58.6 %collective-permute-start.5 = (bf16[256,2048]{1,0:T(8,128)(2,1)S(1)}, bf16[256,2048]{1,0:T(8,128)(2,1)}, u32[]{:S(2)}, u32[]{:S(2)}) collective-permute-start(bf16[256,2048]{1,0:T(8,128)(2,1)S(1)} %copy-done.2), channel_id=1, source_target_pairs={{0,3},{1,0},{2,1},{3,2},{4,7},{5,4},{6,5},{7,6},{8,11},{9,8},{10,9... | collective-permute-start | bytes 3145736 | tf_op jit(solution)/shard_map/ppermute | solution.py:256
  159.4 14.2 %collective-permute-start.6 = (bf16[64,2048]{1,0:T(8,128)(2,1)S(1)}, bf16[64,2048]{1,0:T(8,128)(2,1)S(1)}, u32[]{:S(2)}, u32[]{:S(2)}) collective-permute-start(bf16[64,2048]{1,0:T(8,128)(2,1)S(1)} %merge.1.n0), channel_id=1, source_target_pairs={{0,1},{1,2},{2,3},{3,0},{4,5},{5,6},{6,7},{7,4},{8,9},{9,10},{10,1... | collective-permute-start | bytes 786440 | tf_op jit(solution)/shard_map/ppermute | solution.py:256
  159.5 14.1 %collective-permute-start.7 = (bf16[64,2048]{1,0:T(8,128)(2,1)S(1)}, bf16[64,2048]{1,0:T(8,128)(2,1)S(1)}, u32[]{:S(2)}, u32[]{:S(2)}) collective-permute-start(bf16[64,2048]{1,0:T(8,128)(2,1)S(1)} %merge.1.n0), channel_id=1, source_target_pairs={{0,2},{1,3},{2,0},{3,1},{4,6},{5,7},{6,4},{7,5},{8,10},{9,11},{10,... | collective-permute-start | bytes 786440 | tf_op jit(solution)/shard_map/ppermute | solution.py:256
  161.6 12.7 %collective-permute-start.8 = (bf16[64,2048]{1,0:T(8,128)(2,1)S(1)}, bf16[64,2048]{1,0:T(8,128)(2,1)S(1)}, u32[]{:S(2)}, u32[]{:S(2)}) collective-permute-start(bf16[64,2048]{1,0:T(8,128)(2,1)S(1)} %merge.1.n0), channel_id=1, source_target_pairs={{0,3},{1,0},{2,1},{3,2},{4,7},{5,4},{6,5},{7,6},{8,11},{9,8},{10,9... | collective-permute-start | bytes 786440 | tf_op jit(solution)/shard_map/ppermute | solution.py:256
  174.3 3.4 %copy-start = (bf16[128,32,1024]{2,1,0:T(8,128)(2,1)S(1)}, bf16[128,32,1024]{2,1,0:T(8,128)(2,1)}, u32[]{:S(2)}) copy-start(bf16[128,32,1024]{2,1,0:T(8,128)(2,1)} %all-gather.7.cloned.1.call-done) | copy-start | bytes 25165828
  181.7 10.8 %collective-permute-start.10 = (bf16[64,2048]{1,0:T(8,128)(2,1)S(1)}, bf16[64,2048]{1,0:T(8,128)(2,1)S(1)}, u32[]{:S(2)}, u32[]{:S(2)}) collective-permute-start(bf16[64,2048]{1,0:T(8,128)(2,1)S(1)} %get-tuple-element.15), channel_id=1, source_target_pairs={{0,2},{1,3},{2,0},{3,1},{4,6},{5,7},{6,4},{7,5},{8,10},{9,11},{10,... | collective-permute-start | bytes 786440 | tf_op jit(solution)/shard_map/ppermute | solution.py:256
  182.9 13.1 %collective-permute-start.11 = (bf16[64,2048]{1,0:T(8,128)(2,1)S(1)}, bf16[64,2048]{1,0:T(8,128)(2,1)S(1)}, u32[]{:S(2)}, u32[]{:S(2)}) collective-permute-start(bf16[64,2048]{1,0:T(8,128)(2,1)S(1)} %get-tuple-element.16), channel_id=1, source_target_pairs={{0,1},{1,2},{2,3},{3,0},{4,5},{5,6},{6,7},{7,4},{8,9},{9,10},{10,1... | collective-permute-start | bytes 786440 | tf_op jit(solution)/shard_map/ppermute | solution.py:256
  185.2 11.8 %collective-permute-start.9 = (bf16[64,2048]{1,0:T(8,128)(2,1)S(1)}, bf16[64,2048]{1,0:T(8,128)(2,1)S(1)}, u32[]{:S(2)}, u32[]{:S(2)}) collective-permute-start(bf16[64,2048]{1,0:T(8,128)(2,1)S(1)} %get-tuple-element.14), channel_id=1, source_target_pairs={{0,3},{1,0},{2,1},{3,2},{4,7},{5,4},{6,5},{7,6},{8,11},{9,8},{10,9... | collective-permute-start | bytes 786440 | tf_op jit(solution)/shard_map/ppermute | solution.py:256
Sparse Core Ops, SparseCore 0:
  10.4 44.8 all-gather.4
  58.0 80.7 all-gather.6

commit v2 on v1

--- a/solution.py
+++ b/solution.py
@@ -4,6 +4,7 @@
 from jax.experimental import pallas as pl
 from jax.experimental.pallas import tpu as pltpu
 from jax.sharding import Mesh, PartitionSpec as P
+
 
 F32 = jnp.float32
 BF16 = jnp.bfloat16
@@ -64,12 +65,9 @@
     return hi, mid, rest - mid
 
 
-GROUP = 4
-
-
-def attend_kernel(x_ref, lam_ref, q0, q1, q2, q3, kv_ref, out_ref, qs, sc, acc, top, tot, stat):
+def load_queries(queries, qs):
     lane = lax.broadcasted_iota(jnp.int32, (TOK, 128), 1)
-    for o, q in enumerate((q0, q1, q2, q3)):
+    for o, q in enumerate(queries):
         for m in range(2):
             scaled = q[:, m * 128 : (m + 1) * 128].astype(F32) * (LOG2E * HEAD**-0.5)
             hi = scaled.astype(BF16).astype(F32)
@@ -78,46 +76,46 @@
                 mine = (lane < HEAD) if h == 0 else (lane >= HEAD)
                 qs[o, 2 * h + m, :, 0:128] = jnp.where(mine, hi, 0.0).astype(BF16)
                 qs[o, 2 * h + m, :, 128:256] = jnp.where(mine, lo, 0.0).astype(BF16)
-    top[...] = jnp.full_like(top, -1e30)
-    tot[...] = jnp.zeros_like(tot)
-    acc[...] = jnp.zeros_like(acc)
-
-    def scores(slot, group, o, hm):
+
+
+def absorb(chunks, qs, sc, acc, top, tot, fresh):
+    def scores(slot, o, hm):
         m = hm % 2
-        keys = kv_ref[pl.ds(group * GROUP, GROUP), 0:TOK, m * 128 : (m + 1) * 128]
-        keys = keys.reshape(GROUP * TOK, 128)
+        keys = jnp.concatenate([c[0:TOK, m * 128 : (m + 1) * 128] for c in chunks], axis=0)
         both = jnp.concatenate([keys, keys], axis=1)
-        sc[slot] = lax.dot_general(both, qs[o, hm], NT, preferred_element_type=F32)
-
-    groups = kv_ref.shape[0] // GROUP
-    scores(0, 0, 0, 0)
-
-    def step(i, carry):
-        group, o = i // 4, i % 4
-        after = jnp.minimum(i + 1, groups * 4 - 1)
+        s = lax.dot_general(both, qs[o, hm], NT, preferred_element_type=F32)
+        sc[slot] = s
+        return jnp.max(s, axis=0, keepdims=True)
+
+    def step(o, peak):
+        after = jnp.minimum(o + 1, 3)
         for hm in range(4):
-            if hm < 3:
-                scores((hm + 1) % 2, group, o, hm + 1)
+            here = peak
+            peak = scores((hm + 1) % 2, o, hm + 1) if hm < 3 else scores(0, after, 0)
+            h = hm // 2
+            if fresh:
+                new = here
             else:
-                scores(0, after // 4, after % 4, 0)
-            h = hm // 2
-            s = sc[hm % 2]
-            old = top[o, hm]
-            new = jnp.maximum(old, jnp.max(s, axis=0, keepdims=True))
-            shrink = jnp.exp2(old - new)
-            p = jnp.exp2(s - new)
+                old = top[o, hm]
+                new = jnp.maximum(old, here)
+                shrink = jnp.exp2(old - new)
+            p = jnp.exp2(sc[hm % 2] - new)
+            vals = jnp.concatenate([c[TOK + h * VD : TOK + (h + 1) * VD, :] for c in chunks], axis=1)
+            moved = lax.dot_general(vals, p.astype(BF16), NN, preferred_element_type=F32)
+            total = jnp.sum(p, axis=0, keepdims=True)
             top[o, hm] = new
-            tot[o, hm] = tot[o, hm] * shrink + jnp.sum(p, axis=0, keepdims=True)
-            vals = jnp.concatenate(
-                [kv_ref[group * GROUP + g, TOK + h * VD : TOK + (h + 1) * VD, :] for g in range(GROUP)],
-                axis=1,
-            )
-            acc[o, hm] = acc[o, hm] * shrink + lax.dot_general(
-                vals, p.astype(BF16), NN, preferred_element_type=F32
-            )
-        return carry
-
-    lax.fori_loop(0, groups * 4, step, 0)
+            if fresh:
+                tot[o, hm] = total
+                acc[o, hm] = moved
+            else:
+                tot[o, hm] = tot[o, hm] * shrink + total
+                acc[o, hm] = acc[o, hm] * shrink + moved
+        return peak
+
+    lax.fori_loop(0, 4, step, scores(0, 0, 0))
+
+
+def finish(x_ref, lam_ref, out_ref, stat, acc, top, tot):
     stat[...] = jnp.zeros_like(stat)
     for h in range(2):
         for i, part in enumerate(three_parts(jnp.full((1, TOK), lam_ref[h], F32))):
@@ -132,23 +130,86 @@
         out_ref[home, :, 4 * VD :] = stat[...].T.astype(BF16)
 
 
-def attend(x, lambdas, queries, kv):
-    return pl.pallas_call(
-        attend_kernel,
+STATE = (
+    jax.ShapeDtypeStruct((4, 4, VD, TOK), F32),
+    jax.ShapeDtypeStruct((4, 4, 1, TOK), F32),
+    jax.ShapeDtypeStruct((4, 4, 1, TOK), F32),
+)
+QS = jax.ShapeDtypeStruct((4, 4, TOK, 2 * VD), BF16)
+
+
+def chunks_of(ref):
+    return [ref] if len(ref.shape) == 2 else [ref.at[i] for i in range(ref.shape[0])]
+
+
+def first_kernel(q0, q1, q2, q3, own_ref, other_ref, qs, acc, top, tot, sc):
+    load_queries((q0, q1, q2, q3), qs)
+    absorb([own_ref, other_ref], qs, sc, acc, top, tot, True)
+
+
+def next_kernel(qs, kv_ref, acc_in, top_in, tot_in, acc, top, tot, sc):
+    absorb(chunks_of(kv_ref), qs, sc, acc, top, tot, False)
+
+
+def last_kernel(x_ref, lam_ref, qs, kv_ref, acc_in, top_in, tot_in, out_ref, acc, top, tot, sc, stat):
+    acc[...] = acc_in[...]
+    top[...] = top_in[...]
+    tot[...] = tot_in[...]
+    absorb(chunks_of(kv_ref), qs, sc, acc, top, tot, False)
+    finish(x_ref, lam_ref, out_ref, stat, acc, top, tot)
+
+
+def cost(keys):
+    return pl.CostEstimate(
+        flops=2 * keys * 4 * TOK * 4 * 3 * HEAD,
+        bytes_accessed=keys * 1024,
+        transcendentals=keys * 4 * TOK * 4,
+    )
+
+
+def score_scratch(chunks):
+    return pltpu.VMEM((2, chunks * TOK, TOK), F32)
+
+
+def attend_first(queries, own, other):
+    return pl.pallas_call(
+        first_kernel,
+        out_shape=(QS,) + STATE,
+        in_specs=[VMEM] * 6,
+        out_specs=(VMEM,) * 4,
+        scratch_shapes=[score_scratch(2)],
+        cost_estimate=cost(512),
+        compiler_params=pltpu.CompilerParams(vmem_limit_bytes=24 * 2**20),
+        name="attend_first",
+    )(*queries, own, other)
+
+
+def attend_next(qs, kv, state):
+    return pl.pallas_call(
+        next_kernel,
+        out_shape=STATE,
+        in_specs=[VMEM] * 5,
+        out_specs=(VMEM,) * 3,
+        input_output_aliases={2: 0, 3: 1, 4: 2},
+        scratch_shapes=[score_scratch(kv.shape[0])],
+        cost_estimate=cost(kv.shape[0] * TOK),
+        compiler_params=pltpu.CompilerParams(vmem_limit_bytes=24 * 2**20),
+        name="attend_next",
+    )(qs, kv, *state)
+
+
+def attend_last(x, lambdas, qs, kv, state):
+    return pl.pallas_call(
+        last_kernel,
         out_shape=jax.ShapeDtypeStruct((4, TOK, WIDE), BF16),
         in_specs=[SMEM, SMEM] + [VMEM] * 5,
         out_specs=VMEM,
-        scratch_shapes=[
-            pltpu.VMEM((4, 4, TOK, 256), BF16),
-            pltpu.VMEM((2, GROUP * TOK, TOK), F32),
-            pltpu.VMEM((4, 4, VD, TOK), F32),
-            pltpu.VMEM((4, 4, 1, TOK), F32),
-            pltpu.VMEM((4, 4, 1, TOK), F32),
-            pltpu.VMEM((VD, TOK), F32),
-        ],
-        compiler_params=pltpu.CompilerParams(vmem_limit_bytes=40 * 2**20),
-        name="attend",
-    )(x, lambdas, *queries, kv)
+        scratch_shapes=[pltpu.VMEM(s.shape, s.dtype) for s in STATE]
+        + [score_scratch(kv.shape[0]), pltpu.VMEM((VD, TOK), F32)],
+        cost_estimate=cost(kv.shape[0] * TOK),
+        compiler_params=pltpu.CompilerParams(vmem_limit_bytes=24 * 2**20),
+        name="attend_last",
+    )(x, lambdas, qs, kv, *state)
 
 
 def merge_kernel(y_ref, part_ref, gain_ref, res_ref, norm_ref, w0, w1, w2, w3, out_ref, wbuf, sem):
@@ -274,12 +335,28 @@
     x = lax.axis_index("x").astype(jnp.int32).reshape(1)
     y = lax.axis_index("tp").astype(jnp.int32).reshape(1)
     query, kv = prepare(first_query, second_query, first_key, second_key, values, sp * TOK)
-    kv_all = lax.all_gather(kv, ("z", "c"))
-    both = jnp.stack([up_weight, down_weight.T])
+    ring = ("z", "c")
+    onward = [(2 * z + c, 2 * ((z + 1 - 2 * c) % 8) + c) for z in range(8) for c in range(2)]
+    crossed = [(2 * z + c, 2 * ((z - 1 + 2 * c) % 8) + 1 - c) for z in range(8) for c in range(2)]
+    near = [lax.ppermute(kv, ring, onward), lax.ppermute(kv, ring, crossed)]
+    other = shifted(kv, "c", 1)
     queries = [query] + [shifted(query, "x", o) for o in (1, 2, 3)]
+    mix_weights = jnp.stack([up_weight, down_weight.T])
+    mix_weights = lax.all_gather(mix_weights, ("z", "x", "c"))
+    near = jnp.stack(near)
+    second = lax.ppermute(near, ring, onward)
+    qs, *state = attend_first(queries, kv, other)
     out_weights = [out_weight] + [shifted(out_weight, "tp", o) for o in (1, 2, 3)]
-    mix_weights = lax.all_gather(both, ("z", "x", "c"))
-    part = attend(x, lambdas, queries, kv_all)
+    third = lax.ppermute(second, ring, onward)
+    four = jnp.concatenate([near, second])
+    four_other = shifted(four, "c", 1)
+    state = attend_next(qs, four, state)
+    far = lax.ppermute(third[0], ring, onward)
+    state = attend_next(qs, four_other, state)
+    three = jnp.concatenate([third, far[None]])
+    three_other = shifted(three, "c", 1)
+    state = attend_next(qs, three, state)
+    part = attend_last(x, lambdas, qs, three_other, state)
     part = part.reshape(16, 64, WIDE)
     part = lax.all_to_all(part, ("x", "tp"), split_axis=0, concat_axis=0, tiled=True)
     normed = merge(y, part, head_gain, residual, norm_gain, out_weights)
@@ -309,4 +386,5 @@
         P("tp", sp),
     )
     out_specs = P(sp + ("tp",), None)
+
     return jax.shard_map(local, mesh=fine, in_specs=in_specs, out_specs=out_specs, check_vma=False)

time: 206 us -> 219 us (1.063)
  waiting for transfers between devices: 118 us -> 129 us
  starting transfers between devices: 26.2 us -> 33 us
  local copies, waits for them, and re-layouts: 7.14 us -> 3.43 us
    ppermute x0 -> x5, waiting for transfers between devices: none -> 38.5 us  [the longest x1 12.2 us: local(): second = lax.ppermute(near, ring, onward)]
    all_gather x2 -> x1, waiting for transfers between devices: 33.1 us -> 0.01 us  [local(): mix_weights = lax.all_gather(mix_weights, ('z', 'x', 'c'))]
    ppermute x0 -> x5, starting transfers between devices: none -> 6.19 us  [the longest x2 6.02 us: local(): near = [lax.ppermute(kv, ring, onward), lax.ppermute(kv, ring, crossed)]]
    ppermute x12 -> x15, waiting for transfers between devices: 84.5 us -> 90 us  [shifted(): lax.ppermute(value, axis, [(i, (i + by) % size) for i in range(size)])]
    unnamed x16, local copies, waits for them, and re-layouts: 7.14 us -> 3.41 us
    pallas_call x1 -> x5, Pallas kernels: 27.4 us -> 26.3 us  [the longest x3 15.4 us: attend_next(): pl.pallas_call(next_kernel, out_shape=STATE, in_specs=[VMEM] * 5, out_spe...]
    ppermute x12 -> x15, starting transfers between devices: 18.8 us -> 18.4 us  [shifted(): lax.ppermute(value, axis, [(i, (i + by) % size) for i in range(size)])]
  transfers between devices with their start and end apart: 15 -> 22, of which waited for: 11 -> 13; matrix products, arithmetic and copies ran while one was open for 1% -> 1% of each run, Pallas kernels for 15% -> 14%
where the time goes in v2:
time: 219 us; the launch traced here: 218 us
  waiting for transfers between devices  129 us (59%)
  Pallas kernels  35.4 us (16%)
  starting transfers between devices  33 us (15%)
  between operations  13.6 us (6%)
  other arithmetic  4.19 us (2%)
  local copies, waits for them, and re-layouts  3.43 us (2%)
    ppermute x15, waiting for transfers between devices, shifted(): lax.ppermute(value, axis, [(i, (i + by) % size) for i in range(size)])  90 us
    ppermute x15, starting transfers between devices, shifted(): lax.ppermute(value, axis, [(i, (i + by) % size) for i in range(size)])  18.4 us
    pallas_call x3, Pallas kernels, attend_next(): pl.pallas_call(next_kernel, out_shape=STATE, in_specs=[VMEM] * 5, out_spe...  15.4 us
    ppermute x1, waiting for transfers between devices, local(): second = lax.ppermute(near, ring, onward)  12.2 us
    ppermute x1, waiting for transfers between devices, local(): third = lax.ppermute(second, ring, onward)  11.7 us
    all_to_all x1, starting transfers between devices, local(): lax.all_to_all(part, ('x', 'tp'), split_axis=0, concat_axis=0, tiled=True)  8.44 us
    ppermute x1, waiting for transfers between devices, local(): far = lax.ppermute(third[0], ring, onward)  7.57 us
    ppermute x2, waiting for transfers between devices, local(): near = [lax.ppermute(kv, ring, onward), lax.ppermute(kv, ring, crossed)]  7.11 us
  transfers between devices with their start and end apart: 22, of which 13 were waited for; matrix products, arithmetic and copies ran while one was open for 1% of the time, Pallas kernels for 14%

profile of v2, /device:TPU:2, one launch (start us, length us, event | category | flops | bytes accessed | tf_op | source)
XLA Modules:
  0.0 218.3 jit_solution(14752388039846464296)
XLA Ops:
  6.5 1.5 pad_maximum_fusion.5
  8.1 0.5 fusion
  8.7 1.0 pad_maximum_fusion.3
  9.7 2.2 prep.1
  11.9 1.9 collective-permute-start.4
  13.8 4.1 %collective-permute-start.5 = (bf16[512,256]{1,0:T(8,128)(2,1)}, bf16[512,256]{1,0:T(8,128)(2,1)S(1)}, u32[]{:S(2)}, u32[]{:S(2)}) collective-permute-start(bf16[512,256]{1,0:T(8,128)(2,1)} %get-tuple-element.25.own_ref), channel_id=1, source_target_pairs={{0,228},{4,32},{32,4},{36,64},{64,36},{68,96},{96,68},{100,128},{1... | collective-permute-start | bytes 786440 | tf_op jit(solution)/shard_map/ppermute | solution.py:341
  17.9 7.1 %collective-permute-done.4 = bf16[512,256]{1,0:T(8,128)(2,1)S(1)} collective-permute-done((bf16[512,256]{1,0:T(8,128)(2,1)}, bf16[512,256]{1,0:T(8,128)(2,1)S(1)}, u32[]{:S(2)}, u32[]{:S(2)}) %collective-permute-start.4) | collective-permute-done | bytes 262176 | tf_op jit(solution)/shard_map/ppermute | solution.py:341
  25.0 0.1 pad_maximum_fusion.2
  25.1 0.1 collective-permute-start.6
  25.2 12.2 %collective-permute-done.6 = bf16[2,512,256]{2,1,0:T(8,128)(2,1)S(1)} collective-permute-done((bf16[2,512,256]{2,1,0:T(8,128)(2,1)S(1)}, bf16[2,512,256]{2,1,0:T(8,128)(2,1)S(1)}, u32[]{:S(2)}, u32[]{:S(2)}) %collective-permute-start.6) | collective-permute-done | bytes 524320 | tf_op jit(solution)/shard_map/ppermute | solution.py:347
  37.4 0.1 pad_maximum_fusion.kv_ref
  37.5 0.1 collective-permute-start.10
  37.6 11.7 %collective-permute-done.7 = bf16[2,512,256]{2,1,0:T(8,128)(2,1)S(1)} collective-permute-done((bf16[2,512,256]{2,1,0:T(8,128)(2,1)S(1)}, bf16[2,512,256]{2,1,0:T(8,128)(2,1)S(1)}, u32[]{:S(2)}, u32[]{:S(2)}) %collective-permute-start.7) | collective-permute-done | bytes 524320 | tf_op jit(solution)/shard_map/ppermute | solution.py:350
  49.3 0.1 collective-permute-start.8
  49.3 7.6 %collective-permute-done.8 = bf16[512,256]{1,0:T(8,128)(2,1)S(1)} collective-permute-done((bf16[512,256]{1,0:T(8,128)(2,1)S(1)}, bf16[512,256]{1,0:T(8,128)(2,1)S(1)}, u32[]{:S(2)}, u32[]{:S(2)}) %collective-permute-start.8) | collective-permute-done | bytes 262176 | tf_op jit(solution)/shard_map/ppermute | solution.py:354
  56.9 0.1 pad_maximum_fusion.1.kv_ref
  57.0 0.1 collective-permute-start.9
  57.1 1.6 collective-permute-start
  58.7 0.1 collective-permute-start.3
  58.8 1.3 collective-permute-start.1
  60.1 2.9 %collective-permute-done.q1 = bf16[256,256]{1,0:T(8,128)(2,1)S(1)} collective-permute-done((bf16[256,256]{1,0:T(8,128)(2,1)S(1)}, bf16[256,256]{1,0:T(8,128)(2,1)S(1)}, u32[]{:S(2)}, u32[]{:S(2)}) %collective-permute-start) | collective-permute-done | bytes 131104 | tf_op jit(solution)/shard_map/ppermute | solution.py:317
  63.0 1.9 collective-permute-start.2
  64.9 3.0 %collective-permute-done.1.q2 = bf16[256,256]{1,0:T(8,128)(2,1)S(1)} collective-permute-done((bf16[256,256]{1,0:T(8,128)(2,1)S(1)}, bf16[256,256]{1,0:T(8,128)(2,1)S(1)}, u32[]{:S(2)}, u32[]{:S(2)}) %collective-permute-start.1) | collective-permute-done | bytes 131104 | tf_op jit(solution)/shard_map/ppermute | solution.py:317
  67.9 4.3 %collective-permute-done.2.q3 = bf16[256,256]{1,0:T(8,128)(2,1)S(1)} collective-permute-done((bf16[256,256]{1,0:T(8,128)(2,1)S(1)}, bf16[256,256]{1,0:T(8,128)(2,1)S(1)}, u32[]{:S(2)}, u32[]{:S(2)}) %collective-permute-start.2) | collective-permute-done | bytes 131104 | tf_op jit(solution)/shard_map/ppermute | solution.py:317
  72.3 4.1 %attend_first.1 = (bf16[4,4,256,256]{3,2,1,0:T(8,128)(2,1)S(1)}, f32[4,4,128,256]{3,2,1,0:T(8,128)S(1)}, f32[4,4,1,256]{3,2,1,0:T(1,128)S(1)}, f32[4,4,1,256]{3,2,1,0:T(1,128)S(1)}) custom-call(bf16[256,256]{1,0:T(8,128)(2,1)S(1)} %copy-done.7, bf16[256,256]{1,0:T(8,128)(2,1)S(1)} %collective-permute-done.q1, ...), custom_call_target="tpu_custom_call" | custom-call | flops 805306368 | bytes 524288 | tf_op jit(solution)/shard_map/attend_first/pallas_call | solution.py:175
  76.3 5.4 %attend_next.3 = (f32[4,4,128,256]{3,2,1,0:T(8,128)S(1)}, f32[4,4,1,256]{3,2,1,0:T(1,128)S(1)}, f32[4,4,1,256]{3,2,1,0:T(1,128)S(1)}) custom-call(bf16[4,4,256,256]{3,2,1,0:T(8,128)(2,1)S(1)} %get-tuple-element.26.qs, bf16[4,512,256]{2,1,0:T(8,128)(2,1)S(1)} %pad_maximum_fusion.kv_ref, ...), custom_call_target="tpu_custom_call", output_to_operand_aliasing={{0}: (2, {}), {1}: (3, {}), {2}: (4, {})} | custom-call | flops 1610612736 | bytes 1048576 | tf_op jit(solution)/shard_map/attend_next/pallas_call | solution.py:188
  81.8 5.4 %attend_next.4 = (f32[4,4,128,256]{3,2,1,0:T(8,128)S(1)}, f32[4,4,1,256]{3,2,1,0:T(1,128)S(1)}, f32[4,4,1,256]{3,2,1,0:T(1,128)S(1)}) custom-call(bf16[4,4,256,256]{3,2,1,0:T(8,128)(2,1)S(1)} %get-tuple-element.26.qs, bf16[4,512,256]{2,1,0:T(8,128)(2,1)S(1)} %collective-permute-done.10.kv_ref, ...), custom_call_target="tpu_custom_call", output_to_operand_aliasing={{0}: (2, {}), {1}: (3, {}), {2}: (4, {})} | custom-call | flops 1610612736 | bytes 1048576 | tf_op jit(solution)/shard_map/attend_next/pallas_call | solution.py:188
  87.2 4.5 %attend_next.5 = (f32[4,4,128,256]{3,2,1,0:T(8,128)S(1)}, f32[4,4,1,256]{3,2,1,0:T(1,128)S(1)}, f32[4,4,1,256]{3,2,1,0:T(1,128)S(1)}) custom-call(bf16[4,4,256,256]{3,2,1,0:T(8,128)(2,1)S(1)} %get-tuple-element.26.qs, bf16[3,512,256]{2,1,0:T(8,128)(2,1)S(1)} %pad_maximum_fusion.1.kv_ref, ...), custom_call_target="tpu_custom_call", output_to_operand_aliasing={{0}: (2, {}), {1}: (3, {}), {2}: (4, {})} | custom-call | flops 1207959552 | bytes 786432 | tf_op jit(solution)/shard_map/attend_next/pallas_call | solution.py:188
  91.8 6.8 %attend_last.1 = bf16[4,256,640]{2,1,0:T(8,128)(2,1)} custom-call(s32[1]{0:T(128)} %bitcast.1.x_ref, f32[2]{0:T(128)S(1)} %copy-done.5, bf16[4,4,256,256]{3,2,1,0:T(8,128)(2,1)S(1)} %get-tuple-element.26.qs, bf16[3,512,256]{2,1,0:T(8,128)(2,1)S(1)} %collective-permute-done.9.kv_ref, f32[4,4,128,256]{3,2,1,0:T(8,128)S(1)} %get-tuple-element.36.acc_in, ...), custom_call_target="tpu_custom_call" | custom-call | flops 1207959552 | bytes 786432 | tf_op jit(solution)/shard_map/attend_last/pallas_call | solution.py:202
  98.6 8.4 %all-to-all-start = ((bf16[16,64,640]{2,1,0:T(8,128)(2,1)}), bf16[16,64,640]{2,1,0:T(8,128)(2,1)S(1)}, u32[]{:S(2)}, u32[]{:S(2)}) async-start(bf16[16,64,640]{2,1,0:T(8,128)(2,1)} %bitcast.6), calls=%async_computation | async-start | bytes 2621440 | tf_op jit(solution)/shard_map/all_to_all | solution.py:361
  107.0 1.5 collective-permute-start.11
  108.6 2.7 %collective-permute-start.12 = (bf16[256,2048]{1,0:T(8,128)(2,1)S(1)}, bf16[256,2048]{1,0:T(8,128)(2,1)}, u32[]{:S(2)}, u32[]{:S(2)}) collective-permute-start(bf16[256,2048]{1,0:T(8,128)(2,1)S(1)} %copy-done.1), channel_id=1, source_target_pairs={{0,2},{1,3},{2,0},{3,1},{4,6},{5,7},{6,4},{7,5},{8,10},{9,11},{10,... | collective-permute-start | bytes 3145736 | tf_op jit(solution)/shard_map/ppermute | solution.py:317
  111.3 1.5 collective-permute-start.13
  112.7 33.5 %collective-permute-done.11.w1 = bf16[256,2048]{1,0:T(8,128)(2,1)} collective-permute-done((bf16[256,2048]{1,0:T(8,128)(2,1)S(1)}, bf16[256,2048]{1,0:T(8,128)(2,1)}, u32[]{:S(2)}, u32[]{:S(2)}) %collective-permute-start.11) | collective-permute-done | bytes 1048608 | tf_op jit(solution)/shard_map/ppermute | solution.py:317
  146.2 21.8 %collective-permute-done.12.w2 = bf16[256,2048]{1,0:T(8,128)(2,1)} collective-permute-done((bf16[256,2048]{1,0:T(8,128)(2,1)S(1)}, bf16[256,2048]{1,0:T(8,128)(2,1)}, u32[]{:S(2)}, u32[]{:S(2)}) %collective-permute-start.12) | collective-permute-done | bytes 1048608 | tf_op jit(solution)/shard_map/ppermute | solution.py:317
  168.1 3.0 %merge.1.n0 = bf16[64,2048]{1,0:T(8,128)(2,1)S(1)} custom-call(s32[1]{0:T(128)} %bitcast.y_ref, bf16[16,64,640]{2,1,0:T(8,128)(2,1)S(1)} %all-to-all-done.part_ref, f32[1,128]{1,0:T(1,128)S(1)} %bitcast.17, bf16[64,2048]{1,0:T(8,128)(2,1)S(1)} %copy-done.2, f32[1,2048]{1,0:T(1,128)S(1)} %bitcast.16, bf16[256,2048]{1,0:T(8,128)(2,1)S(1)} %copy-done.1, ...), custom_call_target="tpu_custom_call" | custom-call | tf_op jit(solution)/shard_map/merge/pallas_call | solution.py:257
  171.0 0.1 collective-permute-start.14
  171.1 2.6 %collective-permute-start.15 = (bf16[64,2048]{1,0:T(8,128)(2,1)S(1)}, bf16[64,2048]{1,0:T(8,128)(2,1)S(1)}, u32[]{:S(2)}, u32[]{:S(2)}) collective-permute-start(bf16[64,2048]{1,0:T(8,128)(2,1)S(1)} %merge.1.n0), channel_id=1, source_target_pairs={{0,2},{1,3},{2,0},{3,1},{4,6},{5,7},{6,4},{7,5},{8,10},{9,11},{10,... | collective-permute-start | bytes 786440 | tf_op jit(solution)/shard_map/ppermute | solution.py:317
  173.7 1.2 collective-permute-start.16
  174.9 10.1 %collective-permute-done.14.n1 = bf16[64,2048]{1,0:T(8,128)(2,1)S(1)} collective-permute-done((bf16[64,2048]{1,0:T(8,128)(2,1)S(1)}, bf16[64,2048]{1,0:T(8,128)(2,1)S(1)}, u32[]{:S(2)}, u32[]{:S(2)}) %collective-permute-start.14) | collective-permute-done | bytes 262176 | tf_op jit(solution)/shard_map/ppermute | solution.py:317
  185.1 0.6 collective-permute-done.16.n3
  185.7 3.4 %copy-done = bf16[128,32,1024]{2,1,0:T(8,128)(2,1)S(1)} copy-done((bf16[128,32,1024]{2,1,0:T(8,128)(2,1)S(1)}, bf16[128,32,1024]{2,1,0:T(8,128)(2,1)}, u32[]{:S(2)}) %copy-start) | copy-done | bytes 8388632
  189.1 4.0 %mixer.1 = (f32[64,2048]{1,0:T(8,128)S(1)}, bf16[64,2048]{1,0:T(8,128)(2,1)S(1)}, bf16[64,2048]{1,0:T(8,128)(2,1)S(1)}, bf16[64,2048]{1,0:T(8,128)(2,1)S(1)}) custom-call(bf16[64,2048]{1,0:T(8,128)(2,1)S(1)} %merge.1.n0, bf16[64,2048]{1,0:T(8,128)(2,1)S(1)} %collective-permute-done.14.n1, bf16[64,2048]{1,0:T(8,128)(2,1)S(1)} %collective-permute-done.15.n2, ...), custom_call_target="tpu_custom_call" | custom-call | tf_op jit(solution)/shard_map/mixer/pallas_call | solution.py:300
  193.1 2.7 %collective-permute-start.17 = (bf16[64,2048]{1,0:T(8,128)(2,1)S(1)}, bf16[64,2048]{1,0:T(8,128)(2,1)S(1)}, u32[]{:S(2)}, u32[]{:S(2)}) collective-permute-start(bf16[64,2048]{1,0:T(8,128)(2,1)S(1)} %get-tuple-element.40), channel_id=1, source_target_pairs={{0,3},{1,0},{2,1},{3,2},{4,7},{5,4},{6,5},{7,6},{8,11},{9,8},{10,9... | collective-permute-start | bytes 786440 | tf_op jit(solution)/shard_map/ppermute | solution.py:317
  195.8 1.0 collective-permute-start.19
  196.7 10.4 %collective-permute-done.17 = bf16[64,2048]{1,0:T(8,128)(2,1)S(1)} collective-permute-done((bf16[64,2048]{1,0:T(8,128)(2,1)S(1)}, bf16[64,2048]{1,0:T(8,128)(2,1)S(1)}, u32[]{:S(2)}, u32[]{:S(2)}) %collective-permute-start.17) | collective-permute-done | bytes 262176 | tf_op jit(solution)/shard_map/ppermute | solution.py:317
  207.2 3.4 %collective-permute-done.19 = bf16[64,2048]{1,0:T(8,128)(2,1)S(1)} collective-permute-done((bf16[64,2048]{1,0:T(8,128)(2,1)S(1)}, bf16[64,2048]{1,0:T(8,128)(2,1)S(1)}, u32[]{:S(2)}, u32[]{:S(2)}) %collective-permute-start.19) | collective-permute-done | bytes 262176 | tf_op jit(solution)/shard_map/ppermute | solution.py:317
  210.6 0.9 add_convert_fusion
  (31 shorter events, 0.1 us)
Async XLA Ops:
  6.5 179.1 %all-gather.3.cloned.1.call-start = ((), (), s32[]{:S(2)}) async-start(), calls=%async_computation.1 | async-start | bytes 8519680 | tf_op jit(solution)/shard_map/all_gather | solution.py:345
  11.9 13.1 %collective-permute-start.4 = (bf16[512,256]{1,0:T(8,128)(2,1)}, bf16[512,256]{1,0:T(8,128)(2,1)S(1)}, u32[]{:S(2)}, u32[]{:S(2)}) collective-permute-start(bf16[512,256]{1,0:T(8,128)(2,1)} %get-tuple-element.25.own_ref), channel_id=1, source_target_pairs={{0,32},{4,228},{32,64},{36,4},{64,96},{68,36},{96,128},{100,68},{1... | collective-permute-start | bytes 786440 | tf_op jit(solution)/shard_map/ppermute | solution.py:341
  13.8 11.2 %collective-permute-start.5 = (bf16[512,256]{1,0:T(8,128)(2,1)}, bf16[512,256]{1,0:T(8,128)(2,1)S(1)}, u32[]{:S(2)}, u32[]{:S(2)}) collective-permute-start(bf16[512,256]{1,0:T(8,128)(2,1)} %get-tuple-element.25.own_ref), channel_id=1, source_target_pairs={{0,228},{4,32},{32,4},{36,64},{64,36},{68,96},{96,68},{100,128},{1... | collective-permute-start | bytes 786440 | tf_op jit(solution)/shard_map/ppermute | solution.py:341
  25.0 32.1 %copy-start.7 = (bf16[256,256]{1,0:T(8,128)(2,1)S(1)}, bf16[256,256]{1,0:T(8,128)(2,1)}, u32[]{:S(2)}) copy-start(bf16[256,256]{1,0:T(8,128)(2,1)} %get-tuple-element.24.q0) | copy-start | bytes 393220
  25.0 33.6 %copy-start.6 = (bf16[512,256]{1,0:T(8,128)(2,1)S(1)}, bf16[512,256]{1,0:T(8,128)(2,1)}, u32[]{:S(2)}) copy-start(bf16[512,256]{1,0:T(8,128)(2,1)} %get-tuple-element.25.own_ref) | copy-start | bytes 786436
  25.1 12.3 %collective-permute-start.6 = (bf16[2,512,256]{2,1,0:T(8,128)(2,1)S(1)}, bf16[2,512,256]{2,1,0:T(8,128)(2,1)S(1)}, u32[]{:S(2)}, u32[]{:S(2)}) collective-permute-start(bf16[2,512,256]{2,1,0:T(8,128)(2,1)S(1)} %pad_maximum_fusion.2), channel_id=1, source_target_pairs={{0,32},{4,228},{32,64},{36,4},{64,96},{68,36},{96,128},{100,68},{1... | collective-permute-start | bytes 1572872 | tf_op jit(solution)/shard_map/ppermute | solution.py:347
  37.3 11.9 %collective-permute-start.7 = (bf16[2,512,256]{2,1,0:T(8,128)(2,1)S(1)}, bf16[2,512,256]{2,1,0:T(8,128)(2,1)S(1)}, u32[]{:S(2)}, u32[]{:S(2)}) collective-permute-start(bf16[2,512,256]{2,1,0:T(8,128)(2,1)S(1)} %collective-permute-done.6), channel_id=1, source_target_pairs={{0,32},{4,228},{32,64},{36,4},{64,96},{68,36},{96,128},{100,68},{1... | collective-permute-start | bytes 1572872 | tf_op jit(solution)/shard_map/ppermute | solution.py:350
  37.5 44.3 %collective-permute-start.10 = (bf16[4,512,256]{2,1,0:T(8,128)(2,1)S(1)}, bf16[4,512,256]{2,1,0:T(8,128)(2,1)S(1)}, u32[]{:S(2)}, u32[]{:S(2)}) collective-permute-start(bf16[4,512,256]{2,1,0:T(8,128)(2,1)S(1)} %pad_maximum_fusion.kv_ref), channel_id=1, source_target_pairs={{0,4},{4,0},{1,5},{5,1},{2,6},{6,2},{3,7},{7,3},{8,12},{12,8},{9,1... | collective-permute-start | bytes 3145736 | tf_op jit(solution)/shard_map/ppermute | solution.py:317
  49.3 7.7 %collective-permute-start.8 = (bf16[512,256]{1,0:T(8,128)(2,1)S(1)}, bf16[512,256]{1,0:T(8,128)(2,1)S(1)}, u32[]{:S(2)}, u32[]{:S(2)}) collective-permute-start(bf16[512,256]{1,0:T(8,128)(2,1)S(1)} %slice_bitcast_fusion), channel_id=1, source_target_pairs={{0,32},{4,228},{32,64},{36,4},{64,96},{68,36},{96,128},{100,68},{1... | collective-permute-start | bytes 786440 | tf_op jit(solution)/shard_map/ppermute | solution.py:354
  57.0 34.8 %collective-permute-start.9 = (bf16[3,512,256]{2,1,0:T(8,128)(2,1)S(1)}, bf16[3,512,256]{2,1,0:T(8,128)(2,1)S(1)}, u32[]{:S(2)}, u32[]{:S(2)}) collective-permute-start(bf16[3,512,256]{2,1,0:T(8,128)(2,1)S(1)} %pad_maximum_fusion.1.kv_ref), channel_id=1, source_target_pairs={{0,4},{4,0},{1,5},{5,1},{2,6},{6,2},{3,7},{7,3},{8,12},{12,8},{9,1... | collective-permute-start | bytes 2359304 | tf_op jit(solution)/shard_map/ppermute | solution.py:317
  57.1 5.9 %collective-permute-start = (bf16[256,256]{1,0:T(8,128)(2,1)S(1)}, bf16[256,256]{1,0:T(8,128)(2,1)S(1)}, u32[]{:S(2)}, u32[]{:S(2)}) collective-permute-start(bf16[256,256]{1,0:T(8,128)(2,1)S(1)} %copy-done.7), channel_id=1, source_target_pairs={{0,8},{8,16},{16,24},{24,0},{1,9},{9,17},{17,25},{25,1},{2,10},{10... | collective-permute-start | bytes 393224 | tf_op jit(solution)/shard_map/ppermute | solution.py:317
  58.7 13.6 %collective-permute-start.3 = (bf16[512,256]{1,0:T(8,128)(2,1)S(1)}, bf16[512,256]{1,0:T(8,128)(2,1)S(1)}, u32[]{:S(2)}, u32[]{:S(2)}) collective-permute-start(bf16[512,256]{1,0:T(8,128)(2,1)S(1)} %copy-done.6), channel_id=1, source_target_pairs={{0,4},{4,0},{1,5},{5,1},{2,6},{6,2},{3,7},{7,3},{8,12},{12,8},{9,1... | collective-permute-start | bytes 786440 | tf_op jit(solution)/shard_map/ppermute | solution.py:317
  58.8 9.1 %collective-permute-start.1 = (bf16[256,256]{1,0:T(8,128)(2,1)S(1)}, bf16[256,256]{1,0:T(8,128)(2,1)S(1)}, u32[]{:S(2)}, u32[]{:S(2)}) collective-permute-start(bf16[256,256]{1,0:T(8,128)(2,1)S(1)} %copy-done.7), channel_id=1, source_target_pairs={{0,16},{8,24},{16,0},{24,8},{1,17},{9,25},{17,1},{25,9},{2,18},{10... | collective-permute-start | bytes 393224 | tf_op jit(solution)/shard_map/ppermute | solution.py:317
  63.0 9.3 %collective-permute-start.2 = (bf16[256,256]{1,0:T(8,128)(2,1)S(1)}, bf16[256,256]{1,0:T(8,128)(2,1)S(1)}, u32[]{:S(2)}, u32[]{:S(2)}) collective-permute-start(bf16[256,256]{1,0:T(8,128)(2,1)S(1)} %copy-done.7), channel_id=1, source_target_pairs={{0,24},{8,0},{16,8},{24,16},{1,25},{9,1},{17,9},{25,17},{2,26},{10... | collective-permute-start | bytes 393224 | tf_op jit(solution)/shard_map/ppermute | solution.py:317
  87.2 4.6 %copy-start.5 = (f32[2]{0:T(128)S(1)}, f32[2]{0:T(128)}, u32[]{:S(2)}) copy-start(f32[2]{0:T(128)} %lam_ref.1) | copy-start | bytes 28
  98.6 8.5 %copy-start.1 = (bf16[256,2048]{1,0:T(8,128)(2,1)S(1)}, bf16[256,2048]{1,0:T(8,128)(2,1)}, u32[]{:S(2)}) copy-start(bf16[256,2048]{1,0:T(8,128)(2,1)} %w0.1) | copy-start | bytes 3145732
  98.6 69.5 %copy-start.2 = (bf16[64,2048]{1,0:T(8,128)(2,1)S(1)}, bf16[64,2048]{1,0:T(8,128)(2,1)}, u32[]{:S(2)}) copy-start(bf16[64,2048]{1,0:T(8,128)(2,1)} %res_ref.1) | copy-start | bytes 786436
  98.6 69.5 %copy-start.3 = (f32[2048]{0:T(1024)S(1)}, f32[2048]{0:T(1024)}, u32[]{:S(2)}) copy-start(f32[2048]{0:T(1024)} %param.21) | copy-start | bytes 24580
  98.6 69.5 %copy-start.4 = (f32[128]{0:T(128)S(1)}, f32[128]{0:T(128)}, u32[]{:S(2)}) copy-start(f32[128]{0:T(128)} %param.19) | copy-start | bytes 1540
  98.6 69.4 %all-to-all-start = ((bf16[16,64,640]{2,1,0:T(8,128)(2,1)}), bf16[16,64,640]{2,1,0:T(8,128)(2,1)S(1)}, u32[]{:S(2)}, u32[]{:S(2)}) async-start(bf16[16,64,640]{2,1,0:T(8,128)(2,1)} %bitcast.6), calls=%async_computation | async-start | bytes 2621440 | tf_op jit(solution)/shard_map/all_to_all | solution.py:361
  107.0 39.2 %collective-permute-start.11 = (bf16[256,2048]{1,0:T(8,128)(2,1)S(1)}, bf16[256,2048]{1,0:T(8,128)(2,1)}, u32[]{:S(2)}, u32[]{:S(2)}) collective-permute-start(bf16[256,2048]{1,0:T(8,128)(2,1)S(1)} %copy-done.1), channel_id=1, source_target_pairs={{0,1},{1,2},{2,3},{3,0},{4,5},{5,6},{6,7},{7,4},{8,9},{9,10},{10,1... | collective-permute-start | bytes 3145736 | tf_op jit(solution)/shard_map/ppermute | solution.py:317
  108.6 59.5 %collective-permute-start.12 = (bf16[256,2048]{1,0:T(8,128)(2,1)S(1)}, bf16[256,2048]{1,0:T(8,128)(2,1)}, u32[]{:S(2)}, u32[]{:S(2)}) collective-permute-start(bf16[256,2048]{1,0:T(8,128)(2,1)S(1)} %copy-done.1), channel_id=1, source_target_pairs={{0,2},{1,3},{2,0},{3,1},{4,6},{5,7},{6,4},{7,5},{8,10},{9,11},{10,... | collective-permute-start | bytes 3145736 | tf_op jit(solution)/shard_map/ppermute | solution.py:317
  111.3 56.8 %collective-permute-start.13 = (bf16[256,2048]{1,0:T(8,128)(2,1)S(1)}, bf16[256,2048]{1,0:T(8,128)(2,1)}, u32[]{:S(2)}, u32[]{:S(2)}) collective-permute-start(bf16[256,2048]{1,0:T(8,128)(2,1)S(1)} %copy-done.1), channel_id=1, source_target_pairs={{0,3},{1,0},{2,1},{3,2},{4,7},{5,4},{6,5},{7,6},{8,11},{9,8},{10,9... | collective-permute-start | bytes 3145736 | tf_op jit(solution)/shard_map/ppermute | solution.py:317
  171.0 14.0 %collective-permute-start.14 = (bf16[64,2048]{1,0:T(8,128)(2,1)S(1)}, bf16[64,2048]{1,0:T(8,128)(2,1)S(1)}, u32[]{:S(2)}, u32[]{:S(2)}) collective-permute-start(bf16[64,2048]{1,0:T(8,128)(2,1)S(1)} %merge.1.n0), channel_id=1, source_target_pairs={{0,1},{1,2},{2,3},{3,0},{4,5},{5,6},{6,7},{7,4},{8,9},{9,10},{10,1... | collective-permute-start | bytes 786440 | tf_op jit(solution)/shard_map/ppermute | solution.py:317
  171.1 13.9 %collective-permute-start.15 = (bf16[64,2048]{1,0:T(8,128)(2,1)S(1)}, bf16[64,2048]{1,0:T(8,128)(2,1)S(1)}, u32[]{:S(2)}, u32[]{:S(2)}) collective-permute-start(bf16[64,2048]{1,0:T(8,128)(2,1)S(1)} %merge.1.n0), channel_id=1, source_target_pairs={{0,2},{1,3},{2,0},{3,1},{4,6},{5,7},{6,4},{7,5},{8,10},{9,11},{10,... | collective-permute-start | bytes 786440 | tf_op jit(solution)/shard_map/ppermute | solution.py:317
  173.7 11.9 %collective-permute-start.16 = (bf16[64,2048]{1,0:T(8,128)(2,1)S(1)}, bf16[64,2048]{1,0:T(8,128)(2,1)S(1)}, u32[]{:S(2)}, u32[]{:S(2)}) collective-permute-start(bf16[64,2048]{1,0:T(8,128)(2,1)S(1)} %merge.1.n0), channel_id=1, source_target_pairs={{0,3},{1,0},{2,1},{3,2},{4,7},{5,4},{6,5},{7,6},{8,11},{9,8},{10,9... | collective-permute-start | bytes 786440 | tf_op jit(solution)/shard_map/ppermute | solution.py:317
  185.7 3.4 %copy-start = (bf16[128,32,1024]{2,1,0:T(8,128)(2,1)S(1)}, bf16[128,32,1024]{2,1,0:T(8,128)(2,1)}, u32[]{:S(2)}) copy-start(bf16[128,32,1024]{2,1,0:T(8,128)(2,1)} %all-gather.3.cloned.1.call-done) | copy-start | bytes 25165828
  193.1 14.1 %collective-permute-start.17 = (bf16[64,2048]{1,0:T(8,128)(2,1)S(1)}, bf16[64,2048]{1,0:T(8,128)(2,1)S(1)}, u32[]{:S(2)}, u32[]{:S(2)}) collective-permute-start(bf16[64,2048]{1,0:T(8,128)(2,1)S(1)} %get-tuple-element.40), channel_id=1, source_target_pairs={{0,3},{1,0},{2,1},{3,2},{4,7},{5,4},{6,5},{7,6},{8,11},{9,8},{10,9... | collective-permute-start | bytes 786440 | tf_op jit(solution)/shard_map/ppermute | solution.py:317
  195.8 11.4 %collective-permute-start.18 = (bf16[64,2048]{1,0:T(8,128)(2,1)S(1)}, bf16[64,2048]{1,0:T(8,128)(2,1)S(1)}, u32[]{:S(2)}, u32[]{:S(2)}) collective-permute-start(bf16[64,2048]{1,0:T(8,128)(2,1)S(1)} %get-tuple-element.41), channel_id=1, source_target_pairs={{0,2},{1,3},{2,0},{3,1},{4,6},{5,7},{6,4},{7,5},{8,10},{9,11},{10,... | collective-permute-start | bytes 786440 | tf_op jit(solution)/shard_map/ppermute | solution.py:317
  195.8 14.8 %collective-permute-start.19 = (bf16[64,2048]{1,0:T(8,128)(2,1)S(1)}, bf16[64,2048]{1,0:T(8,128)(2,1)S(1)}, u32[]{:S(2)}, u32[]{:S(2)}) collective-permute-start(bf16[64,2048]{1,0:T(8,128)(2,1)S(1)} %get-tuple-element.42), channel_id=1, source_target_pairs={{0,1},{1,2},{2,3},{3,0},{4,5},{5,6},{6,7},{7,4},{8,9},{9,10},{10,1... | collective-permute-start | bytes 786440 | tf_op jit(solution)/shard_map/ppermute | solution.py:317
Sparse Core Ops, SparseCore 0:
  10.1 86.6 all-gather.2

commit v3 on v2

--- a/solution.py
+++ b/solution.py
@@ -1,3 +1,5 @@
+import functools
+
 import jax
 import jax.numpy as jnp
 from jax import lax
@@ -20,7 +22,7 @@
 WIDE = 5 * VD
 
 
-def prep_kernel(cos_ref, sin_ref, qa_ref, qb_ref, ka_ref, kb_ref, v_ref, q_out, kv_out):
+def prep_kernel(cos_ref, sin_ref, qa_ref, qb_ref, ka_ref, kb_ref, v_ref, q_out, kv_out, q_own, kv_own):
     cos = cos_ref[...]
     sin = sin_ref[...]
     lane = lax.broadcasted_iota(jnp.int32, cos.shape, 1)
@@ -36,6 +38,8 @@
     kv_out[0:TOK, 0:128] = turn(ka_ref)
     kv_out[0:TOK, 128:256] = turn(kb_ref)
     kv_out[TOK : 2 * TOK, :] = v_ref[...].astype(F32).T.astype(BF16)
+    q_own[...] = q_out[...]
+    kv_own[...] = kv_out[...]
 
 
 def prepare(first_query, second_query, first_key, second_key, values, start):
@@ -51,9 +55,10 @@
         out_shape=(
             jax.ShapeDtypeStruct((TOK, 2 * VD), BF16),
             jax.ShapeDtypeStruct((2 * TOK, 2 * VD), BF16),
-        ),
+        )
+        * 2,
         in_specs=[VMEM] * 7,
-        out_specs=(VMEM, VMEM),
+        out_specs=(VMEM,) * 4,
         name="prep",
     )(cos4, sin4, first_query, second_query, first_key, second_key, values)
 
@@ -212,15 +217,24 @@
     )(x, lambdas, qs, kv, *state)
 
 
-def merge_kernel(y_ref, part_ref, gain_ref, res_ref, norm_ref, w0, w1, w2, w3, out_ref, wbuf, sem):
-    copies = [
-        pltpu.make_async_copy(w, wbuf.at[o], sem.at[o]) for o, w in enumerate((w0, w1, w2, w3))
-    ]
-    for copy in copies:
-        copy.start()
+def merge_kernel(at_ref, part_ref, gain_ref, res_ref, norm_ref, own_ref, mine_ref, other_ref, out_ref, wbuf, sem):
+    copies = [[pltpu.make_async_copy(own_ref, wbuf.at[0], sem.at[0])]]
+    mine = at_ref[1] * VD
+    for o in range(3):
+        copies.append(
+            [
+                pltpu.make_async_copy(mine_ref.at[o], wbuf.at[o + 1, pl.ds(mine, VD)], sem.at[2 * o + 1]),
+                pltpu.make_async_copy(
+                    other_ref.at[o], wbuf.at[o + 1, pl.ds(VD - mine, VD)], sem.at[2 * o + 2]
+                ),
+            ]
+        )
+    for pair in copies:
+        for copy in pair:
+            copy.start()
     stream = res_ref[...].astype(F32)
     for o in range(4):
-        y = (y_ref[0] + 4 - o) % 4
+        y = (at_ref[0] + 4 - o) % 4
         parts = [part_ref[4 * k + y] for k in range(4)]
         stats = [p[:, 4 * VD :].astype(F32) for p in parts]
         heads = []
@@ -245,69 +259,59 @@
             scale = lax.rsqrt(jnp.mean(diff * diff, axis=-1, keepdims=True) + 1e-05)
             heads.append((diff * scale * gain_ref[...] * 0.8).astype(BF16))
         flat = jnp.concatenate(heads, axis=1)
-        copies[o].wait()
+        for copy in copies[o]:
+            copy.wait()
         stream = stream + lax.dot_general(flat, wbuf[o], NN, preferred_element_type=F32)
     center = stream - jnp.mean(stream, axis=-1, keepdims=True)
     spread = jnp.mean(center * center, axis=-1, keepdims=True)
     out_ref[...] = (center * lax.rsqrt(spread + 1e-05) * norm_ref[...]).astype(BF16)
 
 
-def merge(y, part, head_gain, residual, norm_gain, weights):
+def merge(at, part, head_gain, residual, norm_gain, weights):
     rows, width = residual.shape
     return pl.pallas_call(
         merge_kernel,
         out_shape=jax.ShapeDtypeStruct((rows, width), BF16),
-        in_specs=[SMEM] + [VMEM] * 4 + [ANY] * 4,
+        in_specs=[SMEM] + [VMEM] * 4 + [ANY] * 3,
         out_specs=VMEM,
-        scratch_shapes=[pltpu.VMEM((4, 2 * VD, width), BF16), pltpu.SemaphoreType.DMA((4,))],
+        scratch_shapes=[pltpu.VMEM((4, 2 * VD, width), BF16), pltpu.SemaphoreType.DMA((7,))],
         compiler_params=pltpu.CompilerParams(vmem_limit_bytes=24 * 2**20),
         name="merge",
-    )(y, part, head_gain.reshape(1, VD), residual, norm_gain.reshape(1, width), *weights)
-
-
-def mixer_kernel(n0, n1, n2, n3, w_ref, o0, o1, o2, o3, up, down, sem):
+    )(at, part, head_gain.reshape(1, VD), residual, norm_gain.reshape(1, width), *weights)
+
+
+def mixer_kernel(count, *refs):
+    pieces, w_ref, outs = refs[:count], refs[count], refs[count + 1 :]
+    devices, _, rows, hidden_width = w_ref.shape
+    x = jnp.concatenate([n[...] for n in pieces], axis=0)
     cuts = 4
-    per = up.shape[0] // cuts
-    copies = []
-    for side, buf in enumerate((up, down)):
-        for i in range(cuts):
-            at = pl.ds(i * per, per)
-            copies.append(pltpu.make_async_copy(w_ref.at[at, side], buf.at[at], sem.at[side * cuts + i]))
-            copies[-1].start()
-    hidden_width = up.shape[2]
-    step = per * up.shape[1]
-    x = jnp.concatenate([n[...] for n in (n0, n1, n2, n3)], axis=0)
-    lifted = jnp.zeros((x.shape[0], hidden_width), F32)
+    per = devices // cuts
+    step = per * rows
+    lifted = None
     for i in range(cuts):
-        copies[i].wait()
-        block = up[i * per : (i + 1) * per].reshape(step, hidden_width)
-        lifted = lifted + lax.dot_general(
-            x[:, i * step : (i + 1) * step], block, NN, preferred_element_type=F32
-        )
+        block = w_ref[i * per : (i + 1) * per, 0].reshape(step, hidden_width)
+        more = lax.dot_general(x[:, i * step : (i + 1) * step], block, NN, preferred_element_type=F32)
+        lifted = more if lifted is None else lifted + more
     pos = jnp.maximum(lifted, 0.0)
     hidden = (pos * pos).astype(BF16)
-    rows = n0.shape[0]
     for i in range(cuts):
-        copies[cuts + i].wait()
-        block = down[i * per : (i + 1) * per].reshape(step, hidden_width)
+        block = w_ref[i * per : (i + 1) * per, 1].reshape(step, hidden_width)
         low = lax.dot_general(hidden, block, NT, preferred_element_type=F32)
-        for k, o in enumerate((o0, o1, o2, o3)):
-            o[:, i * step : (i + 1) * step] = low[k * rows : (k + 1) * rows].astype(o.dtype)
-
-
-def mixer(pieces, weights):
-    rows, width = pieces[0].shape
-    return pl.pallas_call(
-        mixer_kernel,
-        out_shape=[jax.ShapeDtypeStruct((rows, width), F32 if k == 0 else BF16) for k in range(4)],
-        in_specs=[VMEM] * 4 + [ANY],
-        out_specs=[VMEM] * 4,
-        scratch_shapes=[
-            pltpu.VMEM((weights.shape[0],) + weights.shape[2:], BF16),
-            pltpu.VMEM((weights.shape[0],) + weights.shape[2:], BF16),
-            pltpu.SemaphoreType.DMA((8,)),
-        ],
-        compiler_params=pltpu.CompilerParams(vmem_limit_bytes=32 * 2**20),
+        at = 0
+        for n, o in zip(pieces, outs):
+            o[:, i * step : (i + 1) * step] = low[at : at + o.shape[0]].astype(o.dtype)
+            at += o.shape[0]
+
+
+def mixer(pieces, weights, types):
+    width = pieces[0].shape[1]
+    return pl.pallas_call(
+        functools.partial(mixer_kernel, len(pieces)),
+        out_shape=[jax.ShapeDtypeStruct(n.shape, t) for n, t in zip(pieces, types)],
+        in_specs=[VMEM] * (len(pieces) + 1),
+        out_specs=[VMEM] * len(pieces),
+        cost_estimate=pl.CostEstimate(flops=2 * 256 * width * 2048, bytes_accessed=2**23, transcendentals=0),
+        compiler_params=pltpu.CompilerParams(vmem_limit_bytes=24 * 2**20),
         name="mixer",
     )(*pieces, weights)
 
@@ -333,20 +337,22 @@
 ):
     sp = lax.axis_index(("z", "x", "c"))
     x = lax.axis_index("x").astype(jnp.int32).reshape(1)
-    y = lax.axis_index("tp").astype(jnp.int32).reshape(1)
-    query, kv = prepare(first_query, second_query, first_key, second_key, values, sp * TOK)
+    at = jnp.stack([lax.axis_index("tp"), lax.axis_index("c")]).astype(jnp.int32)
+    query, kv, query_own, kv_own = prepare(first_query, second_query, first_key, second_key, values, sp * TOK)
     ring = ("z", "c")
     onward = [(2 * z + c, 2 * ((z + 1 - 2 * c) % 8) + c) for z in range(8) for c in range(2)]
     crossed = [(2 * z + c, 2 * ((z - 1 + 2 * c) % 8) + 1 - c) for z in range(8) for c in range(2)]
     near = [lax.ppermute(kv, ring, onward), lax.ppermute(kv, ring, crossed)]
     other = shifted(kv, "c", 1)
-    queries = [query] + [shifted(query, "x", o) for o in (1, 2, 3)]
+    queries = [query_own] + [shifted(query, "x", o) for o in (1, 2, 3)]
     mix_weights = jnp.stack([up_weight, down_weight.T])
     mix_weights = lax.all_gather(mix_weights, ("z", "x", "c"))
+    half = lax.dynamic_slice_in_dim(out_weight, lax.axis_index("c") * VD, VD, 0)
     near = jnp.stack(near)
     second = lax.ppermute(near, ring, onward)
-    qs, *state = attend_first(queries, kv, other)
-    out_weights = [out_weight] + [shifted(out_weight, "tp", o) for o in (1, 2, 3)]
+    mine = jnp.stack([shifted(half, "tp", o) for o in (1, 2, 3)])
+    out_weights = [out_weight, mine, shifted(mine, "c", 1)]
+    qs, *state = attend_first(queries, kv_own, other)
     third = lax.ppermute(second, ring, onward)
     four = jnp.concatenate([near, second])
     four_other = shifted(four, "c", 1)
@@ -359,12 +365,23 @@
     part = attend_last(x, lambdas, qs, three_other, state)
     part = part.reshape(16, 64, WIDE)
     part = lax.all_to_all(part, ("x", "tp"), split_axis=0, concat_axis=0, tiled=True)
-    normed = merge(y, part, head_gain, residual, norm_gain, out_weights)
-    pieces = [normed] + [shifted(normed, "tp", o) for o in (1, 2, 3)]
-    lows = mixer(pieces, mix_weights)
-    total = normed.astype(F32) + lows[0]
-    for o in (1, 2, 3):
-        total = total + shifted(lows[o], "tp", -o).astype(F32)
+    normed = merge(at, part, head_gain, residual, norm_gain, out_weights)
+    rows = normed.shape[0] // 2
+    before = shifted(normed, "tp", 1)
+    after = shifted(normed, "tp", -1)
+    cut1 = before[:rows]
+    cut3 = after[rows:]
+    across1 = shifted(cut1, "tp", 1)
+    across3 = shifted(cut3, "tp", -1)
+    low0, low1, low3 = mixer([normed, before, after], mix_weights, (F32, BF16, BF16))
+    low1 = shifted(low1, "tp", -1)
+    low3 = shifted(low3, "tp", 1)
+    across = jnp.concatenate([across1, across3])
+    (low2,) = mixer([across], mix_weights, (BF16,))
+    low2 = shifted(low2, "tp", 2)
+    total = normed.astype(F32) + low0
+    for low in (low1, low2, low3):
+        total = total + low.astype(F32)
     return total.astype(BF16)
 
 

time: 219 us -> 173 us (0.79)
  waiting for transfers between devices: 129 us -> 76.4 us
  starting transfers between devices: 33 us -> 35.6 us
  local copies, waits for them, and re-layouts: 3.43 us -> 5.78 us
    ppermute x15 -> x17, waiting for transfers between devices: 90 us -> 29.4 us  [shifted(): lax.ppermute(value, axis, [(i, (i + by) % size) for i in range(size)])]
    all_to_all x1, waiting for transfers between devices: 0.01 us -> 19.1 us  [local(): lax.all_to_all(part, ('x', 'tp'), split_axis=0, concat_axis=0, tiled=True)]
    ppermute x1, waiting for transfers between devices: 7.57 us -> 1.72 us  [local(): far = lax.ppermute(third[0], ring, onward)]
    ppermute x1, waiting for transfers between devices: 11.7 us -> 6.91 us  [local(): third = lax.ppermute(second, ring, onward)]
    ppermute x15 -> x17, starting transfers between devices: 18.4 us -> 22.4 us  [shifted(): lax.ppermute(value, axis, [(i, (i + by) % size) for i in range(size)])]
    unnamed x16 -> x24, local copies, waits for them, and re-layouts: 3.41 us -> 5.7 us
    pallas_call x1 -> x2, Pallas kernels: 4.02 us -> 4.46 us  [mixer(): pl.pallas_call(functools.partial(mixer_kernel, len(pieces)), out_shape=[j...]
  transfers between devices with their start and end apart: 22 -> 24, of which waited for: 13 -> 13; matrix products, arithmetic and copies ran while one was open for 1% -> 1% of each run, Pallas kernels for 14% -> 20%
where the time goes in v3:
time: 173 us; the launch traced here: 172 us
  waiting for transfers between devices  76.4 us (44%)
  starting transfers between devices  35.6 us (21%)
  Pallas kernels  35.6 us (21%)
  between operations  13.7 us (8%)
  local copies, waits for them, and re-layouts  5.78 us (3%)
  other arithmetic  4.41 us (3%)
    ppermute x17, waiting for transfers between devices, shifted(): lax.ppermute(value, axis, [(i, (i + by) % size) for i in range(size)])  29.4 us
    ppermute x17, starting transfers between devices, shifted(): lax.ppermute(value, axis, [(i, (i + by) % size) for i in range(size)])  22.4 us
    all_to_all x1, waiting for transfers between devices, local(): lax.all_to_all(part, ('x', 'tp'), split_axis=0, concat_axis=0, tiled=True)  19.1 us
    pallas_call x3, Pallas kernels, attend_next(): pl.pallas_call(next_kernel, out_shape=STATE, in_specs=[VMEM] * 5, out_spe...  15.6 us
    ppermute x1, waiting for transfers between devices, local(): second = lax.ppermute(near, ring, onward)  12.2 us
    ppermute x2, waiting for transfers between devices, local(): near = [lax.ppermute(kv, ring, onward), lax.ppermute(kv, ring, crossed)]  7.11 us
    all_to_all x1, starting transfers between devices, local(): lax.all_to_all(part, ('x', 'tp'), split_axis=0, concat_axis=0, tiled=True)  7 us
    ppermute x1, waiting for transfers between devices, local(): third = lax.ppermute(second, ring, onward)  6.91 us
  transfers between devices with their start and end apart: 24, of which 13 were waited for; matrix products, arithmetic and copies ran while one was open for 1% of the time, Pallas kernels for 20%

profile of v3, /device:TPU:2, one launch (start us, length us, event | category | flops | bytes accessed | tf_op | source)
XLA Modules:
  0.0 171.5 jit_solution(5175240335360210572)
XLA Ops:
  6.5 1.5 pad_maximum_fusion.7
  8.1 0.5 fusion
  8.7 1.0 pad_maximum_fusion.5
  9.7 2.3 %prep.1 = (bf16[256,256]{1,0:T(8,128)(2,1)}, bf16[512,256]{1,0:T(8,128)(2,1)}, bf16[256,256]{1,0:T(8,128)(2,1)}, bf16[512,256]{1,0:T(8,128)(2,1)}) custom-call(f32[256,128]{1,0:T(8,128)} %get-tuple-element.48.cos_ref, f32[256,128]{1,0:T(8,128)} %get-tuple-element.49.sin_ref, bf16[256,128]{1,0:T(8,128)(2,1)} %qa_ref.1, bf16[256,128]{1,0:T(8,128)(2,1)} %qb_ref.1, ...), custom_call_target="tpu_custom_call" | custom-call | tf_op jit(solution)/shard_map/prep/pallas_call | solution.py:53
  12.0 1.9 %collective-permute-start.4 = (bf16[512,256]{1,0:T(8,128)(2,1)}, bf16[512,256]{1,0:T(8,128)(2,1)S(1)}, u32[]{:S(2)}, u32[]{:S(2)}) collective-permute-start(bf16[512,256]{1,0:T(8,128)(2,1)} %get-tuple-element.28), channel_id=1, source_target_pairs={{0,32},{4,228},{32,64},{36,4},{64,96},{68,36},{96,128},{100,68},{1... | collective-permute-start | bytes 786440 | tf_op jit(solution)/shard_map/ppermute | solution.py:345
  13.9 4.1 %collective-permute-start.5 = (bf16[512,256]{1,0:T(8,128)(2,1)}, bf16[512,256]{1,0:T(8,128)(2,1)S(1)}, u32[]{:S(2)}, u32[]{:S(2)}) collective-permute-start(bf16[512,256]{1,0:T(8,128)(2,1)} %get-tuple-element.28), channel_id=1, source_target_pairs={{0,228},{4,32},{32,4},{36,64},{64,36},{68,96},{96,68},{100,128},{1... | collective-permute-start | bytes 786440 | tf_op jit(solution)/shard_map/ppermute | solution.py:345
  18.0 7.1 %collective-permute-done.4 = bf16[512,256]{1,0:T(8,128)(2,1)S(1)} collective-permute-done((bf16[512,256]{1,0:T(8,128)(2,1)}, bf16[512,256]{1,0:T(8,128)(2,1)S(1)}, u32[]{:S(2)}, u32[]{:S(2)}) %collective-permute-start.4) | collective-permute-done | bytes 262176 | tf_op jit(solution)/shard_map/ppermute | solution.py:345
  25.3 12.2 %collective-permute-done.6 = bf16[2,512,256]{2,1,0:T(8,128)(2,1)S(1)} collective-permute-done((bf16[2,512,256]{2,1,0:T(8,128)(2,1)S(1)}, bf16[2,512,256]{2,1,0:T(8,128)(2,1)S(1)}, u32[]{:S(2)}, u32[]{:S(2)}) %collective-permute-start.6) | collective-permute-done | bytes 524320 | tf_op jit(solution)/shard_map/ppermute | solution.py:352
  37.5 1.5 collective-permute-start
  39.0 1.0 collective-permute-start.1
  40.0 2.2 %collective-permute-start.2 = (bf16[256,256]{1,0:T(8,128)(2,1)}, bf16[256,256]{1,0:T(8,128)(2,1)S(1)}, u32[]{:S(2)}, u32[]{:S(2)}) collective-permute-start(bf16[256,256]{1,0:T(8,128)(2,1)} %get-tuple-element.26), channel_id=1, source_target_pairs={{0,24},{8,0},{16,8},{24,16},{1,25},{9,1},{17,9},{25,17},{2,26},{10... | collective-permute-start | bytes 393224 | tf_op jit(solution)/shard_map/ppermute | solution.py:321
  42.3 0.1 pad_maximum_fusion.1.kv_ref
  42.5 6.9 %collective-permute-done.7 = bf16[2,512,256]{2,1,0:T(8,128)(2,1)S(1)} collective-permute-done((bf16[2,512,256]{2,1,0:T(8,128)(2,1)S(1)}, bf16[2,512,256]{2,1,0:T(8,128)(2,1)S(1)}, u32[]{:S(2)}, u32[]{:S(2)}) %collective-permute-start.7) | collective-permute-done | bytes 524320 | tf_op jit(solution)/shard_map/ppermute | solution.py:356
  49.6 1.6 collective-permute-start.11
  51.2 2.7 %collective-permute-start.12 = (bf16[128,2048]{1,0:T(8,128)(2,1)S(1)}, bf16[128,2048]{1,0:T(8,128)(2,1)S(1)}, u32[]{:S(2)}, u32[]{:S(2)}) collective-permute-start(bf16[128,2048]{1,0:T(8,128)(2,1)S(1)} %constant_dynamic-slice_fusion), channel_id=1, source_target_pairs={{0,2},{1,3},{2,0},{3,1},{4,6},{5,7},{6,4},{7,5},{8,10},{9,11},{10,... | collective-permute-start | bytes 1572872 | tf_op jit(solution)/shard_map/ppermute | solution.py:321
  53.9 1.4 collective-permute-start.13
  55.4 1.7 %collective-permute-done.8 = bf16[512,256]{1,0:T(8,128)(2,1)S(1)} collective-permute-done((bf16[512,256]{1,0:T(8,128)(2,1)S(1)}, bf16[512,256]{1,0:T(8,128)(2,1)S(1)}, u32[]{:S(2)}, u32[]{:S(2)}) %collective-permute-start.8) | collective-permute-done | bytes 262176 | tf_op jit(solution)/shard_map/ppermute | solution.py:360
  57.2 1.5 collective-permute-done.3.other_ref
  58.6 0.1 collective-permute-start.9
  58.8 4.1 %attend_first.1 = (bf16[4,4,256,256]{3,2,1,0:T(8,128)(2,1)S(1)}, f32[4,4,128,256]{3,2,1,0:T(8,128)S(1)}, f32[4,4,1,256]{3,2,1,0:T(1,128)S(1)}, f32[4,4,1,256]{3,2,1,0:T(1,128)S(1)}) custom-call(bf16[256,256]{1,0:T(8,128)(2,1)S(1)} %copy-done.10, bf16[256,256]{1,0:T(8,128)(2,1)S(1)} %collective-permute-done.q1, ...), custom_call_target="tpu_custom_call" | custom-call | flops 805306368 | bytes 524288 | tf_op jit(solution)/shard_map/attend_first/pallas_call | solution.py:180
  62.8 1.5 collective-permute-done.11
  64.3 11.4 %collective-permute-done.12 = bf16[128,2048]{1,0:T(8,128)(2,1)S(1)} collective-permute-done((bf16[128,2048]{1,0:T(8,128)(2,1)S(1)}, bf16[128,2048]{1,0:T(8,128)(2,1)S(1)}, u32[]{:S(2)}, u32[]{:S(2)}) %collective-permute-start.12) | collective-permute-done | bytes 524320 | tf_op jit(solution)/shard_map/ppermute | solution.py:321
  75.7 0.2 pad_maximum_fusion.mine_ref
  75.9 0.1 collective-permute-start.14
  76.0 5.4 %attend_next.3 = (f32[4,4,128,256]{3,2,1,0:T(8,128)S(1)}, f32[4,4,1,256]{3,2,1,0:T(1,128)S(1)}, f32[4,4,1,256]{3,2,1,0:T(1,128)S(1)}) custom-call(bf16[4,4,256,256]{3,2,1,0:T(8,128)(2,1)S(1)} %get-tuple-element.29.qs, bf16[4,512,256]{2,1,0:T(8,128)(2,1)S(1)} %pad_maximum_fusion.1.kv_ref, ...), custom_call_target="tpu_custom_call", output_to_operand_aliasing={{0}: (2, {}), {1}: (3, {}), {2}: (4, {})} | custom-call | flops 1610612736 | bytes 1048576 | tf_op jit(solution)/shard_map/attend_next/pallas_call | solution.py:193
  81.5 5.6 %attend_next.4 = (f32[4,4,128,256]{3,2,1,0:T(8,128)S(1)}, f32[4,4,1,256]{3,2,1,0:T(1,128)S(1)}, f32[4,4,1,256]{3,2,1,0:T(1,128)S(1)}) custom-call(bf16[4,4,256,256]{3,2,1,0:T(8,128)(2,1)S(1)} %get-tuple-element.29.qs, bf16[4,512,256]{2,1,0:T(8,128)(2,1)S(1)} %collective-permute-done.10.kv_ref, ...), custom_call_target="tpu_custom_call", output_to_operand_aliasing={{0}: (2, {}), {1}: (3, {}), {2}: (4, {})} | custom-call | flops 1610612736 | bytes 1048576 | tf_op jit(solution)/shard_map/attend_next/pallas_call | solution.py:193
  87.1 4.6 %attend_next.5 = (f32[4,4,128,256]{3,2,1,0:T(8,128)S(1)}, f32[4,4,1,256]{3,2,1,0:T(1,128)S(1)}, f32[4,4,1,256]{3,2,1,0:T(1,128)S(1)}) custom-call(bf16[4,4,256,256]{3,2,1,0:T(8,128)(2,1)S(1)} %get-tuple-element.29.qs, bf16[3,512,256]{2,1,0:T(8,128)(2,1)S(1)} %pad_maximum_fusion.2.kv_ref, ...), custom_call_target="tpu_custom_call", output_to_operand_aliasing={{0}: (2, {}), {1}: (3, {}), {2}: (4, {})} | custom-call | flops 1207959552 | bytes 786432 | tf_op jit(solution)/shard_map/attend_next/pallas_call | solution.py:193
  91.7 5.7 %attend_last.1 = bf16[4,256,640]{2,1,0:T(8,128)(2,1)S(1)} custom-call(s32[1]{0:T(128)} %bitcast.2.x_ref, f32[2]{0:T(128)S(1)} %copy-done.8, bf16[4,4,256,256]{3,2,1,0:T(8,128)(2,1)S(1)} %get-tuple-element.29.qs, bf16[3,512,256]{2,1,0:T(8,128)(2,1)S(1)} %collective-permute-done.9.kv_ref, f32[4,4,128,256]{3,2,1,0:T(8,128)S(1)} %get-tuple-element.39.acc_in, ...), custom_call_target="tpu_custom_call" | custom-call | flops 1207959552 | bytes 786432 | tf_op jit(solution)/shard_map/attend_last/pallas_call | solution.py:207
  97.4 1.1 copy-done.2
  98.5 7.0 %all-to-all-start = ((bf16[16,64,640]{2,1,0:T(8,128)(2,1)}), bf16[16,64,640]{2,1,0:T(8,128)(2,1)S(1)}, u32[]{:S(2)}, u32[]{:S(2)}) async-start(bf16[16,64,640]{2,1,0:T(8,128)(2,1)} %bitcast.21), calls=%async_computation | async-start | bytes 2621440 | tf_op jit(solution)/shard_map/all_to_all | solution.py:367
  105.5 19.1 %all-to-all-done.part_ref = bf16[16,64,640]{2,1,0:T(8,128)(2,1)S(1)} async-done(((bf16[16,64,640]{2,1,0:T(8,128)(2,1)}), bf16[16,64,640]{2,1,0:T(8,128)(2,1)S(1)}, u32[]{:S(2)}, u32[]{:S(2)}) %all-to-all-start) | async-done | bytes 1310752 | tf_op jit(solution)/shard_map/all_to_all | solution.py:367
  124.6 1.2 copy-done.4
  125.8 3.5 %merge.1.refs_0_ = bf16[64,2048]{1,0:T(8,128)(2,1)S(1)} custom-call(s32[2]{0:T(128)S(1)} %pad_add_fusion.at_ref, bf16[16,64,640]{2,1,0:T(8,128)(2,1)S(1)} %all-to-all-done.part_ref, f32[1,128]{1,0:T(1,128)S(1)} %bitcast.23, bf16[64,2048]{1,0:T(8,128)(2,1)S(1)} %copy-done.5, f32[1,2048]{1,0:T(1,128)S(1)} %bitcast.22, bf16[256,2048]{1,0:T(8,128)(2,1)S(1)} %copy-done.4, ...), custom_call_target="tpu_custom_call" | custom-call | tf_op jit(solution)/shard_map/merge/pallas_call | solution.py:272
  129.3 0.6 collective-permute-start.15
  129.9 2.7 %collective-permute-start.16 = (bf16[64,2048]{1,0:T(8,128)(2,1)S(1)}, bf16[64,2048]{1,0:T(8,128)(2,1)S(1)}, u32[]{:S(2)}, u32[]{:S(2)}) collective-permute-start(bf16[64,2048]{1,0:T(8,128)(2,1)S(1)} %merge.1.refs_0_), channel_id=1, source_target_pairs={{0,3},{1,0},{2,1},{3,2},{4,7},{5,4},{6,5},{7,6},{8,11},{9,8},{10,9... | collective-permute-start | bytes 786440 | tf_op jit(solution)/shard_map/ppermute | solution.py:321
  132.6 4.5 %collective-permute-done.15.refs_1_ = bf16[64,2048]{1,0:T(8,128)(2,1)S(1)} collective-permute-done((bf16[64,2048]{1,0:T(8,128)(2,1)S(1)}, bf16[64,2048]{1,0:T(8,128)(2,1)S(1)}, u32[]{:S(2)}, u32[]{:S(2)}) %collective-permute-start.15) | collective-permute-done | bytes 262176 | tf_op jit(solution)/shard_map/ppermute | solution.py:321
  137.2 0.3 collective-permute-start.18
  137.5 3.3 %collective-permute-start.19 = (bf16[32,2048]{1,0:T(8,128)(2,1)S(1)}, bf16[32,2048]{1,0:T(8,128)(2,1)S(1)}, u32[]{:S(2)}, u32[]{:S(2)}) collective-permute-start(bf16[32,2048]{1,0:T(8,128)(2,1)S(1)} %slice.14), channel_id=1, source_target_pairs={{0,3},{1,0},{2,1},{3,2},{4,7},{5,4},{6,5},{7,6},{8,11},{9,8},{10,9... | collective-permute-start | bytes 393224 | tf_op jit(solution)/shard_map/ppermute | solution.py:321
  140.8 2.8 %collective-permute-done.18 = bf16[32,2048]{1,0:T(8,128)(2,1)S(1)} collective-permute-done((bf16[32,2048]{1,0:T(8,128)(2,1)S(1)}, bf16[32,2048]{1,0:T(8,128)(2,1)S(1)}, u32[]{:S(2)}, u32[]{:S(2)}) %collective-permute-start.18) | collective-permute-done | bytes 131104 | tf_op jit(solution)/shard_map/ppermute | solution.py:321
  143.7 3.4 %copy-done = bf16[128,32,1024]{2,1,0:T(8,128)(2,1)S(1)} copy-done((bf16[128,32,1024]{2,1,0:T(8,128)(2,1)S(1)}, bf16[128,32,1024]{2,1,0:T(8,128)(2,1)}, u32[]{:S(2)}) %copy-start) | copy-done | bytes 8388632
  147.1 2.1 %mixer.3 = bf16[64,2048]{1,0:T(8,128)(2,1)S(1)} custom-call(bf16[64,2048]{1,0:T(8,128)(2,1)S(1)} %pad_maximum_fusion.4.refs_0_, bf16[64,2,32,1024]{3,2,1,0:T(8,128)(2,1)S(1)} %bitcast.19), custom_call_target="tpu_custom_call" | custom-call | flops 2147483648 | bytes 8388608 | tf_op jit(solution)/shard_map/mixer/pallas_call | solution.py:308
  149.2 1.6 collective-permute-start.20
  150.9 2.3 %mixer.2 = (f32[64,2048]{1,0:T(8,128)S(1)}, bf16[64,2048]{1,0:T(8,128)(2,1)S(1)}, bf16[64,2048]{1,0:T(8,128)(2,1)S(1)}) custom-call(bf16[64,2048]{1,0:T(8,128)(2,1)S(1)} %merge.1.refs_0_, bf16[64,2048]{1,0:T(8,128)(2,1)S(1)} %collective-permute-done.15.refs_1_, bf16[64,2048]{1,0:T(8,128)(2,1)S(1)} %collective-permute-done.16.refs_2_, ...), custom_call_target="tpu_custom_call" | custom-call | flops 2147483648 | bytes 8388608 | tf_op jit(solution)/shard_map/mixer/pallas_call | solution.py:308
  153.2 3.0 %collective-permute-start.17 = (bf16[64,2048]{1,0:T(8,128)(2,1)S(1)}, bf16[64,2048]{1,0:T(8,128)(2,1)S(1)}, u32[]{:S(2)}, u32[]{:S(2)}) collective-permute-start(bf16[64,2048]{1,0:T(8,128)(2,1)S(1)} %get-tuple-element.43), channel_id=1, source_target_pairs={{0,3},{1,0},{2,1},{3,2},{4,7},{5,4},{6,5},{7,6},{8,11},{9,8},{10,9... | collective-permute-start | bytes 786440 | tf_op jit(solution)/shard_map/ppermute | solution.py:321
  156.2 3.7 %collective-permute-done.20 = bf16[64,2048]{1,0:T(8,128)(2,1)S(1)} collective-permute-done((bf16[64,2048]{1,0:T(8,128)(2,1)S(1)}, bf16[64,2048]{1,0:T(8,128)(2,1)S(1)}, u32[]{:S(2)}, u32[]{:S(2)}) %collective-permute-start.20) | collective-permute-done | bytes 262176 | tf_op jit(solution)/shard_map/ppermute | solution.py:321
  159.9 1.5 collective-permute-done.17
  161.4 2.4 %collective-permute-done.21 = bf16[64,2048]{1,0:T(8,128)(2,1)S(1)} collective-permute-done((bf16[64,2048]{1,0:T(8,128)(2,1)S(1)}, bf16[64,2048]{1,0:T(8,128)(2,1)S(1)}, u32[]{:S(2)}, u32[]{:S(2)}) %collective-permute-start.21) | collective-permute-done | bytes 262176 | tf_op jit(solution)/shard_map/ppermute | solution.py:321
  163.8 0.9 add_convert_fusion
  (50 shorter events, 0.7 us)
Async XLA Ops:
  6.5 137.2 %all-gather.3.cloned.1.call-start = ((), (), s32[]{:S(2)}) async-start(), calls=%async_computation.1 | async-start | bytes 8519680 | tf_op jit(solution)/shard_map/all_gather | solution.py:349
  12.0 13.1 %collective-permute-start.4 = (bf16[512,256]{1,0:T(8,128)(2,1)}, bf16[512,256]{1,0:T(8,128)(2,1)S(1)}, u32[]{:S(2)}, u32[]{:S(2)}) collective-permute-start(bf16[512,256]{1,0:T(8,128)(2,1)} %get-tuple-element.28), channel_id=1, source_target_pairs={{0,32},{4,228},{32,64},{36,4},{64,96},{68,36},{96,128},{100,68},{1... | collective-permute-start | bytes 786440 | tf_op jit(solution)/shard_map/ppermute | solution.py:345
  13.9 11.2 %collective-permute-start.5 = (bf16[512,256]{1,0:T(8,128)(2,1)}, bf16[512,256]{1,0:T(8,128)(2,1)S(1)}, u32[]{:S(2)}, u32[]{:S(2)}) collective-permute-start(bf16[512,256]{1,0:T(8,128)(2,1)} %get-tuple-element.28), channel_id=1, source_target_pairs={{0,228},{4,32},{32,4},{36,64},{64,36},{68,96},{96,68},{100,128},{1... | collective-permute-start | bytes 786440 | tf_op jit(solution)/shard_map/ppermute | solution.py:345
  25.2 24.3 %copy-start.3 = (bf16[256,2048]{1,0:T(8,128)(2,1)S(1)}, bf16[256,2048]{1,0:T(8,128)(2,1)}, u32[]{:S(2)}) copy-start(bf16[256,2048]{1,0:T(8,128)(2,1)} %own_ref.1) | copy-start | bytes 3145732
  25.2 12.3 %collective-permute-start.6 = (bf16[2,512,256]{2,1,0:T(8,128)(2,1)S(1)}, bf16[2,512,256]{2,1,0:T(8,128)(2,1)S(1)}, u32[]{:S(2)}, u32[]{:S(2)}) collective-permute-start(bf16[2,512,256]{2,1,0:T(8,128)(2,1)S(1)} %pad_maximum_fusion.3), channel_id=1, source_target_pairs={{0,32},{4,228},{32,64},{36,4},{64,96},{68,36},{96,128},{100,68},{1... | collective-permute-start | bytes 1572872 | tf_op jit(solution)/shard_map/ppermute | solution.py:352
  37.5 11.9 %collective-permute-start.7 = (bf16[2,512,256]{2,1,0:T(8,128)(2,1)S(1)}, bf16[2,512,256]{2,1,0:T(8,128)(2,1)S(1)}, u32[]{:S(2)}, u32[]{:S(2)}) collective-permute-start(bf16[2,512,256]{2,1,0:T(8,128)(2,1)S(1)} %collective-permute-done.6), channel_id=1, source_target_pairs={{0,32},{4,228},{32,64},{36,4},{64,96},{68,36},{96,128},{100,68},{1... | collective-permute-start | bytes 1572872 | tf_op jit(solution)/shard_map/ppermute | solution.py:356
  37.5 12.1 %collective-permute-start = (bf16[256,256]{1,0:T(8,128)(2,1)}, bf16[256,256]{1,0:T(8,128)(2,1)S(1)}, u32[]{:S(2)}, u32[]{:S(2)}) collective-permute-start(bf16[256,256]{1,0:T(8,128)(2,1)} %get-tuple-element.26), channel_id=1, source_target_pairs={{0,8},{8,16},{16,24},{24,0},{1,9},{9,17},{17,25},{25,1},{2,10},{10... | collective-permute-start | bytes 393224 | tf_op jit(solution)/shard_map/ppermute | solution.py:321
  39.0 12.2 %collective-permute-start.1 = (bf16[256,256]{1,0:T(8,128)(2,1)}, bf16[256,256]{1,0:T(8,128)(2,1)S(1)}, u32[]{:S(2)}, u32[]{:S(2)}) collective-permute-start(bf16[256,256]{1,0:T(8,128)(2,1)} %get-tuple-element.26), channel_id=1, source_target_pairs={{0,16},{8,24},{16,0},{24,8},{1,17},{9,25},{17,1},{25,9},{2,18},{10... | collective-permute-start | bytes 393224 | tf_op jit(solution)/shard_map/ppermute | solution.py:321
  40.0 13.9 %collective-permute-start.2 = (bf16[256,256]{1,0:T(8,128)(2,1)}, bf16[256,256]{1,0:T(8,128)(2,1)S(1)}, u32[]{:S(2)}, u32[]{:S(2)}) collective-permute-start(bf16[256,256]{1,0:T(8,128)(2,1)} %get-tuple-element.26), channel_id=1, source_target_pairs={{0,24},{8,0},{16,8},{24,16},{1,25},{9,1},{17,9},{25,17},{2,26},{10... | collective-permute-start | bytes 393224 | tf_op jit(solution)/shard_map/ppermute | solution.py:321
  42.3 14.8 %copy-start.11 = (bf16[512,256]{1,0:T(8,128)(2,1)S(1)}, bf16[512,256]{1,0:T(8,128)(2,1)}, u32[]{:S(2)}) copy-start(bf16[512,256]{1,0:T(8,128)(2,1)} %get-tuple-element.28) | copy-start | bytes 786436
  42.4 16.4 %copy-start.9 = (bf16[512,256]{1,0:T(8,128)(2,1)S(1)}, bf16[512,256]{1,0:T(8,128)(2,1)}, u32[]{:S(2)}) copy-start(bf16[512,256]{1,0:T(8,128)(2,1)} %get-tuple-element.27.own_ref) | copy-start | bytes 786436
  42.4 16.4 %copy-start.10 = (bf16[256,256]{1,0:T(8,128)(2,1)S(1)}, bf16[256,256]{1,0:T(8,128)(2,1)}, u32[]{:S(2)}) copy-start(bf16[256,256]{1,0:T(8,128)(2,1)} %get-tuple-element.25.q0) | copy-start | bytes 393220
  42.4 39.1 %collective-permute-start.10 = (bf16[4,512,256]{2,1,0:T(8,128)(2,1)S(1)}, bf16[4,512,256]{2,1,0:T(8,128)(2,1)S(1)}, u32[]{:S(2)}, u32[]{:S(2)}) collective-permute-start(bf16[4,512,256]{2,1,0:T(8,128)(2,1)S(1)} %pad_maximum_fusion.1.kv_ref), channel_id=1, source_target_pairs={{0,4},{4,0},{1,5},{5,1},{2,6},{6,2},{3,7},{7,3},{8,12},{12,8},{9,1... | collective-permute-start | bytes 3145736 | tf_op jit(solution)/shard_map/ppermute | solution.py:321
  49.4 7.7 %collective-permute-start.8 = (bf16[512,256]{1,0:T(8,128)(2,1)S(1)}, bf16[512,256]{1,0:T(8,128)(2,1)S(1)}, u32[]{:S(2)}, u32[]{:S(2)}) collective-permute-start(bf16[512,256]{1,0:T(8,128)(2,1)S(1)} %slice_bitcast_fusion), channel_id=1, source_target_pairs={{0,32},{4,228},{32,64},{36,4},{64,96},{68,36},{96,128},{100,68},{1... | collective-permute-start | bytes 786440 | tf_op jit(solution)/shard_map/ppermute | solution.py:360
  49.6 14.7 %collective-permute-start.11 = (bf16[128,2048]{1,0:T(8,128)(2,1)S(1)}, bf16[128,2048]{1,0:T(8,128)(2,1)S(1)}, u32[]{:S(2)}, u32[]{:S(2)}) collective-permute-start(bf16[128,2048]{1,0:T(8,128)(2,1)S(1)} %constant_dynamic-slice_fusion), channel_id=1, source_target_pairs={{0,1},{1,2},{2,3},{3,0},{4,5},{5,6},{6,7},{7,4},{8,9},{9,10},{10,1... | collective-permute-start | bytes 1572872 | tf_op jit(solution)/shard_map/ppermute | solution.py:321
  51.2 24.5 %collective-permute-start.12 = (bf16[128,2048]{1,0:T(8,128)(2,1)S(1)}, bf16[128,2048]{1,0:T(8,128)(2,1)S(1)}, u32[]{:S(2)}, u32[]{:S(2)}) collective-permute-start(bf16[128,2048]{1,0:T(8,128)(2,1)S(1)} %constant_dynamic-slice_fusion), channel_id=1, source_target_pairs={{0,2},{1,3},{2,0},{3,1},{4,6},{5,7},{6,4},{7,5},{8,10},{9,11},{10,... | collective-permute-start | bytes 1572872 | tf_op jit(solution)/shard_map/ppermute | solution.py:321
  53.9 21.8 %collective-permute-start.13 = (bf16[128,2048]{1,0:T(8,128)(2,1)S(1)}, bf16[128,2048]{1,0:T(8,128)(2,1)S(1)}, u32[]{:S(2)}, u32[]{:S(2)}) collective-permute-start(bf16[128,2048]{1,0:T(8,128)(2,1)S(1)} %constant_dynamic-slice_fusion), channel_id=1, source_target_pairs={{0,3},{1,0},{2,1},{3,2},{4,7},{5,4},{6,5},{7,6},{8,11},{9,8},{10,9... | collective-permute-start | bytes 1572872 | tf_op jit(solution)/shard_map/ppermute | solution.py:321
  57.1 1.5 collective-permute-start.3
  58.6 33.0 %collective-permute-start.9 = (bf16[3,512,256]{2,1,0:T(8,128)(2,1)S(1)}, bf16[3,512,256]{2,1,0:T(8,128)(2,1)S(1)}, u32[]{:S(2)}, u32[]{:S(2)}) collective-permute-start(bf16[3,512,256]{2,1,0:T(8,128)(2,1)S(1)} %pad_maximum_fusion.2.kv_ref), channel_id=1, source_target_pairs={{0,4},{4,0},{1,5},{5,1},{2,6},{6,2},{3,7},{7,3},{8,12},{12,8},{9,1... | collective-permute-start | bytes 2359304 | tf_op jit(solution)/shard_map/ppermute | solution.py:321
  75.9 29.6 %collective-permute-start.14 = (bf16[3,128,2048]{2,1,0:T(8,128)(2,1)S(1)}, bf16[3,128,2048]{2,1,0:T(8,128)(2,1)}, u32[]{:S(2)}, u32[]{:S(2)}) collective-permute-start(bf16[3,128,2048]{2,1,0:T(8,128)(2,1)S(1)} %pad_maximum_fusion.mine_ref), channel_id=1, source_target_pairs={{0,4},{4,0},{1,5},{5,1},{2,6},{6,2},{3,7},{7,3},{8,12},{12,8},{9,1... | collective-permute-start | bytes 4718600 | tf_op jit(solution)/shard_map/ppermute | solution.py:321
  87.1 4.6 %copy-start.8 = (f32[2]{0:T(128)S(1)}, f32[2]{0:T(128)}, u32[]{:S(2)}) copy-start(f32[2]{0:T(128)} %lam_ref.1) | copy-start | bytes 28
  97.4 1.1 copy-start.2
  98.5 26.2 %copy-start.5 = (bf16[64,2048]{1,0:T(8,128)(2,1)S(1)}, bf16[64,2048]{1,0:T(8,128)(2,1)}, u32[]{:S(2)}) copy-start(bf16[64,2048]{1,0:T(8,128)(2,1)} %res_ref.1) | copy-start | bytes 786436
  98.5 26.2 %copy-start.6 = (f32[2048]{0:T(1024)S(1)}, f32[2048]{0:T(1024)}, u32[]{:S(2)}) copy-start(f32[2048]{0:T(1024)} %param.21) | copy-start | bytes 24580
  98.5 26.2 %copy-start.7 = (f32[128]{0:T(128)S(1)}, f32[128]{0:T(128)}, u32[]{:S(2)}) copy-start(f32[128]{0:T(128)} %param.19) | copy-start | bytes 1540
  98.5 26.1 %all-to-all-start = ((bf16[16,64,640]{2,1,0:T(8,128)(2,1)}), bf16[16,64,640]{2,1,0:T(8,128)(2,1)S(1)}, u32[]{:S(2)}, u32[]{:S(2)}) async-start(bf16[16,64,640]{2,1,0:T(8,128)(2,1)} %bitcast.21), calls=%async_computation | async-start | bytes 2621440 | tf_op jit(solution)/shard_map/all_to_all | solution.py:367
  124.6 1.2 copy-start.4
  129.3 7.9 %collective-permute-start.15 = (bf16[64,2048]{1,0:T(8,128)(2,1)S(1)}, bf16[64,2048]{1,0:T(8,128)(2,1)S(1)}, u32[]{:S(2)}, u32[]{:S(2)}) collective-permute-start(bf16[64,2048]{1,0:T(8,128)(2,1)S(1)} %merge.1.refs_0_), channel_id=1, source_target_pairs={{0,1},{1,2},{2,3},{3,0},{4,5},{5,6},{6,7},{7,4},{8,9},{9,10},{10,1... | collective-permute-start | bytes 786440 | tf_op jit(solution)/shard_map/ppermute | solution.py:321
  129.9 7.5 %collective-permute-start.16 = (bf16[64,2048]{1,0:T(8,128)(2,1)S(1)}, bf16[64,2048]{1,0:T(8,128)(2,1)S(1)}, u32[]{:S(2)}, u32[]{:S(2)}) collective-permute-start(bf16[64,2048]{1,0:T(8,128)(2,1)S(1)} %merge.1.refs_0_), channel_id=1, source_target_pairs={{0,3},{1,0},{2,1},{3,2},{4,7},{5,4},{6,5},{7,6},{8,11},{9,8},{10,9... | collective-permute-start | bytes 786440 | tf_op jit(solution)/shard_map/ppermute | solution.py:321
  137.2 6.5 %collective-permute-start.18 = (bf16[32,2048]{1,0:T(8,128)(2,1)S(1)}, bf16[32,2048]{1,0:T(8,128)(2,1)S(1)}, u32[]{:S(2)}, u32[]{:S(2)}) collective-permute-start(bf16[32,2048]{1,0:T(8,128)(2,1)S(1)} %slice.13), channel_id=1, source_target_pairs={{0,1},{1,2},{2,3},{3,0},{4,5},{5,6},{6,7},{7,4},{8,9},{9,10},{10,1... | collective-permute-start | bytes 393224 | tf_op jit(solution)/shard_map/ppermute | solution.py:321
  137.5 6.1 %collective-permute-start.19 = (bf16[32,2048]{1,0:T(8,128)(2,1)S(1)}, bf16[32,2048]{1,0:T(8,128)(2,1)S(1)}, u32[]{:S(2)}, u32[]{:S(2)}) collective-permute-start(bf16[32,2048]{1,0:T(8,128)(2,1)S(1)} %slice.14), channel_id=1, source_target_pairs={{0,3},{1,0},{2,1},{3,2},{4,7},{5,4},{6,5},{7,6},{8,11},{9,8},{10,9... | collective-permute-start | bytes 393224 | tf_op jit(solution)/shard_map/ppermute | solution.py:321
  143.7 3.4 %copy-start = (bf16[128,32,1024]{2,1,0:T(8,128)(2,1)S(1)}, bf16[128,32,1024]{2,1,0:T(8,128)(2,1)}, u32[]{:S(2)}) copy-start(bf16[128,32,1024]{2,1,0:T(8,128)(2,1)} %all-gather.3.cloned.1.call-done) | copy-start | bytes 25165828
  147.1 3.8 %copy-start.1 = (bf16[128,32,1024]{2,1,0:T(8,128)(2,1)S(1)}, bf16[128,32,1024]{2,1,0:T(8,128)(2,1)}, u32[]{:S(2)}) copy-start(bf16[128,32,1024]{2,1,0:T(8,128)(2,1)} %all-gather.3.cloned.1.call-done) | copy-start | bytes 25165828
  149.2 10.7 %collective-permute-start.20 = (bf16[64,2048]{1,0:T(8,128)(2,1)S(1)}, bf16[64,2048]{1,0:T(8,128)(2,1)S(1)}, u32[]{:S(2)}, u32[]{:S(2)}) collective-permute-start(bf16[64,2048]{1,0:T(8,128)(2,1)S(1)} %mixer.3), channel_id=1, source_target_pairs={{0,2},{1,3},{2,0},{3,1},{4,6},{5,7},{6,4},{7,5},{8,10},{9,11},{10,... | collective-permute-start | bytes 786440 | tf_op jit(solution)/shard_map/ppermute | solution.py:321
  153.2 8.2 %collective-permute-start.17 = (bf16[64,2048]{1,0:T(8,128)(2,1)S(1)}, bf16[64,2048]{1,0:T(8,128)(2,1)S(1)}, u32[]{:S(2)}, u32[]{:S(2)}) collective-permute-start(bf16[64,2048]{1,0:T(8,128)(2,1)S(1)} %get-tuple-element.43), channel_id=1, source_target_pairs={{0,3},{1,0},{2,1},{3,2},{4,7},{5,4},{6,5},{7,6},{8,11},{9,8},{10,9... | collective-permute-start | bytes 786440 | tf_op jit(solution)/shard_map/ppermute | solution.py:321
  156.2 7.6 %collective-permute-start.21 = (bf16[64,2048]{1,0:T(8,128)(2,1)S(1)}, bf16[64,2048]{1,0:T(8,128)(2,1)S(1)}, u32[]{:S(2)}, u32[]{:S(2)}) collective-permute-start(bf16[64,2048]{1,0:T(8,128)(2,1)S(1)} %get-tuple-element.44), channel_id=1, source_target_pairs={{0,1},{1,2},{2,3},{3,0},{4,5},{5,6},{6,7},{7,4},{8,9},{9,10},{10,1... | collective-permute-start | bytes 786440 | tf_op jit(solution)/shard_map/ppermute | solution.py:321
Sparse Core Ops, SparseCore 0:
  10.1 84.9 all-gather.2

commit v4 on v3

--- a/solution.py
+++ b/solution.py
@@ -16,15 +16,15 @@
 LOG2E = 1.4426950408889634
 NT = (((1,), (1,)), ((), ()))
 NN = (((1,), (0,)), ((), ()))
-ANY = pl.BlockSpec(memory_space=pl.ANY)
+HBM = pl.BlockSpec(memory_space=pltpu.HBM)
 SMEM = pl.BlockSpec(memory_space=pltpu.SMEM)
 VMEM = pl.BlockSpec(memory_space=pltpu.VMEM)
 WIDE = 5 * VD
 
 
 def prep_kernel(cos_ref, sin_ref, qa_ref, qb_ref, ka_ref, kb_ref, v_ref, q_out, kv_out, q_own, kv_own):
-    cos = cos_ref[...]
-    sin = sin_ref[...]
+    cos = jnp.concatenate([cos_ref[...]] * 4, axis=1)
+    sin = jnp.concatenate([-sin_ref[...], sin_ref[...]] * 2, axis=1)
     lane = lax.broadcasted_iota(jnp.int32, cos.shape, 1)
     front = (lane % HEAD) < HEAD // 2
 
@@ -48,8 +48,6 @@
     inverse = 10000.0 ** (-jnp.arange(0, half, dtype=F32) * 2.0 / HEAD)
     angle = positions[:, None] * inverse[None, :]
     cos, sin = jnp.cos(angle), jnp.sin(angle)
-    cos4 = jnp.concatenate([cos] * 4, axis=1)
-    sin4 = jnp.concatenate([-sin, sin, -sin, sin], axis=1)
     return pl.pallas_call(
         prep_kernel,
         out_shape=(
@@ -60,7 +58,7 @@
         in_specs=[VMEM] * 7,
         out_specs=(VMEM,) * 4,
         name="prep",
-    )(cos4, sin4, first_query, second_query, first_key, second_key, values)
+    )(cos, sin, first_query, second_query, first_key, second_key, values)
 
 
 def three_parts(value):
@@ -83,7 +81,7 @@
                 qs[o, 2 * h + m, :, 128:256] = jnp.where(mine, lo, 0.0).astype(BF16)
 
 
-def absorb(chunks, qs, sc, acc, top, tot, fresh):
+def absorb(chunks, qs, sc, acc, top, tot, fresh, block_done=None):
     def scores(slot, o, hm):
         m = hm % 2
         keys = jnp.concatenate([c[0:TOK, m * 128 : (m + 1) * 128] for c in chunks], axis=0)
@@ -115,24 +113,11 @@
             else:
                 tot[o, hm] = tot[o, hm] * shrink + total
                 acc[o, hm] = acc[o, hm] * shrink + moved
+        if block_done is not None:
+            block_done(o)
         return peak
 
     lax.fori_loop(0, 4, step, scores(0, 0, 0))
-
-
-def finish(x_ref, lam_ref, out_ref, stat, acc, top, tot):
-    stat[...] = jnp.zeros_like(stat)
-    for h in range(2):
-        for i, part in enumerate(three_parts(jnp.full((1, TOK), lam_ref[h], F32))):
-            stat[12 + 3 * h + i : 13 + 3 * h + i, :] = part
-    for o in range(4):
-        home = (x_ref[0] + 4 - o) % 4
-        for hm in range(4):
-            total = tot[o, hm]
-            out_ref[home, :, hm * VD : (hm + 1) * VD] = (acc[o, hm] / total).T.astype(BF16)
-            for i, part in enumerate(three_parts(top[o, hm] + jnp.log2(total))):
-                stat[3 * hm + i : 3 * hm + i + 1, :] = part
-        out_ref[home, :, 4 * VD :] = stat[...].T.astype(BF16)
 
 
 STATE = (
@@ -156,12 +141,34 @@
     absorb(chunks_of(kv_ref), qs, sc, acc, top, tot, False)
 
 
-def last_kernel(x_ref, lam_ref, qs, kv_ref, acc_in, top_in, tot_in, out_ref, acc, top, tot, sc, stat):
+def last_kernel(
+    x_ref, lam_ref, qs, kv_ref, acc_in, top_in, tot_in, out_ref, acc, top, tot, sc, stat, buf, sem
+):
     acc[...] = acc_in[...]
     top[...] = top_in[...]
     tot[...] = tot_in[...]
-    absorb(chunks_of(kv_ref), qs, sc, acc, top, tot, False)
-    finish(x_ref, lam_ref, out_ref, stat, acc, top, tot)
+    stat[...] = jnp.zeros_like(stat)
+    for h in range(2):
+        for i, part in enumerate(three_parts(jnp.full((1, TOK), lam_ref[h], F32))):
+            stat[12 + 3 * h + i : 13 + 3 * h + i, :] = part
+
+    def sending(o):
+        home = (x_ref[0] + 4 - o) % 4
+        return pltpu.make_async_copy(buf.at[o], out_ref.at[pl.ds(4 * home, 4)], sem.at[o])
+
+    def block_done(o):
+        for hm in range(4):
+            total = tot[o, hm]
+            mean = (acc[o, hm] / total).T.astype(BF16)
+            buf[o, :, :, hm * VD : (hm + 1) * VD] = mean.reshape(4, TOK // 4, VD)
+            for i, part in enumerate(three_parts(top[o, hm] + jnp.log2(total))):
+                stat[3 * hm + i : 3 * hm + i + 1, :] = part
+        buf[o, :, :, 4 * VD :] = stat[...].T.astype(BF16).reshape(4, TOK // 4, VD)
+        sending(o).start()
+
+    absorb(chunks_of(kv_ref), qs, sc, acc, top, tot, False, block_done)
+    for o in range(4):
+        sending(o).wait()
 
 
 def cost(keys):
@@ -190,14 +197,15 @@
 
 
 def attend_next(qs, kv, state):
+    keys = kv.shape[0] * TOK if len(kv.shape) == 3 else kv.shape[0] // 2
     return pl.pallas_call(
         next_kernel,
         out_shape=STATE,
         in_specs=[VMEM] * 5,
         out_specs=(VMEM,) * 3,
         input_output_aliases={2: 0, 3: 1, 4: 2},
-        scratch_shapes=[score_scratch(kv.shape[0])],
-        cost_estimate=cost(kv.shape[0] * TOK),
+        scratch_shapes=[score_scratch(keys // TOK)],
+        cost_estimate=cost(keys),
         compiler_params=pltpu.CompilerParams(vmem_limit_bytes=24 * 2**20),
         name="attend_next",
     )(qs, kv, *state)
@@ -206,27 +214,57 @@
 def attend_last(x, lambdas, qs, kv, state):
     return pl.pallas_call(
         last_kernel,
-        out_shape=jax.ShapeDtypeStruct((4, TOK, WIDE), BF16),
+        out_shape=jax.ShapeDtypeStruct((16, TOK // 4, WIDE), BF16),
         in_specs=[SMEM, SMEM] + [VMEM] * 5,
-        out_specs=VMEM,
+        out_specs=HBM,
         scratch_shapes=[pltpu.VMEM(s.shape, s.dtype) for s in STATE]
-        + [score_scratch(kv.shape[0]), pltpu.VMEM((VD, TOK), F32)],
-        cost_estimate=cost(kv.shape[0] * TOK),
+        + [
+            score_scratch(kv.shape[0] // (2 * TOK)),
+            pltpu.VMEM((VD, TOK), F32),
+            pltpu.VMEM((4, 4, TOK // 4, WIDE), BF16),
+            pltpu.SemaphoreType.DMA((4,)),
+        ],
+        cost_estimate=cost(kv.shape[0] // 2),
         compiler_params=pltpu.CompilerParams(vmem_limit_bytes=24 * 2**20),
         name="attend_last",
     )(x, lambdas, qs, kv, *state)
 
 
-def merge_kernel(at_ref, part_ref, gain_ref, res_ref, norm_ref, own_ref, mine_ref, other_ref, out_ref, wbuf, sem):
+def load_mix_kernel(w_ref, out_ref, sem):
+    cuts = 4
+    per = w_ref.shape[0] // cuts
+    copies = []
+    for i in range(cuts):
+        rows = pl.ds(i * per, per)
+        copies.append(pltpu.make_async_copy(w_ref.at[rows], out_ref.at[rows], sem.at[i]))
+        copies[-1].start()
+    for copy in copies:
+        copy.wait()
+
+
+def load_mix(weights):
+    return pl.pallas_call(
+        load_mix_kernel,
+        out_shape=jax.ShapeDtypeStruct(weights.shape, BF16),
+        in_specs=[HBM],
+        out_specs=VMEM,
+        scratch_shapes=[pltpu.SemaphoreType.DMA((4,))],
+        compiler_params=pltpu.CompilerParams(vmem_limit_bytes=20 * 2**20),
+        name="load_mix",
+    )(weights)
+
+
+def merge_kernel(
+    at_ref, part_ref, gain_ref, res_ref, norm_ref, own_ref, mine_ref, other_ref, out_ref, wbuf, sem
+):
+    mine = at_ref[1] * VD
     copies = [[pltpu.make_async_copy(own_ref, wbuf.at[0], sem.at[0])]]
-    mine = at_ref[1] * VD
     for o in range(3):
+        near, far = pl.ds(mine, VD), pl.ds(VD - mine, VD)
         copies.append(
             [
-                pltpu.make_async_copy(mine_ref.at[o], wbuf.at[o + 1, pl.ds(mine, VD)], sem.at[2 * o + 1]),
-                pltpu.make_async_copy(
-                    other_ref.at[o], wbuf.at[o + 1, pl.ds(VD - mine, VD)], sem.at[2 * o + 2]
-                ),
+                pltpu.make_async_copy(mine_ref.at[o], wbuf.at[o + 1, near], sem.at[2 * o + 1]),
+                pltpu.make_async_copy(other_ref.at[o], wbuf.at[o + 1, far], sem.at[2 * o + 2]),
             ]
         )
     for pair in copies:
@@ -272,7 +310,7 @@
     return pl.pallas_call(
         merge_kernel,
         out_shape=jax.ShapeDtypeStruct((rows, width), BF16),
-        in_specs=[SMEM] + [VMEM] * 4 + [ANY] * 3,
+        in_specs=[SMEM] + [VMEM] * 4 + [HBM] * 3,
         out_specs=VMEM,
         scratch_shapes=[pltpu.VMEM((4, 2 * VD, width), BF16), pltpu.SemaphoreType.DMA((7,))],
         compiler_params=pltpu.CompilerParams(vmem_limit_bytes=24 * 2**20),
@@ -357,15 +395,17 @@
     four = jnp.concatenate([near, second])
     four_other = shifted(four, "c", 1)
     state = attend_next(qs, four, state)
+    state = attend_next(qs, four_other, state)
     far = lax.ppermute(third[0], ring, onward)
-    state = attend_next(qs, four_other, state)
-    three = jnp.concatenate([third, far[None]])
-    three_other = shifted(three, "c", 1)
-    state = attend_next(qs, three, state)
-    part = attend_last(x, lambdas, qs, three_other, state)
-    part = part.reshape(16, 64, WIDE)
+    third_other = shifted(third, "c", 1)
+    state = attend_next(qs, third, state)
+    state = attend_next(qs, third_other, state)
+    far_other = shifted(far, "c", 1)
+    state = attend_next(qs, far, state)
+    part = attend_last(x, lambdas, qs, far_other, state)
     part = lax.all_to_all(part, ("x", "tp"), split_axis=0, concat_axis=0, tiled=True)
     normed = merge(at, part, head_gain, residual, norm_gain, out_weights)
+    mix_weights = load_mix(mix_weights)
     rows = normed.shape[0] // 2
     before = shifted(normed, "tp", 1)
     after = shifted(normed, "tp", -1)

time: 173 us -> 170 us (0.983)
  Pallas kernels: 35.6 us -> 40.2 us
  starting transfers between devices: 35.6 us -> 31.3 us
  waiting for transfers between devices: 76.4 us -> 73.4 us
    ppermute x17 -> x18, waiting for transfers between devices: 29.4 us -> 37.5 us  [shifted(): lax.ppermute(value, axis, [(i, (i + by) % size) for i in range(size)])]
    ppermute x1, waiting for transfers between devices: 12.2 us -> 6.63 us  [local(): second = lax.ppermute(near, ring, onward)]
    pallas_call x3 -> x5, Pallas kernels: 15.6 us -> 21 us  [attend_next(): pl.pallas_call(next_kernel, out_shape=STATE, in_specs=[VMEM] * 5, out_spe...]
    ppermute x1, waiting for transfers between devices: 6.91 us -> 3.12 us  [local(): third = lax.ppermute(second, ring, onward)]
    all_to_all x1, starting transfers between devices: 7 us -> 5.13 us  [local(): lax.all_to_all(part, ('x', 'tp'), split_axis=0, concat_axis=0, tiled=True)]
    ppermute x17 -> x18, starting transfers between devices: 22.4 us -> 20.6 us  [shifted(): lax.ppermute(value, axis, [(i, (i + by) % size) for i in range(size)])]
    pallas_call x1 -> x2, Pallas kernels: 5.7 us -> 4.68 us  [the longest x1 4.08 us: attend_last(): pl.pallas_call(last_kernel, out_shape=jax.ShapeDtypeStruct((16, TOK // 4,...]
    unnamed x24 -> x20, local copies, waits for them, and re-layouts: 5.7 us -> 5.69 us
  transfers between devices with their start and end apart: 24 -> 25, of which waited for: 13 -> 12; matrix products, arithmetic and copies ran while one was open for 1% -> 2% of each run, Pallas kernels for 20% -> 22%
where the time goes in v4:
time: 170 us
  waiting for transfers between devices  73.4 us (43%)
  Pallas kernels  40.2 us (24%)
  starting transfers between devices  31.3 us (18%)
  between operations  13.7 us (8%)
  local copies, waits for them, and re-layouts  5.77 us (3%)
  other arithmetic  5.14 us (3%)
    ppermute x18, waiting for transfers between devices, shifted(): lax.ppermute(value, axis, [(i, (i + by) % size) for i in range(size)])  37.5 us
    pallas_call x5, Pallas kernels, attend_next(): pl.pallas_call(next_kernel, out_shape=STATE, in_specs=[VMEM] * 5, out_spe...  21 us
    ppermute x18, starting transfers between devices, shifted(): lax.ppermute(value, axis, [(i, (i + by) % size) for i in range(size)])  20.6 us
    all_to_all x1, waiting for transfers between devices, local(): lax.all_to_all(part, ('x', 'tp'), split_axis=0, concat_axis=0, tiled=True)  18.4 us
    ppermute x2, waiting for transfers between devices, local(): near = [lax.ppermute(kv, ring, onward), lax.ppermute(kv, ring, crossed)]  7.79 us
    ppermute x1, waiting for transfers between devices, local(): second = lax.ppermute(near, ring, onward)  6.63 us
    unnamed x20, local copies, waits for them, and re-layouts  5.69 us
    ppermute x2, starting transfers between devices, local(): near = [lax.ppermute(kv, ring, onward), lax.ppermute(kv, ring, crossed)]  5.3 us
  transfers between devices with their start and end apart: 25, of which 12 were waited for; matrix products, arithmetic and copies ran while one was open for 2% of the time, Pallas kernels for 22%

profile of v4, /device:TPU:2, one launch (start us, length us, event | category | flops | bytes accessed | tf_op | source)
XLA Modules:
  0.0 169.6 jit_solution(18027958521427484112)
XLA Ops:
  6.5 1.5 pad_maximum_fusion.4
  8.1 1.3 multiply_sine_fusion
  9.4 2.5 %prep.1 = (bf16[256,256]{1,0:T(8,128)(2,1)}, bf16[512,256]{1,0:T(8,128)(2,1)}, bf16[256,256]{1,0:T(8,128)(2,1)}, bf16[512,256]{1,0:T(8,128)(2,1)}) custom-call(f32[256,32]{1,0:T(8,128)} %get-tuple-element.58.cos_ref, f32[256,32]{1,0:T(8,128)} %get-tuple-element.57.sin_ref, bf16[256,128]{1,0:T(8,128)(2,1)} %qa_ref.1, bf16[256,128]{1,0:T(8,128)(2,1)} %qb_ref.1, ...), custom_call_target="tpu_custom_call" | custom-call | tf_op jit(solution)/shard_map/prep/pallas_call | solution.py:51
  11.9 5.3 %collective-permute-start.5 = (bf16[512,256]{1,0:T(8,128)(2,1)}, bf16[512,256]{1,0:T(8,128)(2,1)S(1)}, u32[]{:S(2)}, u32[]{:S(2)}) collective-permute-start(bf16[512,256]{1,0:T(8,128)(2,1)} %get-tuple-element.34), channel_id=1, source_target_pairs={{0,228},{4,32},{32,4},{36,64},{64,36},{68,96},{96,68},{100,128},{1... | collective-permute-start | bytes 786440 | tf_op jit(solution)/shard_map/ppermute | solution.py:383
  17.2 6.4 %collective-permute-done.5 = bf16[512,256]{1,0:T(8,128)(2,1)S(1)} collective-permute-done((bf16[512,256]{1,0:T(8,128)(2,1)}, bf16[512,256]{1,0:T(8,128)(2,1)S(1)}, u32[]{:S(2)}, u32[]{:S(2)}) %collective-permute-start.5) | collective-permute-done | bytes 262176 | tf_op jit(solution)/shard_map/ppermute | solution.py:383
  23.7 1.3 collective-permute-done.4
  25.2 1.6 collective-permute-start
  26.7 1.1 collective-permute-start.1
  27.9 2.2 %collective-permute-start.2 = (bf16[256,256]{1,0:T(8,128)(2,1)}, bf16[256,256]{1,0:T(8,128)(2,1)S(1)}, u32[]{:S(2)}, u32[]{:S(2)}) collective-permute-start(bf16[256,256]{1,0:T(8,128)(2,1)} %get-tuple-element.32), channel_id=1, source_target_pairs={{0,24},{8,0},{16,8},{24,16},{1,25},{9,1},{17,9},{25,17},{2,26},{10... | collective-permute-start | bytes 393224 | tf_op jit(solution)/shard_map/ppermute | solution.py:359
  30.0 0.8 collective-permute-start.3
  30.9 6.6 %collective-permute-done.6 = bf16[2,512,256]{2,1,0:T(8,128)(2,1)} collective-permute-done((bf16[2,512,256]{2,1,0:T(8,128)(2,1)S(1)}, bf16[2,512,256]{2,1,0:T(8,128)(2,1)}, u32[]{:S(2)}, u32[]{:S(2)}) %collective-permute-start.6) | collective-permute-done | bytes 524320 | tf_op jit(solution)/shard_map/ppermute | solution.py:390
  37.5 1.1 pad_maximum_fusion.1.kv_ref
  38.9 3.0 %collective-permute-start.14 = (bf16[128,2048]{1,0:T(8,128)(2,1)S(1)}, bf16[128,2048]{1,0:T(8,128)(2,1)S(1)}, u32[]{:S(2)}, u32[]{:S(2)}) collective-permute-start(bf16[128,2048]{1,0:T(8,128)(2,1)S(1)} %constant_dynamic-slice_fusion), channel_id=1, source_target_pairs={{0,3},{1,0},{2,1},{3,2},{4,7},{5,4},{6,5},{7,6},{8,11},{9,8},{10,9... | collective-permute-start | bytes 1572872 | tf_op jit(solution)/shard_map/ppermute | solution.py:359
  41.9 0.7 collective-permute-start.13
  42.7 1.0 collective-permute-start.12
  43.6 4.1 %attend_first.1 = (bf16[4,4,256,256]{3,2,1,0:T(8,128)(2,1)S(1)}, f32[4,4,128,256]{3,2,1,0:T(8,128)S(1)}, f32[4,4,1,256]{3,2,1,0:T(1,128)S(1)}, f32[4,4,1,256]{3,2,1,0:T(1,128)S(1)}) custom-call(bf16[256,256]{1,0:T(8,128)(2,1)S(1)} %copy-done.9, bf16[256,256]{1,0:T(8,128)(2,1)S(1)} %collective-permute-done.q1, ...), custom_call_target="tpu_custom_call" | custom-call | flops 805306368 | bytes 524288 | tf_op jit(solution)/shard_map/attend_first/pallas_call | solution.py:187
  47.7 3.1 %collective-permute-done.7.kv_ref = bf16[2,512,256]{2,1,0:T(8,128)(2,1)S(1)} collective-permute-done((bf16[2,512,256]{2,1,0:T(8,128)(2,1)}, bf16[2,512,256]{2,1,0:T(8,128)(2,1)S(1)}, u32[]{:S(2)}, u32[]{:S(2)}) %collective-permute-start.7) | collective-permute-done | bytes 524320 | tf_op jit(solution)/shard_map/ppermute | solution.py:394
  50.9 14.0 %collective-permute-done.14 = bf16[128,2048]{1,0:T(8,128)(2,1)S(1)} collective-permute-done((bf16[128,2048]{1,0:T(8,128)(2,1)S(1)}, bf16[128,2048]{1,0:T(8,128)(2,1)S(1)}, u32[]{:S(2)}, u32[]{:S(2)}) %collective-permute-start.14) | collective-permute-done | bytes 524320 | tf_op jit(solution)/shard_map/ppermute | solution.py:359
  65.0 3.7 %collective-permute-done.12 = bf16[128,2048]{1,0:T(8,128)(2,1)S(1)} collective-permute-done((bf16[128,2048]{1,0:T(8,128)(2,1)S(1)}, bf16[128,2048]{1,0:T(8,128)(2,1)S(1)}, u32[]{:S(2)}, u32[]{:S(2)}) %collective-permute-start.12) | collective-permute-done | bytes 524320 | tf_op jit(solution)/shard_map/ppermute | solution.py:359
  68.8 0.2 collective-permute-start.15
  69.0 5.4 %attend_next.5 = (f32[4,4,128,256]{3,2,1,0:T(8,128)S(1)}, f32[4,4,1,256]{3,2,1,0:T(1,128)S(1)}, f32[4,4,1,256]{3,2,1,0:T(1,128)S(1)}) custom-call(bf16[4,4,256,256]{3,2,1,0:T(8,128)(2,1)S(1)} %get-tuple-element.35.qs, bf16[4,512,256]{2,1,0:T(8,128)(2,1)S(1)} %pad_maximum_fusion.1.kv_ref, ...), custom_call_target="tpu_custom_call", output_to_operand_aliasing={{0}: (2, {}), {1}: (3, {}), {2}: (4, {})} | custom-call | flops 1610612736 | bytes 1048576 | tf_op jit(solution)/shard_map/attend_next/pallas_call | solution.py:201
  74.5 0.5 collective-permute-start.9
  75.0 5.4 %attend_next.6 = (f32[4,4,128,256]{3,2,1,0:T(8,128)S(1)}, f32[4,4,1,256]{3,2,1,0:T(1,128)S(1)}, f32[4,4,1,256]{3,2,1,0:T(1,128)S(1)}) custom-call(bf16[4,4,256,256]{3,2,1,0:T(8,128)(2,1)S(1)} %get-tuple-element.35.qs, bf16[4,512,256]{2,1,0:T(8,128)(2,1)S(1)} %collective-permute-done.11.kv_ref, ...), custom_call_target="tpu_custom_call", output_to_operand_aliasing={{0}: (2, {}), {1}: (3, {}), {2}: (4, {})} | custom-call | flops 1610612736 | bytes 1048576 | tf_op jit(solution)/shard_map/attend_next/pallas_call | solution.py:201
  80.4 3.7 %attend_next.7 = (f32[4,4,128,256]{3,2,1,0:T(8,128)S(1)}, f32[4,4,1,256]{3,2,1,0:T(1,128)S(1)}, f32[4,4,1,256]{3,2,1,0:T(1,128)S(1)}) custom-call(bf16[4,4,256,256]{3,2,1,0:T(8,128)(2,1)S(1)} %get-tuple-element.35.qs, bf16[2,512,256]{2,1,0:T(8,128)(2,1)S(1)} %collective-permute-done.7.kv_ref, ...), custom_call_target="tpu_custom_call", output_to_operand_aliasing={{0}: (2, {}), {1}: (3, {}), {2}: (4, {})} | custom-call | flops 805306368 | bytes 524288 | tf_op jit(solution)/shard_map/attend_next/pallas_call | solution.py:201
  84.1 3.7 %attend_next.8 = (f32[4,4,128,256]{3,2,1,0:T(8,128)S(1)}, f32[4,4,1,256]{3,2,1,0:T(1,128)S(1)}, f32[4,4,1,256]{3,2,1,0:T(1,128)S(1)}) custom-call(bf16[4,4,256,256]{3,2,1,0:T(8,128)(2,1)S(1)} %get-tuple-element.35.qs, bf16[2,512,256]{2,1,0:T(8,128)(2,1)S(1)} %collective-permute-done.10.kv_ref, ...), custom_call_target="tpu_custom_call", output_to_operand_aliasing={{0}: (2, {}), {1}: (3, {}), {2}: (4, {})} | custom-call | flops 805306368 | bytes 524288 | tf_op jit(solution)/shard_map/attend_next/pallas_call | solution.py:201
  87.8 2.8 %attend_next.9 = (f32[4,4,128,256]{3,2,1,0:T(8,128)S(1)}, f32[4,4,1,256]{3,2,1,0:T(1,128)S(1)}, f32[4,4,1,256]{3,2,1,0:T(1,128)S(1)}) custom-call(bf16[4,4,256,256]{3,2,1,0:T(8,128)(2,1)S(1)} %get-tuple-element.35.qs, bf16[512,256]{1,0:T(8,128)(2,1)S(1)} %collective-permute-done.8.kv_ref, ...), custom_call_target="tpu_custom_call", output_to_operand_aliasing={{0}: (2, {}), {1}: (3, {}), {2}: (4, {})} | custom-call | flops 402653184 | bytes 262144 | tf_op jit(solution)/shard_map/attend_next/pallas_call | solution.py:201
  90.6 4.1 %attend_last.1 = bf16[16,64,640]{2,1,0:T(8,128)(2,1)S(1)} custom-call(s32[1]{0:T(128)} %bitcast.2.x_ref, f32[2]{0:T(128)S(1)} %copy-done.6, bf16[4,4,256,256]{3,2,1,0:T(8,128)(2,1)S(1)} %get-tuple-element.35.qs, bf16[512,256]{1,0:T(8,128)(2,1)S(1)} %collective-permute-done.9.kv_ref, f32[4,4,128,256]{3,2,1,0:T(8,128)S(1)} %get-tuple-element.51.acc_in, ...), custom_call_target="tpu_custom_call" | custom-call | flops 402653184 | bytes 262144 | tf_op jit(solution)/shard_map/attend_last/pallas_call | solution.py:215
  94.7 1.1 copy-done.1
  95.8 5.1 %all-to-all-start = ((bf16[16,64,640]{2,1,0:T(8,128)(2,1)}), bf16[16,64,640]{2,1,0:T(8,128)(2,1)S(1)}, u32[]{:S(2)}, u32[]{:S(2)}) async-start(bf16[16,64,640]{2,1,0:T(8,128)(2,1)} %copy-done.1), calls=%async_computation | async-start | bytes 2621440 | tf_op jit(solution)/shard_map/all_to_all | solution.py:406
  101.0 18.4 %all-to-all-done.part_ref = bf16[16,64,640]{2,1,0:T(8,128)(2,1)S(1)} async-done(((bf16[16,64,640]{2,1,0:T(8,128)(2,1)}), bf16[16,64,640]{2,1,0:T(8,128)(2,1)S(1)}, u32[]{:S(2)}, u32[]{:S(2)}) %all-to-all-start) | async-done | bytes 1310752 | tf_op jit(solution)/shard_map/all_to_all | solution.py:406
  119.4 1.2 copy-done.3
  120.6 3.5 %merge.1.refs_0_ = bf16[64,2048]{1,0:T(8,128)(2,1)S(1)} custom-call(s32[2]{0:T(128)S(1)} %pad_add_fusion.at_ref, bf16[16,64,640]{2,1,0:T(8,128)(2,1)S(1)} %all-to-all-done.part_ref, f32[1,128]{1,0:T(1,128)S(1)} %bitcast.19, bf16[64,2048]{1,0:T(8,128)(2,1)S(1)} %copy-done.4, f32[1,2048]{1,0:T(1,128)S(1)} %bitcast.18, bf16[256,2048]{1,0:T(8,128)(2,1)S(1)} %copy-done.3, ...), custom_call_target="tpu_custom_call" | custom-call | tf_op jit(solution)/shard_map/merge/pallas_call | solution.py:310
  124.0 1.5 collective-permute-start.17
  125.5 0.6 collective-permute-start.16
  126.1 4.4 %collective-permute-done.17.refs_2_ = bf16[64,2048]{1,0:T(8,128)(2,1)S(1)} collective-permute-done((bf16[64,2048]{1,0:T(8,128)(2,1)S(1)}, bf16[64,2048]{1,0:T(8,128)(2,1)S(1)}, u32[]{:S(2)}, u32[]{:S(2)}) %collective-permute-start.17) | collective-permute-done | bytes 262176 | tf_op jit(solution)/shard_map/ppermute | solution.py:359
  130.6 3.6 %collective-permute-start.20 = (bf16[32,2048]{1,0:T(8,128)(2,1)S(1)}, bf16[32,2048]{1,0:T(8,128)(2,1)S(1)}, u32[]{:S(2)}, u32[]{:S(2)}) collective-permute-start(bf16[32,2048]{1,0:T(8,128)(2,1)S(1)} %slice.14), channel_id=1, source_target_pairs={{0,3},{1,0},{2,1},{3,2},{4,7},{5,4},{6,5},{7,6},{8,11},{9,8},{10,9... | collective-permute-start | bytes 393224 | tf_op jit(solution)/shard_map/ppermute | solution.py:359
  134.2 0.3 collective-permute-start.19
  134.5 2.2 %collective-permute-done.20 = bf16[32,2048]{1,0:T(8,128)(2,1)S(1)} collective-permute-done((bf16[32,2048]{1,0:T(8,128)(2,1)S(1)}, bf16[32,2048]{1,0:T(8,128)(2,1)S(1)}, u32[]{:S(2)}, u32[]{:S(2)}) %collective-permute-start.20) | collective-permute-done | bytes 131104 | tf_op jit(solution)/shard_map/ppermute | solution.py:359
  136.7 4.0 %collective-permute-done.19 = bf16[32,2048]{1,0:T(8,128)(2,1)S(1)} collective-permute-done((bf16[32,2048]{1,0:T(8,128)(2,1)S(1)}, bf16[32,2048]{1,0:T(8,128)(2,1)S(1)}, u32[]{:S(2)}, u32[]{:S(2)}) %collective-permute-start.19) | collective-permute-done | bytes 131104 | tf_op jit(solution)/shard_map/ppermute | solution.py:359
  140.7 3.4 %copy-done = bf16[128,32,1024]{2,1,0:T(8,128)(2,1)S(1)} copy-done((bf16[128,32,1024]{2,1,0:T(8,128)(2,1)S(1)}, bf16[128,32,1024]{2,1,0:T(8,128)(2,1)}, u32[]{:S(2)}) %copy-start) | copy-done | bytes 8388632
  144.1 0.6 load_mix.1.refs_3_.refs_1_
  144.7 2.4 %mixer.2 = (f32[64,2048]{1,0:T(8,128)S(1)}, bf16[64,2048]{1,0:T(8,128)(2,1)S(1)}, bf16[64,2048]{1,0:T(8,128)(2,1)S(1)}) custom-call(bf16[64,2048]{1,0:T(8,128)(2,1)S(1)} %merge.1.refs_0_, bf16[64,2048]{1,0:T(8,128)(2,1)S(1)} %collective-permute-done.16.refs_1_, bf16[64,2048]{1,0:T(8,128)(2,1)S(1)} %collective-permute-done.17.refs_2_, ...), custom_call_target="tpu_custom_call" | custom-call | flops 2147483648 | bytes 8388608 | tf_op jit(solution)/shard_map/mixer/pallas_call | solution.py:346
  147.1 2.1 %mixer.3 = bf16[64,2048]{1,0:T(8,128)(2,1)S(1)} custom-call(bf16[64,2048]{1,0:T(8,128)(2,1)S(1)} %pad_maximum_fusion.3.refs_0_, bf16[64,2,32,1024]{3,2,1,0:T(8,128)(2,1)S(1)} %load_mix.1.refs_3_.refs_1_), custom_call_target="tpu_custom_call" | custom-call | flops 2147483648 | bytes 8388608 | tf_op jit(solution)/shard_map/mixer/pallas_call | solution.py:346
  149.3 1.2 collective-permute-start.21
  150.5 2.2 %collective-permute-start.18 = (bf16[64,2048]{1,0:T(8,128)(2,1)S(1)}, bf16[64,2048]{1,0:T(8,128)(2,1)S(1)}, u32[]{:S(2)}, u32[]{:S(2)}) collective-permute-start(bf16[64,2048]{1,0:T(8,128)(2,1)S(1)} %get-tuple-element.55), channel_id=1, source_target_pairs={{0,3},{1,0},{2,1},{3,2},{4,7},{5,4},{6,5},{7,6},{8,11},{9,8},{10,9... | collective-permute-start | bytes 786440 | tf_op jit(solution)/shard_map/ppermute | solution.py:359
  152.7 6.9 %collective-permute-done.22 = bf16[64,2048]{1,0:T(8,128)(2,1)S(1)} collective-permute-done((bf16[64,2048]{1,0:T(8,128)(2,1)S(1)}, bf16[64,2048]{1,0:T(8,128)(2,1)S(1)}, u32[]{:S(2)}, u32[]{:S(2)}) %collective-permute-start.22) | collective-permute-done | bytes 262176 | tf_op jit(solution)/shard_map/ppermute | solution.py:359
  159.5 2.3 %collective-permute-done.18 = bf16[64,2048]{1,0:T(8,128)(2,1)S(1)} collective-permute-done((bf16[64,2048]{1,0:T(8,128)(2,1)S(1)}, bf16[64,2048]{1,0:T(8,128)(2,1)S(1)}, u32[]{:S(2)}, u32[]{:S(2)}) %collective-permute-start.18) | collective-permute-done | bytes 262176 | tf_op jit(solution)/shard_map/ppermute | solution.py:359
  161.9 0.9 add_convert_fusion
  (49 shorter events, 1.0 us)
Async XLA Ops:
  6.5 134.2 %all-gather.3.cloned.1.call-start = ((), (), s32[]{:S(2)}) async-start(), calls=%async_computation.1 | async-start | bytes 8519680 | tf_op jit(solution)/shard_map/all_gather | solution.py:387
  8.1 30.8 %copy-start.2 = (bf16[256,2048]{1,0:T(8,128)(2,1)S(1)}, bf16[256,2048]{1,0:T(8,128)(2,1)}, u32[]{:S(2)}) copy-start(bf16[256,2048]{1,0:T(8,128)(2,1)} %own_ref.1) | copy-start | bytes 3145732
  11.9 11.7 %collective-permute-start.5 = (bf16[512,256]{1,0:T(8,128)(2,1)}, bf16[512,256]{1,0:T(8,128)(2,1)S(1)}, u32[]{:S(2)}, u32[]{:S(2)}) collective-permute-start(bf16[512,256]{1,0:T(8,128)(2,1)} %get-tuple-element.34), channel_id=1, source_target_pairs={{0,228},{4,32},{32,4},{36,64},{64,36},{68,96},{96,68},{100,128},{1... | collective-permute-start | bytes 786440 | tf_op jit(solution)/shard_map/ppermute | solution.py:383
  17.2 7.8 %collective-permute-start.4 = (bf16[512,256]{1,0:T(8,128)(2,1)}, bf16[512,256]{1,0:T(8,128)(2,1)S(1)}, u32[]{:S(2)}, u32[]{:S(2)}) collective-permute-start(bf16[512,256]{1,0:T(8,128)(2,1)} %get-tuple-element.34), channel_id=1, source_target_pairs={{0,32},{4,228},{32,64},{36,4},{64,96},{68,36},{96,128},{100,68},{1... | collective-permute-start | bytes 786440 | tf_op jit(solution)/shard_map/ppermute | solution.py:383
  25.0 18.6 %copy-start.8 = (bf16[512,256]{1,0:T(8,128)(2,1)S(1)}, bf16[512,256]{1,0:T(8,128)(2,1)}, u32[]{:S(2)}) copy-start(bf16[512,256]{1,0:T(8,128)(2,1)} %get-tuple-element.33.own_ref) | copy-start | bytes 786436
  25.0 18.6 %copy-start.9 = (bf16[256,256]{1,0:T(8,128)(2,1)S(1)}, bf16[256,256]{1,0:T(8,128)(2,1)}, u32[]{:S(2)}) copy-start(bf16[256,256]{1,0:T(8,128)(2,1)} %get-tuple-element.31.q0) | copy-start | bytes 393220
  25.1 12.4 %collective-permute-start.6 = (bf16[2,512,256]{2,1,0:T(8,128)(2,1)S(1)}, bf16[2,512,256]{2,1,0:T(8,128)(2,1)}, u32[]{:S(2)}, u32[]{:S(2)}) collective-permute-start(bf16[2,512,256]{2,1,0:T(8,128)(2,1)S(1)} %pad_maximum_fusion.2), channel_id=1, source_target_pairs={{0,32},{4,228},{32,64},{36,4},{64,96},{68,36},{96,128},{100,68},{1... | collective-permute-start | bytes 1572872 | tf_op jit(solution)/shard_map/ppermute | solution.py:390
  25.2 13.6 %collective-permute-start = (bf16[256,256]{1,0:T(8,128)(2,1)}, bf16[256,256]{1,0:T(8,128)(2,1)S(1)}, u32[]{:S(2)}, u32[]{:S(2)}) collective-permute-start(bf16[256,256]{1,0:T(8,128)(2,1)} %get-tuple-element.32), channel_id=1, source_target_pairs={{0,8},{8,16},{16,24},{24,0},{1,9},{9,17},{17,25},{25,1},{2,10},{10... | collective-permute-start | bytes 393224 | tf_op jit(solution)/shard_map/ppermute | solution.py:359
  26.7 12.2 %collective-permute-start.1 = (bf16[256,256]{1,0:T(8,128)(2,1)}, bf16[256,256]{1,0:T(8,128)(2,1)S(1)}, u32[]{:S(2)}, u32[]{:S(2)}) collective-permute-start(bf16[256,256]{1,0:T(8,128)(2,1)} %get-tuple-element.32), channel_id=1, source_target_pairs={{0,16},{8,24},{16,0},{24,8},{1,17},{9,25},{17,1},{25,9},{2,18},{10... | collective-permute-start | bytes 393224 | tf_op jit(solution)/shard_map/ppermute | solution.py:359
  27.9 14.1 %collective-permute-start.2 = (bf16[256,256]{1,0:T(8,128)(2,1)}, bf16[256,256]{1,0:T(8,128)(2,1)S(1)}, u32[]{:S(2)}, u32[]{:S(2)}) collective-permute-start(bf16[256,256]{1,0:T(8,128)(2,1)} %get-tuple-element.32), channel_id=1, source_target_pairs={{0,24},{8,0},{16,8},{24,16},{1,25},{9,1},{17,9},{25,17},{2,26},{10... | collective-permute-start | bytes 393224 | tf_op jit(solution)/shard_map/ppermute | solution.py:359
  30.0 12.6 %collective-permute-start.3 = (bf16[512,256]{1,0:T(8,128)(2,1)}, bf16[512,256]{1,0:T(8,128)(2,1)S(1)}, u32[]{:S(2)}, u32[]{:S(2)}) collective-permute-start(bf16[512,256]{1,0:T(8,128)(2,1)} %get-tuple-element.34), channel_id=1, source_target_pairs={{0,4},{4,0},{1,5},{5,1},{2,6},{6,2},{3,7},{7,3},{8,12},{12,8},{9,1... | collective-permute-start | bytes 786440 | tf_op jit(solution)/shard_map/ppermute | solution.py:359
  38.6 36.3 %collective-permute-start.11 = (bf16[4,512,256]{2,1,0:T(8,128)(2,1)S(1)}, bf16[4,512,256]{2,1,0:T(8,128)(2,1)S(1)}, u32[]{:S(2)}, u32[]{:S(2)}) collective-permute-start(bf16[4,512,256]{2,1,0:T(8,128)(2,1)S(1)} %pad_maximum_fusion.1.kv_ref), channel_id=1, source_target_pairs={{0,4},{4,0},{1,5},{5,1},{2,6},{6,2},{3,7},{7,3},{8,12},{12,8},{9,1... | collective-permute-start | bytes 3145736 | tf_op jit(solution)/shard_map/ppermute | solution.py:359
  38.8 12.1 %collective-permute-start.7 = (bf16[2,512,256]{2,1,0:T(8,128)(2,1)}, bf16[2,512,256]{2,1,0:T(8,128)(2,1)S(1)}, u32[]{:S(2)}, u32[]{:S(2)}) collective-permute-start(bf16[2,512,256]{2,1,0:T(8,128)(2,1)} %collective-permute-done.6), channel_id=1, source_target_pairs={{0,32},{4,228},{32,64},{36,4},{64,96},{68,36},{96,128},{100,68},{1... | collective-permute-start | bytes 1572872 | tf_op jit(solution)/shard_map/ppermute | solution.py:394
  38.9 26.0 %collective-permute-start.14 = (bf16[128,2048]{1,0:T(8,128)(2,1)S(1)}, bf16[128,2048]{1,0:T(8,128)(2,1)S(1)}, u32[]{:S(2)}, u32[]{:S(2)}) collective-permute-start(bf16[128,2048]{1,0:T(8,128)(2,1)S(1)} %constant_dynamic-slice_fusion), channel_id=1, source_target_pairs={{0,3},{1,0},{2,1},{3,2},{4,7},{5,4},{6,5},{7,6},{8,11},{9,8},{10,9... | collective-permute-start | bytes 1572872 | tf_op jit(solution)/shard_map/ppermute | solution.py:359
  41.9 23.0 %collective-permute-start.13 = (bf16[128,2048]{1,0:T(8,128)(2,1)S(1)}, bf16[128,2048]{1,0:T(8,128)(2,1)S(1)}, u32[]{:S(2)}, u32[]{:S(2)}) collective-permute-start(bf16[128,2048]{1,0:T(8,128)(2,1)S(1)} %constant_dynamic-slice_fusion), channel_id=1, source_target_pairs={{0,2},{1,3},{2,0},{3,1},{4,6},{5,7},{6,4},{7,5},{8,10},{9,11},{10,... | collective-permute-start | bytes 1572872 | tf_op jit(solution)/shard_map/ppermute | solution.py:359
  42.7 26.0 %collective-permute-start.12 = (bf16[128,2048]{1,0:T(8,128)(2,1)S(1)}, bf16[128,2048]{1,0:T(8,128)(2,1)S(1)}, u32[]{:S(2)}, u32[]{:S(2)}) collective-permute-start(bf16[128,2048]{1,0:T(8,128)(2,1)S(1)} %constant_dynamic-slice_fusion), channel_id=1, source_target_pairs={{0,1},{1,2},{2,3},{3,0},{4,5},{5,6},{6,7},{7,4},{8,9},{9,10},{10,1... | collective-permute-start | bytes 1572872 | tf_op jit(solution)/shard_map/ppermute | solution.py:359
  50.9 23.6 %collective-permute-start.8 = (bf16[512,256]{1,0:T(8,128)(2,1)S(1)}, bf16[512,256]{1,0:T(8,128)(2,1)S(1)}, u32[]{:S(2)}, u32[]{:S(2)}) collective-permute-start(bf16[512,256]{1,0:T(8,128)(2,1)S(1)} %slice_bitcast_fusion), channel_id=1, source_target_pairs={{0,32},{4,228},{32,64},{36,4},{64,96},{68,36},{96,128},{100,68},{1... | collective-permute-start | bytes 786440 | tf_op jit(solution)/shard_map/ppermute | solution.py:399
  64.9 19.1 %collective-permute-start.10 = (bf16[2,512,256]{2,1,0:T(8,128)(2,1)S(1)}, bf16[2,512,256]{2,1,0:T(8,128)(2,1)S(1)}, u32[]{:S(2)}, u32[]{:S(2)}) collective-permute-start(bf16[2,512,256]{2,1,0:T(8,128)(2,1)S(1)} %collective-permute-done.7.kv_ref), channel_id=1, source_target_pairs={{0,4},{4,0},{1,5},{5,1},{2,6},{6,2},{3,7},{7,3},{8,12},{12,8},{9,1... | collective-permute-start | bytes 1572872 | tf_op jit(solution)/shard_map/ppermute | solution.py:359
  68.8 32.1 %collective-permute-start.15 = (bf16[3,128,2048]{2,1,0:T(8,128)(2,1)S(1)}, bf16[3,128,2048]{2,1,0:T(8,128)(2,1)}, u32[]{:S(2)}, u32[]{:S(2)}) collective-permute-start(bf16[3,128,2048]{2,1,0:T(8,128)(2,1)S(1)} %pad_maximum_fusion.mine_ref), channel_id=1, source_target_pairs={{0,4},{4,0},{1,5},{5,1},{2,6},{6,2},{3,7},{7,3},{8,12},{12,8},{9,1... | collective-permute-start | bytes 4718600 | tf_op jit(solution)/shard_map/ppermute | solution.py:359
  74.5 16.1 %collective-permute-start.9 = (bf16[512,256]{1,0:T(8,128)(2,1)S(1)}, bf16[512,256]{1,0:T(8,128)(2,1)S(1)}, u32[]{:S(2)}, u32[]{:S(2)}) collective-permute-start(bf16[512,256]{1,0:T(8,128)(2,1)S(1)} %collective-permute-done.8.kv_ref), channel_id=1, source_target_pairs={{0,4},{4,0},{1,5},{5,1},{2,6},{6,2},{3,7},{7,3},{8,12},{12,8},{9,1... | collective-permute-start | bytes 786440 | tf_op jit(solution)/shard_map/ppermute | solution.py:359
  87.8 2.8 %copy-start.6 = (f32[2]{0:T(128)S(1)}, f32[2]{0:T(128)}, u32[]{:S(2)}) copy-start(f32[2]{0:T(128)} %lam_ref.1) | copy-start | bytes 28
  94.7 1.1 copy-start.1
  95.8 23.6 %copy-start.4 = (bf16[64,2048]{1,0:T(8,128)(2,1)S(1)}, bf16[64,2048]{1,0:T(8,128)(2,1)}, u32[]{:S(2)}) copy-start(bf16[64,2048]{1,0:T(8,128)(2,1)} %res_ref.1) | copy-start | bytes 786436
  95.8 23.6 %copy-start.5 = (f32[2048]{0:T(1024)S(1)}, f32[2048]{0:T(1024)}, u32[]{:S(2)}) copy-start(f32[2048]{0:T(1024)} %param.21) | copy-start | bytes 24580
  95.8 23.6 %copy-start.7 = (f32[128]{0:T(128)S(1)}, f32[128]{0:T(128)}, u32[]{:S(2)}) copy-start(f32[128]{0:T(128)} %param.19) | copy-start | bytes 1540
  95.8 23.6 %all-to-all-start = ((bf16[16,64,640]{2,1,0:T(8,128)(2,1)}), bf16[16,64,640]{2,1,0:T(8,128)(2,1)S(1)}, u32[]{:S(2)}, u32[]{:S(2)}) async-start(bf16[16,64,640]{2,1,0:T(8,128)(2,1)} %copy-done.1), calls=%async_computation | async-start | bytes 2621440 | tf_op jit(solution)/shard_map/all_to_all | solution.py:406
  119.3 1.2 copy-start.3
  124.0 6.5 %collective-permute-start.17 = (bf16[64,2048]{1,0:T(8,128)(2,1)S(1)}, bf16[64,2048]{1,0:T(8,128)(2,1)S(1)}, u32[]{:S(2)}, u32[]{:S(2)}) collective-permute-start(bf16[64,2048]{1,0:T(8,128)(2,1)S(1)} %merge.1.refs_0_), channel_id=1, source_target_pairs={{0,3},{1,0},{2,1},{3,2},{4,7},{5,4},{6,5},{7,6},{8,11},{9,8},{10,9... | collective-permute-start | bytes 786440 | tf_op jit(solution)/shard_map/ppermute | solution.py:359
  125.5 8.6 %collective-permute-start.16 = (bf16[64,2048]{1,0:T(8,128)(2,1)S(1)}, bf16[64,2048]{1,0:T(8,128)(2,1)S(1)}, u32[]{:S(2)}, u32[]{:S(2)}) collective-permute-start(bf16[64,2048]{1,0:T(8,128)(2,1)S(1)} %merge.1.refs_0_), channel_id=1, source_target_pairs={{0,1},{1,2},{2,3},{3,0},{4,5},{5,6},{6,7},{7,4},{8,9},{9,10},{10,1... | collective-permute-start | bytes 786440 | tf_op jit(solution)/shard_map/ppermute | solution.py:359
  130.6 6.1 %collective-permute-start.20 = (bf16[32,2048]{1,0:T(8,128)(2,1)S(1)}, bf16[32,2048]{1,0:T(8,128)(2,1)S(1)}, u32[]{:S(2)}, u32[]{:S(2)}) collective-permute-start(bf16[32,2048]{1,0:T(8,128)(2,1)S(1)} %slice.14), channel_id=1, source_target_pairs={{0,3},{1,0},{2,1},{3,2},{4,7},{5,4},{6,5},{7,6},{8,11},{9,8},{10,9... | collective-permute-start | bytes 393224 | tf_op jit(solution)/shard_map/ppermute | solution.py:359
  134.2 6.5 %collective-permute-start.19 = (bf16[32,2048]{1,0:T(8,128)(2,1)S(1)}, bf16[32,2048]{1,0:T(8,128)(2,1)S(1)}, u32[]{:S(2)}, u32[]{:S(2)}) collective-permute-start(bf16[32,2048]{1,0:T(8,128)(2,1)S(1)} %slice.13), channel_id=1, source_target_pairs={{0,1},{1,2},{2,3},{3,0},{4,5},{5,6},{6,7},{7,4},{8,9},{9,10},{10,1... | collective-permute-start | bytes 393224 | tf_op jit(solution)/shard_map/ppermute | solution.py:359
  140.7 3.4 %copy-start = (bf16[128,32,1024]{2,1,0:T(8,128)(2,1)S(1)}, bf16[128,32,1024]{2,1,0:T(8,128)(2,1)}, u32[]{:S(2)}) copy-start(bf16[128,32,1024]{2,1,0:T(8,128)(2,1)} %all-gather.3.cloned.1.call-done) | copy-start | bytes 25165828
  147.1 12.5 %collective-permute-start.22 = (bf16[64,2048]{1,0:T(8,128)(2,1)S(1)}, bf16[64,2048]{1,0:T(8,128)(2,1)S(1)}, u32[]{:S(2)}, u32[]{:S(2)}) collective-permute-start(bf16[64,2048]{1,0:T(8,128)(2,1)S(1)} %get-tuple-element.56), channel_id=1, source_target_pairs={{0,1},{1,2},{2,3},{3,0},{4,5},{5,6},{6,7},{7,4},{8,9},{9,10},{10,1... | collective-permute-start | bytes 786440 | tf_op jit(solution)/shard_map/ppermute | solution.py:359
  149.3 10.3 %collective-permute-start.21 = (bf16[64,2048]{1,0:T(8,128)(2,1)S(1)}, bf16[64,2048]{1,0:T(8,128)(2,1)S(1)}, u32[]{:S(2)}, u32[]{:S(2)}) collective-permute-start(bf16[64,2048]{1,0:T(8,128)(2,1)S(1)} %mixer.3), channel_id=1, source_target_pairs={{0,2},{1,3},{2,0},{3,1},{4,6},{5,7},{6,4},{7,5},{8,10},{9,11},{10,... | collective-permute-start | bytes 786440 | tf_op jit(solution)/shard_map/ppermute | solution.py:359
  150.5 11.4 %collective-permute-start.18 = (bf16[64,2048]{1,0:T(8,128)(2,1)S(1)}, bf16[64,2048]{1,0:T(8,128)(2,1)S(1)}, u32[]{:S(2)}, u32[]{:S(2)}) collective-permute-start(bf16[64,2048]{1,0:T(8,128)(2,1)S(1)} %get-tuple-element.55), channel_id=1, source_target_pairs={{0,3},{1,0},{2,1},{3,2},{4,7},{5,4},{6,5},{7,6},{8,11},{9,8},{10,9... | collective-permute-start | bytes 786440 | tf_op jit(solution)/shard_map/ppermute | solution.py:359
Sparse Core Ops, SparseCore 0:
  10.1 84.8 all-gather.2

commit v5 on v4

--- a/solution.py
+++ b/solution.py
@@ -19,7 +19,6 @@
 HBM = pl.BlockSpec(memory_space=pltpu.HBM)
 SMEM = pl.BlockSpec(memory_space=pltpu.SMEM)
 VMEM = pl.BlockSpec(memory_space=pltpu.VMEM)
-WIDE = 5 * VD
 
 
 def prep_kernel(cos_ref, sin_ref, qa_ref, qb_ref, ka_ref, kb_ref, v_ref, q_out, kv_out, q_own, kv_own):
@@ -59,13 +58,6 @@
         out_specs=(VMEM,) * 4,
         name="prep",
     )(cos, sin, first_query, second_query, first_key, second_key, values)
-
-
-def three_parts(value):
-    hi = value.astype(BF16).astype(F32)
-    rest = value - hi
-    mid = rest.astype(BF16).astype(F32)
-    return hi, mid, rest - mid
 
 
 def load_queries(queries, qs):
@@ -81,7 +73,7 @@
                 qs[o, 2 * h + m, :, 128:256] = jnp.where(mine, lo, 0.0).astype(BF16)
 
 
-def absorb(chunks, qs, sc, acc, top, tot, fresh, block_done=None):
+def absorb(chunks, qs, sc, acc, top, tot, fresh):
     def scores(slot, o, hm):
         m = hm % 2
         keys = jnp.concatenate([c[0:TOK, m * 128 : (m + 1) * 128] for c in chunks], axis=0)
@@ -113,8 +105,6 @@
             else:
                 tot[o, hm] = tot[o, hm] * shrink + total
                 acc[o, hm] = acc[o, hm] * shrink + moved
-        if block_done is not None:
-            block_done(o)
         return peak
 
     lax.fori_loop(0, 4, step, scores(0, 0, 0))
@@ -141,34 +131,30 @@
     absorb(chunks_of(kv_ref), qs, sc, acc, top, tot, False)
 
 
-def last_kernel(
-    x_ref, lam_ref, qs, kv_ref, acc_in, top_in, tot_in, out_ref, acc, top, tot, sc, stat, buf, sem
-):
-    acc[...] = acc_in[...]
-    top[...] = top_in[...]
-    tot[...] = tot_in[...]
-    stat[...] = jnp.zeros_like(stat)
-    for h in range(2):
-        for i, part in enumerate(three_parts(jnp.full((1, TOK), lam_ref[h], F32))):
-            stat[12 + 3 * h + i : 13 + 3 * h + i, :] = part
-
-    def sending(o):
+def last_kernel(qs, kv_ref, acc_in, top_in, tot_in, acc, top, tot, lse, sc):
+    absorb(chunks_of(kv_ref), qs, sc, acc, top, tot, False)
+    for o in range(4):
+        for hm in range(4):
+            row = 4 * o + hm
+            lse[row : row + 1, :] = top[o, hm] + jnp.log2(tot[o, hm])
+
+
+def share_kernel(x_ref, lam_ref, lse0, lse1, lse2, lse3, acc, tot, out_ref):
+    lses = (lse0, lse1, lse2, lse3)
+    for o in range(4):
         home = (x_ref[0] + 4 - o) % 4
-        return pltpu.make_async_copy(buf.at[o], out_ref.at[pl.ds(4 * home, 4)], sem.at[o])
-
-    def block_done(o):
+        factors = []
         for hm in range(4):
-            total = tot[o, hm]
-            mean = (acc[o, hm] / total).T.astype(BF16)
-            buf[o, :, :, hm * VD : (hm + 1) * VD] = mean.reshape(4, TOK // 4, VD)
-            for i, part in enumerate(three_parts(top[o, hm] + jnp.log2(total))):
-                stat[3 * hm + i : 3 * hm + i + 1, :] = part
-        buf[o, :, :, 4 * VD :] = stat[...].T.astype(BF16).reshape(4, TOK // 4, VD)
-        sending(o).start()
-
-    absorb(chunks_of(kv_ref), qs, sc, acc, top, tot, False, block_done)
-    for o in range(4):
-        sending(o).wait()
+            rows = [4 * ((o - k) % 4) + hm for k in range(4)]
+            here = [ref[row : row + 1, :] for ref, row in zip(lses, rows)]
+            peak = jnp.maximum(jnp.maximum(here[0], here[1]), jnp.maximum(here[2], here[3]))
+            terms = [jnp.exp2(e - peak) for e in here]
+            factors.append(terms[0] / ((terms[0] + terms[1] + terms[2] + terms[3]) * tot[o, hm]))
+        for h in range(2):
+            diff = acc[o, 2 * h] * factors[2 * h] - acc[o, 2 * h + 1] * (lam_ref[h] * factors[2 * h + 1])
+            out_ref[pl.ds(4 * home, 4), :, h * VD : (h + 1) * VD] = diff.T.astype(BF16).reshape(
+                4, TOK // 4, VD
+            )
 
 
 def cost(keys):
@@ -211,23 +197,29 @@
     )(qs, kv, *state)
 
 
-def attend_last(x, lambdas, qs, kv, state):
+def attend_last(qs, kv, state):
     return pl.pallas_call(
         last_kernel,
-        out_shape=jax.ShapeDtypeStruct((16, TOK // 4, WIDE), BF16),
-        in_specs=[SMEM, SMEM] + [VMEM] * 5,
-        out_specs=HBM,
-        scratch_shapes=[pltpu.VMEM(s.shape, s.dtype) for s in STATE]
-        + [
-            score_scratch(kv.shape[0] // (2 * TOK)),
-            pltpu.VMEM((VD, TOK), F32),
-            pltpu.VMEM((4, 4, TOK // 4, WIDE), BF16),
-            pltpu.SemaphoreType.DMA((4,)),
-        ],
+        out_shape=STATE + (jax.ShapeDtypeStruct((16, TOK), F32),),
+        in_specs=[VMEM] * 5,
+        out_specs=(VMEM,) * 4,
+        input_output_aliases={2: 0, 3: 1, 4: 2},
+        scratch_shapes=[score_scratch(kv.shape[0] // (2 * TOK))],
         cost_estimate=cost(kv.shape[0] // 2),
         compiler_params=pltpu.CompilerParams(vmem_limit_bytes=24 * 2**20),
         name="attend_last",
-    )(x, lambdas, qs, kv, *state)
+    )(qs, kv, *state)
+
+
+def share(x, lambdas, lses, acc, tot):
+    return pl.pallas_call(
+        share_kernel,
+        out_shape=jax.ShapeDtypeStruct((16, TOK // 4, 2 * VD), BF16),
+        in_specs=[SMEM, SMEM] + [VMEM] * 6,
+        out_specs=VMEM,
+        compiler_params=pltpu.CompilerParams(vmem_limit_bytes=16 * 2**20),
+        name="share",
+    )(x, lambdas, *lses, acc, tot)
 
 
 def load_mix_kernel(w_ref, out_ref, sem):
@@ -254,17 +246,15 @@
     )(weights)
 
 
-def merge_kernel(
-    at_ref, part_ref, gain_ref, res_ref, norm_ref, own_ref, mine_ref, other_ref, out_ref, wbuf, sem
-):
+def merge_kernel(at_ref, part_ref, gain_ref, res_ref, norm_ref, mine_ref, other_ref, out_ref, wbuf, sem):
     mine = at_ref[1] * VD
-    copies = [[pltpu.make_async_copy(own_ref, wbuf.at[0], sem.at[0])]]
-    for o in range(3):
+    copies = []
+    for o in range(4):
         near, far = pl.ds(mine, VD), pl.ds(VD - mine, VD)
         copies.append(
             [
-                pltpu.make_async_copy(mine_ref.at[o], wbuf.at[o + 1, near], sem.at[2 * o + 1]),
-                pltpu.make_async_copy(other_ref.at[o], wbuf.at[o + 1, far], sem.at[2 * o + 2]),
+                pltpu.make_async_copy(mine_ref.at[o], wbuf.at[o, near], sem.at[2 * o]),
+                pltpu.make_async_copy(other_ref.at[o], wbuf.at[o, far], sem.at[2 * o + 1]),
             ]
         )
     for pair in copies:
@@ -273,27 +263,10 @@
     stream = res_ref[...].astype(F32)
     for o in range(4):
         y = (at_ref[0] + 4 - o) % 4
-        parts = [part_ref[4 * k + y] for k in range(4)]
-        stats = [p[:, 4 * VD :].astype(F32) for p in parts]
+        both = sum(part_ref[4 * k + y].astype(F32) for k in range(4))
         heads = []
         for h in range(2):
-            maps = []
-            for m in range(2):
-                hm = 2 * h + m
-                at = 3 * hm
-                lse = [s[:, at : at + 1] + s[:, at + 1 : at + 2] + s[:, at + 2 : at + 3] for s in stats]
-                peak = jnp.maximum(jnp.maximum(lse[0], lse[1]), jnp.maximum(lse[2], lse[3]))
-                share = [jnp.exp2(e - peak) for e in lse]
-                inv = 1.0 / (share[0] + share[1] + share[2] + share[3])
-                maps.append(
-                    sum(
-                        p[:, hm * VD : (hm + 1) * VD].astype(F32) * (w * inv)
-                        for p, w in zip(parts, share)
-                    )
-                )
-            at = 12 + 3 * h
-            lam = stats[0][:, at : at + 1] + stats[0][:, at + 1 : at + 2] + stats[0][:, at + 2 : at + 3]
-            diff = maps[0] - lam * maps[1]
+            diff = both[:, h * VD : (h + 1) * VD]
             scale = lax.rsqrt(jnp.mean(diff * diff, axis=-1, keepdims=True) + 1e-05)
             heads.append((diff * scale * gain_ref[...] * 0.8).astype(BF16))
         flat = jnp.concatenate(heads, axis=1)
@@ -310,9 +283,9 @@
     return pl.pallas_call(
         merge_kernel,
         out_shape=jax.ShapeDtypeStruct((rows, width), BF16),
-        in_specs=[SMEM] + [VMEM] * 4 + [HBM] * 3,
+        in_specs=[SMEM] + [VMEM] * 4 + [HBM] * 2,
         out_specs=VMEM,
-        scratch_shapes=[pltpu.VMEM((4, 2 * VD, width), BF16), pltpu.SemaphoreType.DMA((7,))],
+        scratch_shapes=[pltpu.VMEM((4, 2 * VD, width), BF16), pltpu.SemaphoreType.DMA((8,))],
         compiler_params=pltpu.CompilerParams(vmem_limit_bytes=24 * 2**20),
         name="merge",
     )(at, part, head_gain.reshape(1, VD), residual, norm_gain.reshape(1, width), *weights)
@@ -388,8 +361,8 @@
     half = lax.dynamic_slice_in_dim(out_weight, lax.axis_index("c") * VD, VD, 0)
     near = jnp.stack(near)
     second = lax.ppermute(near, ring, onward)
-    mine = jnp.stack([shifted(half, "tp", o) for o in (1, 2, 3)])
-    out_weights = [out_weight, mine, shifted(mine, "c", 1)]
+    mine = jnp.stack([half] + [shifted(half, "tp", o) for o in (1, 2, 3)])
+    out_weights = [mine, shifted(mine, "c", 1)]
     qs, *state = attend_first(queries, kv_own, other)
     third = lax.ppermute(second, ring, onward)
     four = jnp.concatenate([near, second])
@@ -401,8 +374,10 @@
     state = attend_next(qs, third, state)
     state = attend_next(qs, third_other, state)
     far_other = shifted(far, "c", 1)
-    state = attend_next(qs, far, state)
-    part = attend_last(x, lambdas, qs, far_other, state)
+    *state, _ = attend_last(qs, far, state)
+    acc, _, tot, lse = attend_last(qs, far_other, state)
+    lses = [lse] + [shifted(lse, "x", k) for k in (1, 2, 3)]
+    part = share(x, lambdas, lses, acc, tot)
     part = lax.all_to_all(part, ("x", "tp"), split_axis=0, concat_axis=0, tiled=True)
     normed = merge(at, part, head_gain, residual, norm_gain, out_weights)
     mix_weights = load_mix(mix_weights)

time: 170 us -> 162 us (0.953)
  waiting for transfers between devices: 73.4 us -> 61.1 us
  starting transfers between devices: 31.3 us -> 35.7 us
    ppermute x18 -> x21, waiting for transfers between devices: 37.5 us -> 48.4 us  [shifted(): lax.ppermute(value, axis, [(i, (i + by) % size) for i in range(size)])]
    all_to_all x1, waiting for transfers between devices: 18.4 us -> 8.52 us  [local(): lax.all_to_all(part, ('x', 'tp'), split_axis=0, concat_axis=0, tiled=True)]
    ppermute x1, waiting for transfers between devices: 6.63 us -> 0.01 us  [local(): second = lax.ppermute(near, ring, onward)]
    ppermute x2, waiting for transfers between devices: 7.79 us -> 3.05 us  [local(): near = [lax.ppermute(kv, ring, onward), lax.ppermute(kv, ring, crossed)]]
    ppermute x18 -> x21, starting transfers between devices: 20.6 us -> 24.2 us  [shifted(): lax.ppermute(value, axis, [(i, (i + by) % size) for i in range(size)])]
    pallas_call x1 -> x3, Pallas kernels: 4.08 us -> 7.05 us  [the longest x2 6.22 us: attend_last(): pl.pallas_call(last_kernel, out_shape=STATE + (jax.ShapeDtypeStruct((16,...]
    pallas_call x5 -> x4, Pallas kernels: 21 us -> 18.2 us  [attend_next(): pl.pallas_call(next_kernel, out_shape=STATE, in_specs=[VMEM] * 5, out_spe...]
    ppermute x1, waiting for transfers between devices: 3.12 us -> 0.8 us  [local(): third = lax.ppermute(second, ring, onward)]
  transfers between devices with their start and end apart: 25 -> 28, of which waited for: 12 -> 18; matrix products, arithmetic and copies ran while one was open for 2% -> 1% of each run, Pallas kernels for 22% -> 23%
where the time goes in v5:
time: 162 us; the launch traced here: 161 us
  waiting for transfers between devices  61.1 us (38%)
  Pallas kernels  40.2 us (25%)
  starting transfers between devices  35.7 us (22%)
  between operations  13.7 us (8%)
  local copies, waits for them, and re-layouts  5.79 us (4%)
  other arithmetic  4.25 us (3%)
    ppermute x21, waiting for transfers between devices, shifted(): lax.ppermute(value, axis, [(i, (i + by) % size) for i in range(size)])  48.4 us
    ppermute x21, starting transfers between devices, shifted(): lax.ppermute(value, axis, [(i, (i + by) % size) for i in range(size)])  24.2 us
    pallas_call x4, Pallas kernels, attend_next(): pl.pallas_call(next_kernel, out_shape=STATE, in_specs=[VMEM] * 5, out_spe...  18.2 us
    all_to_all x1, waiting for transfers between devices, local(): lax.all_to_all(part, ('x', 'tp'), split_axis=0, concat_axis=0, tiled=True)  8.52 us
    pallas_call x2, Pallas kernels, attend_last(): pl.pallas_call(last_kernel, out_shape=STATE + (jax.ShapeDtypeStruct((16,...  6.22 us
    all_to_all x1, starting transfers between devices, local(): lax.all_to_all(part, ('x', 'tp'), split_axis=0, concat_axis=0, tiled=True)  5.67 us
    unnamed x26, local copies, waits for them, and re-layouts  5.67 us
    ppermute x2, starting transfers between devices, local(): near = [lax.ppermute(kv, ring, onward), lax.ppermute(kv, ring, crossed)]  5.3 us
  transfers between devices with their start and end apart: 28, of which 18 were waited for; matrix products, arithmetic and copies ran while one was open for 1% of the time, Pallas kernels for 23%

profile of v5, /device:TPU:2, one launch (start us, length us, event | category | flops | bytes accessed | tf_op | source)
XLA Modules:
  0.0 160.8 jit_solution(16191409381361272252)
XLA Ops:
  6.5 1.6 %pad_maximum_fusion.4 = bf16[2,32,1024]{2,1,0:T(8,128)(2,1)} fusion(bf16[1,32,1024]{2,1,0:T(8,128)(2,1)} %bitcast.29, bf16[1,32,1024]{2,1,0:T(8,128)(2,1)} %bitcast.30), kind=kLoop, calls=%fused_computation.8 | loop fusion | flops 65536 | bytes 262144 | tf_op jit(solution)/shard_map/stack | solution.py:359
  8.2 1.2 multiply_sine_fusion
  9.5 2.5 %prep.1 = (bf16[256,256]{1,0:T(8,128)(2,1)}, bf16[512,256]{1,0:T(8,128)(2,1)}, bf16[256,256]{1,0:T(8,128)(2,1)}, bf16[512,256]{1,0:T(8,128)(2,1)}) custom-call(f32[256,32]{1,0:T(8,128)} %get-tuple-element.64.cos_ref, f32[256,32]{1,0:T(8,128)} %get-tuple-element.63.sin_ref, bf16[256,128]{1,0:T(8,128)(2,1)} %qa_ref.1, bf16[256,128]{1,0:T(8,128)(2,1)} %qb_ref.1, ...), custom_call_target="tpu_custom_call" | custom-call | tf_op jit(solution)/shard_map/prep/pallas_call | solution.py:50
  12.0 5.3 %collective-permute-start.5 = (bf16[512,256]{1,0:T(8,128)(2,1)}, bf16[512,256]{1,0:T(8,128)(2,1)S(1)}, u32[]{:S(2)}, u32[]{:S(2)}) collective-permute-start(bf16[512,256]{1,0:T(8,128)(2,1)} %get-tuple-element.37), channel_id=1, source_target_pairs={{0,228},{4,32},{32,4},{36,64},{64,36},{68,96},{96,68},{100,128},{1... | collective-permute-start | bytes 786440 | tf_op jit(solution)/shard_map/ppermute | solution.py:356
  17.3 3.1 %collective-permute-start.17 = (bf16[128,2048]{1,0:T(8,128)(2,1)S(1)}, bf16[128,2048]{1,0:T(8,128)(2,1)S(1)}, u32[]{:S(2)}, u32[]{:S(2)}) collective-permute-start(bf16[128,2048]{1,0:T(8,128)(2,1)S(1)} %constant_dynamic-slice_fusion), channel_id=1, source_target_pairs={{0,3},{1,0},{2,1},{3,2},{4,7},{5,4},{6,5},{7,6},{8,11},{9,8},{10,9... | collective-permute-start | bytes 1572872 | tf_op jit(solution)/shard_map/ppermute | solution.py:332
  21.1 1.0 collective-permute-start.15
  22.0 1.7 %collective-permute-done.5 = bf16[512,256]{1,0:T(8,128)(2,1)S(1)} collective-permute-done((bf16[512,256]{1,0:T(8,128)(2,1)}, bf16[512,256]{1,0:T(8,128)(2,1)S(1)}, u32[]{:S(2)}, u32[]{:S(2)}) %collective-permute-start.5) | collective-permute-done | bytes 262176 | tf_op jit(solution)/shard_map/ppermute | solution.py:356
  23.7 1.3 collective-permute-done.4
  25.3 17.8 %collective-permute-done.17 = bf16[128,2048]{1,0:T(8,128)(2,1)S(1)} collective-permute-done((bf16[128,2048]{1,0:T(8,128)(2,1)S(1)}, bf16[128,2048]{1,0:T(8,128)(2,1)S(1)}, u32[]{:S(2)}, u32[]{:S(2)}) %collective-permute-start.17) | collective-permute-done | bytes 524320 | tf_op jit(solution)/shard_map/ppermute | solution.py:332
  43.1 3.7 %collective-permute-done.15 = bf16[128,2048]{1,0:T(8,128)(2,1)S(1)} collective-permute-done((bf16[128,2048]{1,0:T(8,128)(2,1)S(1)}, bf16[128,2048]{1,0:T(8,128)(2,1)S(1)}, u32[]{:S(2)}, u32[]{:S(2)}) %collective-permute-start.15) | collective-permute-done | bytes 524320 | tf_op jit(solution)/shard_map/ppermute | solution.py:332
  48.1 1.6 collective-permute-start
  49.7 1.1 collective-permute-start.1
  50.8 2.4 %collective-permute-done.q1 = bf16[256,256]{1,0:T(8,128)(2,1)S(1)} collective-permute-done((bf16[256,256]{1,0:T(8,128)(2,1)S(1)}, bf16[256,256]{1,0:T(8,128)(2,1)S(1)}, u32[]{:S(2)}, u32[]{:S(2)}) %collective-permute-start) | collective-permute-done | bytes 131104 | tf_op jit(solution)/shard_map/ppermute | solution.py:332
  53.2 1.7 %collective-permute-start.2 = (bf16[256,256]{1,0:T(8,128)(2,1)S(1)}, bf16[256,256]{1,0:T(8,128)(2,1)S(1)}, u32[]{:S(2)}, u32[]{:S(2)}) collective-permute-start(bf16[256,256]{1,0:T(8,128)(2,1)S(1)} %copy-done.12), channel_id=1, source_target_pairs={{0,24},{8,0},{16,8},{24,16},{1,25},{9,1},{17,9},{25,17},{2,26},{10... | collective-permute-start | bytes 393224 | tf_op jit(solution)/shard_map/ppermute | solution.py:332
  54.9 1.5 collective-permute-done.1.q2
  56.5 1.2 collective-permute-start.3
  57.7 0.8 collective-permute-done.7.kv_ref
  58.5 1.8 %collective-permute-done.2.q3 = bf16[256,256]{1,0:T(8,128)(2,1)S(1)} collective-permute-done((bf16[256,256]{1,0:T(8,128)(2,1)S(1)}, bf16[256,256]{1,0:T(8,128)(2,1)S(1)}, u32[]{:S(2)}, u32[]{:S(2)}) %collective-permute-start.2) | collective-permute-done | bytes 131104 | tf_op jit(solution)/shard_map/ppermute | solution.py:332
  60.7 4.1 %attend_first.1 = (bf16[4,4,256,256]{3,2,1,0:T(8,128)(2,1)S(1)}, f32[4,4,128,256]{3,2,1,0:T(8,128)S(1)}, f32[4,4,1,256]{3,2,1,0:T(1,128)S(1)}, f32[4,4,1,256]{3,2,1,0:T(1,128)S(1)}) custom-call(bf16[256,256]{1,0:T(8,128)(2,1)S(1)} %copy-done.8, bf16[256,256]{1,0:T(8,128)(2,1)S(1)} %collective-permute-done.q1, ...), custom_call_target="tpu_custom_call" | custom-call | flops 805306368 | bytes 524288 | tf_op jit(solution)/shard_map/attend_first/pallas_call | solution.py:173
  64.8 5.4 %attend_next.4 = (f32[4,4,128,256]{3,2,1,0:T(8,128)S(1)}, f32[4,4,1,256]{3,2,1,0:T(1,128)S(1)}, f32[4,4,1,256]{3,2,1,0:T(1,128)S(1)}) custom-call(bf16[4,4,256,256]{3,2,1,0:T(8,128)(2,1)S(1)} %get-tuple-element.38.qs, bf16[4,512,256]{2,1,0:T(8,128)(2,1)S(1)} %pad_maximum_fusion.1.kv_ref, ...), custom_call_target="tpu_custom_call", output_to_operand_aliasing={{0}: (2, {}), {1}: (3, {}), {2}: (4, {})} | custom-call | flops 1610612736 | bytes 1048576 | tf_op jit(solution)/shard_map/attend_next/pallas_call | solution.py:187
  70.7 5.4 %attend_next.5 = (f32[4,4,128,256]{3,2,1,0:T(8,128)S(1)}, f32[4,4,1,256]{3,2,1,0:T(1,128)S(1)}, f32[4,4,1,256]{3,2,1,0:T(1,128)S(1)}) custom-call(bf16[4,4,256,256]{3,2,1,0:T(8,128)(2,1)S(1)} %get-tuple-element.38.qs, bf16[4,512,256]{2,1,0:T(8,128)(2,1)S(1)} %collective-permute-done.11.kv_ref, ...), custom_call_target="tpu_custom_call", output_to_operand_aliasing={{0}: (2, {}), {1}: (3, {}), {2}: (4, {})} | custom-call | flops 1610612736 | bytes 1048576 | tf_op jit(solution)/shard_map/attend_next/pallas_call | solution.py:187
  76.1 3.7 %attend_next.6 = (f32[4,4,128,256]{3,2,1,0:T(8,128)S(1)}, f32[4,4,1,256]{3,2,1,0:T(1,128)S(1)}, f32[4,4,1,256]{3,2,1,0:T(1,128)S(1)}) custom-call(bf16[4,4,256,256]{3,2,1,0:T(8,128)(2,1)S(1)} %get-tuple-element.38.qs, bf16[2,512,256]{2,1,0:T(8,128)(2,1)S(1)} %collective-permute-done.7.kv_ref, ...), custom_call_target="tpu_custom_call", output_to_operand_aliasing={{0}: (2, {}), {1}: (3, {}), {2}: (4, {})} | custom-call | flops 805306368 | bytes 524288 | tf_op jit(solution)/shard_map/attend_next/pallas_call | solution.py:187
  79.8 3.7 %attend_next.7 = (f32[4,4,128,256]{3,2,1,0:T(8,128)S(1)}, f32[4,4,1,256]{3,2,1,0:T(1,128)S(1)}, f32[4,4,1,256]{3,2,1,0:T(1,128)S(1)}) custom-call(bf16[4,4,256,256]{3,2,1,0:T(8,128)(2,1)S(1)} %get-tuple-element.38.qs, bf16[2,512,256]{2,1,0:T(8,128)(2,1)S(1)} %collective-permute-done.10.kv_ref, ...), custom_call_target="tpu_custom_call", output_to_operand_aliasing={{0}: (2, {}), {1}: (3, {}), {2}: (4, {})} | custom-call | flops 805306368 | bytes 524288 | tf_op jit(solution)/shard_map/attend_next/pallas_call | solution.py:187
  83.5 3.4 %attend_last.2 = (f32[4,4,128,256]{3,2,1,0:T(8,128)S(1)}, f32[4,4,1,256]{3,2,1,0:T(1,128)S(1)}, f32[4,4,1,256]{3,2,1,0:T(1,128)S(1)}, f32[16,256]{1,0:T(8,128)}) custom-call(bf16[4,4,256,256]{3,2,1,0:T(8,128)(2,1)S(1)} %get-tuple-element.38.qs, ...), custom_call_target="tpu_custom_call", output_to_operand_aliasing={{0}: (2, {}), {1}: (3, {}), {2}: (4, {})} | custom-call | flops 402653184 | bytes 262144 | tf_op jit(solution)/shard_map/attend_last/pallas_call | solution.py:201
  86.9 2.8 %attend_last.3 = (f32[4,4,128,256]{3,2,1,0:T(8,128)S(1)}, f32[4,4,1,256]{3,2,1,0:T(1,128)S(1)}, f32[4,4,1,256]{3,2,1,0:T(1,128)S(1)}, f32[16,256]{1,0:T(8,128)S(1)}) custom-call(bf16[4,4,256,256]{3,2,1,0:T(8,128)(2,1)S(1)} %get-tuple-element.38.qs, ...), custom_call_target="tpu_custom_call", output_to_operand_aliasing={{0}: (2, {}), {1}: (3, {}), {2}: (4, {})} | custom-call | flops 402653184 | bytes 262144 | tf_op jit(solution)/shard_map/attend_last/pallas_call | solution.py:201
  89.8 1.0 collective-permute-start.12
  90.8 3.2 %collective-permute-start.13 = (f32[16,256]{1,0:T(8,128)S(1)}, f32[16,256]{1,0:T(8,128)S(1)}, u32[]{:S(2)}, u32[]{:S(2)}) collective-permute-start(f32[16,256]{1,0:T(8,128)S(1)} %get-tuple-element.57.lse0), channel_id=1, source_target_pairs={{0,16},{8,24},{16,0},{24,8},{1,17},{9,25},{17,1},{25,9},{2,18},{10... | collective-permute-start | bytes 49160 | tf_op jit(solution)/shard_map/ppermute | solution.py:332
  93.9 1.7 %collective-permute-start.14 = (f32[16,256]{1,0:T(8,128)S(1)}, f32[16,256]{1,0:T(8,128)S(1)}, u32[]{:S(2)}, u32[]{:S(2)}) collective-permute-start(f32[16,256]{1,0:T(8,128)S(1)} %get-tuple-element.57.lse0), channel_id=1, source_target_pairs={{0,24},{8,0},{16,8},{24,16},{1,25},{9,1},{17,9},{25,17},{2,26},{10... | collective-permute-start | bytes 49160 | tf_op jit(solution)/shard_map/ppermute | solution.py:332
  96.2 1.4 collective-permute-done.14.lse3
  97.7 0.8 share.1
  99.3 5.7 %all-to-all-start = ((bf16[16,64,256]{2,1,0:T(8,128)(2,1)}), bf16[16,64,256]{2,1,0:T(8,128)(2,1)}, u32[]{:S(2)}, u32[]{:S(2)}) async-start(bf16[16,64,256]{2,1,0:T(8,128)(2,1)} %copy-done.2), calls=%async_computation | async-start | bytes 1048576 | tf_op jit(solution)/shard_map/all_to_all | solution.py:381
  105.0 8.5 %all-to-all-done.part_ref = bf16[16,64,256]{2,1,0:T(8,128)(2,1)} async-done(((bf16[16,64,256]{2,1,0:T(8,128)(2,1)}), bf16[16,64,256]{2,1,0:T(8,128)(2,1)}, u32[]{:S(2)}, u32[]{:S(2)}) %all-to-all-start) | async-done | bytes 524320 | tf_op jit(solution)/shard_map/all_to_all | solution.py:381
  113.6 0.9 copy-done.3
  114.5 3.3 %merge.1.refs_0_ = bf16[64,2048]{1,0:T(8,128)(2,1)S(1)} custom-call(s32[2]{0:T(128)S(1)} %pad_add_fusion.at_ref, bf16[16,64,256]{2,1,0:T(8,128)(2,1)} %all-to-all-done.part_ref, f32[1,128]{1,0:T(1,128)S(1)} %bitcast.21, bf16[64,2048]{1,0:T(8,128)(2,1)S(1)} %copy-done.3, f32[1,2048]{1,0:T(1,128)S(1)} %bitcast.20, ...), custom_call_target="tpu_custom_call" | custom-call | tf_op jit(solution)/shard_map/merge/pallas_call | solution.py:283
  117.9 1.2 collective-permute-start.20
  119.1 0.9 collective-permute-start.19
  120.0 5.3 %collective-permute-done.20.refs_2_ = bf16[64,2048]{1,0:T(8,128)(2,1)S(1)} collective-permute-done((bf16[64,2048]{1,0:T(8,128)(2,1)S(1)}, bf16[64,2048]{1,0:T(8,128)(2,1)S(1)}, u32[]{:S(2)}, u32[]{:S(2)}) %collective-permute-start.20) | collective-permute-done | bytes 262176 | tf_op jit(solution)/shard_map/ppermute | solution.py:332
  125.3 1.5 collective-permute-start.23
  127.5 2.8 %collective-permute-done.23 = bf16[32,2048]{1,0:T(8,128)(2,1)S(1)} collective-permute-done((bf16[32,2048]{1,0:T(8,128)(2,1)S(1)}, bf16[32,2048]{1,0:T(8,128)(2,1)S(1)}, u32[]{:S(2)}, u32[]{:S(2)}) %collective-permute-start.23) | collective-permute-done | bytes 131104 | tf_op jit(solution)/shard_map/ppermute | solution.py:332
  130.3 2.8 %collective-permute-done.22 = bf16[32,2048]{1,0:T(8,128)(2,1)S(1)} collective-permute-done((bf16[32,2048]{1,0:T(8,128)(2,1)S(1)}, bf16[32,2048]{1,0:T(8,128)(2,1)S(1)}, u32[]{:S(2)}, u32[]{:S(2)}) %collective-permute-start.22) | collective-permute-done | bytes 131104 | tf_op jit(solution)/shard_map/ppermute | solution.py:332
  133.2 3.4 %copy-done.1 = bf16[128,32,1024]{2,1,0:T(8,128)(2,1)S(1)} copy-done((bf16[128,32,1024]{2,1,0:T(8,128)(2,1)S(1)}, bf16[128,32,1024]{2,1,0:T(8,128)(2,1)}, u32[]{:S(2)}) %copy-start.1) | copy-done | bytes 8388632
  137.2 2.4 %mixer.2 = (f32[64,2048]{1,0:T(8,128)S(1)}, bf16[64,2048]{1,0:T(8,128)(2,1)S(1)}, bf16[64,2048]{1,0:T(8,128)(2,1)S(1)}) custom-call(bf16[64,2048]{1,0:T(8,128)(2,1)S(1)} %merge.1.refs_0_, bf16[64,2048]{1,0:T(8,128)(2,1)S(1)} %collective-permute-done.19.refs_1_, bf16[64,2048]{1,0:T(8,128)(2,1)S(1)} %collective-permute-done.20.refs_2_, ...), custom_call_target="tpu_custom_call" | custom-call | flops 2147483648 | bytes 8388608 | tf_op jit(solution)/shard_map/mixer/pallas_call | solution.py:319
  139.6 2.1 %mixer.3 = bf16[64,2048]{1,0:T(8,128)(2,1)S(1)} custom-call(bf16[64,2048]{1,0:T(8,128)(2,1)S(1)} %pad_maximum_fusion.3.refs_0_, bf16[64,2,32,1024]{3,2,1,0:T(8,128)(2,1)S(1)} %load_mix.1.refs_3_.refs_1_), custom_call_target="tpu_custom_call" | custom-call | flops 2147483648 | bytes 8388608 | tf_op jit(solution)/shard_map/mixer/pallas_call | solution.py:319
  141.8 1.4 collective-permute-start.24
  143.1 2.0 %collective-permute-start.21 = (bf16[64,2048]{1,0:T(8,128)(2,1)S(1)}, bf16[64,2048]{1,0:T(8,128)(2,1)S(1)}, u32[]{:S(2)}, u32[]{:S(2)}) collective-permute-start(bf16[64,2048]{1,0:T(8,128)(2,1)S(1)} %get-tuple-element.61), channel_id=1, source_target_pairs={{0,3},{1,0},{2,1},{3,2},{4,7},{5,4},{6,5},{7,6},{8,11},{9,8},{10,9... | collective-permute-start | bytes 786440 | tf_op jit(solution)/shard_map/ppermute | solution.py:332
  145.1 5.0 %collective-permute-done.25 = bf16[64,2048]{1,0:T(8,128)(2,1)S(1)} collective-permute-done((bf16[64,2048]{1,0:T(8,128)(2,1)S(1)}, bf16[64,2048]{1,0:T(8,128)(2,1)S(1)}, u32[]{:S(2)}, u32[]{:S(2)}) %collective-permute-start.25) | collective-permute-done | bytes 262176 | tf_op jit(solution)/shard_map/ppermute | solution.py:332
  150.1 3.0 %collective-permute-done.21 = bf16[64,2048]{1,0:T(8,128)(2,1)S(1)} collective-permute-done((bf16[64,2048]{1,0:T(8,128)(2,1)S(1)}, bf16[64,2048]{1,0:T(8,128)(2,1)S(1)}, u32[]{:S(2)}, u32[]{:S(2)}) %collective-permute-start.21) | collective-permute-done | bytes 262176 | tf_op jit(solution)/shard_map/ppermute | solution.py:332
  153.1 0.9 add_convert_fusion
  (63 shorter events, 5.9 us)
Async XLA Ops:
  6.5 10.8 %copy-start = (bf16[256,2048]{1,0:T(8,128)(2,1)S(1)}, bf16[256,2048]{1,0:T(8,128)(2,1)}, u32[]{:S(2)}) copy-start(bf16[256,2048]{1,0:T(8,128)(2,1)} %param.20) | copy-start | bytes 3145732
  6.5 126.7 %all-gather.3.cloned.1.call-start = ((), (), s32[]{:S(2)}) async-start(), calls=%async_computation.1 | async-start | bytes 8519680 | tf_op jit(solution)/shard_map/all_gather | solution.py:360
  12.0 11.7 %collective-permute-start.5 = (bf16[512,256]{1,0:T(8,128)(2,1)}, bf16[512,256]{1,0:T(8,128)(2,1)S(1)}, u32[]{:S(2)}, u32[]{:S(2)}) collective-permute-start(bf16[512,256]{1,0:T(8,128)(2,1)} %get-tuple-element.37), channel_id=1, source_target_pairs={{0,228},{4,32},{32,4},{36,64},{64,36},{68,96},{96,68},{100,128},{1... | collective-permute-start | bytes 786440 | tf_op jit(solution)/shard_map/ppermute | solution.py:356
  17.3 7.8 %collective-permute-start.4 = (bf16[512,256]{1,0:T(8,128)(2,1)}, bf16[512,256]{1,0:T(8,128)(2,1)S(1)}, u32[]{:S(2)}, u32[]{:S(2)}) collective-permute-start(bf16[512,256]{1,0:T(8,128)(2,1)} %get-tuple-element.37), channel_id=1, source_target_pairs={{0,32},{4,228},{32,64},{36,4},{64,96},{68,36},{96,128},{100,68},{1... | collective-permute-start | bytes 786440 | tf_op jit(solution)/shard_map/ppermute | solution.py:356
  17.3 25.8 %collective-permute-start.17 = (bf16[128,2048]{1,0:T(8,128)(2,1)S(1)}, bf16[128,2048]{1,0:T(8,128)(2,1)S(1)}, u32[]{:S(2)}, u32[]{:S(2)}) collective-permute-start(bf16[128,2048]{1,0:T(8,128)(2,1)S(1)} %constant_dynamic-slice_fusion), channel_id=1, source_target_pairs={{0,3},{1,0},{2,1},{3,2},{4,7},{5,4},{6,5},{7,6},{8,11},{9,8},{10,9... | collective-permute-start | bytes 1572872 | tf_op jit(solution)/shard_map/ppermute | solution.py:332
  20.4 22.7 %collective-permute-start.16 = (bf16[128,2048]{1,0:T(8,128)(2,1)S(1)}, bf16[128,2048]{1,0:T(8,128)(2,1)S(1)}, u32[]{:S(2)}, u32[]{:S(2)}) collective-permute-start(bf16[128,2048]{1,0:T(8,128)(2,1)S(1)} %constant_dynamic-slice_fusion), channel_id=1, source_target_pairs={{0,2},{1,3},{2,0},{3,1},{4,6},{5,7},{6,4},{7,5},{8,10},{9,11},{10,... | collective-permute-start | bytes 1572872 | tf_op jit(solution)/shard_map/ppermute | solution.py:332
  21.1 25.8 %collective-permute-start.15 = (bf16[128,2048]{1,0:T(8,128)(2,1)S(1)}, bf16[128,2048]{1,0:T(8,128)(2,1)S(1)}, u32[]{:S(2)}, u32[]{:S(2)}) collective-permute-start(bf16[128,2048]{1,0:T(8,128)(2,1)S(1)} %constant_dynamic-slice_fusion), channel_id=1, source_target_pairs={{0,1},{1,2},{2,3},{3,0},{4,5},{5,6},{6,7},{7,4},{8,9},{9,10},{10,1... | collective-permute-start | bytes 1572872 | tf_op jit(solution)/shard_map/ppermute | solution.py:332
  25.1 21.7 %copy-start.9 = (bf16[512,256]{1,0:T(8,128)(2,1)}, bf16[512,256]{1,0:T(8,128)(2,1)S(1)}, u32[]{:S(2)}) copy-start(bf16[512,256]{1,0:T(8,128)(2,1)S(1)} %collective-permute-done.4) | copy-start | bytes 786436
  25.1 22.1 %collective-permute-start.6 = (bf16[2,512,256]{2,1,0:T(8,128)(2,1)S(1)}, bf16[2,512,256]{2,1,0:T(8,128)(2,1)S(1)}, u32[]{:S(2)}, u32[]{:S(2)}) collective-permute-start(bf16[2,512,256]{2,1,0:T(8,128)(2,1)S(1)} %pad_maximum_fusion.2), channel_id=1, source_target_pairs={{0,32},{4,228},{32,64},{36,4},{64,96},{68,36},{96,128},{100,68},{1... | collective-permute-start | bytes 1572872 | tf_op jit(solution)/shard_map/ppermute | solution.py:363
  46.8 1.0 copy-start.10
  47.1 1.0 copy-start.12
  47.1 9.3 %copy-start.11 = (bf16[512,256]{1,0:T(8,128)(2,1)S(1)}, bf16[512,256]{1,0:T(8,128)(2,1)}, u32[]{:S(2)}) copy-start(bf16[512,256]{1,0:T(8,128)(2,1)} %get-tuple-element.37) | copy-start | bytes 786436
  47.1 13.6 %copy-start.7 = (bf16[512,256]{1,0:T(8,128)(2,1)S(1)}, bf16[512,256]{1,0:T(8,128)(2,1)}, u32[]{:S(2)}) copy-start(bf16[512,256]{1,0:T(8,128)(2,1)} %get-tuple-element.36.own_ref) | copy-start | bytes 786436
  47.1 13.6 %copy-start.8 = (bf16[256,256]{1,0:T(8,128)(2,1)S(1)}, bf16[256,256]{1,0:T(8,128)(2,1)}, u32[]{:S(2)}) copy-start(bf16[256,256]{1,0:T(8,128)(2,1)} %get-tuple-element.34.q0) | copy-start | bytes 393220
  47.1 66.4 %collective-permute-start.18 = (bf16[4,128,2048]{2,1,0:T(8,128)(2,1)S(1)}, bf16[4,128,2048]{2,1,0:T(8,128)(2,1)}, u32[]{:S(2)}, u32[]{:S(2)}) collective-permute-start(bf16[4,128,2048]{2,1,0:T(8,128)(2,1)S(1)} %pad_maximum_fusion.mine_ref), channel_id=1, source_target_pairs={{0,4},{4,0},{1,5},{5,1},{2,6},{6,2},{3,7},{7,3},{8,12},{12,8},{9,1... | collective-permute-start | bytes 6291464 | tf_op jit(solution)/shard_map/ppermute | solution.py:332
  47.9 22.8 %collective-permute-start.11 = (bf16[4,512,256]{2,1,0:T(8,128)(2,1)S(1)}, bf16[4,512,256]{2,1,0:T(8,128)(2,1)S(1)}, u32[]{:S(2)}, u32[]{:S(2)}) collective-permute-start(bf16[4,512,256]{2,1,0:T(8,128)(2,1)S(1)} %pad_maximum_fusion.1.kv_ref), channel_id=1, source_target_pairs={{0,4},{4,0},{1,5},{5,1},{2,6},{6,2},{3,7},{7,3},{8,12},{12,8},{9,1... | collective-permute-start | bytes 3145736 | tf_op jit(solution)/shard_map/ppermute | solution.py:332
  48.0 10.5 %collective-permute-start.7 = (bf16[2,512,256]{2,1,0:T(8,128)(2,1)S(1)}, bf16[2,512,256]{2,1,0:T(8,128)(2,1)S(1)}, u32[]{:S(2)}, u32[]{:S(2)}) collective-permute-start(bf16[2,512,256]{2,1,0:T(8,128)(2,1)S(1)} %collective-permute-done.6), channel_id=1, source_target_pairs={{0,32},{4,228},{32,64},{36,4},{64,96},{68,36},{96,128},{100,68},{1... | collective-permute-start | bytes 1572872 | tf_op jit(solution)/shard_map/ppermute | solution.py:367
  48.1 5.1 %collective-permute-start = (bf16[256,256]{1,0:T(8,128)(2,1)S(1)}, bf16[256,256]{1,0:T(8,128)(2,1)S(1)}, u32[]{:S(2)}, u32[]{:S(2)}) collective-permute-start(bf16[256,256]{1,0:T(8,128)(2,1)S(1)} %copy-done.12), channel_id=1, source_target_pairs={{0,8},{8,16},{16,24},{24,0},{1,9},{9,17},{17,25},{25,1},{2,10},{10... | collective-permute-start | bytes 393224 | tf_op jit(solution)/shard_map/ppermute | solution.py:332
  49.7 6.8 %collective-permute-start.1 = (bf16[256,256]{1,0:T(8,128)(2,1)S(1)}, bf16[256,256]{1,0:T(8,128)(2,1)S(1)}, u32[]{:S(2)}, u32[]{:S(2)}) collective-permute-start(bf16[256,256]{1,0:T(8,128)(2,1)S(1)} %copy-done.12), channel_id=1, source_target_pairs={{0,16},{8,24},{16,0},{24,8},{1,17},{9,25},{17,1},{25,9},{2,18},{10... | collective-permute-start | bytes 393224 | tf_op jit(solution)/shard_map/ppermute | solution.py:332
  53.2 7.1 %collective-permute-start.2 = (bf16[256,256]{1,0:T(8,128)(2,1)S(1)}, bf16[256,256]{1,0:T(8,128)(2,1)S(1)}, u32[]{:S(2)}, u32[]{:S(2)}) collective-permute-start(bf16[256,256]{1,0:T(8,128)(2,1)S(1)} %copy-done.12), channel_id=1, source_target_pairs={{0,24},{8,0},{16,8},{24,16},{1,25},{9,1},{17,9},{25,17},{2,26},{10... | collective-permute-start | bytes 393224 | tf_op jit(solution)/shard_map/ppermute | solution.py:332
  56.5 4.3 %collective-permute-start.3 = (bf16[512,256]{1,0:T(8,128)(2,1)S(1)}, bf16[512,256]{1,0:T(8,128)(2,1)S(1)}, u32[]{:S(2)}, u32[]{:S(2)}) collective-permute-start(bf16[512,256]{1,0:T(8,128)(2,1)S(1)} %copy-done.11), channel_id=1, source_target_pairs={{0,4},{4,0},{1,5},{5,1},{2,6},{6,2},{3,7},{7,3},{8,12},{12,8},{9,1... | collective-permute-start | bytes 786440 | tf_op jit(solution)/shard_map/ppermute | solution.py:332
  58.5 21.4 %collective-permute-start.10 = (bf16[2,512,256]{2,1,0:T(8,128)(2,1)S(1)}, bf16[2,512,256]{2,1,0:T(8,128)(2,1)S(1)}, u32[]{:S(2)}, u32[]{:S(2)}) collective-permute-start(bf16[2,512,256]{2,1,0:T(8,128)(2,1)S(1)} %collective-permute-done.7.kv_ref), channel_id=1, source_target_pairs={{0,4},{4,0},{1,5},{5,1},{2,6},{6,2},{3,7},{7,3},{8,12},{12,8},{9,1... | collective-permute-start | bytes 1572872 | tf_op jit(solution)/shard_map/ppermute | solution.py:332
  60.3 10.3 %collective-permute-start.8 = (bf16[512,256]{1,0:T(8,128)(2,1)S(1)}, bf16[512,256]{1,0:T(8,128)(2,1)S(1)}, u32[]{:S(2)}, u32[]{:S(2)}) collective-permute-start(bf16[512,256]{1,0:T(8,128)(2,1)S(1)} %slice_bitcast_fusion), channel_id=1, source_target_pairs={{0,32},{4,228},{32,64},{36,4},{64,96},{68,36},{96,128},{100,68},{1... | collective-permute-start | bytes 786440 | tf_op jit(solution)/shard_map/ppermute | solution.py:372
  70.6 16.3 %collective-permute-start.9 = (bf16[512,256]{1,0:T(8,128)(2,1)S(1)}, bf16[512,256]{1,0:T(8,128)(2,1)S(1)}, u32[]{:S(2)}, u32[]{:S(2)}) collective-permute-start(bf16[512,256]{1,0:T(8,128)(2,1)S(1)} %collective-permute-done.8.kv_ref), channel_id=1, source_target_pairs={{0,4},{4,0},{1,5},{5,1},{2,6},{6,2},{3,7},{7,3},{8,12},{12,8},{9,1... | collective-permute-start | bytes 786440 | tf_op jit(solution)/shard_map/ppermute | solution.py:332
  86.9 10.7 %copy-start.5 = (f32[2]{0:T(128)S(1)}, f32[2]{0:T(128)}, u32[]{:S(2)}) copy-start(f32[2]{0:T(128)} %lam_ref.1) | copy-start | bytes 28
  89.7 23.8 %copy-start.4 = (f32[2048]{0:T(1024)S(1)}, f32[2048]{0:T(1024)}, u32[]{:S(2)}) copy-start(f32[2048]{0:T(1024)} %param.21) | copy-start | bytes 24580
  89.7 23.8 %copy-start.6 = (f32[128]{0:T(128)S(1)}, f32[128]{0:T(128)}, u32[]{:S(2)}) copy-start(f32[128]{0:T(128)} %param.19) | copy-start | bytes 1540
  89.8 5.9 %collective-permute-start.12 = (f32[16,256]{1,0:T(8,128)S(1)}, f32[16,256]{1,0:T(8,128)S(1)}, u32[]{:S(2)}, u32[]{:S(2)}) collective-permute-start(f32[16,256]{1,0:T(8,128)S(1)} %get-tuple-element.57.lse0), channel_id=1, source_target_pairs={{0,8},{8,16},{16,24},{24,0},{1,9},{9,17},{17,25},{25,1},{2,10},{10... | collective-permute-start | bytes 49160 | tf_op jit(solution)/shard_map/ppermute | solution.py:332
  90.8 5.5 %collective-permute-start.13 = (f32[16,256]{1,0:T(8,128)S(1)}, f32[16,256]{1,0:T(8,128)S(1)}, u32[]{:S(2)}, u32[]{:S(2)}) collective-permute-start(f32[16,256]{1,0:T(8,128)S(1)} %get-tuple-element.57.lse0), channel_id=1, source_target_pairs={{0,16},{8,24},{16,0},{24,8},{1,17},{9,25},{17,1},{25,9},{2,18},{10... | collective-permute-start | bytes 49160 | tf_op jit(solution)/shard_map/ppermute | solution.py:332
  93.9 3.7 %collective-permute-start.14 = (f32[16,256]{1,0:T(8,128)S(1)}, f32[16,256]{1,0:T(8,128)S(1)}, u32[]{:S(2)}, u32[]{:S(2)}) collective-permute-start(f32[16,256]{1,0:T(8,128)S(1)} %get-tuple-element.57.lse0), channel_id=1, source_target_pairs={{0,24},{8,0},{16,8},{24,16},{1,25},{9,1},{17,9},{25,17},{2,26},{10... | collective-permute-start | bytes 49160 | tf_op jit(solution)/shard_map/ppermute | solution.py:332
  98.5 0.8 copy-start.2
  99.3 14.3 %all-to-all-start = ((bf16[16,64,256]{2,1,0:T(8,128)(2,1)}), bf16[16,64,256]{2,1,0:T(8,128)(2,1)}, u32[]{:S(2)}, u32[]{:S(2)}) async-start(bf16[16,64,256]{2,1,0:T(8,128)(2,1)} %copy-done.2), calls=%async_computation | async-start | bytes 1048576 | tf_op jit(solution)/shard_map/all_to_all | solution.py:381
  113.6 1.0 copy-start.3
  117.9 7.4 %collective-permute-start.20 = (bf16[64,2048]{1,0:T(8,128)(2,1)S(1)}, bf16[64,2048]{1,0:T(8,128)(2,1)S(1)}, u32[]{:S(2)}, u32[]{:S(2)}) collective-permute-start(bf16[64,2048]{1,0:T(8,128)(2,1)S(1)} %merge.1.refs_0_), channel_id=1, source_target_pairs={{0,3},{1,0},{2,1},{3,2},{4,7},{5,4},{6,5},{7,6},{8,11},{9,8},{10,9... | collective-permute-start | bytes 786440 | tf_op jit(solution)/shard_map/ppermute | solution.py:332
  119.1 7.8 %collective-permute-start.19 = (bf16[64,2048]{1,0:T(8,128)(2,1)S(1)}, bf16[64,2048]{1,0:T(8,128)(2,1)S(1)}, u32[]{:S(2)}, u32[]{:S(2)}) collective-permute-start(bf16[64,2048]{1,0:T(8,128)(2,1)S(1)} %merge.1.refs_0_), channel_id=1, source_target_pairs={{0,1},{1,2},{2,3},{3,0},{4,5},{5,6},{6,7},{7,4},{8,9},{9,10},{10,1... | collective-permute-start | bytes 786440 | tf_op jit(solution)/shard_map/ppermute | solution.py:332
  125.3 5.0 %collective-permute-start.23 = (bf16[32,2048]{1,0:T(8,128)(2,1)S(1)}, bf16[32,2048]{1,0:T(8,128)(2,1)S(1)}, u32[]{:S(2)}, u32[]{:S(2)}) collective-permute-start(bf16[32,2048]{1,0:T(8,128)(2,1)S(1)} %slice.14), channel_id=1, source_target_pairs={{0,3},{1,0},{2,1},{3,2},{4,7},{5,4},{6,5},{7,6},{8,11},{9,8},{10,9... | collective-permute-start | bytes 393224 | tf_op jit(solution)/shard_map/ppermute | solution.py:332
  126.9 6.3 %collective-permute-start.22 = (bf16[32,2048]{1,0:T(8,128)(2,1)S(1)}, bf16[32,2048]{1,0:T(8,128)(2,1)S(1)}, u32[]{:S(2)}, u32[]{:S(2)}) collective-permute-start(bf16[32,2048]{1,0:T(8,128)(2,1)S(1)} %slice.13), channel_id=1, source_target_pairs={{0,1},{1,2},{2,3},{3,0},{4,5},{5,6},{6,7},{7,4},{8,9},{9,10},{10,1... | collective-permute-start | bytes 393224 | tf_op jit(solution)/shard_map/ppermute | solution.py:332
  133.2 3.4 %copy-start.1 = (bf16[128,32,1024]{2,1,0:T(8,128)(2,1)S(1)}, bf16[128,32,1024]{2,1,0:T(8,128)(2,1)}, u32[]{:S(2)}) copy-start(bf16[128,32,1024]{2,1,0:T(8,128)(2,1)} %all-gather.3.cloned.1.call-done) | copy-start | bytes 25165828
  139.5 10.6 %collective-permute-start.25 = (bf16[64,2048]{1,0:T(8,128)(2,1)S(1)}, bf16[64,2048]{1,0:T(8,128)(2,1)S(1)}, u32[]{:S(2)}, u32[]{:S(2)}) collective-permute-start(bf16[64,2048]{1,0:T(8,128)(2,1)S(1)} %get-tuple-element.62), channel_id=1, source_target_pairs={{0,1},{1,2},{2,3},{3,0},{4,5},{5,6},{6,7},{7,4},{8,9},{9,10},{10,1... | collective-permute-start | bytes 786440 | tf_op jit(solution)/shard_map/ppermute | solution.py:332
  141.8 8.4 %collective-permute-start.24 = (bf16[64,2048]{1,0:T(8,128)(2,1)S(1)}, bf16[64,2048]{1,0:T(8,128)(2,1)S(1)}, u32[]{:S(2)}, u32[]{:S(2)}) collective-permute-start(bf16[64,2048]{1,0:T(8,128)(2,1)S(1)} %mixer.3), channel_id=1, source_target_pairs={{0,2},{1,3},{2,0},{3,1},{4,6},{5,7},{6,4},{7,5},{8,10},{9,11},{10,... | collective-permute-start | bytes 786440 | tf_op jit(solution)/shard_map/ppermute | solution.py:332
  143.1 10.0 %collective-permute-start.21 = (bf16[64,2048]{1,0:T(8,128)(2,1)S(1)}, bf16[64,2048]{1,0:T(8,128)(2,1)S(1)}, u32[]{:S(2)}, u32[]{:S(2)}) collective-permute-start(bf16[64,2048]{1,0:T(8,128)(2,1)S(1)} %get-tuple-element.61), channel_id=1, source_target_pairs={{0,3},{1,0},{2,1},{3,2},{4,7},{5,4},{6,5},{7,6},{8,11},{9,8},{10,9... | collective-permute-start | bytes 786440 | tf_op jit(solution)/shard_map/ppermute | solution.py:332
Sparse Core Ops, SparseCore 0:
  10.1 84.8 all-gather.2

commit v6 on v5

--- a/solution.py
+++ b/solution.py
@@ -21,27 +21,44 @@
 VMEM = pl.BlockSpec(memory_space=pltpu.VMEM)
 
 
-def prep_kernel(cos_ref, sin_ref, qa_ref, qb_ref, ka_ref, kb_ref, v_ref, q_out, kv_out, q_own, kv_own):
-    cos = jnp.concatenate([cos_ref[...]] * 4, axis=1)
-    sin = jnp.concatenate([-sin_ref[...], sin_ref[...]] * 2, axis=1)
-    lane = lax.broadcasted_iota(jnp.int32, cos.shape, 1)
+def prep_kernel(
+    cos_ref, sin_ref, qa_ref, qb_ref, ka_ref, kb_ref, v_ref, up_ref, down_ref,
+    q_out, kv_out, q_own, kv_own, mix_out, sem,
+):
+    copies = [
+        pltpu.make_async_copy(ref, mix_out.at[i], sem.at[i]) for i, ref in enumerate((up_ref, down_ref))
+    ]
+    for copy in copies:
+        copy.start()
+    rows = TOK // 4
+    lane = lax.broadcasted_iota(jnp.int32, (rows, 128), 1)
     front = (lane % HEAD) < HEAD // 2
 
-    def turn(ref):
-        x = ref[...].astype(F32)
-        other = jnp.where(front, pltpu.roll(x, 128 - 32, 1), pltpu.roll(x, 32, 1))
-        return (x * cos + other * sin).astype(BF16)
-
-    q_out[:, 0:128] = turn(qa_ref)
-    q_out[:, 128:256] = turn(qb_ref)
-    kv_out[0:TOK, 0:128] = turn(ka_ref)
-    kv_out[0:TOK, 128:256] = turn(kb_ref)
+    def turn_rows(i, carry):
+        at = pl.ds(pl.multiple_of(i * rows, rows), rows)
+        cos = jnp.concatenate([cos_ref[at, :]] * 4, axis=1)
+        sin = jnp.concatenate([-sin_ref[at, :], sin_ref[at, :]] * 2, axis=1)
+
+        def turn(ref):
+            x = ref[at, :].astype(F32)
+            other = jnp.where(front, pltpu.roll(x, 128 - 32, 1), pltpu.roll(x, 32, 1))
+            return (x * cos + other * sin).astype(BF16)
+
+        q_out[at, 0:128] = turn(qa_ref)
+        q_out[at, 128:256] = turn(qb_ref)
+        kv_out[at, 0:128] = turn(ka_ref)
+        kv_out[at, 128:256] = turn(kb_ref)
+        return carry
+
+    lax.fori_loop(0, 4, turn_rows, 0)
     kv_out[TOK : 2 * TOK, :] = v_ref[...].astype(F32).T.astype(BF16)
     q_own[...] = q_out[...]
     kv_own[...] = kv_out[...]
-
-
-def prepare(first_query, second_query, first_key, second_key, values, start):
+    for copy in copies:
+        copy.wait()
+
+
+def prepare(first_query, second_query, first_key, second_key, values, up, down, start):
     positions = (start + jnp.arange(TOK)).astype(F32)
     half = HEAD // 2
     inverse = 10000.0 ** (-jnp.arange(0, half, dtype=F32) * 2.0 / HEAD)
@@ -53,24 +70,33 @@
             jax.ShapeDtypeStruct((TOK, 2 * VD), BF16),
             jax.ShapeDtypeStruct((2 * TOK, 2 * VD), BF16),
         )
-        * 2,
-        in_specs=[VMEM] * 7,
-        out_specs=(VMEM,) * 4,
+        * 2
+        + (jax.ShapeDtypeStruct((2,) + up.shape, BF16),),
+        in_specs=[VMEM] * 7 + [HBM] * 2,
+        out_specs=(VMEM,) * 4 + (HBM,),
+        scratch_shapes=[pltpu.SemaphoreType.DMA((2,))],
         name="prep",
-    )(cos, sin, first_query, second_query, first_key, second_key, values)
+    )(cos, sin, first_query, second_query, first_key, second_key, values, up, down)
 
 
 def load_queries(queries, qs):
-    lane = lax.broadcasted_iota(jnp.int32, (TOK, 128), 1)
-    for o, q in enumerate(queries):
-        for m in range(2):
-            scaled = q[:, m * 128 : (m + 1) * 128].astype(F32) * (LOG2E * HEAD**-0.5)
-            hi = scaled.astype(BF16).astype(F32)
-            lo = scaled - hi
-            for h in range(2):
-                mine = (lane < HEAD) if h == 0 else (lane >= HEAD)
-                qs[o, 2 * h + m, :, 0:128] = jnp.where(mine, hi, 0.0).astype(BF16)
-                qs[o, 2 * h + m, :, 128:256] = jnp.where(mine, lo, 0.0).astype(BF16)
+    rows = TOK // 4
+    lane = lax.broadcasted_iota(jnp.int32, (rows, 128), 1)
+
+    def load(i, carry):
+        at = pl.ds(pl.multiple_of(i * rows, rows), rows)
+        for o, q in enumerate(queries):
+            for m in range(2):
+                scaled = q[at, m * 128 : (m + 1) * 128].astype(F32) * (LOG2E * HEAD**-0.5)
+                hi = scaled.astype(BF16).astype(F32)
+                lo = scaled - hi
+                for h in range(2):
+                    mine = (lane < HEAD) if h == 0 else (lane >= HEAD)
+                    qs[o, 2 * h + m, at, 0:128] = jnp.where(mine, hi, 0.0).astype(BF16)
+                    qs[o, 2 * h + m, at, 128:256] = jnp.where(mine, lo, 0.0).astype(BF16)
+        return carry
+
+    lax.fori_loop(0, 4, load, 0)
 
 
 def absorb(chunks, qs, sc, acc, top, tot, fresh):
@@ -131,7 +157,7 @@
     absorb(chunks_of(kv_ref), qs, sc, acc, top, tot, False)
 
 
-def last_kernel(qs, kv_ref, acc_in, top_in, tot_in, acc, top, tot, lse, sc):
+def last_kernel(qs, kv_ref, acc_in, top_in, tot_in, lse_in, acc, top, tot, lse, sc):
     absorb(chunks_of(kv_ref), qs, sc, acc, top, tot, False)
     for o in range(4):
         for hm in range(4):
@@ -139,10 +165,9 @@
             lse[row : row + 1, :] = top[o, hm] + jnp.log2(tot[o, hm])
 
 
-def share_kernel(x_ref, lam_ref, lse0, lse1, lse2, lse3, acc, tot, out_ref):
+def share_kernel(lam_ref, lse0, lse1, lse2, lse3, acc, tot, *outs):
     lses = (lse0, lse1, lse2, lse3)
     for o in range(4):
-        home = (x_ref[0] + 4 - o) % 4
         factors = []
         for hm in range(4):
             rows = [4 * ((o - k) % 4) + hm for k in range(4)]
@@ -152,9 +177,7 @@
             factors.append(terms[0] / ((terms[0] + terms[1] + terms[2] + terms[3]) * tot[o, hm]))
         for h in range(2):
             diff = acc[o, 2 * h] * factors[2 * h] - acc[o, 2 * h + 1] * (lam_ref[h] * factors[2 * h + 1])
-            out_ref[pl.ds(4 * home, 4), :, h * VD : (h + 1) * VD] = diff.T.astype(BF16).reshape(
-                4, TOK // 4, VD
-            )
+            outs[o][:, h * VD : (h + 1) * VD] = diff.T.astype(BF16)
 
 
 def cost(keys):
@@ -201,9 +224,9 @@
     return pl.pallas_call(
         last_kernel,
         out_shape=STATE + (jax.ShapeDtypeStruct((16, TOK), F32),),
-        in_specs=[VMEM] * 5,
+        in_specs=[VMEM] * 6,
         out_specs=(VMEM,) * 4,
-        input_output_aliases={2: 0, 3: 1, 4: 2},
+        input_output_aliases={2: 0, 3: 1, 4: 2, 5: 3},
         scratch_shapes=[score_scratch(kv.shape[0] // (2 * TOK))],
         cost_estimate=cost(kv.shape[0] // 2),
         compiler_params=pltpu.CompilerParams(vmem_limit_bytes=24 * 2**20),
@@ -211,15 +234,39 @@
     )(qs, kv, *state)
 
 
-def share(x, lambdas, lses, acc, tot):
+def share(lambdas, lses, acc, tot):
     return pl.pallas_call(
         share_kernel,
-        out_shape=jax.ShapeDtypeStruct((16, TOK // 4, 2 * VD), BF16),
-        in_specs=[SMEM, SMEM] + [VMEM] * 6,
-        out_specs=VMEM,
+        out_shape=[jax.ShapeDtypeStruct((TOK, 2 * VD), BF16)] * 4,
+        in_specs=[SMEM] + [VMEM] * 6,
+        out_specs=[VMEM] * 4,
         compiler_params=pltpu.CompilerParams(vmem_limit_bytes=16 * 2**20),
         name="share",
-    )(x, lambdas, *lses, acc, tot)
+    )(lambdas, *lses, acc, tot)
+
+
+def heads_kernel(at_ref, gain_ref, p0, p1, p2, p3, *refs):
+    outs, buf = refs[:4], refs[4]
+    whole = sum(p[...].astype(F32) for p in (p0, p1, p2, p3))
+    for h in range(2):
+        diff = whole[:, h * VD : (h + 1) * VD]
+        scale = lax.rsqrt(jnp.mean(diff * diff, axis=-1, keepdims=True) + 1e-05)
+        buf[:, h * VD : (h + 1) * VD] = (diff * scale * gain_ref[...] * 0.8).astype(BF16)
+    for o in range(4):
+        y = (at_ref[0] + o) % 4
+        outs[o][...] = buf[pl.ds(y * (TOK // 4), TOK // 4), :]
+
+
+def heads(at, head_gain, parts):
+    return pl.pallas_call(
+        heads_kernel,
+        out_shape=[jax.ShapeDtypeStruct((TOK // 4, 2 * VD), BF16)] * 4,
+        in_specs=[SMEM] + [VMEM] * 5,
+        out_specs=[VMEM] * 4,
+        scratch_shapes=[pltpu.VMEM((TOK, 2 * VD), BF16)],
+        compiler_params=pltpu.CompilerParams(vmem_limit_bytes=12 * 2**20),
+        name="heads",
+    )(at, head_gain.reshape(1, VD), *parts)
 
 
 def load_mix_kernel(w_ref, out_ref, sem):
@@ -246,7 +293,7 @@
     )(weights)
 
 
-def merge_kernel(at_ref, part_ref, gain_ref, res_ref, norm_ref, mine_ref, other_ref, out_ref, wbuf, sem):
+def merge_kernel(at_ref, f0, f1, f2, f3, res_ref, norm_ref, mine_ref, other_ref, out_ref, wbuf, sums, sem):
     mine = at_ref[1] * VD
     copies = []
     for o in range(4):
@@ -260,58 +307,71 @@
     for pair in copies:
         for copy in pair:
             copy.start()
-    stream = res_ref[...].astype(F32)
-    for o in range(4):
-        y = (at_ref[0] + 4 - o) % 4
-        both = sum(part_ref[4 * k + y].astype(F32) for k in range(4))
-        heads = []
-        for h in range(2):
-            diff = both[:, h * VD : (h + 1) * VD]
-            scale = lax.rsqrt(jnp.mean(diff * diff, axis=-1, keepdims=True) + 1e-05)
-            heads.append((diff * scale * gain_ref[...] * 0.8).astype(BF16))
-        flat = jnp.concatenate(heads, axis=1)
-        for copy in copies[o]:
+    flat = jnp.concatenate([f[...] for f in (f0, f1, f2, f3)], axis=1)
+    for pair in copies:
+        for copy in pair:
             copy.wait()
-        stream = stream + lax.dot_general(flat, wbuf[o], NN, preferred_element_type=F32)
+    width = out_ref.shape[1] // 8
+
+    def project(i, carry):
+        at = pl.ds(pl.multiple_of(i * width, 128), width)
+        weight = wbuf[:, :, at].reshape(flat.shape[1], width)
+        added = lax.dot_general(flat, weight, NN, preferred_element_type=F32)
+        sums[:, at] = res_ref[:, at].astype(F32) + added
+        return carry
+
+    lax.fori_loop(0, 8, project, 0)
+    stream = sums[...]
     center = stream - jnp.mean(stream, axis=-1, keepdims=True)
     spread = jnp.mean(center * center, axis=-1, keepdims=True)
     out_ref[...] = (center * lax.rsqrt(spread + 1e-05) * norm_ref[...]).astype(BF16)
 
 
-def merge(at, part, head_gain, residual, norm_gain, weights):
+def merge(at, flats, residual, norm_gain, weights):
     rows, width = residual.shape
     return pl.pallas_call(
         merge_kernel,
         out_shape=jax.ShapeDtypeStruct((rows, width), BF16),
-        in_specs=[SMEM] + [VMEM] * 4 + [HBM] * 2,
+        in_specs=[SMEM] + [VMEM] * 6 + [HBM] * 2,
         out_specs=VMEM,
-        scratch_shapes=[pltpu.VMEM((4, 2 * VD, width), BF16), pltpu.SemaphoreType.DMA((8,))],
+        scratch_shapes=[pltpu.VMEM((4, 2 * VD, width), BF16), pltpu.VMEM((rows, width), F32), pltpu.SemaphoreType.DMA((8,))],
         compiler_params=pltpu.CompilerParams(vmem_limit_bytes=24 * 2**20),
         name="merge",
-    )(at, part, head_gain.reshape(1, VD), residual, norm_gain.reshape(1, width), *weights)
+    )(at, *flats, residual, norm_gain.reshape(1, width), *weights)
+
+
+CUTS = 4
 
 
 def mixer_kernel(count, *refs):
-    pieces, w_ref, outs = refs[:count], refs[count], refs[count + 1 :]
+    pieces, w_ref, outs = refs[:count], refs[count], refs[count + 1 : -2]
+    lifted, hidden = refs[-2:]
     devices, _, rows, hidden_width = w_ref.shape
-    x = jnp.concatenate([n[...] for n in pieces], axis=0)
-    cuts = 4
-    per = devices // cuts
+    per = devices // CUTS
     step = per * rows
-    lifted = None
-    for i in range(cuts):
-        block = w_ref[i * per : (i + 1) * per, 0].reshape(step, hidden_width)
-        more = lax.dot_general(x[:, i * step : (i + 1) * step], block, NN, preferred_element_type=F32)
-        lifted = more if lifted is None else lifted + more
-    pos = jnp.maximum(lifted, 0.0)
-    hidden = (pos * pos).astype(BF16)
-    for i in range(cuts):
-        block = w_ref[i * per : (i + 1) * per, 1].reshape(step, hidden_width)
-        low = lax.dot_general(hidden, block, NT, preferred_element_type=F32)
-        at = 0
-        for n, o in zip(pieces, outs):
-            o[:, i * step : (i + 1) * step] = low[at : at + o.shape[0]].astype(o.dtype)
-            at += o.shape[0]
+
+    def lift(i, carry):
+        at = pl.ds(pl.multiple_of(i * step, 128), step)
+        x = jnp.concatenate([n[:, at] for n in pieces], axis=0)
+        block = w_ref[pl.ds(i * per, per), 0].reshape(step, hidden_width)
+        lifted[...] += lax.dot_general(x, block, NN, preferred_element_type=F32)
+        return carry
+
+    def lower(i, carry):
+        at = pl.ds(pl.multiple_of(i * (step // 2), 128), step // 2)
+        block = w_ref[pl.ds(i * (per // 2), per // 2), 1].reshape(step // 2, hidden_width)
+        low = lax.dot_general(hidden[...], block, NT, preferred_element_type=F32)
+        first = 0
+        for o in outs:
+            o[:, at] = low[first : first + o.shape[0]].astype(o.dtype)
+            first += o.shape[0]
+        return carry
+
+    lifted[...] = jnp.zeros_like(lifted)
+    lax.fori_loop(0, CUTS, lift, 0)
+    pos = jnp.maximum(lifted[...], 0.0)
+    hidden[...] = (pos * pos).astype(BF16)
+    lax.fori_loop(0, 2 * CUTS, lower, 0)
 
 
 def mixer(pieces, weights, types):
@@ -321,6 +381,7 @@
         out_shape=[jax.ShapeDtypeStruct(n.shape, t) for n, t in zip(pieces, types)],
         in_specs=[VMEM] * (len(pieces) + 1),
         out_specs=[VMEM] * len(pieces),
+        scratch_shapes=[pltpu.VMEM((sum(n.shape[0] for n in pieces), weights.shape[3]), t) for t in (F32, BF16)],
         cost_estimate=pl.CostEstimate(flops=2 * 256 * width * 2048, bytes_accessed=2**23, transcendentals=0),
         compiler_params=pltpu.CompilerParams(vmem_limit_bytes=24 * 2**20),
         name="mixer",
@@ -347,16 +408,16 @@
     down_weight,
 ):
     sp = lax.axis_index(("z", "x", "c"))
-    x = lax.axis_index("x").astype(jnp.int32).reshape(1)
     at = jnp.stack([lax.axis_index("tp"), lax.axis_index("c")]).astype(jnp.int32)
-    query, kv, query_own, kv_own = prepare(first_query, second_query, first_key, second_key, values, sp * TOK)
+    query, kv, query_own, kv_own, mix_weights = prepare(
+        first_query, second_query, first_key, second_key, values, up_weight, down_weight.T, sp * TOK
+    )
     ring = ("z", "c")
     onward = [(2 * z + c, 2 * ((z + 1 - 2 * c) % 8) + c) for z in range(8) for c in range(2)]
     crossed = [(2 * z + c, 2 * ((z - 1 + 2 * c) % 8) + 1 - c) for z in range(8) for c in range(2)]
     near = [lax.ppermute(kv, ring, onward), lax.ppermute(kv, ring, crossed)]
     other = shifted(kv, "c", 1)
     queries = [query_own] + [shifted(query, "x", o) for o in (1, 2, 3)]
-    mix_weights = jnp.stack([up_weight, down_weight.T])
     mix_weights = lax.all_gather(mix_weights, ("z", "x", "c"))
     half = lax.dynamic_slice_in_dim(out_weight, lax.axis_index("c") * VD, VD, 0)
     near = jnp.stack(near)
@@ -374,12 +435,14 @@
     state = attend_next(qs, third, state)
     state = attend_next(qs, third_other, state)
     far_other = shifted(far, "c", 1)
-    *state, _ = attend_last(qs, far, state)
+    state = attend_last(qs, far, (*state, jnp.zeros((16, TOK), F32)))
     acc, _, tot, lse = attend_last(qs, far_other, state)
     lses = [lse] + [shifted(lse, "x", k) for k in (1, 2, 3)]
-    part = share(x, lambdas, lses, acc, tot)
-    part = lax.all_to_all(part, ("x", "tp"), split_axis=0, concat_axis=0, tiled=True)
-    normed = merge(at, part, head_gain, residual, norm_gain, out_weights)
+    parts = share(lambdas, lses, acc, tot)
+    parts = [parts[0]] + [shifted(parts[o], "x", -o) for o in (1, 2, 3)]
+    flats = heads(at, head_gain, parts)
+    flats = [flats[0]] + [shifted(flats[o], "tp", o) for o in (1, 2, 3)]
+    normed = merge(at, flats, residual, norm_gain, out_weights)
     mix_weights = load_mix(mix_weights)
     rows = normed.shape[0] // 2
     before = shifted(normed, "tp", 1)

time: 162 us -> 172 us (1.062)
  Pallas kernels: 40.2 us -> 50.1 us
  starting transfers between devices: 35.7 us -> 45.4 us
  waiting for transfers between devices: 61.1 us -> 52.9 us
    ppermute x21 -> x27, starting transfers between devices: 24.2 us -> 37.6 us  [shifted(): lax.ppermute(value, axis, [(i, (i + by) % size) for i in range(size)])]
    all_to_all x1 -> x0, waiting for transfers between devices: 8.52 us -> none  [local(): lax.all_to_all(part, ('x', 'tp'), split_axis=0, concat_axis=0, tiled=True)]
    all_to_all x1 -> x0, starting transfers between devices: 5.67 us -> none  [local(): lax.all_to_all(part, ('x', 'tp'), split_axis=0, concat_axis=0, tiled=True)]
    ppermute x2, waiting for transfers between devices: 3.05 us -> 7.75 us  [local(): near = [lax.ppermute(kv, ring, onward), lax.ppermute(kv, ring, crossed)]]
    pallas_call x1, Pallas kernels: 2.53 us -> 7.13 us  [prepare(): pl.pallas_call(prep_kernel, out_shape=(jax.ShapeDtypeStruct((TOK, 2 * VD)...]
    ppermute x21 -> x27, waiting for transfers between devices: 48.4 us -> 45 us  [shifted(): lax.ppermute(value, axis, [(i, (i + by) % size) for i in range(size)])]
    pallas_call x2, Pallas kernels: 4.47 us -> 7.81 us  [mixer(): pl.pallas_call(functools.partial(mixer_kernel, len(pieces)), out_shape=[j...]
    ppermute x1, starting transfers between devices: 0.08 us -> 1.92 us  [local(): third = lax.ppermute(second, ring, onward)]
  transfers between devices with their start and end apart: 28 -> 33, of which waited for: 18 -> 22; matrix products, arithmetic and copies ran while one was open for 1% -> 0% of each run, Pallas kernels for 23% -> 23%
where the time goes in v6:
time: 172 us; the launch traced here: 169 us
  waiting for transfers between devices  52.9 us (31%)
  Pallas kernels  50.1 us (29%)
  starting transfers between devices  45.4 us (26%)
  between operations  13.7 us (8%)
  local copies, waits for them, and re-layouts  4.49 us (3%)
  other arithmetic  2.62 us (2%)
    ppermute x27, waiting for transfers between devices, shifted(): lax.ppermute(value, axis, [(i, (i + by) % size) for i in range(size)])  45 us
    ppermute x27, starting transfers between devices, shifted(): lax.ppermute(value, axis, [(i, (i + by) % size) for i in range(size)])  37.6 us
    pallas_call x4, Pallas kernels, attend_next(): pl.pallas_call(next_kernel, out_shape=STATE, in_specs=[VMEM] * 5, out_spe...  18.2 us
    pallas_call x2, Pallas kernels, mixer(): pl.pallas_call(functools.partial(mixer_kernel, len(pieces)), out_shape=[j...  7.81 us
    ppermute x2, waiting for transfers between devices, local(): near = [lax.ppermute(kv, ring, onward), lax.ppermute(kv, ring, crossed)]  7.75 us
    pallas_call x1, Pallas kernels, prepare(): pl.pallas_call(prep_kernel, out_shape=(jax.ShapeDtypeStruct((TOK, 2 * VD)...  7.13 us
    pallas_call x2, Pallas kernels, attend_last(): pl.pallas_call(last_kernel, out_shape=STATE + (jax.ShapeDtypeStruct((16,...  5.61 us
    ppermute x2, starting transfers between devices, local(): near = [lax.ppermute(kv, ring, onward), lax.ppermute(kv, ring, crossed)]  4.46 us
  transfers between devices with their start and end apart: 33, of which 22 were waited for; matrix products, arithmetic and copies ran while one was open for 0% of the time, Pallas kernels for 23%

profile of v6, /device:TPU:2, one launch (start us, length us, event | category | flops | bytes accessed | tf_op | source)
XLA Modules:
  0.0 169.3 jit_solution(17195912886633462593)
XLA Ops:
  6.6 1.2 multiply_sine_fusion
  7.8 7.1 %prep.1 = (bf16[256,256]{1,0:T(8,128)(2,1)}, bf16[512,256]{1,0:T(8,128)(2,1)}, bf16[256,256]{1,0:T(8,128)(2,1)}, bf16[512,256]{1,0:T(8,128)(2,1)}, bf16[2,32,1024]{2,1,0:T(8,128)(2,1)}) custom-call(f32[256,32]{1,0:T(8,128)} %get-tuple-element.84.cos_ref, f32[256,32]{1,0:T(8,128)} %get-tuple-element.83.sin_ref, bf16[256,128]{1,0:T(8,128)(2,1)} %qa_ref.1, ...), custom_call_target="tpu_custom_call" | custom-call | tf_op jit(solution)/shard_map/prep/pallas_call | solution.py:67
  15.0 3.1 %collective-permute-start.23 = (bf16[128,2048]{1,0:T(8,128)(2,1)S(1)}, bf16[128,2048]{1,0:T(8,128)(2,1)S(1)}, u32[]{:S(2)}, u32[]{:S(2)}) collective-permute-start(bf16[128,2048]{1,0:T(8,128)(2,1)S(1)} %constant_dynamic-slice_fusion), channel_id=1, source_target_pairs={{0,3},{1,0},{2,1},{3,2},{4,7},{5,4},{6,5},{7,6},{8,11},{9,8},{10,9... | collective-permute-start | bytes 1572872 | tf_op jit(solution)/shard_map/ppermute | solution.py:393
  19.7 4.5 %collective-permute-start.5 = (bf16[512,256]{1,0:T(8,128)(2,1)}, bf16[512,256]{1,0:T(8,128)(2,1)S(1)}, u32[]{:S(2)}, u32[]{:S(2)}) collective-permute-start(bf16[512,256]{1,0:T(8,128)(2,1)} %get-tuple-element.47), channel_id=1, source_target_pairs={{0,228},{4,32},{32,4},{36,64},{64,36},{68,96},{96,68},{100,128},{1... | collective-permute-start | bytes 786440 | tf_op jit(solution)/shard_map/ppermute | solution.py:418
  24.2 6.4 %collective-permute-done.5 = bf16[512,256]{1,0:T(8,128)(2,1)S(1)} collective-permute-done((bf16[512,256]{1,0:T(8,128)(2,1)}, bf16[512,256]{1,0:T(8,128)(2,1)S(1)}, u32[]{:S(2)}, u32[]{:S(2)}) %collective-permute-start.5) | collective-permute-done | bytes 262176 | tf_op jit(solution)/shard_map/ppermute | solution.py:418
  30.6 1.3 collective-permute-done.4
  32.1 8.4 %collective-permute-done.23 = bf16[128,2048]{1,0:T(8,128)(2,1)S(1)} collective-permute-done((bf16[128,2048]{1,0:T(8,128)(2,1)S(1)}, bf16[128,2048]{1,0:T(8,128)(2,1)S(1)}, u32[]{:S(2)}, u32[]{:S(2)}) %collective-permute-start.23) | collective-permute-done | bytes 524320 | tf_op jit(solution)/shard_map/ppermute | solution.py:393
  40.5 3.7 %collective-permute-done.21 = bf16[128,2048]{1,0:T(8,128)(2,1)S(1)} collective-permute-done((bf16[128,2048]{1,0:T(8,128)(2,1)S(1)}, bf16[128,2048]{1,0:T(8,128)(2,1)S(1)}, u32[]{:S(2)}, u32[]{:S(2)}) %collective-permute-start.21) | collective-permute-done | bytes 524320 | tf_op jit(solution)/shard_map/ppermute | solution.py:393
  45.4 1.9 %collective-permute-start.7 = (bf16[2,512,256]{2,1,0:T(8,128)(2,1)S(1)}, bf16[2,512,256]{2,1,0:T(8,128)(2,1)S(1)}, u32[]{:S(2)}, u32[]{:S(2)}) collective-permute-start(bf16[2,512,256]{2,1,0:T(8,128)(2,1)S(1)} %collective-permute-done.6), channel_id=1, source_target_pairs={{0,32},{4,228},{32,64},{36,4},{64,96},{68,36},{96,128},{100,68},{1... | collective-permute-start | bytes 1572872 | tf_op jit(solution)/shard_map/ppermute | solution.py:428
  47.3 1.5 collective-permute-start
  49.9 2.4 %collective-permute-done.q1 = bf16[256,256]{1,0:T(8,128)(2,1)S(1)} collective-permute-done((bf16[256,256]{1,0:T(8,128)(2,1)S(1)}, bf16[256,256]{1,0:T(8,128)(2,1)S(1)}, u32[]{:S(2)}, u32[]{:S(2)}) %collective-permute-start) | collective-permute-done | bytes 131104 | tf_op jit(solution)/shard_map/ppermute | solution.py:393
  52.2 1.7 %collective-permute-start.2 = (bf16[256,256]{1,0:T(8,128)(2,1)S(1)}, bf16[256,256]{1,0:T(8,128)(2,1)S(1)}, u32[]{:S(2)}, u32[]{:S(2)}) collective-permute-start(bf16[256,256]{1,0:T(8,128)(2,1)S(1)} %copy-done.9), channel_id=1, source_target_pairs={{0,24},{8,0},{16,8},{24,16},{1,25},{9,1},{17,9},{25,17},{2,26},{10... | collective-permute-start | bytes 393224 | tf_op jit(solution)/shard_map/ppermute | solution.py:393
  54.0 1.2 collective-permute-done.1.q2
  55.2 3.6 %collective-permute-start.3 = (bf16[512,256]{1,0:T(8,128)(2,1)S(1)}, bf16[512,256]{1,0:T(8,128)(2,1)S(1)}, u32[]{:S(2)}, u32[]{:S(2)}) collective-permute-start(bf16[512,256]{1,0:T(8,128)(2,1)S(1)} %copy-done.8), channel_id=1, source_target_pairs={{0,4},{4,0},{1,5},{5,1},{2,6},{6,2},{3,7},{7,3},{8,12},{12,8},{9,1... | collective-permute-start | bytes 786440 | tf_op jit(solution)/shard_map/ppermute | solution.py:393
  59.0 1.3 collective-permute-start.8
  60.3 4.0 %attend_first.1 = (bf16[4,4,256,256]{3,2,1,0:T(8,128)(2,1)S(1)}, f32[4,4,128,256]{3,2,1,0:T(8,128)S(1)}, f32[4,4,1,256]{3,2,1,0:T(1,128)S(1)}, f32[4,4,1,256]{3,2,1,0:T(1,128)S(1)}) custom-call(bf16[256,256]{1,0:T(8,128)(2,1)S(1)} %copy-done.7, bf16[256,256]{1,0:T(8,128)(2,1)S(1)} %collective-permute-done.q1, ...), custom_call_target="tpu_custom_call" | custom-call | flops 805306368 | bytes 524288 | tf_op jit(solution)/shard_map/attend_first/pallas_call | solution.py:196
  64.3 5.4 %attend_next.4 = (f32[4,4,128,256]{3,2,1,0:T(8,128)S(1)}, f32[4,4,1,256]{3,2,1,0:T(1,128)S(1)}, f32[4,4,1,256]{3,2,1,0:T(1,128)S(1)}) custom-call(bf16[4,4,256,256]{3,2,1,0:T(8,128)(2,1)S(1)} %get-tuple-element.48.qs, bf16[4,512,256]{2,1,0:T(8,128)(2,1)S(1)} %pad_maximum_fusion.1.kv_ref, ...), custom_call_target="tpu_custom_call", output_to_operand_aliasing={{0}: (2, {}), {1}: (3, {}), {2}: (4, {})} | custom-call | flops 1610612736 | bytes 1048576 | tf_op jit(solution)/shard_map/attend_next/pallas_call | solution.py:210
  69.8 1.5 collective-permute-start.9
  71.3 5.4 %attend_next.5 = (f32[4,4,128,256]{3,2,1,0:T(8,128)S(1)}, f32[4,4,1,256]{3,2,1,0:T(1,128)S(1)}, f32[4,4,1,256]{3,2,1,0:T(1,128)S(1)}) custom-call(bf16[4,4,256,256]{3,2,1,0:T(8,128)(2,1)S(1)} %get-tuple-element.48.qs, bf16[4,512,256]{2,1,0:T(8,128)(2,1)S(1)} %collective-permute-done.11.kv_ref, ...), custom_call_target="tpu_custom_call", output_to_operand_aliasing={{0}: (2, {}), {1}: (3, {}), {2}: (4, {})} | custom-call | flops 1610612736 | bytes 1048576 | tf_op jit(solution)/shard_map/attend_next/pallas_call | solution.py:210
  76.8 3.7 %attend_next.6 = (f32[4,4,128,256]{3,2,1,0:T(8,128)S(1)}, f32[4,4,1,256]{3,2,1,0:T(1,128)S(1)}, f32[4,4,1,256]{3,2,1,0:T(1,128)S(1)}) custom-call(bf16[4,4,256,256]{3,2,1,0:T(8,128)(2,1)S(1)} %get-tuple-element.48.qs, bf16[2,512,256]{2,1,0:T(8,128)(2,1)S(1)} %collective-permute-done.7.kv_ref, ...), custom_call_target="tpu_custom_call", output_to_operand_aliasing={{0}: (2, {}), {1}: (3, {}), {2}: (4, {})} | custom-call | flops 805306368 | bytes 524288 | tf_op jit(solution)/shard_map/attend_next/pallas_call | solution.py:210
  80.5 3.7 %attend_next.7 = (f32[4,4,128,256]{3,2,1,0:T(8,128)S(1)}, f32[4,4,1,256]{3,2,1,0:T(1,128)S(1)}, f32[4,4,1,256]{3,2,1,0:T(1,128)S(1)}) custom-call(bf16[4,4,256,256]{3,2,1,0:T(8,128)(2,1)S(1)} %get-tuple-element.48.qs, bf16[2,512,256]{2,1,0:T(8,128)(2,1)S(1)} %collective-permute-done.10.kv_ref, ...), custom_call_target="tpu_custom_call", output_to_operand_aliasing={{0}: (2, {}), {1}: (3, {}), {2}: (4, {})} | custom-call | flops 805306368 | bytes 524288 | tf_op jit(solution)/shard_map/attend_next/pallas_call | solution.py:210
  84.1 2.8 %attend_last.2 = (f32[4,4,128,256]{3,2,1,0:T(8,128)S(1)}, f32[4,4,1,256]{3,2,1,0:T(1,128)S(1)}, f32[4,4,1,256]{3,2,1,0:T(1,128)S(1)}, f32[16,256]{1,0:T(8,128)S(1)}) custom-call(bf16[4,4,256,256]{3,2,1,0:T(8,128)(2,1)S(1)} %get-tuple-element.48.qs, ...), custom_call_target="tpu_custom_call", output_to_operand_aliasing={{0}: (2, {}), {1}: (3, {}), {2}: (4, {}), {3}: (5, {})} | custom-call | flops 402653184 | bytes 262144 | tf_op jit(solution)/shard_map/attend_last/pallas_call | solution.py:224
  87.0 2.8 %attend_last.3 = (f32[4,4,128,256]{3,2,1,0:T(8,128)S(1)}, f32[4,4,1,256]{3,2,1,0:T(1,128)S(1)}, f32[4,4,1,256]{3,2,1,0:T(1,128)S(1)}, f32[16,256]{1,0:T(8,128)S(1)}) custom-call(bf16[4,4,256,256]{3,2,1,0:T(8,128)(2,1)S(1)} %get-tuple-element.48.qs, ...), custom_call_target="tpu_custom_call", output_to_operand_aliasing={{0}: (2, {}), {1}: (3, {}), {2}: (4, {}), {3}: (5, {})} | custom-call | flops 402653184 | bytes 262144 | tf_op jit(solution)/shard_map/attend_last/pallas_call | solution.py:224
  91.0 2.9 %collective-permute-start.13 = (f32[16,256]{1,0:T(8,128)S(1)}, f32[16,256]{1,0:T(8,128)S(1)}, u32[]{:S(2)}, u32[]{:S(2)}) collective-permute-start(f32[16,256]{1,0:T(8,128)S(1)} %get-tuple-element.68.lse0), channel_id=1, source_target_pairs={{0,16},{8,24},{16,0},{24,8},{1,17},{9,25},{17,1},{25,9},{2,18},{10... | collective-permute-start | bytes 49160 | tf_op jit(solution)/shard_map/ppermute | solution.py:393
  93.8 1.6 collective-permute-start.14
  96.3 1.3 collective-permute-done.14.lse3
  97.6 1.5 share.1
  99.1 1.6 collective-permute-start.15
  101.6 2.0 %collective-permute-start.17 = (bf16[256,256]{1,0:T(8,128)(2,1)}, bf16[256,256]{1,0:T(8,128)(2,1)}, u32[]{:S(2)}, u32[]{:S(2)}) collective-permute-start(bf16[256,256]{1,0:T(8,128)(2,1)} %get-tuple-element.74), channel_id=1, source_target_pairs={{0,8},{8,16},{16,24},{24,0},{1,9},{9,17},{17,25},{25,1},{2,10},{10... | collective-permute-start | bytes 393224 | tf_op jit(solution)/shard_map/ppermute | solution.py:393
  103.7 1.6 collective-permute-done.15.p1
  105.3 2.2 %collective-permute-done.16.p2 = bf16[256,256]{1,0:T(8,128)(2,1)S(1)} collective-permute-done((bf16[256,256]{1,0:T(8,128)(2,1)}, bf16[256,256]{1,0:T(8,128)(2,1)S(1)}, u32[]{:S(2)}, u32[]{:S(2)}) %collective-permute-start.16) | collective-permute-done | bytes 131104 | tf_op jit(solution)/shard_map/ppermute | solution.py:393
  109.5 2.0 %collective-permute-start.19 = (bf16[64,256]{1,0:T(8,128)(2,1)S(1)}, bf16[64,256]{1,0:T(8,128)(2,1)S(1)}, u32[]{:S(2)}, u32[]{:S(2)}) collective-permute-start(bf16[64,256]{1,0:T(8,128)(2,1)S(1)} %get-tuple-element.77), channel_id=1, source_target_pairs={{0,2},{1,3},{2,0},{3,1},{4,6},{5,7},{6,4},{7,5},{8,10},{9,11},{10,... | collective-permute-start | bytes 98312 | tf_op jit(solution)/shard_map/ppermute | solution.py:393
  111.6 1.2 collective-permute-start.20
  112.8 1.9 %collective-permute-done.18.f1 = bf16[64,256]{1,0:T(8,128)(2,1)S(1)} collective-permute-done((bf16[64,256]{1,0:T(8,128)(2,1)S(1)}, bf16[64,256]{1,0:T(8,128)(2,1)S(1)}, u32[]{:S(2)}, u32[]{:S(2)}) %collective-permute-start.18) | collective-permute-done | bytes 32800 | tf_op jit(solution)/shard_map/ppermute | solution.py:393
  116.8 4.2 %merge.1.refs_0_ = bf16[64,2048]{1,0:T(8,128)(2,1)S(1)} custom-call(s32[2]{0:T(128)S(1)} %pad_add_fusion.at_ref, bf16[64,256]{1,0:T(8,128)(2,1)S(1)} %get-tuple-element.75.f0, bf16[64,256]{1,0:T(8,128)(2,1)S(1)} %collective-permute-done.18.f1, bf16[64,256]{1,0:T(8,128)(2,1)S(1)} %collective-permute-done.19.f2, ...), custom_call_target="tpu_custom_call" | custom-call | tf_op jit(solution)/shard_map/merge/pallas_call | solution.py:332
  121.0 2.5 %collective-permute-start.26 = (bf16[64,2048]{1,0:T(8,128)(2,1)S(1)}, bf16[64,2048]{1,0:T(8,128)(2,1)S(1)}, u32[]{:S(2)}, u32[]{:S(2)}) collective-permute-start(bf16[64,2048]{1,0:T(8,128)(2,1)S(1)} %merge.1.refs_0_), channel_id=1, source_target_pairs={{0,3},{1,0},{2,1},{3,2},{4,7},{5,4},{6,5},{7,6},{8,11},{9,8},{10,9... | collective-permute-start | bytes 786440 | tf_op jit(solution)/shard_map/ppermute | solution.py:393
  123.5 5.3 %collective-permute-done.26.refs_2_ = bf16[64,2048]{1,0:T(8,128)(2,1)S(1)} collective-permute-done((bf16[64,2048]{1,0:T(8,128)(2,1)S(1)}, bf16[64,2048]{1,0:T(8,128)(2,1)S(1)}, u32[]{:S(2)}, u32[]{:S(2)}) %collective-permute-start.26) | collective-permute-done | bytes 262176 | tf_op jit(solution)/shard_map/ppermute | solution.py:393
  128.8 3.0 %collective-permute-start.29 = (bf16[32,2048]{1,0:T(8,128)(2,1)S(1)}, bf16[32,2048]{1,0:T(8,128)(2,1)S(1)}, u32[]{:S(2)}, u32[]{:S(2)}) collective-permute-start(bf16[32,2048]{1,0:T(8,128)(2,1)S(1)} %slice.14), channel_id=1, source_target_pairs={{0,3},{1,0},{2,1},{3,2},{4,7},{5,4},{6,5},{7,6},{8,11},{9,8},{10,9... | collective-permute-start | bytes 393224 | tf_op jit(solution)/shard_map/ppermute | solution.py:393
  132.1 2.3 %collective-permute-done.29 = bf16[32,2048]{1,0:T(8,128)(2,1)S(1)} collective-permute-done((bf16[32,2048]{1,0:T(8,128)(2,1)S(1)}, bf16[32,2048]{1,0:T(8,128)(2,1)S(1)}, u32[]{:S(2)}, u32[]{:S(2)}) %collective-permute-start.29) | collective-permute-done | bytes 131104 | tf_op jit(solution)/shard_map/ppermute | solution.py:393
  134.4 3.8 %collective-permute-done.28 = bf16[32,2048]{1,0:T(8,128)(2,1)S(1)} collective-permute-done((bf16[32,2048]{1,0:T(8,128)(2,1)S(1)}, bf16[32,2048]{1,0:T(8,128)(2,1)S(1)}, u32[]{:S(2)}, u32[]{:S(2)}) %collective-permute-start.28) | collective-permute-done | bytes 131104 | tf_op jit(solution)/shard_map/ppermute | solution.py:393
  138.3 3.4 %copy-done.1 = bf16[128,32,1024]{2,1,0:T(8,128)(2,1)S(1)} copy-done((bf16[128,32,1024]{2,1,0:T(8,128)(2,1)S(1)}, bf16[128,32,1024]{2,1,0:T(8,128)(2,1)}, u32[]{:S(2)}) %copy-start.1) | copy-done | bytes 8388632
  142.3 4.3 %mixer.2 = (f32[64,2048]{1,0:T(8,128)S(1)}, bf16[64,2048]{1,0:T(8,128)(2,1)S(1)}, bf16[64,2048]{1,0:T(8,128)(2,1)S(1)}) custom-call(bf16[64,2048]{1,0:T(8,128)(2,1)S(1)} %merge.1.refs_0_, bf16[64,2048]{1,0:T(8,128)(2,1)S(1)} %collective-permute-done.25.refs_1_, bf16[64,2048]{1,0:T(8,128)(2,1)S(1)} %collective-permute-done.26.refs_2_, ...), custom_call_target="tpu_custom_call" | custom-call | flops 2147483648 | bytes 8388608 | tf_op jit(solution)/shard_map/mixer/pallas_call | solution.py:379
  146.7 3.5 %mixer.3 = bf16[64,2048]{1,0:T(8,128)(2,1)S(1)} custom-call(bf16[64,2048]{1,0:T(8,128)(2,1)S(1)} %pad_maximum_fusion.3.refs_0_, bf16[64,2,32,1024]{3,2,1,0:T(8,128)(2,1)S(1)} %load_mix.1.refs_3_.refs_1_), custom_call_target="tpu_custom_call" | custom-call | flops 2147483648 | bytes 8388608 | tf_op jit(solution)/shard_map/mixer/pallas_call | solution.py:379
  150.2 1.4 collective-permute-start.30
  151.6 2.0 %collective-permute-start.27 = (bf16[64,2048]{1,0:T(8,128)(2,1)S(1)}, bf16[64,2048]{1,0:T(8,128)(2,1)S(1)}, u32[]{:S(2)}, u32[]{:S(2)}) collective-permute-start(bf16[64,2048]{1,0:T(8,128)(2,1)S(1)} %get-tuple-element.81), channel_id=1, source_target_pairs={{0,3},{1,0},{2,1},{3,2},{4,7},{5,4},{6,5},{7,6},{8,11},{9,8},{10,9... | collective-permute-start | bytes 786440 | tf_op jit(solution)/shard_map/ppermute | solution.py:393
  153.6 1.4 collective-permute-done.31
  155.0 3.1 %collective-permute-done.30 = bf16[64,2048]{1,0:T(8,128)(2,1)S(1)} collective-permute-done((bf16[64,2048]{1,0:T(8,128)(2,1)S(1)}, bf16[64,2048]{1,0:T(8,128)(2,1)S(1)}, u32[]{:S(2)}, u32[]{:S(2)}) %collective-permute-start.30) | collective-permute-done | bytes 262176 | tf_op jit(solution)/shard_map/ppermute | solution.py:393
  158.1 3.4 %collective-permute-done.27 = bf16[64,2048]{1,0:T(8,128)(2,1)S(1)} collective-permute-done((bf16[64,2048]{1,0:T(8,128)(2,1)S(1)}, bf16[64,2048]{1,0:T(8,128)(2,1)S(1)}, u32[]{:S(2)}, u32[]{:S(2)}) %collective-permute-start.27) | collective-permute-done | bytes 262176 | tf_op jit(solution)/shard_map/ppermute | solution.py:393
  (68 shorter events, 13.2 us)
Async XLA Ops:
  6.5 8.4 %copy-start = (bf16[256,2048]{1,0:T(8,128)(2,1)S(1)}, bf16[256,2048]{1,0:T(8,128)(2,1)}, u32[]{:S(2)}) copy-start(bf16[256,2048]{1,0:T(8,128)(2,1)} %param.20) | copy-start | bytes 3145732
  6.5 131.7 %all-gather.3.cloned.1.call-start = ((), (), s32[]{:S(2)}) async-start(), calls=%async_computation | async-start | bytes 8519680 | tf_op jit(solution)/shard_map/all_gather | solution.py:421
  15.0 25.5 %collective-permute-start.23 = (bf16[128,2048]{1,0:T(8,128)(2,1)S(1)}, bf16[128,2048]{1,0:T(8,128)(2,1)S(1)}, u32[]{:S(2)}, u32[]{:S(2)}) collective-permute-start(bf16[128,2048]{1,0:T(8,128)(2,1)S(1)} %constant_dynamic-slice_fusion), channel_id=1, source_target_pairs={{0,3},{1,0},{2,1},{3,2},{4,7},{5,4},{6,5},{7,6},{8,11},{9,8},{10,9... | collective-permute-start | bytes 1572872 | tf_op jit(solution)/shard_map/ppermute | solution.py:393
  18.1 22.4 %collective-permute-start.22 = (bf16[128,2048]{1,0:T(8,128)(2,1)S(1)}, bf16[128,2048]{1,0:T(8,128)(2,1)S(1)}, u32[]{:S(2)}, u32[]{:S(2)}) collective-permute-start(bf16[128,2048]{1,0:T(8,128)(2,1)S(1)} %constant_dynamic-slice_fusion), channel_id=1, source_target_pairs={{0,2},{1,3},{2,0},{3,1},{4,6},{5,7},{6,4},{7,5},{8,10},{9,11},{10,... | collective-permute-start | bytes 1572872 | tf_op jit(solution)/shard_map/ppermute | solution.py:393
  18.8 25.5 %collective-permute-start.21 = (bf16[128,2048]{1,0:T(8,128)(2,1)S(1)}, bf16[128,2048]{1,0:T(8,128)(2,1)S(1)}, u32[]{:S(2)}, u32[]{:S(2)}) collective-permute-start(bf16[128,2048]{1,0:T(8,128)(2,1)S(1)} %constant_dynamic-slice_fusion), channel_id=1, source_target_pairs={{0,1},{1,2},{2,3},{3,0},{4,5},{5,6},{6,7},{7,4},{8,9},{9,10},{10,1... | collective-permute-start | bytes 1572872 | tf_op jit(solution)/shard_map/ppermute | solution.py:393
  19.7 10.9 %collective-permute-start.5 = (bf16[512,256]{1,0:T(8,128)(2,1)}, bf16[512,256]{1,0:T(8,128)(2,1)S(1)}, u32[]{:S(2)}, u32[]{:S(2)}) collective-permute-start(bf16[512,256]{1,0:T(8,128)(2,1)} %get-tuple-element.47), channel_id=1, source_target_pairs={{0,228},{4,32},{32,4},{36,64},{64,36},{68,96},{96,68},{100,128},{1... | collective-permute-start | bytes 786440 | tf_op jit(solution)/shard_map/ppermute | solution.py:418
  24.2 7.8 %collective-permute-start.4 = (bf16[512,256]{1,0:T(8,128)(2,1)}, bf16[512,256]{1,0:T(8,128)(2,1)S(1)}, u32[]{:S(2)}, u32[]{:S(2)}) collective-permute-start(bf16[512,256]{1,0:T(8,128)(2,1)} %get-tuple-element.47), channel_id=1, source_target_pairs={{0,32},{4,228},{32,64},{36,4},{64,96},{68,36},{96,128},{100,68},{1... | collective-permute-start | bytes 786440 | tf_op jit(solution)/shard_map/ppermute | solution.py:418
  32.0 12.6 %collective-permute-start.6 = (bf16[2,512,256]{2,1,0:T(8,128)(2,1)S(1)}, bf16[2,512,256]{2,1,0:T(8,128)(2,1)S(1)}, u32[]{:S(2)}, u32[]{:S(2)}) collective-permute-start(bf16[2,512,256]{2,1,0:T(8,128)(2,1)S(1)} %pad_maximum_fusion.2), channel_id=1, source_target_pairs={{0,32},{4,228},{32,64},{36,4},{64,96},{68,36},{96,128},{100,68},{1... | collective-permute-start | bytes 1572872 | tf_op jit(solution)/shard_map/ppermute | solution.py:424
  44.5 2.8 %copy-start.9 = (bf16[256,256]{1,0:T(8,128)(2,1)S(1)}, bf16[256,256]{1,0:T(8,128)(2,1)}, u32[]{:S(2)}) copy-start(bf16[256,256]{1,0:T(8,128)(2,1)} %get-tuple-element.45) | copy-start | bytes 393220
  44.5 10.7 %copy-start.8 = (bf16[512,256]{1,0:T(8,128)(2,1)S(1)}, bf16[512,256]{1,0:T(8,128)(2,1)}, u32[]{:S(2)}) copy-start(bf16[512,256]{1,0:T(8,128)(2,1)} %get-tuple-element.47) | copy-start | bytes 786436
  44.5 15.8 %copy-start.6 = (bf16[512,256]{1,0:T(8,128)(2,1)S(1)}, bf16[512,256]{1,0:T(8,128)(2,1)}, u32[]{:S(2)}) copy-start(bf16[512,256]{1,0:T(8,128)(2,1)} %get-tuple-element.46.own_ref) | copy-start | bytes 786436
  44.5 15.7 %copy-start.7 = (bf16[256,256]{1,0:T(8,128)(2,1)S(1)}, bf16[256,256]{1,0:T(8,128)(2,1)}, u32[]{:S(2)}) copy-start(bf16[256,256]{1,0:T(8,128)(2,1)} %get-tuple-element.44.q0) | copy-start | bytes 393220
  44.6 71.3 %collective-permute-start.24 = (bf16[4,128,2048]{2,1,0:T(8,128)(2,1)S(1)}, bf16[4,128,2048]{2,1,0:T(8,128)(2,1)}, u32[]{:S(2)}, u32[]{:S(2)}) collective-permute-start(bf16[4,128,2048]{2,1,0:T(8,128)(2,1)S(1)} %pad_maximum_fusion.mine_ref), channel_id=1, source_target_pairs={{0,4},{4,0},{1,5},{5,1},{2,6},{6,2},{3,7},{7,3},{8,12},{12,8},{9,1... | collective-permute-start | bytes 6291464 | tf_op jit(solution)/shard_map/ppermute | solution.py:393
  44.8 26.5 %collective-permute-start.11 = (bf16[4,512,256]{2,1,0:T(8,128)(2,1)S(1)}, bf16[4,512,256]{2,1,0:T(8,128)(2,1)S(1)}, u32[]{:S(2)}, u32[]{:S(2)}) collective-permute-start(bf16[4,512,256]{2,1,0:T(8,128)(2,1)S(1)} %pad_maximum_fusion.1.kv_ref), channel_id=1, source_target_pairs={{0,4},{4,0},{1,5},{5,1},{2,6},{6,2},{3,7},{7,3},{8,12},{12,8},{9,1... | collective-permute-start | bytes 3145736 | tf_op jit(solution)/shard_map/ppermute | solution.py:393
  45.4 13.6 %collective-permute-start.7 = (bf16[2,512,256]{2,1,0:T(8,128)(2,1)S(1)}, bf16[2,512,256]{2,1,0:T(8,128)(2,1)S(1)}, u32[]{:S(2)}, u32[]{:S(2)}) collective-permute-start(bf16[2,512,256]{2,1,0:T(8,128)(2,1)S(1)} %collective-permute-done.6), channel_id=1, source_target_pairs={{0,32},{4,228},{32,64},{36,4},{64,96},{68,36},{96,128},{100,68},{1... | collective-permute-start | bytes 1572872 | tf_op jit(solution)/shard_map/ppermute | solution.py:428
  47.3 5.0 %collective-permute-start = (bf16[256,256]{1,0:T(8,128)(2,1)S(1)}, bf16[256,256]{1,0:T(8,128)(2,1)S(1)}, u32[]{:S(2)}, u32[]{:S(2)}) collective-permute-start(bf16[256,256]{1,0:T(8,128)(2,1)S(1)} %copy-done.9), channel_id=1, source_target_pairs={{0,8},{8,16},{16,24},{24,0},{1,9},{9,17},{17,25},{25,1},{2,10},{10... | collective-permute-start | bytes 393224 | tf_op jit(solution)/shard_map/ppermute | solution.py:393
  48.8 6.5 %collective-permute-start.1 = (bf16[256,256]{1,0:T(8,128)(2,1)S(1)}, bf16[256,256]{1,0:T(8,128)(2,1)S(1)}, u32[]{:S(2)}, u32[]{:S(2)}) collective-permute-start(bf16[256,256]{1,0:T(8,128)(2,1)S(1)} %copy-done.9), channel_id=1, source_target_pairs={{0,16},{8,24},{16,0},{24,8},{1,17},{9,25},{17,1},{25,9},{2,18},{10... | collective-permute-start | bytes 393224 | tf_op jit(solution)/shard_map/ppermute | solution.py:393
  52.2 6.8 %collective-permute-start.2 = (bf16[256,256]{1,0:T(8,128)(2,1)S(1)}, bf16[256,256]{1,0:T(8,128)(2,1)S(1)}, u32[]{:S(2)}, u32[]{:S(2)}) collective-permute-start(bf16[256,256]{1,0:T(8,128)(2,1)S(1)} %copy-done.9), channel_id=1, source_target_pairs={{0,24},{8,0},{16,8},{24,16},{1,25},{9,1},{17,9},{25,17},{2,26},{10... | collective-permute-start | bytes 393224 | tf_op jit(solution)/shard_map/ppermute | solution.py:393
  55.2 5.0 %collective-permute-start.3 = (bf16[512,256]{1,0:T(8,128)(2,1)S(1)}, bf16[512,256]{1,0:T(8,128)(2,1)S(1)}, u32[]{:S(2)}, u32[]{:S(2)}) collective-permute-start(bf16[512,256]{1,0:T(8,128)(2,1)S(1)} %copy-done.8), channel_id=1, source_target_pairs={{0,4},{4,0},{1,5},{5,1},{2,6},{6,2},{3,7},{7,3},{8,12},{12,8},{9,1... | collective-permute-start | bytes 786440 | tf_op jit(solution)/shard_map/ppermute | solution.py:393
  59.0 21.5 %collective-permute-start.10 = (bf16[2,512,256]{2,1,0:T(8,128)(2,1)S(1)}, bf16[2,512,256]{2,1,0:T(8,128)(2,1)S(1)}, u32[]{:S(2)}, u32[]{:S(2)}) collective-permute-start(bf16[2,512,256]{2,1,0:T(8,128)(2,1)S(1)} %collective-permute-done.7.kv_ref), channel_id=1, source_target_pairs={{0,4},{4,0},{1,5},{5,1},{2,6},{6,2},{3,7},{7,3},{8,12},{12,8},{9,1... | collective-permute-start | bytes 1572872 | tf_op jit(solution)/shard_map/ppermute | solution.py:393
  59.0 10.8 %collective-permute-start.8 = (bf16[512,256]{1,0:T(8,128)(2,1)S(1)}, bf16[512,256]{1,0:T(8,128)(2,1)S(1)}, u32[]{:S(2)}, u32[]{:S(2)}) collective-permute-start(bf16[512,256]{1,0:T(8,128)(2,1)S(1)} %slice_bitcast_fusion), channel_id=1, source_target_pairs={{0,32},{4,228},{32,64},{36,4},{64,96},{68,36},{96,128},{100,68},{1... | collective-permute-start | bytes 786440 | tf_op jit(solution)/shard_map/ppermute | solution.py:433
  69.8 17.2 %collective-permute-start.9 = (bf16[512,256]{1,0:T(8,128)(2,1)S(1)}, bf16[512,256]{1,0:T(8,128)(2,1)S(1)}, u32[]{:S(2)}, u32[]{:S(2)}) collective-permute-start(bf16[512,256]{1,0:T(8,128)(2,1)S(1)} %collective-permute-done.8.kv_ref), channel_id=1, source_target_pairs={{0,4},{4,0},{1,5},{5,1},{2,6},{6,2},{3,7},{7,3},{8,12},{12,8},{9,1... | collective-permute-start | bytes 786440 | tf_op jit(solution)/shard_map/ppermute | solution.py:393
  87.0 10.6 %copy-start.4 = (f32[2]{0:T(128)S(1)}, f32[2]{0:T(128)}, u32[]{:S(2)}) copy-start(f32[2]{0:T(128)} %lam_ref.1) | copy-start | bytes 28
  89.8 18.3 %copy-start.5 = (f32[128]{0:T(128)S(1)}, f32[128]{0:T(128)}, u32[]{:S(2)}) copy-start(f32[128]{0:T(128)} %param.19) | copy-start | bytes 1540
  89.8 26.1 %copy-start.3 = (f32[2048]{0:T(1024)S(1)}, f32[2048]{0:T(1024)}, u32[]{:S(2)}) copy-start(f32[2048]{0:T(1024)} %param.21) | copy-start | bytes 24580
  89.8 5.6 %collective-permute-start.12 = (f32[16,256]{1,0:T(8,128)S(1)}, f32[16,256]{1,0:T(8,128)S(1)}, u32[]{:S(2)}, u32[]{:S(2)}) collective-permute-start(f32[16,256]{1,0:T(8,128)S(1)} %get-tuple-element.68.lse0), channel_id=1, source_target_pairs={{0,8},{8,16},{16,24},{24,0},{1,9},{9,17},{17,25},{25,1},{2,10},{10... | collective-permute-start | bytes 49160 | tf_op jit(solution)/shard_map/ppermute | solution.py:393
  91.0 5.3 %collective-permute-start.13 = (f32[16,256]{1,0:T(8,128)S(1)}, f32[16,256]{1,0:T(8,128)S(1)}, u32[]{:S(2)}, u32[]{:S(2)}) collective-permute-start(f32[16,256]{1,0:T(8,128)S(1)} %get-tuple-element.68.lse0), channel_id=1, source_target_pairs={{0,16},{8,24},{16,0},{24,8},{1,17},{9,25},{17,1},{25,9},{2,18},{10... | collective-permute-start | bytes 49160 | tf_op jit(solution)/shard_map/ppermute | solution.py:393
  93.8 3.7 %collective-permute-start.14 = (f32[16,256]{1,0:T(8,128)S(1)}, f32[16,256]{1,0:T(8,128)S(1)}, u32[]{:S(2)}, u32[]{:S(2)}) collective-permute-start(f32[16,256]{1,0:T(8,128)S(1)} %get-tuple-element.68.lse0), channel_id=1, source_target_pairs={{0,24},{8,0},{16,8},{24,16},{1,25},{9,1},{17,9},{25,17},{2,26},{10... | collective-permute-start | bytes 49160 | tf_op jit(solution)/shard_map/ppermute | solution.py:393
  99.1 6.2 %collective-permute-start.15 = (bf16[256,256]{1,0:T(8,128)(2,1)}, bf16[256,256]{1,0:T(8,128)(2,1)S(1)}, u32[]{:S(2)}, u32[]{:S(2)}) collective-permute-start(bf16[256,256]{1,0:T(8,128)(2,1)} %get-tuple-element.72), channel_id=1, source_target_pairs={{0,24},{8,0},{16,8},{24,16},{1,25},{9,1},{17,9},{25,17},{2,26},{10... | collective-permute-start | bytes 393224 | tf_op jit(solution)/shard_map/ppermute | solution.py:393
  100.7 6.8 %collective-permute-start.16 = (bf16[256,256]{1,0:T(8,128)(2,1)}, bf16[256,256]{1,0:T(8,128)(2,1)S(1)}, u32[]{:S(2)}, u32[]{:S(2)}) collective-permute-start(bf16[256,256]{1,0:T(8,128)(2,1)} %get-tuple-element.73), channel_id=1, source_target_pairs={{0,16},{8,24},{16,0},{24,8},{1,17},{9,25},{17,1},{25,9},{2,18},{10... | collective-permute-start | bytes 393224 | tf_op jit(solution)/shard_map/ppermute | solution.py:393
  101.6 6.6 %collective-permute-start.17 = (bf16[256,256]{1,0:T(8,128)(2,1)}, bf16[256,256]{1,0:T(8,128)(2,1)}, u32[]{:S(2)}, u32[]{:S(2)}) collective-permute-start(bf16[256,256]{1,0:T(8,128)(2,1)} %get-tuple-element.74), channel_id=1, source_target_pairs={{0,8},{8,16},{16,24},{24,0},{1,9},{9,17},{17,25},{25,1},{2,10},{10... | collective-permute-start | bytes 393224 | tf_op jit(solution)/shard_map/ppermute | solution.py:393
  109.2 5.4 %collective-permute-start.18 = (bf16[64,256]{1,0:T(8,128)(2,1)S(1)}, bf16[64,256]{1,0:T(8,128)(2,1)S(1)}, u32[]{:S(2)}, u32[]{:S(2)}) collective-permute-start(bf16[64,256]{1,0:T(8,128)(2,1)S(1)} %get-tuple-element.76), channel_id=1, source_target_pairs={{0,1},{1,2},{2,3},{3,0},{4,5},{5,6},{6,7},{7,4},{8,9},{9,10},{10,1... | collective-permute-start | bytes 98312 | tf_op jit(solution)/shard_map/ppermute | solution.py:393
  109.5 5.5 %collective-permute-start.19 = (bf16[64,256]{1,0:T(8,128)(2,1)S(1)}, bf16[64,256]{1,0:T(8,128)(2,1)S(1)}, u32[]{:S(2)}, u32[]{:S(2)}) collective-permute-start(bf16[64,256]{1,0:T(8,128)(2,1)S(1)} %get-tuple-element.77), channel_id=1, source_target_pairs={{0,2},{1,3},{2,0},{3,1},{4,6},{5,7},{6,4},{7,5},{8,10},{9,11},{10,... | collective-permute-start | bytes 98312 | tf_op jit(solution)/shard_map/ppermute | solution.py:393
  111.6 4.3 %collective-permute-start.20 = (bf16[64,256]{1,0:T(8,128)(2,1)S(1)}, bf16[64,256]{1,0:T(8,128)(2,1)S(1)}, u32[]{:S(2)}, u32[]{:S(2)}) collective-permute-start(bf16[64,256]{1,0:T(8,128)(2,1)S(1)} %get-tuple-element.78), channel_id=1, source_target_pairs={{0,3},{1,0},{2,1},{3,2},{4,7},{5,4},{6,5},{7,6},{8,11},{9,8},{10,9... | collective-permute-start | bytes 98312 | tf_op jit(solution)/shard_map/ppermute | solution.py:393
  115.9 1.0 copy-start.2
  121.0 7.9 %collective-permute-start.26 = (bf16[64,2048]{1,0:T(8,128)(2,1)S(1)}, bf16[64,2048]{1,0:T(8,128)(2,1)S(1)}, u32[]{:S(2)}, u32[]{:S(2)}) collective-permute-start(bf16[64,2048]{1,0:T(8,128)(2,1)S(1)} %merge.1.refs_0_), channel_id=1, source_target_pairs={{0,3},{1,0},{2,1},{3,2},{4,7},{5,4},{6,5},{7,6},{8,11},{9,8},{10,9... | collective-permute-start | bytes 786440 | tf_op jit(solution)/shard_map/ppermute | solution.py:393
  123.5 8.5 %collective-permute-start.25 = (bf16[64,2048]{1,0:T(8,128)(2,1)S(1)}, bf16[64,2048]{1,0:T(8,128)(2,1)S(1)}, u32[]{:S(2)}, u32[]{:S(2)}) collective-permute-start(bf16[64,2048]{1,0:T(8,128)(2,1)S(1)} %merge.1.refs_0_), channel_id=1, source_target_pairs={{0,1},{1,2},{2,3},{3,0},{4,5},{5,6},{6,7},{7,4},{8,9},{9,10},{10,1... | collective-permute-start | bytes 786440 | tf_op jit(solution)/shard_map/ppermute | solution.py:393
  128.8 5.5 %collective-permute-start.29 = (bf16[32,2048]{1,0:T(8,128)(2,1)S(1)}, bf16[32,2048]{1,0:T(8,128)(2,1)S(1)}, u32[]{:S(2)}, u32[]{:S(2)}) collective-permute-start(bf16[32,2048]{1,0:T(8,128)(2,1)S(1)} %slice.14), channel_id=1, source_target_pairs={{0,3},{1,0},{2,1},{3,2},{4,7},{5,4},{6,5},{7,6},{8,11},{9,8},{10,9... | collective-permute-start | bytes 393224 | tf_op jit(solution)/shard_map/ppermute | solution.py:393
  132.0 6.3 %collective-permute-start.28 = (bf16[32,2048]{1,0:T(8,128)(2,1)S(1)}, bf16[32,2048]{1,0:T(8,128)(2,1)S(1)}, u32[]{:S(2)}, u32[]{:S(2)}) collective-permute-start(bf16[32,2048]{1,0:T(8,128)(2,1)S(1)} %slice.13), channel_id=1, source_target_pairs={{0,1},{1,2},{2,3},{3,0},{4,5},{5,6},{6,7},{7,4},{8,9},{9,10},{10,1... | collective-permute-start | bytes 393224 | tf_op jit(solution)/shard_map/ppermute | solution.py:393
  138.3 3.4 %copy-start.1 = (bf16[128,32,1024]{2,1,0:T(8,128)(2,1)S(1)}, bf16[128,32,1024]{2,1,0:T(8,128)(2,1)}, u32[]{:S(2)}) copy-start(bf16[128,32,1024]{2,1,0:T(8,128)(2,1)} %all-gather.3.cloned.1.call-done) | copy-start | bytes 25165828
  146.6 8.4 %collective-permute-start.31 = (bf16[64,2048]{1,0:T(8,128)(2,1)S(1)}, bf16[64,2048]{1,0:T(8,128)(2,1)S(1)}, u32[]{:S(2)}, u32[]{:S(2)}) collective-permute-start(bf16[64,2048]{1,0:T(8,128)(2,1)S(1)} %get-tuple-element.82), channel_id=1, source_target_pairs={{0,1},{1,2},{2,3},{3,0},{4,5},{5,6},{6,7},{7,4},{8,9},{9,10},{10,1... | collective-permute-start | bytes 786440 | tf_op jit(solution)/shard_map/ppermute | solution.py:393
  150.2 8.0 %collective-permute-start.30 = (bf16[64,2048]{1,0:T(8,128)(2,1)S(1)}, bf16[64,2048]{1,0:T(8,128)(2,1)S(1)}, u32[]{:S(2)}, u32[]{:S(2)}) collective-permute-start(bf16[64,2048]{1,0:T(8,128)(2,1)S(1)} %mixer.3), channel_id=1, source_target_pairs={{0,2},{1,3},{2,0},{3,1},{4,6},{5,7},{6,4},{7,5},{8,10},{9,11},{10,... | collective-permute-start | bytes 786440 | tf_op jit(solution)/shard_map/ppermute | solution.py:393
  151.6 10.0 %collective-permute-start.27 = (bf16[64,2048]{1,0:T(8,128)(2,1)S(1)}, bf16[64,2048]{1,0:T(8,128)(2,1)S(1)}, u32[]{:S(2)}, u32[]{:S(2)}) collective-permute-start(bf16[64,2048]{1,0:T(8,128)(2,1)S(1)} %get-tuple-element.81), channel_id=1, source_target_pairs={{0,3},{1,0},{2,1},{3,2},{4,7},{5,4},{6,5},{7,6},{8,11},{9,8},{10,9... | collective-permute-start | bytes 786440 | tf_op jit(solution)/shard_map/ppermute | solution.py:393
Sparse Core Ops, SparseCore 0:
  15.1 85.0 all-gather.2

commit v7 on v5

--- a/solution.py
+++ b/solution.py
@@ -21,7 +21,12 @@
 VMEM = pl.BlockSpec(memory_space=pltpu.VMEM)
 
 
-def prep_kernel(cos_ref, sin_ref, qa_ref, qb_ref, ka_ref, kb_ref, v_ref, q_out, kv_out, q_own, kv_own):
+def prep_kernel(
+    cos_ref, sin_ref, qa_ref, qb_ref, ka_ref, kb_ref, v_ref, up_ref, down_ref,
+    q_out, kv_out, q_own, kv_own, mix_out,
+):
+    mix_out[0] = up_ref[...]
+    mix_out[1] = down_ref[...]
     cos = jnp.concatenate([cos_ref[...]] * 4, axis=1)
     sin = jnp.concatenate([-sin_ref[...], sin_ref[...]] * 2, axis=1)
     lane = lax.broadcasted_iota(jnp.int32, cos.shape, 1)
@@ -41,7 +46,7 @@
     kv_own[...] = kv_out[...]
 
 
-def prepare(first_query, second_query, first_key, second_key, values, start):
+def prepare(first_query, second_query, first_key, second_key, values, up, down, start):
     positions = (start + jnp.arange(TOK)).astype(F32)
     half = HEAD // 2
     inverse = 10000.0 ** (-jnp.arange(0, half, dtype=F32) * 2.0 / HEAD)
@@ -53,11 +58,12 @@
             jax.ShapeDtypeStruct((TOK, 2 * VD), BF16),
             jax.ShapeDtypeStruct((2 * TOK, 2 * VD), BF16),
         )
-        * 2,
-        in_specs=[VMEM] * 7,
-        out_specs=(VMEM,) * 4,
+        * 2
+        + (jax.ShapeDtypeStruct((2,) + up.shape, BF16),),
+        in_specs=[VMEM] * 9,
+        out_specs=(VMEM,) * 5,
         name="prep",
-    )(cos, sin, first_query, second_query, first_key, second_key, values)
+    )(cos, sin, first_query, second_query, first_key, second_key, values, up, down)
 
 
 def load_queries(queries, qs):
@@ -204,8 +210,8 @@
         in_specs=[VMEM] * 5,
         out_specs=(VMEM,) * 4,
         input_output_aliases={2: 0, 3: 1, 4: 2},
-        scratch_shapes=[score_scratch(kv.shape[0] // (2 * TOK))],
-        cost_estimate=cost(kv.shape[0] // 2),
+        scratch_shapes=[score_scratch(kv.shape[0])],
+        cost_estimate=cost(kv.shape[0] * TOK),
         compiler_params=pltpu.CompilerParams(vmem_limit_bytes=24 * 2**20),
         name="attend_last",
     )(qs, kv, *state)
@@ -349,14 +355,15 @@
     sp = lax.axis_index(("z", "x", "c"))
     x = lax.axis_index("x").astype(jnp.int32).reshape(1)
     at = jnp.stack([lax.axis_index("tp"), lax.axis_index("c")]).astype(jnp.int32)
-    query, kv, query_own, kv_own = prepare(first_query, second_query, first_key, second_key, values, sp * TOK)
+    query, kv, query_own, kv_own, mix_weights = prepare(
+        first_query, second_query, first_key, second_key, values, up_weight, down_weight.T, sp * TOK
+    )
     ring = ("z", "c")
     onward = [(2 * z + c, 2 * ((z + 1 - 2 * c) % 8) + c) for z in range(8) for c in range(2)]
     crossed = [(2 * z + c, 2 * ((z - 1 + 2 * c) % 8) + 1 - c) for z in range(8) for c in range(2)]
     near = [lax.ppermute(kv, ring, onward), lax.ppermute(kv, ring, crossed)]
     other = shifted(kv, "c", 1)
     queries = [query_own] + [shifted(query, "x", o) for o in (1, 2, 3)]
-    mix_weights = jnp.stack([up_weight, down_weight.T])
     mix_weights = lax.all_gather(mix_weights, ("z", "x", "c"))
     half = lax.dynamic_slice_in_dim(out_weight, lax.axis_index("c") * VD, VD, 0)
     near = jnp.stack(near)
@@ -369,13 +376,11 @@
     four_other = shifted(four, "c", 1)
     state = attend_next(qs, four, state)
     state = attend_next(qs, four_other, state)
-    far = lax.ppermute(third[0], ring, onward)
+    far = lax.ppermute(third, ring, onward)
     third_other = shifted(third, "c", 1)
     state = attend_next(qs, third, state)
     state = attend_next(qs, third_other, state)
-    far_other = shifted(far, "c", 1)
-    *state, _ = attend_last(qs, far, state)
-    acc, _, tot, lse = attend_last(qs, far_other, state)
+    acc, _, tot, lse = attend_last(qs, far, state)
     lses = [lse] + [shifted(lse, "x", k) for k in (1, 2, 3)]
     part = share(x, lambdas, lses, acc, tot)
     part = lax.all_to_all(part, ("x", "tp"), split_axis=0, concat_axis=0, tiled=True)

time: 162 us -> 161 us (level)
  Pallas kernels: 40.2 us -> 37.7 us
  other arithmetic: 4.25 us -> 2.61 us
    pallas_call x2 -> x1, Pallas kernels: 6.22 us -> 3.66 us  [attend_last(): pl.pallas_call(last_kernel, out_shape=STATE + (jax.ShapeDtypeStruct((16,...]
    ppermute x21 -> x20, waiting for transfers between devices: 48.4 us -> 50.7 us  [shifted(): lax.ppermute(value, axis, [(i, (i + by) % size) for i in range(size)])]
    another operation x1 -> x0, other arithmetic: 1.63 us -> none  [local(): mix_weights = jnp.stack([up_weight, down_weight.T])]
    ppermute x21 -> x20, starting transfers between devices: 24.2 us -> 25.7 us  [shifted(): lax.ppermute(value, axis, [(i, (i + by) % size) for i in range(size)])]
  transfers between devices with their start and end apart: 28 -> 27, of which waited for: 18 -> 15; matrix products, arithmetic and copies ran while one was open for 1% -> 0% of each run, Pallas kernels for 23% -> 20%
where the time goes in v7:
time: 161 us; the launch traced here: 158 us
  waiting for transfers between devices  62 us (39%)
  Pallas kernels  37.7 us (23%)
  starting transfers between devices  36.5 us (23%)
  between operations  13.7 us (9%)
  local copies, waits for them, and re-layouts  5.78 us (4%)
  other arithmetic  2.61 us (2%)
    ppermute x20, waiting for transfers between devices, shifted(): lax.ppermute(value, axis, [(i, (i + by) % size) for i in range(size)])  50.7 us
    ppermute x20, starting transfers between devices, shifted(): lax.ppermute(value, axis, [(i, (i + by) % size) for i in range(size)])  25.7 us
    pallas_call x4, Pallas kernels, attend_next(): pl.pallas_call(next_kernel, out_shape=STATE, in_specs=[VMEM] * 5, out_spe...  18.2 us
    all_to_all x1, waiting for transfers between devices, local(): lax.all_to_all(part, ('x', 'tp'), split_axis=0, concat_axis=0, tiled=True)  8.26 us
    unnamed x26, local copies, waits for them, and re-layouts  5.68 us
    ppermute x2, starting transfers between devices, local(): near = [lax.ppermute(kv, ring, onward), lax.ppermute(kv, ring, crossed)]  5.38 us
    all_to_all x1, starting transfers between devices, local(): lax.all_to_all(part, ('x', 'tp'), split_axis=0, concat_axis=0, tiled=True)  4.89 us
    pallas_call x2, Pallas kernels, mixer(): pl.pallas_call(functools.partial(mixer_kernel, len(pieces)), out_shape=[j...  4.47 us
  transfers between devices with their start and end apart: 27, of which 15 were waited for; matrix products, arithmetic and copies ran while one was open for 0% of the time, Pallas kernels for 20%

profile of v7, /device:TPU:2, one launch (start us, length us, event | category | flops | bytes accessed | tf_op | source)
XLA Modules:
  0.0 158.3 jit_solution(9904568328610910193)
XLA Ops:
  6.6 1.2 multiply_sine_fusion
  7.8 2.6 %prep.1 = (bf16[256,256]{1,0:T(8,128)(2,1)}, bf16[512,256]{1,0:T(8,128)(2,1)}, bf16[256,256]{1,0:T(8,128)(2,1)}, bf16[512,256]{1,0:T(8,128)(2,1)}, bf16[2,32,1024]{2,1,0:T(8,128)(2,1)}) custom-call(f32[256,32]{1,0:T(8,128)} %get-tuple-element.60.cos_ref, f32[256,32]{1,0:T(8,128)} %get-tuple-element.59.sin_ref, bf16[256,128]{1,0:T(8,128)(2,1)} %qa_ref.1, ...), custom_call_target="tpu_custom_call" | custom-call | tf_op jit(solution)/shard_map/prep/pallas_call | solution.py:55
  10.4 5.4 %collective-permute-start.5 = (bf16[512,256]{1,0:T(8,128)(2,1)}, bf16[512,256]{1,0:T(8,128)(2,1)S(1)}, u32[]{:S(2)}, u32[]{:S(2)}) collective-permute-start(bf16[512,256]{1,0:T(8,128)(2,1)} %get-tuple-element.35), channel_id=1, source_target_pairs={{0,228},{4,32},{32,4},{36,64},{64,36},{68,96},{96,68},{100,128},{1... | collective-permute-start | bytes 786440 | tf_op jit(solution)/shard_map/ppermute | solution.py:364
  15.8 3.1 %collective-permute-start.16 = (bf16[128,2048]{1,0:T(8,128)(2,1)S(1)}, bf16[128,2048]{1,0:T(8,128)(2,1)S(1)}, u32[]{:S(2)}, u32[]{:S(2)}) collective-permute-start(bf16[128,2048]{1,0:T(8,128)(2,1)S(1)} %constant_dynamic-slice_fusion), channel_id=1, source_target_pairs={{0,3},{1,0},{2,1},{3,2},{4,7},{5,4},{6,5},{7,6},{8,11},{9,8},{10,9... | collective-permute-start | bytes 1572872 | tf_op jit(solution)/shard_map/ppermute | solution.py:338
  19.6 1.0 collective-permute-start.14
  20.5 1.8 %collective-permute-done.5 = bf16[512,256]{1,0:T(8,128)(2,1)S(1)} collective-permute-done((bf16[512,256]{1,0:T(8,128)(2,1)}, bf16[512,256]{1,0:T(8,128)(2,1)S(1)}, u32[]{:S(2)}, u32[]{:S(2)}) %collective-permute-start.5) | collective-permute-done | bytes 262176 | tf_op jit(solution)/shard_map/ppermute | solution.py:364
  22.3 1.3 collective-permute-done.4
  23.8 17.9 %collective-permute-done.16 = bf16[128,2048]{1,0:T(8,128)(2,1)S(1)} collective-permute-done((bf16[128,2048]{1,0:T(8,128)(2,1)S(1)}, bf16[128,2048]{1,0:T(8,128)(2,1)S(1)}, u32[]{:S(2)}, u32[]{:S(2)}) %collective-permute-start.16) | collective-permute-done | bytes 524320 | tf_op jit(solution)/shard_map/ppermute | solution.py:338
  41.7 3.7 %collective-permute-done.14 = bf16[128,2048]{1,0:T(8,128)(2,1)S(1)} collective-permute-done((bf16[128,2048]{1,0:T(8,128)(2,1)S(1)}, bf16[128,2048]{1,0:T(8,128)(2,1)S(1)}, u32[]{:S(2)}, u32[]{:S(2)}) %collective-permute-start.14) | collective-permute-done | bytes 524320 | tf_op jit(solution)/shard_map/ppermute | solution.py:338
  46.7 1.6 collective-permute-start
  48.2 1.1 collective-permute-start.1
  49.4 2.5 %collective-permute-done.q1 = bf16[256,256]{1,0:T(8,128)(2,1)S(1)} collective-permute-done((bf16[256,256]{1,0:T(8,128)(2,1)S(1)}, bf16[256,256]{1,0:T(8,128)(2,1)S(1)}, u32[]{:S(2)}, u32[]{:S(2)}) %collective-permute-start) | collective-permute-done | bytes 131104 | tf_op jit(solution)/shard_map/ppermute | solution.py:338
  51.8 1.5 collective-permute-start.3
  53.3 1.8 %collective-permute-done.1.q2 = bf16[256,256]{1,0:T(8,128)(2,1)S(1)} collective-permute-done((bf16[256,256]{1,0:T(8,128)(2,1)S(1)}, bf16[256,256]{1,0:T(8,128)(2,1)S(1)}, u32[]{:S(2)}, u32[]{:S(2)}) %collective-permute-start.1) | collective-permute-done | bytes 131104 | tf_op jit(solution)/shard_map/ppermute | solution.py:338
  55.1 2.3 %collective-permute-start.2 = (bf16[256,256]{1,0:T(8,128)(2,1)S(1)}, bf16[256,256]{1,0:T(8,128)(2,1)S(1)}, u32[]{:S(2)}, u32[]{:S(2)}) collective-permute-start(bf16[256,256]{1,0:T(8,128)(2,1)S(1)} %copy-done.12), channel_id=1, source_target_pairs={{0,24},{8,0},{16,8},{24,16},{1,25},{9,1},{17,9},{25,17},{2,26},{10... | collective-permute-start | bytes 393224 | tf_op jit(solution)/shard_map/ppermute | solution.py:338
  57.4 0.8 collective-permute-start.9
  58.2 3.1 %collective-permute-done.2.q3 = bf16[256,256]{1,0:T(8,128)(2,1)S(1)} collective-permute-done((bf16[256,256]{1,0:T(8,128)(2,1)S(1)}, bf16[256,256]{1,0:T(8,128)(2,1)S(1)}, u32[]{:S(2)}, u32[]{:S(2)}) %collective-permute-start.2) | collective-permute-done | bytes 131104 | tf_op jit(solution)/shard_map/ppermute | solution.py:338
  61.7 4.1 %attend_first.1 = (bf16[4,4,256,256]{3,2,1,0:T(8,128)(2,1)S(1)}, f32[4,4,128,256]{3,2,1,0:T(8,128)S(1)}, f32[4,4,1,256]{3,2,1,0:T(1,128)S(1)}, f32[4,4,1,256]{3,2,1,0:T(1,128)S(1)}) custom-call(bf16[256,256]{1,0:T(8,128)(2,1)S(1)} %copy-done.8, bf16[256,256]{1,0:T(8,128)(2,1)S(1)} %collective-permute-done.q1, ...), custom_call_target="tpu_custom_call" | custom-call | flops 805306368 | bytes 524288 | tf_op jit(solution)/shard_map/attend_first/pallas_call | solution.py:179
  65.8 5.4 %attend_next.4 = (f32[4,4,128,256]{3,2,1,0:T(8,128)S(1)}, f32[4,4,1,256]{3,2,1,0:T(1,128)S(1)}, f32[4,4,1,256]{3,2,1,0:T(1,128)S(1)}) custom-call(bf16[4,4,256,256]{3,2,1,0:T(8,128)(2,1)S(1)} %get-tuple-element.36.qs, bf16[4,512,256]{2,1,0:T(8,128)(2,1)S(1)} %pad_maximum_fusion.1.kv_ref, ...), custom_call_target="tpu_custom_call", output_to_operand_aliasing={{0}: (2, {}), {1}: (3, {}), {2}: (4, {})} | custom-call | flops 1610612736 | bytes 1048576 | tf_op jit(solution)/shard_map/attend_next/pallas_call | solution.py:193
  71.2 5.4 %attend_next.5 = (f32[4,4,128,256]{3,2,1,0:T(8,128)S(1)}, f32[4,4,1,256]{3,2,1,0:T(1,128)S(1)}, f32[4,4,1,256]{3,2,1,0:T(1,128)S(1)}) custom-call(bf16[4,4,256,256]{3,2,1,0:T(8,128)(2,1)S(1)} %get-tuple-element.36.qs, bf16[4,512,256]{2,1,0:T(8,128)(2,1)S(1)} %collective-permute-done.10.kv_ref, ...), custom_call_target="tpu_custom_call", output_to_operand_aliasing={{0}: (2, {}), {1}: (3, {}), {2}: (4, {})} | custom-call | flops 1610612736 | bytes 1048576 | tf_op jit(solution)/shard_map/attend_next/pallas_call | solution.py:193
  76.7 3.7 %attend_next.6 = (f32[4,4,128,256]{3,2,1,0:T(8,128)S(1)}, f32[4,4,1,256]{3,2,1,0:T(1,128)S(1)}, f32[4,4,1,256]{3,2,1,0:T(1,128)S(1)}) custom-call(bf16[4,4,256,256]{3,2,1,0:T(8,128)(2,1)S(1)} %get-tuple-element.36.qs, bf16[2,512,256]{2,1,0:T(8,128)(2,1)S(1)} %collective-permute-done.7.kv_ref, ...), custom_call_target="tpu_custom_call", output_to_operand_aliasing={{0}: (2, {}), {1}: (3, {}), {2}: (4, {})} | custom-call | flops 805306368 | bytes 524288 | tf_op jit(solution)/shard_map/attend_next/pallas_call | solution.py:193
  80.3 3.7 %attend_next.7 = (f32[4,4,128,256]{3,2,1,0:T(8,128)S(1)}, f32[4,4,1,256]{3,2,1,0:T(1,128)S(1)}, f32[4,4,1,256]{3,2,1,0:T(1,128)S(1)}) custom-call(bf16[4,4,256,256]{3,2,1,0:T(8,128)(2,1)S(1)} %get-tuple-element.36.qs, bf16[2,512,256]{2,1,0:T(8,128)(2,1)S(1)} %collective-permute-done.9.kv_ref, ...), custom_call_target="tpu_custom_call", output_to_operand_aliasing={{0}: (2, {}), {1}: (3, {}), {2}: (4, {})} | custom-call | flops 805306368 | bytes 524288 | tf_op jit(solution)/shard_map/attend_next/pallas_call | solution.py:193
  84.0 3.7 %attend_last.1 = (f32[4,4,128,256]{3,2,1,0:T(8,128)S(1)}, f32[4,4,1,256]{3,2,1,0:T(1,128)S(1)}, f32[4,4,1,256]{3,2,1,0:T(1,128)S(1)}, f32[16,256]{1,0:T(8,128)S(1)}) custom-call(bf16[4,4,256,256]{3,2,1,0:T(8,128)(2,1)S(1)} %get-tuple-element.36.qs, ...), custom_call_target="tpu_custom_call", output_to_operand_aliasing={{0}: (2, {}), {1}: (3, {}), {2}: (4, {})} | custom-call | flops 805306368 | bytes 524288 | tf_op jit(solution)/shard_map/attend_last/pallas_call | solution.py:207
  87.7 1.3 collective-permute-start.11
  89.1 3.3 %collective-permute-start.12 = (f32[16,256]{1,0:T(8,128)S(1)}, f32[16,256]{1,0:T(8,128)S(1)}, u32[]{:S(2)}, u32[]{:S(2)}) collective-permute-start(f32[16,256]{1,0:T(8,128)S(1)} %get-tuple-element.52.lse0), channel_id=1, source_target_pairs={{0,16},{8,24},{16,0},{24,8},{1,17},{9,25},{17,1},{25,9},{2,18},{10... | collective-permute-start | bytes 49160 | tf_op jit(solution)/shard_map/ppermute | solution.py:338
  92.4 0.9 collective-permute-start.13
  93.3 1.1 collective-permute-done.12.lse2
  94.4 1.8 %collective-permute-done.13.lse3 = f32[16,256]{1,0:T(8,128)S(1)} collective-permute-done((f32[16,256]{1,0:T(8,128)S(1)}, f32[16,256]{1,0:T(8,128)S(1)}, u32[]{:S(2)}, u32[]{:S(2)}) %collective-permute-start.13) | collective-permute-done | bytes 16416 | tf_op jit(solution)/shard_map/ppermute | solution.py:338
  96.1 0.8 share.1
  97.0 0.8 copy-done.2
  97.8 4.9 %all-to-all-start = ((bf16[16,64,256]{2,1,0:T(8,128)(2,1)}), bf16[16,64,256]{2,1,0:T(8,128)(2,1)}, u32[]{:S(2)}, u32[]{:S(2)}) async-start(bf16[16,64,256]{2,1,0:T(8,128)(2,1)} %copy-done.2), calls=%async_computation | async-start | bytes 1048576 | tf_op jit(solution)/shard_map/all_to_all | solution.py:386
  102.7 8.3 %all-to-all-done.part_ref = bf16[16,64,256]{2,1,0:T(8,128)(2,1)} async-done(((bf16[16,64,256]{2,1,0:T(8,128)(2,1)}), bf16[16,64,256]{2,1,0:T(8,128)(2,1)}, u32[]{:S(2)}, u32[]{:S(2)}) %all-to-all-start) | async-done | bytes 524320 | tf_op jit(solution)/shard_map/all_to_all | solution.py:386
  111.0 0.9 copy-done.3
  111.9 3.3 %merge.1.refs_0_ = bf16[64,2048]{1,0:T(8,128)(2,1)S(1)} custom-call(s32[2]{0:T(128)S(1)} %pad_add_fusion.at_ref, bf16[16,64,256]{2,1,0:T(8,128)(2,1)} %all-to-all-done.part_ref, f32[1,128]{1,0:T(1,128)S(1)} %bitcast.16, bf16[64,2048]{1,0:T(8,128)(2,1)S(1)} %copy-done.3, f32[1,2048]{1,0:T(1,128)S(1)} %bitcast.15, ...), custom_call_target="tpu_custom_call" | custom-call | tf_op jit(solution)/shard_map/merge/pallas_call | solution.py:289
  115.3 1.2 collective-permute-start.19
  116.5 0.9 collective-permute-start.18
  117.4 5.4 %collective-permute-done.19.refs_2_ = bf16[64,2048]{1,0:T(8,128)(2,1)S(1)} collective-permute-done((bf16[64,2048]{1,0:T(8,128)(2,1)S(1)}, bf16[64,2048]{1,0:T(8,128)(2,1)S(1)}, u32[]{:S(2)}, u32[]{:S(2)}) %collective-permute-start.19) | collective-permute-done | bytes 262176 | tf_op jit(solution)/shard_map/ppermute | solution.py:338
  122.8 1.6 %collective-permute-start.22 = (bf16[32,2048]{1,0:T(8,128)(2,1)S(1)}, bf16[32,2048]{1,0:T(8,128)(2,1)S(1)}, u32[]{:S(2)}, u32[]{:S(2)}) collective-permute-start(bf16[32,2048]{1,0:T(8,128)(2,1)S(1)} %slice.9), channel_id=1, source_target_pairs={{0,3},{1,0},{2,1},{3,2},{4,7},{5,4},{6,5},{7,6},{8,11},{9,8},{10,9... | collective-permute-start | bytes 393224 | tf_op jit(solution)/shard_map/ppermute | solution.py:338
  125.2 2.8 %collective-permute-done.22 = bf16[32,2048]{1,0:T(8,128)(2,1)S(1)} collective-permute-done((bf16[32,2048]{1,0:T(8,128)(2,1)S(1)}, bf16[32,2048]{1,0:T(8,128)(2,1)S(1)}, u32[]{:S(2)}, u32[]{:S(2)}) %collective-permute-start.22) | collective-permute-done | bytes 131104 | tf_op jit(solution)/shard_map/ppermute | solution.py:338
  128.0 2.6 %collective-permute-done.21 = bf16[32,2048]{1,0:T(8,128)(2,1)S(1)} collective-permute-done((bf16[32,2048]{1,0:T(8,128)(2,1)S(1)}, bf16[32,2048]{1,0:T(8,128)(2,1)S(1)}, u32[]{:S(2)}, u32[]{:S(2)}) %collective-permute-start.21) | collective-permute-done | bytes 131104 | tf_op jit(solution)/shard_map/ppermute | solution.py:338
  130.7 3.4 %copy-done.1 = bf16[128,32,1024]{2,1,0:T(8,128)(2,1)S(1)} copy-done((bf16[128,32,1024]{2,1,0:T(8,128)(2,1)S(1)}, bf16[128,32,1024]{2,1,0:T(8,128)(2,1)}, u32[]{:S(2)}) %copy-start.1) | copy-done | bytes 8388632
  134.7 2.4 %mixer.2 = (f32[64,2048]{1,0:T(8,128)S(1)}, bf16[64,2048]{1,0:T(8,128)(2,1)S(1)}, bf16[64,2048]{1,0:T(8,128)(2,1)S(1)}) custom-call(bf16[64,2048]{1,0:T(8,128)(2,1)S(1)} %merge.1.refs_0_, bf16[64,2048]{1,0:T(8,128)(2,1)S(1)} %collective-permute-done.18.refs_1_, bf16[64,2048]{1,0:T(8,128)(2,1)S(1)} %collective-permute-done.19.refs_2_, ...), custom_call_target="tpu_custom_call" | custom-call | flops 2147483648 | bytes 8388608 | tf_op jit(solution)/shard_map/mixer/pallas_call | solution.py:325
  137.2 2.1 %mixer.3 = bf16[64,2048]{1,0:T(8,128)(2,1)S(1)} custom-call(bf16[64,2048]{1,0:T(8,128)(2,1)S(1)} %pad_maximum_fusion.3.refs_0_, bf16[64,2,32,1024]{3,2,1,0:T(8,128)(2,1)S(1)} %load_mix.1.refs_3_.refs_1_), custom_call_target="tpu_custom_call" | custom-call | flops 2147483648 | bytes 8388608 | tf_op jit(solution)/shard_map/mixer/pallas_call | solution.py:325
  139.3 1.4 collective-permute-start.23
  140.7 2.0 %collective-permute-start.20 = (bf16[64,2048]{1,0:T(8,128)(2,1)S(1)}, bf16[64,2048]{1,0:T(8,128)(2,1)S(1)}, u32[]{:S(2)}, u32[]{:S(2)}) collective-permute-start(bf16[64,2048]{1,0:T(8,128)(2,1)S(1)} %get-tuple-element.57), channel_id=1, source_target_pairs={{0,3},{1,0},{2,1},{3,2},{4,7},{5,4},{6,5},{7,6},{8,11},{9,8},{10,9... | collective-permute-start | bytes 786440 | tf_op jit(solution)/shard_map/ppermute | solution.py:338
  142.7 4.9 %collective-permute-done.24 = bf16[64,2048]{1,0:T(8,128)(2,1)S(1)} collective-permute-done((bf16[64,2048]{1,0:T(8,128)(2,1)S(1)}, bf16[64,2048]{1,0:T(8,128)(2,1)S(1)}, u32[]{:S(2)}, u32[]{:S(2)}) %collective-permute-start.24) | collective-permute-done | bytes 262176 | tf_op jit(solution)/shard_map/ppermute | solution.py:338
  147.5 3.1 %collective-permute-done.20 = bf16[64,2048]{1,0:T(8,128)(2,1)S(1)} collective-permute-done((bf16[64,2048]{1,0:T(8,128)(2,1)S(1)}, bf16[64,2048]{1,0:T(8,128)(2,1)S(1)}, u32[]{:S(2)}, u32[]{:S(2)}) %collective-permute-start.20) | collective-permute-done | bytes 262176 | tf_op jit(solution)/shard_map/ppermute | solution.py:338
  150.6 0.9 add_convert_fusion
  (58 shorter events, 4.1 us)
Async XLA Ops:
  6.5 9.3 %copy-start = (bf16[256,2048]{1,0:T(8,128)(2,1)S(1)}, bf16[256,2048]{1,0:T(8,128)(2,1)}, u32[]{:S(2)}) copy-start(bf16[256,2048]{1,0:T(8,128)(2,1)} %param.20) | copy-start | bytes 3145732
  6.5 124.2 %all-gather.3.cloned.1.call-start = ((), (), s32[]{:S(2)}) async-start(), calls=%async_computation.1 | async-start | bytes 8519680 | tf_op jit(solution)/shard_map/all_gather | solution.py:367
  10.4 11.9 %collective-permute-start.5 = (bf16[512,256]{1,0:T(8,128)(2,1)}, bf16[512,256]{1,0:T(8,128)(2,1)S(1)}, u32[]{:S(2)}, u32[]{:S(2)}) collective-permute-start(bf16[512,256]{1,0:T(8,128)(2,1)} %get-tuple-element.35), channel_id=1, source_target_pairs={{0,228},{4,32},{32,4},{36,64},{64,36},{68,96},{96,68},{100,128},{1... | collective-permute-start | bytes 786440 | tf_op jit(solution)/shard_map/ppermute | solution.py:364
  15.8 7.8 %collective-permute-start.4 = (bf16[512,256]{1,0:T(8,128)(2,1)}, bf16[512,256]{1,0:T(8,128)(2,1)S(1)}, u32[]{:S(2)}, u32[]{:S(2)}) collective-permute-start(bf16[512,256]{1,0:T(8,128)(2,1)} %get-tuple-element.35), channel_id=1, source_target_pairs={{0,32},{4,228},{32,64},{36,4},{64,96},{68,36},{96,128},{100,68},{1... | collective-permute-start | bytes 786440 | tf_op jit(solution)/shard_map/ppermute | solution.py:364
  15.8 25.9 %collective-permute-start.16 = (bf16[128,2048]{1,0:T(8,128)(2,1)S(1)}, bf16[128,2048]{1,0:T(8,128)(2,1)S(1)}, u32[]{:S(2)}, u32[]{:S(2)}) collective-permute-start(bf16[128,2048]{1,0:T(8,128)(2,1)S(1)} %constant_dynamic-slice_fusion), channel_id=1, source_target_pairs={{0,3},{1,0},{2,1},{3,2},{4,7},{5,4},{6,5},{7,6},{8,11},{9,8},{10,9... | collective-permute-start | bytes 1572872 | tf_op jit(solution)/shard_map/ppermute | solution.py:338
  18.9 22.8 %collective-permute-start.15 = (bf16[128,2048]{1,0:T(8,128)(2,1)S(1)}, bf16[128,2048]{1,0:T(8,128)(2,1)S(1)}, u32[]{:S(2)}, u32[]{:S(2)}) collective-permute-start(bf16[128,2048]{1,0:T(8,128)(2,1)S(1)} %constant_dynamic-slice_fusion), channel_id=1, source_target_pairs={{0,2},{1,3},{2,0},{3,1},{4,6},{5,7},{6,4},{7,5},{8,10},{9,11},{10,... | collective-permute-start | bytes 1572872 | tf_op jit(solution)/shard_map/ppermute | solution.py:338
  19.6 25.9 %collective-permute-start.14 = (bf16[128,2048]{1,0:T(8,128)(2,1)S(1)}, bf16[128,2048]{1,0:T(8,128)(2,1)S(1)}, u32[]{:S(2)}, u32[]{:S(2)}) collective-permute-start(bf16[128,2048]{1,0:T(8,128)(2,1)S(1)} %constant_dynamic-slice_fusion), channel_id=1, source_target_pairs={{0,1},{1,2},{2,3},{3,0},{4,5},{5,6},{6,7},{7,4},{8,9},{9,10},{10,1... | collective-permute-start | bytes 1572872 | tf_op jit(solution)/shard_map/ppermute | solution.py:338
  23.6 21.8 %copy-start.9 = (bf16[512,256]{1,0:T(8,128)(2,1)}, bf16[512,256]{1,0:T(8,128)(2,1)S(1)}, u32[]{:S(2)}) copy-start(bf16[512,256]{1,0:T(8,128)(2,1)S(1)} %collective-permute-done.4) | copy-start | bytes 786436
  23.6 22.2 %collective-permute-start.6 = (bf16[2,512,256]{2,1,0:T(8,128)(2,1)S(1)}, bf16[2,512,256]{2,1,0:T(8,128)(2,1)S(1)}, u32[]{:S(2)}, u32[]{:S(2)}) collective-permute-start(bf16[2,512,256]{2,1,0:T(8,128)(2,1)S(1)} %pad_maximum_fusion.2), channel_id=1, source_target_pairs={{0,32},{4,228},{32,64},{36,4},{64,96},{68,36},{96,128},{100,68},{1... | collective-permute-start | bytes 1572872 | tf_op jit(solution)/shard_map/ppermute | solution.py:370
  45.4 1.0 copy-start.10
  45.7 1.0 copy-start.12
  45.7 6.1 %copy-start.11 = (bf16[512,256]{1,0:T(8,128)(2,1)S(1)}, bf16[512,256]{1,0:T(8,128)(2,1)}, u32[]{:S(2)}) copy-start(bf16[512,256]{1,0:T(8,128)(2,1)} %get-tuple-element.35) | copy-start | bytes 786436
  45.7 16.0 %copy-start.7 = (bf16[512,256]{1,0:T(8,128)(2,1)S(1)}, bf16[512,256]{1,0:T(8,128)(2,1)}, u32[]{:S(2)}) copy-start(bf16[512,256]{1,0:T(8,128)(2,1)} %get-tuple-element.34.own_ref) | copy-start | bytes 786436
  45.7 16.0 %copy-start.8 = (bf16[256,256]{1,0:T(8,128)(2,1)S(1)}, bf16[256,256]{1,0:T(8,128)(2,1)}, u32[]{:S(2)}) copy-start(bf16[256,256]{1,0:T(8,128)(2,1)} %get-tuple-element.32.q0) | copy-start | bytes 393220
  45.7 65.3 %collective-permute-start.17 = (bf16[4,128,2048]{2,1,0:T(8,128)(2,1)S(1)}, bf16[4,128,2048]{2,1,0:T(8,128)(2,1)}, u32[]{:S(2)}, u32[]{:S(2)}) collective-permute-start(bf16[4,128,2048]{2,1,0:T(8,128)(2,1)S(1)} %pad_maximum_fusion.mine_ref), channel_id=1, source_target_pairs={{0,4},{4,0},{1,5},{5,1},{2,6},{6,2},{3,7},{7,3},{8,12},{12,8},{9,1... | collective-permute-start | bytes 6291464 | tf_op jit(solution)/shard_map/ppermute | solution.py:338
  46.5 24.7 %collective-permute-start.10 = (bf16[4,512,256]{2,1,0:T(8,128)(2,1)S(1)}, bf16[4,512,256]{2,1,0:T(8,128)(2,1)S(1)}, u32[]{:S(2)}, u32[]{:S(2)}) collective-permute-start(bf16[4,512,256]{2,1,0:T(8,128)(2,1)S(1)} %pad_maximum_fusion.1.kv_ref), channel_id=1, source_target_pairs={{0,4},{4,0},{1,5},{5,1},{2,6},{6,2},{3,7},{7,3},{8,12},{12,8},{9,1... | collective-permute-start | bytes 3145736 | tf_op jit(solution)/shard_map/ppermute | solution.py:338
  46.6 10.8 %collective-permute-start.7 = (bf16[2,512,256]{2,1,0:T(8,128)(2,1)S(1)}, bf16[2,512,256]{2,1,0:T(8,128)(2,1)S(1)}, u32[]{:S(2)}, u32[]{:S(2)}) collective-permute-start(bf16[2,512,256]{2,1,0:T(8,128)(2,1)S(1)} %collective-permute-done.6), channel_id=1, source_target_pairs={{0,32},{4,228},{32,64},{36,4},{64,96},{68,36},{96,128},{100,68},{1... | collective-permute-start | bytes 1572872 | tf_op jit(solution)/shard_map/ppermute | solution.py:374
  46.7 5.2 %collective-permute-start = (bf16[256,256]{1,0:T(8,128)(2,1)S(1)}, bf16[256,256]{1,0:T(8,128)(2,1)S(1)}, u32[]{:S(2)}, u32[]{:S(2)}) collective-permute-start(bf16[256,256]{1,0:T(8,128)(2,1)S(1)} %copy-done.12), channel_id=1, source_target_pairs={{0,8},{8,16},{16,24},{24,0},{1,9},{9,17},{17,25},{25,1},{2,10},{10... | collective-permute-start | bytes 393224 | tf_op jit(solution)/shard_map/ppermute | solution.py:338
  48.2 6.9 %collective-permute-start.1 = (bf16[256,256]{1,0:T(8,128)(2,1)S(1)}, bf16[256,256]{1,0:T(8,128)(2,1)S(1)}, u32[]{:S(2)}, u32[]{:S(2)}) collective-permute-start(bf16[256,256]{1,0:T(8,128)(2,1)S(1)} %copy-done.12), channel_id=1, source_target_pairs={{0,16},{8,24},{16,0},{24,8},{1,17},{9,25},{17,1},{25,9},{2,18},{10... | collective-permute-start | bytes 393224 | tf_op jit(solution)/shard_map/ppermute | solution.py:338
  51.8 9.8 %collective-permute-start.3 = (bf16[512,256]{1,0:T(8,128)(2,1)S(1)}, bf16[512,256]{1,0:T(8,128)(2,1)S(1)}, u32[]{:S(2)}, u32[]{:S(2)}) collective-permute-start(bf16[512,256]{1,0:T(8,128)(2,1)S(1)} %copy-done.11), channel_id=1, source_target_pairs={{0,4},{4,0},{1,5},{5,1},{2,6},{6,2},{3,7},{7,3},{8,12},{12,8},{9,1... | collective-permute-start | bytes 786440 | tf_op jit(solution)/shard_map/ppermute | solution.py:338
  55.1 6.2 %collective-permute-start.2 = (bf16[256,256]{1,0:T(8,128)(2,1)S(1)}, bf16[256,256]{1,0:T(8,128)(2,1)S(1)}, u32[]{:S(2)}, u32[]{:S(2)}) collective-permute-start(bf16[256,256]{1,0:T(8,128)(2,1)S(1)} %copy-done.12), channel_id=1, source_target_pairs={{0,24},{8,0},{16,8},{24,16},{1,25},{9,1},{17,9},{25,17},{2,26},{10... | collective-permute-start | bytes 393224 | tf_op jit(solution)/shard_map/ppermute | solution.py:338
  57.4 23.0 %collective-permute-start.9 = (bf16[2,512,256]{2,1,0:T(8,128)(2,1)S(1)}, bf16[2,512,256]{2,1,0:T(8,128)(2,1)S(1)}, u32[]{:S(2)}, u32[]{:S(2)}) collective-permute-start(bf16[2,512,256]{2,1,0:T(8,128)(2,1)S(1)} %collective-permute-done.7.kv_ref), channel_id=1, source_target_pairs={{0,4},{4,0},{1,5},{5,1},{2,6},{6,2},{3,7},{7,3},{8,12},{12,8},{9,1... | collective-permute-start | bytes 1572872 | tf_op jit(solution)/shard_map/ppermute | solution.py:338
  61.3 22.7 %collective-permute-start.8 = (bf16[2,512,256]{2,1,0:T(8,128)(2,1)S(1)}, bf16[2,512,256]{2,1,0:T(8,128)(2,1)S(1)}, u32[]{:S(2)}, u32[]{:S(2)}) collective-permute-start(bf16[2,512,256]{2,1,0:T(8,128)(2,1)S(1)} %collective-permute-done.7.kv_ref), channel_id=1, source_target_pairs={{0,32},{4,228},{32,64},{36,4},{64,96},{68,36},{96,128},{100,68},{1... | collective-permute-start | bytes 1572872 | tf_op jit(solution)/shard_map/ppermute | solution.py:379
  84.0 12.1 %copy-start.5 = (f32[2]{0:T(128)S(1)}, f32[2]{0:T(128)}, u32[]{:S(2)}) copy-start(f32[2]{0:T(128)} %lam_ref.1) | copy-start | bytes 28
  87.7 23.3 %copy-start.4 = (f32[2048]{0:T(1024)S(1)}, f32[2048]{0:T(1024)}, u32[]{:S(2)}) copy-start(f32[2048]{0:T(1024)} %param.21) | copy-start | bytes 24580
  87.7 23.3 %copy-start.6 = (f32[128]{0:T(128)S(1)}, f32[128]{0:T(128)}, u32[]{:S(2)}) copy-start(f32[128]{0:T(128)} %param.19) | copy-start | bytes 1540
  87.7 5.6 %collective-permute-start.11 = (f32[16,256]{1,0:T(8,128)S(1)}, f32[16,256]{1,0:T(8,128)S(1)}, u32[]{:S(2)}, u32[]{:S(2)}) collective-permute-start(f32[16,256]{1,0:T(8,128)S(1)} %get-tuple-element.52.lse0), channel_id=1, source_target_pairs={{0,8},{8,16},{16,24},{24,0},{1,9},{9,17},{17,25},{25,1},{2,10},{10... | collective-permute-start | bytes 49160 | tf_op jit(solution)/shard_map/ppermute | solution.py:338
  89.1 5.3 %collective-permute-start.12 = (f32[16,256]{1,0:T(8,128)S(1)}, f32[16,256]{1,0:T(8,128)S(1)}, u32[]{:S(2)}, u32[]{:S(2)}) collective-permute-start(f32[16,256]{1,0:T(8,128)S(1)} %get-tuple-element.52.lse0), channel_id=1, source_target_pairs={{0,16},{8,24},{16,0},{24,8},{1,17},{9,25},{17,1},{25,9},{2,18},{10... | collective-permute-start | bytes 49160 | tf_op jit(solution)/shard_map/ppermute | solution.py:338
  92.4 3.7 %collective-permute-start.13 = (f32[16,256]{1,0:T(8,128)S(1)}, f32[16,256]{1,0:T(8,128)S(1)}, u32[]{:S(2)}, u32[]{:S(2)}) collective-permute-start(f32[16,256]{1,0:T(8,128)S(1)} %get-tuple-element.52.lse0), channel_id=1, source_target_pairs={{0,24},{8,0},{16,8},{24,16},{1,25},{9,1},{17,9},{25,17},{2,26},{10... | collective-permute-start | bytes 49160 | tf_op jit(solution)/shard_map/ppermute | solution.py:338
  97.0 0.8 copy-start.2
  97.8 13.2 %all-to-all-start = ((bf16[16,64,256]{2,1,0:T(8,128)(2,1)}), bf16[16,64,256]{2,1,0:T(8,128)(2,1)}, u32[]{:S(2)}, u32[]{:S(2)}) async-start(bf16[16,64,256]{2,1,0:T(8,128)(2,1)} %copy-done.2), calls=%async_computation | async-start | bytes 1048576 | tf_op jit(solution)/shard_map/all_to_all | solution.py:386
  111.0 1.0 copy-start.3
  115.3 7.5 %collective-permute-start.19 = (bf16[64,2048]{1,0:T(8,128)(2,1)S(1)}, bf16[64,2048]{1,0:T(8,128)(2,1)S(1)}, u32[]{:S(2)}, u32[]{:S(2)}) collective-permute-start(bf16[64,2048]{1,0:T(8,128)(2,1)S(1)} %merge.1.refs_0_), channel_id=1, source_target_pairs={{0,3},{1,0},{2,1},{3,2},{4,7},{5,4},{6,5},{7,6},{8,11},{9,8},{10,9... | collective-permute-start | bytes 786440 | tf_op jit(solution)/shard_map/ppermute | solution.py:338
  116.5 7.9 %collective-permute-start.18 = (bf16[64,2048]{1,0:T(8,128)(2,1)S(1)}, bf16[64,2048]{1,0:T(8,128)(2,1)S(1)}, u32[]{:S(2)}, u32[]{:S(2)}) collective-permute-start(bf16[64,2048]{1,0:T(8,128)(2,1)S(1)} %merge.1.refs_0_), channel_id=1, source_target_pairs={{0,1},{1,2},{2,3},{3,0},{4,5},{5,6},{6,7},{7,4},{8,9},{9,10},{10,1... | collective-permute-start | bytes 786440 | tf_op jit(solution)/shard_map/ppermute | solution.py:338
  122.8 5.3 %collective-permute-start.22 = (bf16[32,2048]{1,0:T(8,128)(2,1)S(1)}, bf16[32,2048]{1,0:T(8,128)(2,1)S(1)}, u32[]{:S(2)}, u32[]{:S(2)}) collective-permute-start(bf16[32,2048]{1,0:T(8,128)(2,1)S(1)} %slice.9), channel_id=1, source_target_pairs={{0,3},{1,0},{2,1},{3,2},{4,7},{5,4},{6,5},{7,6},{8,11},{9,8},{10,9... | collective-permute-start | bytes 393224 | tf_op jit(solution)/shard_map/ppermute | solution.py:338
  124.4 6.3 %collective-permute-start.21 = (bf16[32,2048]{1,0:T(8,128)(2,1)S(1)}, bf16[32,2048]{1,0:T(8,128)(2,1)S(1)}, u32[]{:S(2)}, u32[]{:S(2)}) collective-permute-start(bf16[32,2048]{1,0:T(8,128)(2,1)S(1)} %slice.8), channel_id=1, source_target_pairs={{0,1},{1,2},{2,3},{3,0},{4,5},{5,6},{6,7},{7,4},{8,9},{9,10},{10,1... | collective-permute-start | bytes 393224 | tf_op jit(solution)/shard_map/ppermute | solution.py:338
  130.7 3.4 %copy-start.1 = (bf16[128,32,1024]{2,1,0:T(8,128)(2,1)S(1)}, bf16[128,32,1024]{2,1,0:T(8,128)(2,1)}, u32[]{:S(2)}) copy-start(bf16[128,32,1024]{2,1,0:T(8,128)(2,1)} %all-gather.3.cloned.1.call-done) | copy-start | bytes 25165828
  137.1 10.5 %collective-permute-start.24 = (bf16[64,2048]{1,0:T(8,128)(2,1)S(1)}, bf16[64,2048]{1,0:T(8,128)(2,1)S(1)}, u32[]{:S(2)}, u32[]{:S(2)}) collective-permute-start(bf16[64,2048]{1,0:T(8,128)(2,1)S(1)} %get-tuple-element.58), channel_id=1, source_target_pairs={{0,1},{1,2},{2,3},{3,0},{4,5},{5,6},{6,7},{7,4},{8,9},{9,10},{10,1... | collective-permute-start | bytes 786440 | tf_op jit(solution)/shard_map/ppermute | solution.py:338
  139.3 8.3 %collective-permute-start.23 = (bf16[64,2048]{1,0:T(8,128)(2,1)S(1)}, bf16[64,2048]{1,0:T(8,128)(2,1)S(1)}, u32[]{:S(2)}, u32[]{:S(2)}) collective-permute-start(bf16[64,2048]{1,0:T(8,128)(2,1)S(1)} %mixer.3), channel_id=1, source_target_pairs={{0,2},{1,3},{2,0},{3,1},{4,6},{5,7},{6,4},{7,5},{8,10},{9,11},{10,... | collective-permute-start | bytes 786440 | tf_op jit(solution)/shard_map/ppermute | solution.py:338
  140.7 9.9 %collective-permute-start.20 = (bf16[64,2048]{1,0:T(8,128)(2,1)S(1)}, bf16[64,2048]{1,0:T(8,128)(2,1)S(1)}, u32[]{:S(2)}, u32[]{:S(2)}) collective-permute-start(bf16[64,2048]{1,0:T(8,128)(2,1)S(1)} %get-tuple-element.57), channel_id=1, source_target_pairs={{0,3},{1,0},{2,1},{3,2},{4,7},{5,4},{6,5},{7,6},{8,11},{9,8},{10,9... | collective-permute-start | bytes 786440 | tf_op jit(solution)/shard_map/ppermute | solution.py:338
Sparse Core Ops, SparseCore 0:
  10.5 86.3 all-gather.2

commit v8 on v7

--- a/solution.py
+++ b/solution.py
@@ -21,12 +21,7 @@
 VMEM = pl.BlockSpec(memory_space=pltpu.VMEM)
 
 
-def prep_kernel(
-    cos_ref, sin_ref, qa_ref, qb_ref, ka_ref, kb_ref, v_ref, up_ref, down_ref,
-    q_out, kv_out, q_own, kv_own, mix_out,
-):
-    mix_out[0] = up_ref[...]
-    mix_out[1] = down_ref[...]
+def turner(cos_ref, sin_ref):
     cos = jnp.concatenate([cos_ref[...]] * 4, axis=1)
     sin = jnp.concatenate([-sin_ref[...], sin_ref[...]] * 2, axis=1)
     lane = lax.broadcasted_iota(jnp.int32, cos.shape, 1)
@@ -37,33 +32,54 @@
         other = jnp.where(front, pltpu.roll(x, 128 - 32, 1), pltpu.roll(x, 32, 1))
         return (x * cos + other * sin).astype(BF16)
 
-    q_out[:, 0:128] = turn(qa_ref)
-    q_out[:, 128:256] = turn(qb_ref)
+    return turn
+
+
+def prep_keys_kernel(cos_ref, sin_ref, ka_ref, kb_ref, v_ref, up_ref, down_ref, kv_out, kv_own, mix_out):
+    mix_out[0] = up_ref[...]
+    mix_out[1] = down_ref[...]
+    turn = turner(cos_ref, sin_ref)
     kv_out[0:TOK, 0:128] = turn(ka_ref)
     kv_out[0:TOK, 128:256] = turn(kb_ref)
     kv_out[TOK : 2 * TOK, :] = v_ref[...].astype(F32).T.astype(BF16)
+    kv_own[...] = kv_out[...]
+
+
+def prep_queries_kernel(cos_ref, sin_ref, qa_ref, qb_ref, q_out, q_own):
+    turn = turner(cos_ref, sin_ref)
+    q_out[:, 0:128] = turn(qa_ref)
+    q_out[:, 128:256] = turn(qb_ref)
     q_own[...] = q_out[...]
-    kv_own[...] = kv_out[...]
-
-
-def prepare(first_query, second_query, first_key, second_key, values, up, down, start):
+
+
+def tables(start):
     positions = (start + jnp.arange(TOK)).astype(F32)
     half = HEAD // 2
     inverse = 10000.0 ** (-jnp.arange(0, half, dtype=F32) * 2.0 / HEAD)
     angle = positions[:, None] * inverse[None, :]
-    cos, sin = jnp.cos(angle), jnp.sin(angle)
-    return pl.pallas_call(
-        prep_kernel,
-        out_shape=(
-            jax.ShapeDtypeStruct((TOK, 2 * VD), BF16),
-            jax.ShapeDtypeStruct((2 * TOK, 2 * VD), BF16),
-        )
-        * 2
-        + (jax.ShapeDtypeStruct((2,) + up.shape, BF16),),
-        in_specs=[VMEM] * 9,
-        out_specs=(VMEM,) * 5,
-        name="prep",
-    )(cos, sin, first_query, second_query, first_key, second_key, values, up, down)
+    return jnp.cos(angle), jnp.sin(angle)
+
+
+def prepare_keys(cos, sin, first_key, second_key, values, up, down):
+    kv = jax.ShapeDtypeStruct((2 * TOK, 2 * VD), BF16)
+    return pl.pallas_call(
+        prep_keys_kernel,
+        out_shape=(kv, kv, jax.ShapeDtypeStruct((2,) + up.shape, BF16)),
+        in_specs=[VMEM] * 7,
+        out_specs=(VMEM,) * 3,
+        name="prep_keys",
+    )(cos, sin, first_key, second_key, values, up, down)
+
+
+def prepare_queries(cos, sin, first_query, second_query):
+    q = jax.ShapeDtypeStruct((TOK, 2 * VD), BF16)
+    return pl.pallas_call(
+        prep_queries_kernel,
+        out_shape=(q, q),
+        in_specs=[VMEM] * 4,
+        out_specs=(VMEM,) * 2,
+        name="prep_queries",
+    )(cos, sin, first_query, second_query)
 
 
 def load_queries(queries, qs):
@@ -355,9 +371,11 @@
     sp = lax.axis_index(("z", "x", "c"))
     x = lax.axis_index("x").astype(jnp.int32).reshape(1)
     at = jnp.stack([lax.axis_index("tp"), lax.axis_index("c")]).astype(jnp.int32)
-    query, kv, query_own, kv_own, mix_weights = prepare(
-        first_query, second_query, first_key, second_key, values, up_weight, down_weight.T, sp * TOK
+    cos, sin = tables(sp * TOK)
+    kv, kv_own, mix_weights = prepare_keys(
+        cos, sin, first_key, second_key, values, up_weight, down_weight.T
     )
+    query, query_own = prepare_queries(cos, sin, first_query, second_query)
     ring = ("z", "c")
     onward = [(2 * z + c, 2 * ((z + 1 - 2 * c) % 8) + c) for z in range(8) for c in range(2)]
     crossed = [(2 * z + c, 2 * ((z - 1 + 2 * c) % 8) + 1 - c) for z in range(8) for c in range(2)]

time: 161 us -> 173 us (1.075)
  the two profiles are of different devices: /device:TPU:2 before, /device:TPU:32 now
where the time goes in v8:
time: 173 us; the launch traced here: 172 us
  waiting for transfers between devices  72.7 us (42%)
  Pallas kernels  43.2 us (25%)
  starting transfers between devices  31.5 us (18%)
  between operations  13.7 us (8%)
  local copies, waits for them, and re-layouts  6.67 us (4%)
  other arithmetic  4.63 us (3%)
    ppermute x20, waiting for transfers between devices, shifted(): lax.ppermute(value, axis, [(i, (i + by) % size) for i in range(size)])  57.5 us
    ppermute x20, starting transfers between devices, shifted(): lax.ppermute(value, axis, [(i, (i + by) % size) for i in range(size)])  22.5 us
    pallas_call x4, Pallas kernels, attend_next(): pl.pallas_call(next_kernel, out_shape=STATE, in_specs=[VMEM] * 5, out_spe...  21.7 us
    all_to_all x1, waiting for transfers between devices, local(): lax.all_to_all(part, ('x', 'tp'), split_axis=0, concat_axis=0, tiled=True)  11.9 us
    unnamed x26, local copies, waits for them, and re-layouts  6.58 us
    pallas_call x2, Pallas kernels, mixer(): pl.pallas_call(functools.partial(mixer_kernel, len(pieces)), out_shape=[j...  4.47 us
    all_to_all x1, starting transfers between devices, local(): lax.all_to_all(part, ('x', 'tp'), split_axis=0, concat_axis=0, tiled=True)  4.24 us
    pallas_call x1, Pallas kernels, attend_first(): pl.pallas_call(first_kernel, out_shape=(QS,) + STATE, in_specs=[VMEM] * 6...  4.05 us
  transfers between devices with their start and end apart: 27, of which 15 were waited for; matrix products, arithmetic and copies ran while one was open for 2% of the time, Pallas kernels for 22%

profile of v8, /device:TPU:32, one launch (start us, length us, event | category | flops | bytes accessed | tf_op | source)
XLA Modules:
  0.0 172.3 jit_solution(17547155241689466281)
XLA Ops:
  6.6 1.2 multiply_sine_fusion
  7.8 2.4 %prep_keys.1 = (bf16[512,256]{1,0:T(8,128)(2,1)}, bf16[512,256]{1,0:T(8,128)(2,1)}, bf16[2,32,1024]{2,1,0:T(8,128)(2,1)}) custom-call(f32[256,32]{1,0:T(8,128)} %get-tuple-element.60.cos_ref, f32[256,32]{1,0:T(8,128)} %get-tuple-element.59.sin_ref, bf16[256,128]{1,0:T(8,128)(2,1)} %ka_ref.1, bf16[256,128]{1,0:T(8,128)(2,1)} %kb_ref.1, ...), custom_call_target="tpu_custom_call" | custom-call | tf_op jit(solution)/shard_map/prep_keys/pallas_call | solution.py:65
  10.3 2.0 %collective-permute-start.4 = (bf16[512,256]{1,0:T(8,128)(2,1)}, bf16[512,256]{1,0:T(8,128)(2,1)S(1)}, u32[]{:S(2)}, u32[]{:S(2)}) collective-permute-start(bf16[512,256]{1,0:T(8,128)(2,1)} %get-tuple-element.35), channel_id=1, source_target_pairs={{0,32},{4,228},{32,64},{36,4},{64,96},{68,36},{96,128},{100,68},{1... | collective-permute-start | bytes 786440 | tf_op jit(solution)/shard_map/ppermute | solution.py:382
  12.4 3.1 %collective-permute-start.16 = (bf16[128,2048]{1,0:T(8,128)(2,1)S(1)}, bf16[128,2048]{1,0:T(8,128)(2,1)S(1)}, u32[]{:S(2)}, u32[]{:S(2)}) collective-permute-start(bf16[128,2048]{1,0:T(8,128)(2,1)S(1)} %constant_dynamic-slice_fusion), channel_id=1, source_target_pairs={{0,3},{1,0},{2,1},{3,2},{4,7},{5,4},{6,5},{7,6},{8,11},{9,8},{10,9... | collective-permute-start | bytes 1572872 | tf_op jit(solution)/shard_map/ppermute | solution.py:354
  16.1 1.0 collective-permute-start.14
  17.1 3.2 %collective-permute-done.4 = bf16[512,256]{1,0:T(8,128)(2,1)S(1)} collective-permute-done((bf16[512,256]{1,0:T(8,128)(2,1)}, bf16[512,256]{1,0:T(8,128)(2,1)S(1)}, u32[]{:S(2)}, u32[]{:S(2)}) %collective-permute-start.4) | collective-permute-done | bytes 262176 | tf_op jit(solution)/shard_map/ppermute | solution.py:382
  20.4 0.8 collective-permute-start.6
  21.2 16.8 %collective-permute-done.16 = bf16[128,2048]{1,0:T(8,128)(2,1)S(1)} collective-permute-done((bf16[128,2048]{1,0:T(8,128)(2,1)S(1)}, bf16[128,2048]{1,0:T(8,128)(2,1)S(1)}, u32[]{:S(2)}, u32[]{:S(2)}) %collective-permute-start.16) | collective-permute-done | bytes 524320 | tf_op jit(solution)/shard_map/ppermute | solution.py:354
  38.1 3.7 %collective-permute-done.14 = bf16[128,2048]{1,0:T(8,128)(2,1)S(1)} collective-permute-done((bf16[128,2048]{1,0:T(8,128)(2,1)S(1)}, bf16[128,2048]{1,0:T(8,128)(2,1)S(1)}, u32[]{:S(2)}, u32[]{:S(2)}) %collective-permute-start.14) | collective-permute-done | bytes 524320 | tf_op jit(solution)/shard_map/ppermute | solution.py:354
  42.8 2.1 %pad_maximum_fusion.1.kv_ref = bf16[4,512,256]{2,1,0:T(8,128)(2,1)} fusion(bf16[2,512,256]{2,1,0:T(8,128)(2,1)} %collective-permute-done.6, bf16[1,512,256]{2,1,0:T(8,128)(2,1)S(1)} %bitcast.18, bf16[1,512,256]{2,1,0:T(8,128)(2,1)S(1)} %bitcast.20), kind=kLoop, calls=%fused_computation.1 | loop fusion | flops 1048576 | bytes 2097152 | tf_op jit(solution)/shard_map/concatenate | solution.py:393
  45.0 1.8 %collective-permute-start.7 = (bf16[2,512,256]{2,1,0:T(8,128)(2,1)}, bf16[2,512,256]{2,1,0:T(8,128)(2,1)}, u32[]{:S(2)}, u32[]{:S(2)}) collective-permute-start(bf16[2,512,256]{2,1,0:T(8,128)(2,1)} %collective-permute-done.6), channel_id=1, source_target_pairs={{0,32},{4,228},{32,64},{36,4},{64,96},{68,36},{96,128},{100,68},{1... | collective-permute-start | bytes 1572872 | tf_op jit(solution)/shard_map/ppermute | solution.py:392
  46.8 2.1 %prep_queries.1 = (bf16[256,256]{1,0:T(8,128)(2,1)}, bf16[256,256]{1,0:T(8,128)(2,1)}) custom-call(f32[256,32]{1,0:T(8,128)} %get-tuple-element.60.cos_ref, f32[256,32]{1,0:T(8,128)} %get-tuple-element.59.sin_ref, bf16[256,128]{1,0:T(8,128)(2,1)} %qa_ref.1, bf16[256,128]{1,0:T(8,128)(2,1)} %qb_ref.1), custom_call_target="tpu_custom_call" | custom-call | tf_op jit(solution)/shard_map/prep_queries/pallas_call | solution.py:76
  48.9 1.5 collective-permute-start
  50.4 2.7 %collective-permute-start.1 = (bf16[256,256]{1,0:T(8,128)(2,1)}, bf16[256,256]{1,0:T(8,128)(2,1)S(1)}, u32[]{:S(2)}, u32[]{:S(2)}) collective-permute-start(bf16[256,256]{1,0:T(8,128)(2,1)} %get-tuple-element.33), channel_id=1, source_target_pairs={{0,16},{8,24},{16,0},{24,8},{1,17},{9,25},{17,1},{25,9},{2,18},{10... | collective-permute-start | bytes 393224 | tf_op jit(solution)/shard_map/ppermute | solution.py:354
  53.1 2.7 %collective-permute-done.q1 = bf16[256,256]{1,0:T(8,128)(2,1)S(1)} collective-permute-done((bf16[256,256]{1,0:T(8,128)(2,1)}, bf16[256,256]{1,0:T(8,128)(2,1)S(1)}, u32[]{:S(2)}, u32[]{:S(2)}) %collective-permute-start) | collective-permute-done | bytes 131104 | tf_op jit(solution)/shard_map/ppermute | solution.py:354
  55.8 0.7 collective-permute-start.3
  56.5 3.1 %collective-permute-done.1.q2 = bf16[256,256]{1,0:T(8,128)(2,1)S(1)} collective-permute-done((bf16[256,256]{1,0:T(8,128)(2,1)}, bf16[256,256]{1,0:T(8,128)(2,1)S(1)}, u32[]{:S(2)}, u32[]{:S(2)}) %collective-permute-start.1) | collective-permute-done | bytes 131104 | tf_op jit(solution)/shard_map/ppermute | solution.py:354
  59.6 0.7 collective-permute-start.9
  60.3 7.2 %collective-permute-done.2.q3 = bf16[256,256]{1,0:T(8,128)(2,1)S(1)} collective-permute-done((bf16[256,256]{1,0:T(8,128)(2,1)}, bf16[256,256]{1,0:T(8,128)(2,1)S(1)}, u32[]{:S(2)}, u32[]{:S(2)}) %collective-permute-start.2) | collective-permute-done | bytes 131104 | tf_op jit(solution)/shard_map/ppermute | solution.py:354
  67.6 0.9 copy-done.8
  68.5 4.0 %attend_first.1 = (bf16[4,4,256,256]{3,2,1,0:T(8,128)(2,1)S(1)}, f32[4,4,128,256]{3,2,1,0:T(8,128)S(1)}, f32[4,4,1,256]{3,2,1,0:T(1,128)S(1)}, f32[4,4,1,256]{3,2,1,0:T(1,128)S(1)}) custom-call(bf16[256,256]{1,0:T(8,128)(2,1)S(1)} %copy-done.8, bf16[256,256]{1,0:T(8,128)(2,1)S(1)} %collective-permute-done.q1, ...), custom_call_target="tpu_custom_call" | custom-call | flops 805306368 | bytes 524288 | tf_op jit(solution)/shard_map/attend_first/pallas_call | solution.py:195
  72.5 6.7 %attend_next.4 = (f32[4,4,128,256]{3,2,1,0:T(8,128)S(1)}, f32[4,4,1,256]{3,2,1,0:T(1,128)S(1)}, f32[4,4,1,256]{3,2,1,0:T(1,128)S(1)}) custom-call(bf16[4,4,256,256]{3,2,1,0:T(8,128)(2,1)S(1)} %get-tuple-element.36.qs, bf16[4,512,256]{2,1,0:T(8,128)(2,1)} %pad_maximum_fusion.1.kv_ref, ...), custom_call_target="tpu_custom_call", output_to_operand_aliasing={{0}: (2, {}), {1}: (3, {}), {2}: (4, {})} | custom-call | flops 1610612736 | bytes 1048576 | tf_op jit(solution)/shard_map/attend_next/pallas_call | solution.py:209
  79.2 6.7 %attend_next.5 = (f32[4,4,128,256]{3,2,1,0:T(8,128)S(1)}, f32[4,4,1,256]{3,2,1,0:T(1,128)S(1)}, f32[4,4,1,256]{3,2,1,0:T(1,128)S(1)}) custom-call(bf16[4,4,256,256]{3,2,1,0:T(8,128)(2,1)S(1)} %get-tuple-element.36.qs, bf16[4,512,256]{2,1,0:T(8,128)(2,1)} %collective-permute-done.10.kv_ref, ...), custom_call_target="tpu_custom_call", output_to_operand_aliasing={{0}: (2, {}), {1}: (3, {}), {2}: (4, {})} | custom-call | flops 1610612736 | bytes 1048576 | tf_op jit(solution)/shard_map/attend_next/pallas_call | solution.py:209
  85.9 4.7 %attend_next.6 = (f32[4,4,128,256]{3,2,1,0:T(8,128)S(1)}, f32[4,4,1,256]{3,2,1,0:T(1,128)S(1)}, f32[4,4,1,256]{3,2,1,0:T(1,128)S(1)}) custom-call(bf16[4,4,256,256]{3,2,1,0:T(8,128)(2,1)S(1)} %get-tuple-element.36.qs, bf16[2,512,256]{2,1,0:T(8,128)(2,1)} %collective-permute-done.7.kv_ref, ...), custom_call_target="tpu_custom_call", output_to_operand_aliasing={{0}: (2, {}), {1}: (3, {}), {2}: (4, {})} | custom-call | flops 805306368 | bytes 524288 | tf_op jit(solution)/shard_map/attend_next/pallas_call | solution.py:209
  90.6 3.7 %attend_next.7 = (f32[4,4,128,256]{3,2,1,0:T(8,128)S(1)}, f32[4,4,1,256]{3,2,1,0:T(1,128)S(1)}, f32[4,4,1,256]{3,2,1,0:T(1,128)S(1)}) custom-call(bf16[4,4,256,256]{3,2,1,0:T(8,128)(2,1)S(1)} %get-tuple-element.36.qs, bf16[2,512,256]{2,1,0:T(8,128)(2,1)S(1)} %collective-permute-done.9.kv_ref, ...), custom_call_target="tpu_custom_call", output_to_operand_aliasing={{0}: (2, {}), {1}: (3, {}), {2}: (4, {})} | custom-call | flops 805306368 | bytes 524288 | tf_op jit(solution)/shard_map/attend_next/pallas_call | solution.py:209
  94.3 3.7 %attend_last.1 = (f32[4,4,128,256]{3,2,1,0:T(8,128)S(1)}, f32[4,4,1,256]{3,2,1,0:T(1,128)S(1)}, f32[4,4,1,256]{3,2,1,0:T(1,128)S(1)}, f32[16,256]{1,0:T(8,128)S(1)}) custom-call(bf16[4,4,256,256]{3,2,1,0:T(8,128)(2,1)S(1)} %get-tuple-element.36.qs, ...), custom_call_target="tpu_custom_call", output_to_operand_aliasing={{0}: (2, {}), {1}: (3, {}), {2}: (4, {})} | custom-call | flops 805306368 | bytes 524288 | tf_op jit(solution)/shard_map/attend_last/pallas_call | solution.py:223
  98.1 3.2 %collective-permute-start.12 = (f32[16,256]{1,0:T(8,128)S(1)}, f32[16,256]{1,0:T(8,128)S(1)}, u32[]{:S(2)}, u32[]{:S(2)}) collective-permute-start(f32[16,256]{1,0:T(8,128)S(1)} %get-tuple-element.52.lse0), channel_id=1, source_target_pairs={{0,16},{8,24},{16,0},{24,8},{1,17},{9,25},{17,1},{25,9},{2,18},{10... | collective-permute-start | bytes 49160 | tf_op jit(solution)/shard_map/ppermute | solution.py:354
  101.4 1.7 collective-permute-done.11.lse1
  103.6 1.6 collective-permute-done.13.lse3
  105.2 0.8 share.1
  106.0 0.8 copy-done.2
  106.8 4.2 %all-to-all-start = ((bf16[16,64,256]{2,1,0:T(8,128)(2,1)}), bf16[16,64,256]{2,1,0:T(8,128)(2,1)}, u32[]{:S(2)}, u32[]{:S(2)}) async-start(bf16[16,64,256]{2,1,0:T(8,128)(2,1)} %copy-done.2), calls=%async_computation | async-start | bytes 1048576 | tf_op jit(solution)/shard_map/all_to_all | solution.py:404
  111.2 11.9 %all-to-all-done.part_ref = bf16[16,64,256]{2,1,0:T(8,128)(2,1)} async-done(((bf16[16,64,256]{2,1,0:T(8,128)(2,1)}), bf16[16,64,256]{2,1,0:T(8,128)(2,1)}, u32[]{:S(2)}, u32[]{:S(2)}) %all-to-all-start) | async-done | bytes 524320 | tf_op jit(solution)/shard_map/all_to_all | solution.py:404
  123.1 0.9 copy-done.3
  124.0 3.3 %merge.1.refs_0_ = bf16[64,2048]{1,0:T(8,128)(2,1)S(1)} custom-call(s32[2]{0:T(128)S(1)} %pad_add_fusion.at_ref, bf16[16,64,256]{2,1,0:T(8,128)(2,1)} %all-to-all-done.part_ref, f32[1,128]{1,0:T(1,128)S(1)} %bitcast.16, bf16[64,2048]{1,0:T(8,128)(2,1)S(1)} %copy-done.3, f32[1,2048]{1,0:T(1,128)S(1)} %bitcast.15, ...), custom_call_target="tpu_custom_call" | custom-call | tf_op jit(solution)/shard_map/merge/pallas_call | solution.py:305
  127.9 1.5 collective-permute-start.18
  129.4 4.7 %collective-permute-done.19.refs_2_ = bf16[64,2048]{1,0:T(8,128)(2,1)S(1)} collective-permute-done((bf16[64,2048]{1,0:T(8,128)(2,1)S(1)}, bf16[64,2048]{1,0:T(8,128)(2,1)S(1)}, u32[]{:S(2)}, u32[]{:S(2)}) %collective-permute-start.19) | collective-permute-done | bytes 262176 | tf_op jit(solution)/shard_map/ppermute | solution.py:354
  134.1 2.8 %collective-permute-start.22 = (bf16[32,2048]{1,0:T(8,128)(2,1)S(1)}, bf16[32,2048]{1,0:T(8,128)(2,1)S(1)}, u32[]{:S(2)}, u32[]{:S(2)}) collective-permute-start(bf16[32,2048]{1,0:T(8,128)(2,1)S(1)} %slice.9), channel_id=1, source_target_pairs={{0,3},{1,0},{2,1},{3,2},{4,7},{5,4},{6,5},{7,6},{8,11},{9,8},{10,9... | collective-permute-start | bytes 393224 | tf_op jit(solution)/shard_map/ppermute | solution.py:354
  137.1 2.4 %collective-permute-done.22 = bf16[32,2048]{1,0:T(8,128)(2,1)S(1)} collective-permute-done((bf16[32,2048]{1,0:T(8,128)(2,1)S(1)}, bf16[32,2048]{1,0:T(8,128)(2,1)S(1)}, u32[]{:S(2)}, u32[]{:S(2)}) %collective-permute-start.22) | collective-permute-done | bytes 131104 | tf_op jit(solution)/shard_map/ppermute | solution.py:354
  139.5 3.8 %collective-permute-done.21 = bf16[32,2048]{1,0:T(8,128)(2,1)S(1)} collective-permute-done((bf16[32,2048]{1,0:T(8,128)(2,1)S(1)}, bf16[32,2048]{1,0:T(8,128)(2,1)S(1)}, u32[]{:S(2)}, u32[]{:S(2)}) %collective-permute-start.21) | collective-permute-done | bytes 131104 | tf_op jit(solution)/shard_map/ppermute | solution.py:354
  143.3 3.4 %copy-done.1 = bf16[128,32,1024]{2,1,0:T(8,128)(2,1)S(1)} copy-done((bf16[128,32,1024]{2,1,0:T(8,128)(2,1)S(1)}, bf16[128,32,1024]{2,1,0:T(8,128)(2,1)}, u32[]{:S(2)}) %copy-start.1) | copy-done | bytes 8388632
  147.3 2.4 %mixer.2 = (f32[64,2048]{1,0:T(8,128)S(1)}, bf16[64,2048]{1,0:T(8,128)(2,1)S(1)}, bf16[64,2048]{1,0:T(8,128)(2,1)S(1)}) custom-call(bf16[64,2048]{1,0:T(8,128)(2,1)S(1)} %merge.1.refs_0_, bf16[64,2048]{1,0:T(8,128)(2,1)S(1)} %collective-permute-done.18.refs_1_, bf16[64,2048]{1,0:T(8,128)(2,1)S(1)} %collective-permute-done.19.refs_2_, ...), custom_call_target="tpu_custom_call" | custom-call | flops 2147483648 | bytes 8388608 | tf_op jit(solution)/shard_map/mixer/pallas_call | solution.py:341
  149.7 2.1 %mixer.3 = bf16[64,2048]{1,0:T(8,128)(2,1)S(1)} custom-call(bf16[64,2048]{1,0:T(8,128)(2,1)S(1)} %pad_maximum_fusion.3.refs_0_, bf16[64,2,32,1024]{3,2,1,0:T(8,128)(2,1)S(1)} %load_mix.1.refs_3_.refs_1_), custom_call_target="tpu_custom_call" | custom-call | flops 2147483648 | bytes 8388608 | tf_op jit(solution)/shard_map/mixer/pallas_call | solution.py:341
  151.8 1.4 collective-permute-start.23
  153.3 2.0 %collective-permute-start.20 = (bf16[64,2048]{1,0:T(8,128)(2,1)S(1)}, bf16[64,2048]{1,0:T(8,128)(2,1)S(1)}, u32[]{:S(2)}, u32[]{:S(2)}) collective-permute-start(bf16[64,2048]{1,0:T(8,128)(2,1)S(1)} %get-tuple-element.57), channel_id=1, source_target_pairs={{0,3},{1,0},{2,1},{3,2},{4,7},{5,4},{6,5},{7,6},{8,11},{9,8},{10,9... | collective-permute-start | bytes 786440 | tf_op jit(solution)/shard_map/ppermute | solution.py:354
  155.2 6.9 %collective-permute-done.24 = bf16[64,2048]{1,0:T(8,128)(2,1)S(1)} collective-permute-done((bf16[64,2048]{1,0:T(8,128)(2,1)S(1)}, bf16[64,2048]{1,0:T(8,128)(2,1)S(1)}, u32[]{:S(2)}, u32[]{:S(2)}) %collective-permute-start.24) | collective-permute-done | bytes 262176 | tf_op jit(solution)/shard_map/ppermute | solution.py:354
  162.2 2.4 %collective-permute-done.20 = bf16[64,2048]{1,0:T(8,128)(2,1)S(1)} collective-permute-done((bf16[64,2048]{1,0:T(8,128)(2,1)S(1)}, bf16[64,2048]{1,0:T(8,128)(2,1)S(1)}, u32[]{:S(2)}, u32[]{:S(2)}) %collective-permute-start.20) | collective-permute-done | bytes 262176 | tf_op jit(solution)/shard_map/ppermute | solution.py:354
  164.6 0.9 add_convert_fusion
  (59 shorter events, 4.1 us)
Async XLA Ops:
  6.5 5.8 %copy-start = (bf16[256,2048]{1,0:T(8,128)(2,1)S(1)}, bf16[256,2048]{1,0:T(8,128)(2,1)}, u32[]{:S(2)}) copy-start(bf16[256,2048]{1,0:T(8,128)(2,1)} %param.20) | copy-start | bytes 3145732
  6.5 136.7 %all-gather.3.cloned.1.call-start = ((), (), s32[]{:S(2)}) async-start(), calls=%async_computation.1 | async-start | bytes 8519680 | tf_op jit(solution)/shard_map/all_gather | solution.py:385
  10.2 6.8 %collective-permute-start.5 = (bf16[512,256]{1,0:T(8,128)(2,1)}, bf16[512,256]{1,0:T(8,128)(2,1)S(1)}, u32[]{:S(2)}, u32[]{:S(2)}) collective-permute-start(bf16[512,256]{1,0:T(8,128)(2,1)} %get-tuple-element.35), channel_id=1, source_target_pairs={{0,228},{4,32},{32,4},{36,64},{64,36},{68,96},{96,68},{100,128},{1... | collective-permute-start | bytes 786440 | tf_op jit(solution)/shard_map/ppermute | solution.py:382
  10.3 10.0 %collective-permute-start.4 = (bf16[512,256]{1,0:T(8,128)(2,1)}, bf16[512,256]{1,0:T(8,128)(2,1)S(1)}, u32[]{:S(2)}, u32[]{:S(2)}) collective-permute-start(bf16[512,256]{1,0:T(8,128)(2,1)} %get-tuple-element.35), channel_id=1, source_target_pairs={{0,32},{4,228},{32,64},{36,4},{64,96},{68,36},{96,128},{100,68},{1... | collective-permute-start | bytes 786440 | tf_op jit(solution)/shard_map/ppermute | solution.py:382
  12.4 25.7 %collective-permute-start.16 = (bf16[128,2048]{1,0:T(8,128)(2,1)S(1)}, bf16[128,2048]{1,0:T(8,128)(2,1)S(1)}, u32[]{:S(2)}, u32[]{:S(2)}) collective-permute-start(bf16[128,2048]{1,0:T(8,128)(2,1)S(1)} %constant_dynamic-slice_fusion), channel_id=1, source_target_pairs={{0,3},{1,0},{2,1},{3,2},{4,7},{5,4},{6,5},{7,6},{8,11},{9,8},{10,9... | collective-permute-start | bytes 1572872 | tf_op jit(solution)/shard_map/ppermute | solution.py:354
  15.5 22.6 %collective-permute-start.15 = (bf16[128,2048]{1,0:T(8,128)(2,1)S(1)}, bf16[128,2048]{1,0:T(8,128)(2,1)S(1)}, u32[]{:S(2)}, u32[]{:S(2)}) collective-permute-start(bf16[128,2048]{1,0:T(8,128)(2,1)S(1)} %constant_dynamic-slice_fusion), channel_id=1, source_target_pairs={{0,2},{1,3},{2,0},{3,1},{4,6},{5,7},{6,4},{7,5},{8,10},{9,11},{10,... | collective-permute-start | bytes 1572872 | tf_op jit(solution)/shard_map/ppermute | solution.py:354
  16.1 25.7 %collective-permute-start.14 = (bf16[128,2048]{1,0:T(8,128)(2,1)S(1)}, bf16[128,2048]{1,0:T(8,128)(2,1)S(1)}, u32[]{:S(2)}, u32[]{:S(2)}) collective-permute-start(bf16[128,2048]{1,0:T(8,128)(2,1)S(1)} %constant_dynamic-slice_fusion), channel_id=1, source_target_pairs={{0,1},{1,2},{2,3},{3,0},{4,5},{5,6},{6,7},{7,4},{8,9},{9,10},{10,1... | collective-permute-start | bytes 1572872 | tf_op jit(solution)/shard_map/ppermute | solution.py:354
  17.1 24.7 %copy-start.9 = (bf16[512,256]{1,0:T(8,128)(2,1)}, bf16[512,256]{1,0:T(8,128)(2,1)S(1)}, u32[]{:S(2)}) copy-start(bf16[512,256]{1,0:T(8,128)(2,1)S(1)} %collective-permute-done.5) | copy-start | bytes 786436
  20.3 21.5 %copy-start.11 = (bf16[512,256]{1,0:T(8,128)(2,1)}, bf16[512,256]{1,0:T(8,128)(2,1)S(1)}, u32[]{:S(2)}) copy-start(bf16[512,256]{1,0:T(8,128)(2,1)S(1)} %collective-permute-done.4) | copy-start | bytes 786436
  20.4 21.9 %collective-permute-start.6 = (bf16[2,512,256]{2,1,0:T(8,128)(2,1)S(1)}, bf16[2,512,256]{2,1,0:T(8,128)(2,1)}, u32[]{:S(2)}, u32[]{:S(2)}) collective-permute-start(bf16[2,512,256]{2,1,0:T(8,128)(2,1)S(1)} %pad_maximum_fusion.2), channel_id=1, source_target_pairs={{0,32},{4,228},{32,64},{36,4},{64,96},{68,36},{96,128},{100,68},{1... | collective-permute-start | bytes 1572872 | tf_op jit(solution)/shard_map/ppermute | solution.py:388
  41.8 1.0 copy-start.10
  41.8 1.0 copy-start.12
  42.1 25.5 %copy-start.7 = (bf16[512,256]{1,0:T(8,128)(2,1)S(1)}, bf16[512,256]{1,0:T(8,128)(2,1)}, u32[]{:S(2)}) copy-start(bf16[512,256]{1,0:T(8,128)(2,1)} %get-tuple-element.34.own_ref) | copy-start | bytes 786436
  42.1 81.0 %collective-permute-start.17 = (bf16[4,128,2048]{2,1,0:T(8,128)(2,1)S(1)}, bf16[4,128,2048]{2,1,0:T(8,128)(2,1)}, u32[]{:S(2)}, u32[]{:S(2)}) collective-permute-start(bf16[4,128,2048]{2,1,0:T(8,128)(2,1)S(1)} %pad_maximum_fusion.mine_ref), channel_id=1, source_target_pairs={{0,4},{4,0},{1,5},{5,1},{2,6},{6,2},{3,7},{7,3},{8,12},{12,8},{9,1... | collective-permute-start | bytes 6291464 | tf_op jit(solution)/shard_map/ppermute | solution.py:354
  44.9 34.3 %collective-permute-start.10 = (bf16[4,512,256]{2,1,0:T(8,128)(2,1)}, bf16[4,512,256]{2,1,0:T(8,128)(2,1)}, u32[]{:S(2)}, u32[]{:S(2)}) collective-permute-start(bf16[4,512,256]{2,1,0:T(8,128)(2,1)} %pad_maximum_fusion.1.kv_ref), channel_id=1, source_target_pairs={{0,4},{4,0},{1,5},{5,1},{2,6},{6,2},{3,7},{7,3},{8,12},{12,8},{9,1... | collective-permute-start | bytes 3145736 | tf_op jit(solution)/shard_map/ppermute | solution.py:354
  45.0 14.6 %collective-permute-start.7 = (bf16[2,512,256]{2,1,0:T(8,128)(2,1)}, bf16[2,512,256]{2,1,0:T(8,128)(2,1)}, u32[]{:S(2)}, u32[]{:S(2)}) collective-permute-start(bf16[2,512,256]{2,1,0:T(8,128)(2,1)} %collective-permute-done.6), channel_id=1, source_target_pairs={{0,32},{4,228},{32,64},{36,4},{64,96},{68,36},{96,128},{100,68},{1... | collective-permute-start | bytes 1572872 | tf_op jit(solution)/shard_map/ppermute | solution.py:392
  48.9 6.9 %collective-permute-start = (bf16[256,256]{1,0:T(8,128)(2,1)}, bf16[256,256]{1,0:T(8,128)(2,1)S(1)}, u32[]{:S(2)}, u32[]{:S(2)}) collective-permute-start(bf16[256,256]{1,0:T(8,128)(2,1)} %get-tuple-element.33), channel_id=1, source_target_pairs={{0,8},{8,16},{16,24},{24,0},{1,9},{9,17},{17,25},{25,1},{2,10},{10... | collective-permute-start | bytes 393224 | tf_op jit(solution)/shard_map/ppermute | solution.py:354
  50.4 9.2 %collective-permute-start.1 = (bf16[256,256]{1,0:T(8,128)(2,1)}, bf16[256,256]{1,0:T(8,128)(2,1)S(1)}, u32[]{:S(2)}, u32[]{:S(2)}) collective-permute-start(bf16[256,256]{1,0:T(8,128)(2,1)} %get-tuple-element.33), channel_id=1, source_target_pairs={{0,16},{8,24},{16,0},{24,8},{1,17},{9,25},{17,1},{25,9},{2,18},{10... | collective-permute-start | bytes 393224 | tf_op jit(solution)/shard_map/ppermute | solution.py:354
  55.8 11.8 %collective-permute-start.3 = (bf16[512,256]{1,0:T(8,128)(2,1)}, bf16[512,256]{1,0:T(8,128)(2,1)S(1)}, u32[]{:S(2)}, u32[]{:S(2)}) collective-permute-start(bf16[512,256]{1,0:T(8,128)(2,1)} %get-tuple-element.35), channel_id=1, source_target_pairs={{0,4},{4,0},{1,5},{5,1},{2,6},{6,2},{3,7},{7,3},{8,12},{12,8},{9,1... | collective-permute-start | bytes 786440 | tf_op jit(solution)/shard_map/ppermute | solution.py:354
  59.6 8.0 %collective-permute-start.2 = (bf16[256,256]{1,0:T(8,128)(2,1)}, bf16[256,256]{1,0:T(8,128)(2,1)S(1)}, u32[]{:S(2)}, u32[]{:S(2)}) collective-permute-start(bf16[256,256]{1,0:T(8,128)(2,1)} %get-tuple-element.33), channel_id=1, source_target_pairs={{0,24},{8,0},{16,8},{24,16},{1,25},{9,1},{17,9},{25,17},{2,26},{10... | collective-permute-start | bytes 393224 | tf_op jit(solution)/shard_map/ppermute | solution.py:354
  59.6 31.0 %collective-permute-start.9 = (bf16[2,512,256]{2,1,0:T(8,128)(2,1)}, bf16[2,512,256]{2,1,0:T(8,128)(2,1)S(1)}, u32[]{:S(2)}, u32[]{:S(2)}) collective-permute-start(bf16[2,512,256]{2,1,0:T(8,128)(2,1)} %collective-permute-done.7.kv_ref), channel_id=1, source_target_pairs={{0,4},{4,0},{1,5},{5,1},{2,6},{6,2},{3,7},{7,3},{8,12},{12,8},{9,1... | collective-permute-start | bytes 1572872 | tf_op jit(solution)/shard_map/ppermute | solution.py:354
  67.5 26.8 %collective-permute-start.8 = (bf16[2,512,256]{2,1,0:T(8,128)(2,1)}, bf16[2,512,256]{2,1,0:T(8,128)(2,1)S(1)}, u32[]{:S(2)}, u32[]{:S(2)}) collective-permute-start(bf16[2,512,256]{2,1,0:T(8,128)(2,1)} %collective-permute-done.7.kv_ref), channel_id=1, source_target_pairs={{0,32},{4,228},{32,64},{36,4},{64,96},{68,36},{96,128},{100,68},{1... | collective-permute-start | bytes 1572872 | tf_op jit(solution)/shard_map/ppermute | solution.py:397
  67.6 0.9 copy-start.8
  94.3 10.9 %copy-start.5 = (f32[2]{0:T(128)S(1)}, f32[2]{0:T(128)}, u32[]{:S(2)}) copy-start(f32[2]{0:T(128)} %lam_ref.1) | copy-start | bytes 28
  98.0 25.0 %copy-start.4 = (f32[2048]{0:T(1024)S(1)}, f32[2048]{0:T(1024)}, u32[]{:S(2)}) copy-start(f32[2048]{0:T(1024)} %param.21) | copy-start | bytes 24580
  98.0 25.0 %copy-start.6 = (f32[128]{0:T(128)S(1)}, f32[128]{0:T(128)}, u32[]{:S(2)}) copy-start(f32[128]{0:T(128)} %param.19) | copy-start | bytes 1540
  98.1 5.0 %collective-permute-start.11 = (f32[16,256]{1,0:T(8,128)S(1)}, f32[16,256]{1,0:T(8,128)S(1)}, u32[]{:S(2)}, u32[]{:S(2)}) collective-permute-start(f32[16,256]{1,0:T(8,128)S(1)} %get-tuple-element.52.lse0), channel_id=1, source_target_pairs={{0,8},{8,16},{16,24},{24,0},{1,9},{9,17},{17,25},{25,1},{2,10},{10... | collective-permute-start | bytes 49160 | tf_op jit(solution)/shard_map/ppermute | solution.py:354
  98.1 5.4 %collective-permute-start.12 = (f32[16,256]{1,0:T(8,128)S(1)}, f32[16,256]{1,0:T(8,128)S(1)}, u32[]{:S(2)}, u32[]{:S(2)}) collective-permute-start(f32[16,256]{1,0:T(8,128)S(1)} %get-tuple-element.52.lse0), channel_id=1, source_target_pairs={{0,16},{8,24},{16,0},{24,8},{1,17},{9,25},{17,1},{25,9},{2,18},{10... | collective-permute-start | bytes 49160 | tf_op jit(solution)/shard_map/ppermute | solution.py:354
  101.4 3.8 %collective-permute-start.13 = (f32[16,256]{1,0:T(8,128)S(1)}, f32[16,256]{1,0:T(8,128)S(1)}, u32[]{:S(2)}, u32[]{:S(2)}) collective-permute-start(f32[16,256]{1,0:T(8,128)S(1)} %get-tuple-element.52.lse0), channel_id=1, source_target_pairs={{0,24},{8,0},{16,8},{24,16},{1,25},{9,1},{17,9},{25,17},{2,26},{10... | collective-permute-start | bytes 49160 | tf_op jit(solution)/shard_map/ppermute | solution.py:354
  106.0 0.8 copy-start.2
  106.8 16.2 %all-to-all-start = ((bf16[16,64,256]{2,1,0:T(8,128)(2,1)}), bf16[16,64,256]{2,1,0:T(8,128)(2,1)}, u32[]{:S(2)}, u32[]{:S(2)}) async-start(bf16[16,64,256]{2,1,0:T(8,128)(2,1)} %copy-done.2), calls=%async_computation | async-start | bytes 1048576 | tf_op jit(solution)/shard_map/all_to_all | solution.py:404
  123.0 1.0 copy-start.3
  127.3 6.8 %collective-permute-start.19 = (bf16[64,2048]{1,0:T(8,128)(2,1)S(1)}, bf16[64,2048]{1,0:T(8,128)(2,1)S(1)}, u32[]{:S(2)}, u32[]{:S(2)}) collective-permute-start(bf16[64,2048]{1,0:T(8,128)(2,1)S(1)} %merge.1.refs_0_), channel_id=1, source_target_pairs={{0,3},{1,0},{2,1},{3,2},{4,7},{5,4},{6,5},{7,6},{8,11},{9,8},{10,9... | collective-permute-start | bytes 786440 | tf_op jit(solution)/shard_map/ppermute | solution.py:354
  127.9 9.0 %collective-permute-start.18 = (bf16[64,2048]{1,0:T(8,128)(2,1)S(1)}, bf16[64,2048]{1,0:T(8,128)(2,1)S(1)}, u32[]{:S(2)}, u32[]{:S(2)}) collective-permute-start(bf16[64,2048]{1,0:T(8,128)(2,1)S(1)} %merge.1.refs_0_), channel_id=1, source_target_pairs={{0,1},{1,2},{2,3},{3,0},{4,5},{5,6},{6,7},{7,4},{8,9},{9,10},{10,1... | collective-permute-start | bytes 786440 | tf_op jit(solution)/shard_map/ppermute | solution.py:354
  134.1 5.3 %collective-permute-start.22 = (bf16[32,2048]{1,0:T(8,128)(2,1)S(1)}, bf16[32,2048]{1,0:T(8,128)(2,1)S(1)}, u32[]{:S(2)}, u32[]{:S(2)}) collective-permute-start(bf16[32,2048]{1,0:T(8,128)(2,1)S(1)} %slice.9), channel_id=1, source_target_pairs={{0,3},{1,0},{2,1},{3,2},{4,7},{5,4},{6,5},{7,6},{8,11},{9,8},{10,9... | collective-permute-start | bytes 393224 | tf_op jit(solution)/shard_map/ppermute | solution.py:354
  137.0 6.3 %collective-permute-start.21 = (bf16[32,2048]{1,0:T(8,128)(2,1)S(1)}, bf16[32,2048]{1,0:T(8,128)(2,1)S(1)}, u32[]{:S(2)}, u32[]{:S(2)}) collective-permute-start(bf16[32,2048]{1,0:T(8,128)(2,1)S(1)} %slice.8), channel_id=1, source_target_pairs={{0,1},{1,2},{2,3},{3,0},{4,5},{5,6},{6,7},{7,4},{8,9},{9,10},{10,1... | collective-permute-start | bytes 393224 | tf_op jit(solution)/shard_map/ppermute | solution.py:354
  143.3 3.4 %copy-start.1 = (bf16[128,32,1024]{2,1,0:T(8,128)(2,1)S(1)}, bf16[128,32,1024]{2,1,0:T(8,128)(2,1)}, u32[]{:S(2)}) copy-start(bf16[128,32,1024]{2,1,0:T(8,128)(2,1)} %all-gather.3.cloned.1.call-done) | copy-start | bytes 25165828
  149.6 12.5 %collective-permute-start.24 = (bf16[64,2048]{1,0:T(8,128)(2,1)S(1)}, bf16[64,2048]{1,0:T(8,128)(2,1)S(1)}, u32[]{:S(2)}, u32[]{:S(2)}) collective-permute-start(bf16[64,2048]{1,0:T(8,128)(2,1)S(1)} %get-tuple-element.58), channel_id=1, source_target_pairs={{0,1},{1,2},{2,3},{3,0},{4,5},{5,6},{6,7},{7,4},{8,9},{9,10},{10,1... | collective-permute-start | bytes 786440 | tf_op jit(solution)/shard_map/ppermute | solution.py:354
  151.8 10.3 %collective-permute-start.23 = (bf16[64,2048]{1,0:T(8,128)(2,1)S(1)}, bf16[64,2048]{1,0:T(8,128)(2,1)S(1)}, u32[]{:S(2)}, u32[]{:S(2)}) collective-permute-start(bf16[64,2048]{1,0:T(8,128)(2,1)S(1)} %mixer.3), channel_id=1, source_target_pairs={{0,2},{1,3},{2,0},{3,1},{4,6},{5,7},{6,4},{7,5},{8,10},{9,11},{10,... | collective-permute-start | bytes 786440 | tf_op jit(solution)/shard_map/ppermute | solution.py:354
  153.3 11.3 %collective-permute-start.20 = (bf16[64,2048]{1,0:T(8,128)(2,1)S(1)}, bf16[64,2048]{1,0:T(8,128)(2,1)S(1)}, u32[]{:S(2)}, u32[]{:S(2)}) collective-permute-start(bf16[64,2048]{1,0:T(8,128)(2,1)S(1)} %get-tuple-element.57), channel_id=1, source_target_pairs={{0,3},{1,0},{2,1},{3,2},{4,7},{5,4},{6,5},{7,6},{8,11},{9,8},{10,9... | collective-permute-start | bytes 786440 | tf_op jit(solution)/shard_map/ppermute | solution.py:354
Sparse Core Ops, SparseCore 0:
  10.4 87.3 all-gather.2

commit v9 on v8

--- a/solution.py
+++ b/solution.py
@@ -174,9 +174,9 @@
             factors.append(terms[0] / ((terms[0] + terms[1] + terms[2] + terms[3]) * tot[o, hm]))
         for h in range(2):
             diff = acc[o, 2 * h] * factors[2 * h] - acc[o, 2 * h + 1] * (lam_ref[h] * factors[2 * h + 1])
-            out_ref[pl.ds(4 * home, 4), :, h * VD : (h + 1) * VD] = diff.T.astype(BF16).reshape(
-                4, TOK // 4, VD
-            )
+            block = diff.T.astype(BF16).reshape(4, TOK // 4, VD)
+            for y in range(4):
+                out_ref[4 * y + home, :, h * VD : (h + 1) * VD] = block[y]
 
 
 def cost(keys):
@@ -285,7 +285,7 @@
     stream = res_ref[...].astype(F32)
     for o in range(4):
         y = (at_ref[0] + 4 - o) % 4
-        both = sum(part_ref[4 * k + y].astype(F32) for k in range(4))
+        both = sum(part_ref[4 * y + k].astype(F32) for k in range(4))
         heads = []
         for h in range(2):
             diff = both[:, h * VD : (h + 1) * VD]
@@ -401,7 +401,7 @@
     acc, _, tot, lse = attend_last(qs, far, state)
     lses = [lse] + [shifted(lse, "x", k) for k in (1, 2, 3)]
     part = share(x, lambdas, lses, acc, tot)
-    part = lax.all_to_all(part, ("x", "tp"), split_axis=0, concat_axis=0, tiled=True)
+    part = lax.all_to_all(part, ("tp", "x"), split_axis=0, concat_axis=0, tiled=True)
     normed = merge(at, part, head_gain, residual, norm_gain, out_weights)
     mix_weights = load_mix(mix_weights)
     rows = normed.shape[0] // 2

time: 173 us -> 174 us (level)
  the two profiles are of different devices: /device:TPU:32 before, /device:TPU:98 now
where the time goes in v9:
time: 174 us; the launch traced here: 173 us
  waiting for transfers between devices  66.4 us (38%)
  Pallas kernels  43.2 us (25%)
  starting transfers between devices  38.5 us (22%)
  between operations  13.7 us (8%)
  local copies, waits for them, and re-layouts  6.77 us (4%)
  other arithmetic  4.63 us (3%)
    ppermute x20, waiting for transfers between devices, shifted(): lax.ppermute(value, axis, [(i, (i + by) % size) for i in range(size)])  55.8 us
    pallas_call x4, Pallas kernels, attend_next(): pl.pallas_call(next_kernel, out_shape=STATE, in_specs=[VMEM] * 5, out_spe...  21.7 us
    ppermute x20, starting transfers between devices, shifted(): lax.ppermute(value, axis, [(i, (i + by) % size) for i in range(size)])  21.4 us
    all_to_all x1, waiting for transfers between devices, local(): lax.all_to_all(part, ('tp', 'x'), split_axis=0, concat_axis=0, tiled=True)  8.92 us
    unnamed x26, local copies, waits for them, and re-layouts  6.68 us
    pallas_call x2, Pallas kernels, mixer(): pl.pallas_call(functools.partial(mixer_kernel, len(pieces)), out_shape=[j...  4.47 us
    all_to_all x1, starting transfers between devices, local(): lax.all_to_all(part, ('tp', 'x'), split_axis=0, concat_axis=0, tiled=True)  4.33 us
    pallas_call x1, Pallas kernels, attend_first(): pl.pallas_call(first_kernel, out_shape=(QS,) + STATE, in_specs=[VMEM] * 6...  4.07 us
  transfers between devices with their start and end apart: 27, of which 15 were waited for; matrix products, arithmetic and copies ran while one was open for 1% of the time, Pallas kernels for 22%

profile of v9, /device:TPU:98, one launch (start us, length us, event | category | flops | bytes accessed | tf_op | source)
XLA Modules:
  0.0 173.1 jit_solution(14253863282808955696)
XLA Ops:
  6.6 1.2 multiply_sine_fusion
  7.8 2.4 %prep_keys.1 = (bf16[512,256]{1,0:T(8,128)(2,1)}, bf16[512,256]{1,0:T(8,128)(2,1)}, bf16[2,32,1024]{2,1,0:T(8,128)(2,1)}) custom-call(f32[256,32]{1,0:T(8,128)} %get-tuple-element.60.cos_ref, f32[256,32]{1,0:T(8,128)} %get-tuple-element.59.sin_ref, bf16[256,128]{1,0:T(8,128)(2,1)} %ka_ref.1, bf16[256,128]{1,0:T(8,128)(2,1)} %kb_ref.1, ...), custom_call_target="tpu_custom_call" | custom-call | tf_op jit(solution)/shard_map/prep_keys/pallas_call | solution.py:65
  10.3 3.2 %collective-permute-start.4 = (bf16[512,256]{1,0:T(8,128)(2,1)}, bf16[512,256]{1,0:T(8,128)(2,1)S(1)}, u32[]{:S(2)}, u32[]{:S(2)}) collective-permute-start(bf16[512,256]{1,0:T(8,128)(2,1)} %get-tuple-element.35), channel_id=1, source_target_pairs={{0,32},{4,228},{32,64},{36,4},{64,96},{68,36},{96,128},{100,68},{1... | collective-permute-start | bytes 786440 | tf_op jit(solution)/shard_map/ppermute | solution.py:382
  13.6 3.1 %collective-permute-start.16 = (bf16[128,2048]{1,0:T(8,128)(2,1)S(1)}, bf16[128,2048]{1,0:T(8,128)(2,1)S(1)}, u32[]{:S(2)}, u32[]{:S(2)}) collective-permute-start(bf16[128,2048]{1,0:T(8,128)(2,1)S(1)} %constant_dynamic-slice_fusion), channel_id=1, source_target_pairs={{0,3},{1,0},{2,1},{3,2},{4,7},{5,4},{6,5},{7,6},{8,11},{9,8},{10,9... | collective-permute-start | bytes 1572872 | tf_op jit(solution)/shard_map/ppermute | solution.py:354
  17.3 1.0 collective-permute-start.14
  18.5 1.4 collective-permute-done.4
  19.9 3.7 %collective-permute-start.6 = (bf16[2,512,256]{2,1,0:T(8,128)(2,1)S(1)}, bf16[2,512,256]{2,1,0:T(8,128)(2,1)}, u32[]{:S(2)}, u32[]{:S(2)}) collective-permute-start(bf16[2,512,256]{2,1,0:T(8,128)(2,1)S(1)} %pad_maximum_fusion.2), channel_id=1, source_target_pairs={{0,32},{4,228},{32,64},{36,4},{64,96},{68,36},{96,128},{100,68},{1... | collective-permute-start | bytes 1572872 | tf_op jit(solution)/shard_map/ppermute | solution.py:388
  23.7 15.6 %collective-permute-done.16 = bf16[128,2048]{1,0:T(8,128)(2,1)S(1)} collective-permute-done((bf16[128,2048]{1,0:T(8,128)(2,1)S(1)}, bf16[128,2048]{1,0:T(8,128)(2,1)S(1)}, u32[]{:S(2)}, u32[]{:S(2)}) %collective-permute-start.16) | collective-permute-done | bytes 524320 | tf_op jit(solution)/shard_map/ppermute | solution.py:354
  39.3 3.7 %collective-permute-done.14 = bf16[128,2048]{1,0:T(8,128)(2,1)S(1)} collective-permute-done((bf16[128,2048]{1,0:T(8,128)(2,1)S(1)}, bf16[128,2048]{1,0:T(8,128)(2,1)S(1)}, u32[]{:S(2)}, u32[]{:S(2)}) %collective-permute-start.14) | collective-permute-done | bytes 524320 | tf_op jit(solution)/shard_map/ppermute | solution.py:354
  44.0 2.1 %pad_maximum_fusion.1.kv_ref = bf16[4,512,256]{2,1,0:T(8,128)(2,1)} fusion(bf16[2,512,256]{2,1,0:T(8,128)(2,1)} %collective-permute-done.6, bf16[1,512,256]{2,1,0:T(8,128)(2,1)S(1)} %bitcast.18, bf16[1,512,256]{2,1,0:T(8,128)(2,1)S(1)} %bitcast.20), kind=kLoop, calls=%fused_computation.1 | loop fusion | flops 1048576 | bytes 2097152 | tf_op jit(solution)/shard_map/concatenate | solution.py:393
  46.1 2.8 %collective-permute-start.7 = (bf16[2,512,256]{2,1,0:T(8,128)(2,1)}, bf16[2,512,256]{2,1,0:T(8,128)(2,1)}, u32[]{:S(2)}, u32[]{:S(2)}) collective-permute-start(bf16[2,512,256]{2,1,0:T(8,128)(2,1)} %collective-permute-done.6), channel_id=1, source_target_pairs={{0,32},{4,228},{32,64},{36,4},{64,96},{68,36},{96,128},{100,68},{1... | collective-permute-start | bytes 1572872 | tf_op jit(solution)/shard_map/ppermute | solution.py:392
  48.9 2.1 %prep_queries.1 = (bf16[256,256]{1,0:T(8,128)(2,1)}, bf16[256,256]{1,0:T(8,128)(2,1)}) custom-call(f32[256,32]{1,0:T(8,128)} %get-tuple-element.60.cos_ref, f32[256,32]{1,0:T(8,128)} %get-tuple-element.59.sin_ref, bf16[256,128]{1,0:T(8,128)(2,1)} %qa_ref.1, bf16[256,128]{1,0:T(8,128)(2,1)} %qb_ref.1), custom_call_target="tpu_custom_call" | custom-call | tf_op jit(solution)/shard_map/prep_queries/pallas_call | solution.py:76
  51.0 1.4 collective-permute-start
  52.4 1.1 collective-permute-start.1
  53.5 3.3 %collective-permute-done.q1 = bf16[256,256]{1,0:T(8,128)(2,1)S(1)} collective-permute-done((bf16[256,256]{1,0:T(8,128)(2,1)}, bf16[256,256]{1,0:T(8,128)(2,1)S(1)}, u32[]{:S(2)}, u32[]{:S(2)}) %collective-permute-start) | collective-permute-done | bytes 131104 | tf_op jit(solution)/shard_map/ppermute | solution.py:354
  56.8 2.3 %collective-permute-done.1.q2 = bf16[256,256]{1,0:T(8,128)(2,1)S(1)} collective-permute-done((bf16[256,256]{1,0:T(8,128)(2,1)}, bf16[256,256]{1,0:T(8,128)(2,1)S(1)}, u32[]{:S(2)}, u32[]{:S(2)}) %collective-permute-start.1) | collective-permute-done | bytes 131104 | tf_op jit(solution)/shard_map/ppermute | solution.py:354
  59.1 1.1 collective-permute-start.2
  60.2 4.9 %collective-permute-done.2.q3 = bf16[256,256]{1,0:T(8,128)(2,1)S(1)} collective-permute-done((bf16[256,256]{1,0:T(8,128)(2,1)}, bf16[256,256]{1,0:T(8,128)(2,1)S(1)}, u32[]{:S(2)}, u32[]{:S(2)}) %collective-permute-start.2) | collective-permute-done | bytes 131104 | tf_op jit(solution)/shard_map/ppermute | solution.py:354
  65.1 3.0 %collective-permute-start.8 = (bf16[2,512,256]{2,1,0:T(8,128)(2,1)}, bf16[2,512,256]{2,1,0:T(8,128)(2,1)S(1)}, u32[]{:S(2)}, u32[]{:S(2)}) collective-permute-start(bf16[2,512,256]{2,1,0:T(8,128)(2,1)} %collective-permute-done.7.kv_ref), channel_id=1, source_target_pairs={{0,32},{4,228},{32,64},{36,4},{64,96},{68,36},{96,128},{100,68},{1... | collective-permute-start | bytes 1572872 | tf_op jit(solution)/shard_map/ppermute | solution.py:397
  68.1 0.9 copy-done.8
  69.0 4.1 %attend_first.1 = (bf16[4,4,256,256]{3,2,1,0:T(8,128)(2,1)S(1)}, f32[4,4,128,256]{3,2,1,0:T(8,128)S(1)}, f32[4,4,1,256]{3,2,1,0:T(1,128)S(1)}, f32[4,4,1,256]{3,2,1,0:T(1,128)S(1)}) custom-call(bf16[256,256]{1,0:T(8,128)(2,1)S(1)} %copy-done.8, bf16[256,256]{1,0:T(8,128)(2,1)S(1)} %collective-permute-done.q1, ...), custom_call_target="tpu_custom_call" | custom-call | flops 805306368 | bytes 524288 | tf_op jit(solution)/shard_map/attend_first/pallas_call | solution.py:195
  73.1 6.7 %attend_next.4 = (f32[4,4,128,256]{3,2,1,0:T(8,128)S(1)}, f32[4,4,1,256]{3,2,1,0:T(1,128)S(1)}, f32[4,4,1,256]{3,2,1,0:T(1,128)S(1)}) custom-call(bf16[4,4,256,256]{3,2,1,0:T(8,128)(2,1)S(1)} %get-tuple-element.36.qs, bf16[4,512,256]{2,1,0:T(8,128)(2,1)} %pad_maximum_fusion.1.kv_ref, ...), custom_call_target="tpu_custom_call", output_to_operand_aliasing={{0}: (2, {}), {1}: (3, {}), {2}: (4, {})} | custom-call | flops 1610612736 | bytes 1048576 | tf_op jit(solution)/shard_map/attend_next/pallas_call | solution.py:209
  79.8 6.7 %attend_next.5 = (f32[4,4,128,256]{3,2,1,0:T(8,128)S(1)}, f32[4,4,1,256]{3,2,1,0:T(1,128)S(1)}, f32[4,4,1,256]{3,2,1,0:T(1,128)S(1)}) custom-call(bf16[4,4,256,256]{3,2,1,0:T(8,128)(2,1)S(1)} %get-tuple-element.36.qs, bf16[4,512,256]{2,1,0:T(8,128)(2,1)} %collective-permute-done.10.kv_ref, ...), custom_call_target="tpu_custom_call", output_to_operand_aliasing={{0}: (2, {}), {1}: (3, {}), {2}: (4, {})} | custom-call | flops 1610612736 | bytes 1048576 | tf_op jit(solution)/shard_map/attend_next/pallas_call | solution.py:209
  86.5 4.7 %attend_next.6 = (f32[4,4,128,256]{3,2,1,0:T(8,128)S(1)}, f32[4,4,1,256]{3,2,1,0:T(1,128)S(1)}, f32[4,4,1,256]{3,2,1,0:T(1,128)S(1)}) custom-call(bf16[4,4,256,256]{3,2,1,0:T(8,128)(2,1)S(1)} %get-tuple-element.36.qs, bf16[2,512,256]{2,1,0:T(8,128)(2,1)} %collective-permute-done.7.kv_ref, ...), custom_call_target="tpu_custom_call", output_to_operand_aliasing={{0}: (2, {}), {1}: (3, {}), {2}: (4, {})} | custom-call | flops 805306368 | bytes 524288 | tf_op jit(solution)/shard_map/attend_next/pallas_call | solution.py:209
  91.2 3.7 %attend_next.7 = (f32[4,4,128,256]{3,2,1,0:T(8,128)S(1)}, f32[4,4,1,256]{3,2,1,0:T(1,128)S(1)}, f32[4,4,1,256]{3,2,1,0:T(1,128)S(1)}) custom-call(bf16[4,4,256,256]{3,2,1,0:T(8,128)(2,1)S(1)} %get-tuple-element.36.qs, bf16[2,512,256]{2,1,0:T(8,128)(2,1)S(1)} %collective-permute-done.9.kv_ref, ...), custom_call_target="tpu_custom_call", output_to_operand_aliasing={{0}: (2, {}), {1}: (3, {}), {2}: (4, {})} | custom-call | flops 805306368 | bytes 524288 | tf_op jit(solution)/shard_map/attend_next/pallas_call | solution.py:209
  94.9 3.7 %attend_last.1 = (f32[4,4,128,256]{3,2,1,0:T(8,128)S(1)}, f32[4,4,1,256]{3,2,1,0:T(1,128)S(1)}, f32[4,4,1,256]{3,2,1,0:T(1,128)S(1)}, f32[16,256]{1,0:T(8,128)S(1)}) custom-call(bf16[4,4,256,256]{3,2,1,0:T(8,128)(2,1)S(1)} %get-tuple-element.36.qs, ...), custom_call_target="tpu_custom_call", output_to_operand_aliasing={{0}: (2, {}), {1}: (3, {}), {2}: (4, {})} | custom-call | flops 805306368 | bytes 524288 | tf_op jit(solution)/shard_map/attend_last/pallas_call | solution.py:223
  98.7 4.4 %collective-permute-start.12 = (f32[16,256]{1,0:T(8,128)S(1)}, f32[16,256]{1,0:T(8,128)S(1)}, u32[]{:S(2)}, u32[]{:S(2)}) collective-permute-start(f32[16,256]{1,0:T(8,128)S(1)} %get-tuple-element.52.lse0), channel_id=1, source_target_pairs={{0,16},{8,24},{16,0},{24,8},{1,17},{9,25},{17,1},{25,9},{2,18},{10... | collective-permute-start | bytes 49160 | tf_op jit(solution)/shard_map/ppermute | solution.py:354
  103.5 1.4 collective-permute-done.12.lse2
  104.8 2.0 %collective-permute-done.13.lse3 = f32[16,256]{1,0:T(8,128)S(1)} collective-permute-done((f32[16,256]{1,0:T(8,128)S(1)}, f32[16,256]{1,0:T(8,128)S(1)}, u32[]{:S(2)}, u32[]{:S(2)}) %collective-permute-start.13) | collective-permute-done | bytes 16416 | tf_op jit(solution)/shard_map/ppermute | solution.py:354
  106.8 0.8 share.1
  107.7 0.8 copy-done.2
  108.5 4.3 %all-to-all-start = ((bf16[16,64,256]{2,1,0:T(8,128)(2,1)}), bf16[16,64,256]{2,1,0:T(8,128)(2,1)}, u32[]{:S(2)}, u32[]{:S(2)}) async-start(bf16[16,64,256]{2,1,0:T(8,128)(2,1)} %copy-done.2), calls=%async_computation | async-start | bytes 1048576 | tf_op jit(solution)/shard_map/all_to_all | solution.py:404
  112.9 8.9 %all-to-all-done.part_ref = bf16[16,64,256]{2,1,0:T(8,128)(2,1)} async-done(((bf16[16,64,256]{2,1,0:T(8,128)(2,1)}), bf16[16,64,256]{2,1,0:T(8,128)(2,1)}, u32[]{:S(2)}, u32[]{:S(2)}) %all-to-all-start) | async-done | bytes 524320 | tf_op jit(solution)/shard_map/all_to_all | solution.py:404
  121.8 0.9 copy-done.3
  122.8 3.3 %merge.1.refs_0_ = bf16[64,2048]{1,0:T(8,128)(2,1)S(1)} custom-call(s32[2]{0:T(128)S(1)} %pad_add_fusion.at_ref, bf16[16,64,256]{2,1,0:T(8,128)(2,1)} %all-to-all-done.part_ref, f32[1,128]{1,0:T(1,128)S(1)} %bitcast.16, bf16[64,2048]{1,0:T(8,128)(2,1)S(1)} %copy-done.3, f32[1,2048]{1,0:T(1,128)S(1)} %bitcast.15, ...), custom_call_target="tpu_custom_call" | custom-call | tf_op jit(solution)/shard_map/merge/pallas_call | solution.py:305
  126.1 1.0 collective-permute-start.19
  127.1 1.1 collective-permute-start.18
  128.2 4.3 %collective-permute-done.19.refs_2_ = bf16[64,2048]{1,0:T(8,128)(2,1)S(1)} collective-permute-done((bf16[64,2048]{1,0:T(8,128)(2,1)S(1)}, bf16[64,2048]{1,0:T(8,128)(2,1)S(1)}, u32[]{:S(2)}, u32[]{:S(2)}) %collective-permute-start.19) | collective-permute-done | bytes 262176 | tf_op jit(solution)/shard_map/ppermute | solution.py:354
  132.6 2.4 %collective-permute-start.22 = (bf16[32,2048]{1,0:T(8,128)(2,1)S(1)}, bf16[32,2048]{1,0:T(8,128)(2,1)S(1)}, u32[]{:S(2)}, u32[]{:S(2)}) collective-permute-start(bf16[32,2048]{1,0:T(8,128)(2,1)S(1)} %slice.9), channel_id=1, source_target_pairs={{0,3},{1,0},{2,1},{3,2},{4,7},{5,4},{6,5},{7,6},{8,11},{9,8},{10,9... | collective-permute-start | bytes 393224 | tf_op jit(solution)/shard_map/ppermute | solution.py:354
  135.1 2.7 %collective-permute-done.22 = bf16[32,2048]{1,0:T(8,128)(2,1)S(1)} collective-permute-done((bf16[32,2048]{1,0:T(8,128)(2,1)S(1)}, bf16[32,2048]{1,0:T(8,128)(2,1)S(1)}, u32[]{:S(2)}, u32[]{:S(2)}) %collective-permute-start.22) | collective-permute-done | bytes 131104 | tf_op jit(solution)/shard_map/ppermute | solution.py:354
  137.8 7.6 %collective-permute-done.21 = bf16[32,2048]{1,0:T(8,128)(2,1)S(1)} collective-permute-done((bf16[32,2048]{1,0:T(8,128)(2,1)S(1)}, bf16[32,2048]{1,0:T(8,128)(2,1)S(1)}, u32[]{:S(2)}, u32[]{:S(2)}) %collective-permute-start.21) | collective-permute-done | bytes 131104 | tf_op jit(solution)/shard_map/ppermute | solution.py:354
  145.5 3.4 %copy-done.1 = bf16[128,32,1024]{2,1,0:T(8,128)(2,1)S(1)} copy-done((bf16[128,32,1024]{2,1,0:T(8,128)(2,1)S(1)}, bf16[128,32,1024]{2,1,0:T(8,128)(2,1)}, u32[]{:S(2)}) %copy-start.1) | copy-done | bytes 8388632
  149.5 2.4 %mixer.2 = (f32[64,2048]{1,0:T(8,128)S(1)}, bf16[64,2048]{1,0:T(8,128)(2,1)S(1)}, bf16[64,2048]{1,0:T(8,128)(2,1)S(1)}) custom-call(bf16[64,2048]{1,0:T(8,128)(2,1)S(1)} %merge.1.refs_0_, bf16[64,2048]{1,0:T(8,128)(2,1)S(1)} %collective-permute-done.18.refs_1_, bf16[64,2048]{1,0:T(8,128)(2,1)S(1)} %collective-permute-done.19.refs_2_, ...), custom_call_target="tpu_custom_call" | custom-call | flops 2147483648 | bytes 8388608 | tf_op jit(solution)/shard_map/mixer/pallas_call | solution.py:341
  151.9 2.1 %mixer.3 = bf16[64,2048]{1,0:T(8,128)(2,1)S(1)} custom-call(bf16[64,2048]{1,0:T(8,128)(2,1)S(1)} %pad_maximum_fusion.3.refs_0_, bf16[64,2,32,1024]{3,2,1,0:T(8,128)(2,1)S(1)} %load_mix.1.refs_3_.refs_1_), custom_call_target="tpu_custom_call" | custom-call | flops 2147483648 | bytes 8388608 | tf_op jit(solution)/shard_map/mixer/pallas_call | solution.py:341
  154.2 3.3 %collective-permute-start.20 = (bf16[64,2048]{1,0:T(8,128)(2,1)S(1)}, bf16[64,2048]{1,0:T(8,128)(2,1)S(1)}, u32[]{:S(2)}, u32[]{:S(2)}) collective-permute-start(bf16[64,2048]{1,0:T(8,128)(2,1)S(1)} %get-tuple-element.57), channel_id=1, source_target_pairs={{0,3},{1,0},{2,1},{3,2},{4,7},{5,4},{6,5},{7,6},{8,11},{9,8},{10,9... | collective-permute-start | bytes 786440 | tf_op jit(solution)/shard_map/ppermute | solution.py:354
  157.5 4.9 %collective-permute-done.24 = bf16[64,2048]{1,0:T(8,128)(2,1)S(1)} collective-permute-done((bf16[64,2048]{1,0:T(8,128)(2,1)S(1)}, bf16[64,2048]{1,0:T(8,128)(2,1)S(1)}, u32[]{:S(2)}, u32[]{:S(2)}) %collective-permute-start.24) | collective-permute-done | bytes 262176 | tf_op jit(solution)/shard_map/ppermute | solution.py:354
  162.3 3.1 %collective-permute-done.20 = bf16[64,2048]{1,0:T(8,128)(2,1)S(1)} collective-permute-done((bf16[64,2048]{1,0:T(8,128)(2,1)S(1)}, bf16[64,2048]{1,0:T(8,128)(2,1)S(1)}, u32[]{:S(2)}, u32[]{:S(2)}) %collective-permute-start.20) | collective-permute-done | bytes 262176 | tf_op jit(solution)/shard_map/ppermute | solution.py:354
  165.4 0.9 add_convert_fusion
  (59 shorter events, 3.6 us)
Async XLA Ops:
  6.5 7.0 %copy-start = (bf16[256,2048]{1,0:T(8,128)(2,1)S(1)}, bf16[256,2048]{1,0:T(8,128)(2,1)}, u32[]{:S(2)}) copy-start(bf16[256,2048]{1,0:T(8,128)(2,1)} %param.20) | copy-start | bytes 3145732
  6.5 139.0 %all-gather.3.cloned.1.call-start = ((), (), s32[]{:S(2)}) async-start(), calls=%async_computation.1 | async-start | bytes 8519680 | tf_op jit(solution)/shard_map/all_gather | solution.py:385
  10.2 8.2 %collective-permute-start.5 = (bf16[512,256]{1,0:T(8,128)(2,1)}, bf16[512,256]{1,0:T(8,128)(2,1)S(1)}, u32[]{:S(2)}, u32[]{:S(2)}) collective-permute-start(bf16[512,256]{1,0:T(8,128)(2,1)} %get-tuple-element.35), channel_id=1, source_target_pairs={{0,228},{4,32},{32,4},{36,64},{64,36},{68,96},{96,68},{100,128},{1... | collective-permute-start | bytes 786440 | tf_op jit(solution)/shard_map/ppermute | solution.py:382
  10.3 9.6 %collective-permute-start.4 = (bf16[512,256]{1,0:T(8,128)(2,1)}, bf16[512,256]{1,0:T(8,128)(2,1)S(1)}, u32[]{:S(2)}, u32[]{:S(2)}) collective-permute-start(bf16[512,256]{1,0:T(8,128)(2,1)} %get-tuple-element.35), channel_id=1, source_target_pairs={{0,32},{4,228},{32,64},{36,4},{64,96},{68,36},{96,128},{100,68},{1... | collective-permute-start | bytes 786440 | tf_op jit(solution)/shard_map/ppermute | solution.py:382
  13.6 25.7 %collective-permute-start.16 = (bf16[128,2048]{1,0:T(8,128)(2,1)S(1)}, bf16[128,2048]{1,0:T(8,128)(2,1)S(1)}, u32[]{:S(2)}, u32[]{:S(2)}) collective-permute-start(bf16[128,2048]{1,0:T(8,128)(2,1)S(1)} %constant_dynamic-slice_fusion), channel_id=1, source_target_pairs={{0,3},{1,0},{2,1},{3,2},{4,7},{5,4},{6,5},{7,6},{8,11},{9,8},{10,9... | collective-permute-start | bytes 1572872 | tf_op jit(solution)/shard_map/ppermute | solution.py:354
  16.7 22.6 %collective-permute-start.15 = (bf16[128,2048]{1,0:T(8,128)(2,1)S(1)}, bf16[128,2048]{1,0:T(8,128)(2,1)S(1)}, u32[]{:S(2)}, u32[]{:S(2)}) collective-permute-start(bf16[128,2048]{1,0:T(8,128)(2,1)S(1)} %constant_dynamic-slice_fusion), channel_id=1, source_target_pairs={{0,2},{1,3},{2,0},{3,1},{4,6},{5,7},{6,4},{7,5},{8,10},{9,11},{10,... | collective-permute-start | bytes 1572872 | tf_op jit(solution)/shard_map/ppermute | solution.py:354
  17.3 25.7 %collective-permute-start.14 = (bf16[128,2048]{1,0:T(8,128)(2,1)S(1)}, bf16[128,2048]{1,0:T(8,128)(2,1)S(1)}, u32[]{:S(2)}, u32[]{:S(2)}) collective-permute-start(bf16[128,2048]{1,0:T(8,128)(2,1)S(1)} %constant_dynamic-slice_fusion), channel_id=1, source_target_pairs={{0,1},{1,2},{2,3},{3,0},{4,5},{5,6},{6,7},{7,4},{8,9},{9,10},{10,1... | collective-permute-start | bytes 1572872 | tf_op jit(solution)/shard_map/ppermute | solution.py:354
  18.5 24.5 %copy-start.9 = (bf16[512,256]{1,0:T(8,128)(2,1)}, bf16[512,256]{1,0:T(8,128)(2,1)S(1)}, u32[]{:S(2)}) copy-start(bf16[512,256]{1,0:T(8,128)(2,1)S(1)} %collective-permute-done.5) | copy-start | bytes 786436
  19.9 23.1 %copy-start.11 = (bf16[512,256]{1,0:T(8,128)(2,1)}, bf16[512,256]{1,0:T(8,128)(2,1)S(1)}, u32[]{:S(2)}) copy-start(bf16[512,256]{1,0:T(8,128)(2,1)S(1)} %collective-permute-done.4) | copy-start | bytes 786436
  19.9 23.4 %collective-permute-start.6 = (bf16[2,512,256]{2,1,0:T(8,128)(2,1)S(1)}, bf16[2,512,256]{2,1,0:T(8,128)(2,1)}, u32[]{:S(2)}, u32[]{:S(2)}) collective-permute-start(bf16[2,512,256]{2,1,0:T(8,128)(2,1)S(1)} %pad_maximum_fusion.2), channel_id=1, source_target_pairs={{0,32},{4,228},{32,64},{36,4},{64,96},{68,36},{96,128},{100,68},{1... | collective-permute-start | bytes 1572872 | tf_op jit(solution)/shard_map/ppermute | solution.py:388
  43.0 1.0 copy-start.10
  43.0 1.0 copy-start.12
  43.3 24.8 %copy-start.7 = (bf16[512,256]{1,0:T(8,128)(2,1)S(1)}, bf16[512,256]{1,0:T(8,128)(2,1)}, u32[]{:S(2)}) copy-start(bf16[512,256]{1,0:T(8,128)(2,1)} %get-tuple-element.34.own_ref) | copy-start | bytes 786436
  43.3 78.5 %collective-permute-start.17 = (bf16[4,128,2048]{2,1,0:T(8,128)(2,1)S(1)}, bf16[4,128,2048]{2,1,0:T(8,128)(2,1)}, u32[]{:S(2)}, u32[]{:S(2)}) collective-permute-start(bf16[4,128,2048]{2,1,0:T(8,128)(2,1)S(1)} %pad_maximum_fusion.mine_ref), channel_id=1, source_target_pairs={{0,4},{4,0},{1,5},{5,1},{2,6},{6,2},{3,7},{7,3},{8,12},{12,8},{9,1... | collective-permute-start | bytes 6291464 | tf_op jit(solution)/shard_map/ppermute | solution.py:354
  46.1 33.6 %collective-permute-start.10 = (bf16[4,512,256]{2,1,0:T(8,128)(2,1)}, bf16[4,512,256]{2,1,0:T(8,128)(2,1)}, u32[]{:S(2)}, u32[]{:S(2)}) collective-permute-start(bf16[4,512,256]{2,1,0:T(8,128)(2,1)} %pad_maximum_fusion.1.kv_ref), channel_id=1, source_target_pairs={{0,4},{4,0},{1,5},{5,1},{2,6},{6,2},{3,7},{7,3},{8,12},{12,8},{9,1... | collective-permute-start | bytes 3145736 | tf_op jit(solution)/shard_map/ppermute | solution.py:354
  46.1 14.1 %collective-permute-start.7 = (bf16[2,512,256]{2,1,0:T(8,128)(2,1)}, bf16[2,512,256]{2,1,0:T(8,128)(2,1)}, u32[]{:S(2)}, u32[]{:S(2)}) collective-permute-start(bf16[2,512,256]{2,1,0:T(8,128)(2,1)} %collective-permute-done.6), channel_id=1, source_target_pairs={{0,32},{4,228},{32,64},{36,4},{64,96},{68,36},{96,128},{100,68},{1... | collective-permute-start | bytes 1572872 | tf_op jit(solution)/shard_map/ppermute | solution.py:392
  51.0 5.8 %collective-permute-start = (bf16[256,256]{1,0:T(8,128)(2,1)}, bf16[256,256]{1,0:T(8,128)(2,1)S(1)}, u32[]{:S(2)}, u32[]{:S(2)}) collective-permute-start(bf16[256,256]{1,0:T(8,128)(2,1)} %get-tuple-element.33), channel_id=1, source_target_pairs={{0,8},{8,16},{16,24},{24,0},{1,9},{9,17},{17,25},{25,1},{2,10},{10... | collective-permute-start | bytes 393224 | tf_op jit(solution)/shard_map/ppermute | solution.py:354
  52.4 6.7 %collective-permute-start.1 = (bf16[256,256]{1,0:T(8,128)(2,1)}, bf16[256,256]{1,0:T(8,128)(2,1)S(1)}, u32[]{:S(2)}, u32[]{:S(2)}) collective-permute-start(bf16[256,256]{1,0:T(8,128)(2,1)} %get-tuple-element.33), channel_id=1, source_target_pairs={{0,16},{8,24},{16,0},{24,8},{1,17},{9,25},{17,1},{25,9},{2,18},{10... | collective-permute-start | bytes 393224 | tf_op jit(solution)/shard_map/ppermute | solution.py:354
  56.8 11.3 %collective-permute-start.3 = (bf16[512,256]{1,0:T(8,128)(2,1)}, bf16[512,256]{1,0:T(8,128)(2,1)S(1)}, u32[]{:S(2)}, u32[]{:S(2)}) collective-permute-start(bf16[512,256]{1,0:T(8,128)(2,1)} %get-tuple-element.35), channel_id=1, source_target_pairs={{0,4},{4,0},{1,5},{5,1},{2,6},{6,2},{3,7},{7,3},{8,12},{12,8},{9,1... | collective-permute-start | bytes 786440 | tf_op jit(solution)/shard_map/ppermute | solution.py:354
  59.1 6.0 %collective-permute-start.2 = (bf16[256,256]{1,0:T(8,128)(2,1)}, bf16[256,256]{1,0:T(8,128)(2,1)S(1)}, u32[]{:S(2)}, u32[]{:S(2)}) collective-permute-start(bf16[256,256]{1,0:T(8,128)(2,1)} %get-tuple-element.33), channel_id=1, source_target_pairs={{0,24},{8,0},{16,8},{24,16},{1,25},{9,1},{17,9},{25,17},{2,26},{10... | collective-permute-start | bytes 393224 | tf_op jit(solution)/shard_map/ppermute | solution.py:354
  60.2 31.0 %collective-permute-start.9 = (bf16[2,512,256]{2,1,0:T(8,128)(2,1)}, bf16[2,512,256]{2,1,0:T(8,128)(2,1)S(1)}, u32[]{:S(2)}, u32[]{:S(2)}) collective-permute-start(bf16[2,512,256]{2,1,0:T(8,128)(2,1)} %collective-permute-done.7.kv_ref), channel_id=1, source_target_pairs={{0,4},{4,0},{1,5},{5,1},{2,6},{6,2},{3,7},{7,3},{8,12},{12,8},{9,1... | collective-permute-start | bytes 1572872 | tf_op jit(solution)/shard_map/ppermute | solution.py:354
  65.1 29.8 %collective-permute-start.8 = (bf16[2,512,256]{2,1,0:T(8,128)(2,1)}, bf16[2,512,256]{2,1,0:T(8,128)(2,1)S(1)}, u32[]{:S(2)}, u32[]{:S(2)}) collective-permute-start(bf16[2,512,256]{2,1,0:T(8,128)(2,1)} %collective-permute-done.7.kv_ref), channel_id=1, source_target_pairs={{0,32},{4,228},{32,64},{36,4},{64,96},{68,36},{96,128},{100,68},{1... | collective-permute-start | bytes 1572872 | tf_op jit(solution)/shard_map/ppermute | solution.py:397
  68.1 0.9 copy-start.8
  94.9 12.0 %copy-start.5 = (f32[2]{0:T(128)S(1)}, f32[2]{0:T(128)}, u32[]{:S(2)}) copy-start(f32[2]{0:T(128)} %lam_ref.1) | copy-start | bytes 28
  98.6 23.2 %copy-start.4 = (f32[2048]{0:T(1024)S(1)}, f32[2048]{0:T(1024)}, u32[]{:S(2)}) copy-start(f32[2048]{0:T(1024)} %param.21) | copy-start | bytes 24580
  98.6 23.2 %copy-start.6 = (f32[128]{0:T(128)S(1)}, f32[128]{0:T(128)}, u32[]{:S(2)}) copy-start(f32[128]{0:T(128)} %param.19) | copy-start | bytes 1540
  98.6 4.9 %collective-permute-start.11 = (f32[16,256]{1,0:T(8,128)S(1)}, f32[16,256]{1,0:T(8,128)S(1)}, u32[]{:S(2)}, u32[]{:S(2)}) collective-permute-start(f32[16,256]{1,0:T(8,128)S(1)} %get-tuple-element.52.lse0), channel_id=1, source_target_pairs={{0,8},{8,16},{16,24},{24,0},{1,9},{9,17},{17,25},{25,1},{2,10},{10... | collective-permute-start | bytes 49160 | tf_op jit(solution)/shard_map/ppermute | solution.py:354
  98.7 6.1 %collective-permute-start.12 = (f32[16,256]{1,0:T(8,128)S(1)}, f32[16,256]{1,0:T(8,128)S(1)}, u32[]{:S(2)}, u32[]{:S(2)}) collective-permute-start(f32[16,256]{1,0:T(8,128)S(1)} %get-tuple-element.52.lse0), channel_id=1, source_target_pairs={{0,16},{8,24},{16,0},{24,8},{1,17},{9,25},{17,1},{25,9},{2,18},{10... | collective-permute-start | bytes 49160 | tf_op jit(solution)/shard_map/ppermute | solution.py:354
  103.1 3.7 %collective-permute-start.13 = (f32[16,256]{1,0:T(8,128)S(1)}, f32[16,256]{1,0:T(8,128)S(1)}, u32[]{:S(2)}, u32[]{:S(2)}) collective-permute-start(f32[16,256]{1,0:T(8,128)S(1)} %get-tuple-element.52.lse0), channel_id=1, source_target_pairs={{0,24},{8,0},{16,8},{24,16},{1,25},{9,1},{17,9},{25,17},{2,26},{10... | collective-permute-start | bytes 49160 | tf_op jit(solution)/shard_map/ppermute | solution.py:354
  107.7 0.8 copy-start.2
  108.5 13.3 %all-to-all-start = ((bf16[16,64,256]{2,1,0:T(8,128)(2,1)}), bf16[16,64,256]{2,1,0:T(8,128)(2,1)}, u32[]{:S(2)}, u32[]{:S(2)}) async-start(bf16[16,64,256]{2,1,0:T(8,128)(2,1)} %copy-done.2), calls=%async_computation | async-start | bytes 1048576 | tf_op jit(solution)/shard_map/all_to_all | solution.py:404
  121.8 1.0 copy-start.3
  126.1 6.4 %collective-permute-start.19 = (bf16[64,2048]{1,0:T(8,128)(2,1)S(1)}, bf16[64,2048]{1,0:T(8,128)(2,1)S(1)}, u32[]{:S(2)}, u32[]{:S(2)}) collective-permute-start(bf16[64,2048]{1,0:T(8,128)(2,1)S(1)} %merge.1.refs_0_), channel_id=1, source_target_pairs={{0,3},{1,0},{2,1},{3,2},{4,7},{5,4},{6,5},{7,6},{8,11},{9,8},{10,9... | collective-permute-start | bytes 786440 | tf_op jit(solution)/shard_map/ppermute | solution.py:354
  127.1 7.9 %collective-permute-start.18 = (bf16[64,2048]{1,0:T(8,128)(2,1)S(1)}, bf16[64,2048]{1,0:T(8,128)(2,1)S(1)}, u32[]{:S(2)}, u32[]{:S(2)}) collective-permute-start(bf16[64,2048]{1,0:T(8,128)(2,1)S(1)} %merge.1.refs_0_), channel_id=1, source_target_pairs={{0,1},{1,2},{2,3},{3,0},{4,5},{5,6},{6,7},{7,4},{8,9},{9,10},{10,1... | collective-permute-start | bytes 786440 | tf_op jit(solution)/shard_map/ppermute | solution.py:354
  132.6 5.3 %collective-permute-start.22 = (bf16[32,2048]{1,0:T(8,128)(2,1)S(1)}, bf16[32,2048]{1,0:T(8,128)(2,1)S(1)}, u32[]{:S(2)}, u32[]{:S(2)}) collective-permute-start(bf16[32,2048]{1,0:T(8,128)(2,1)S(1)} %slice.9), channel_id=1, source_target_pairs={{0,3},{1,0},{2,1},{3,2},{4,7},{5,4},{6,5},{7,6},{8,11},{9,8},{10,9... | collective-permute-start | bytes 393224 | tf_op jit(solution)/shard_map/ppermute | solution.py:354
  135.0 10.5 %collective-permute-start.21 = (bf16[32,2048]{1,0:T(8,128)(2,1)S(1)}, bf16[32,2048]{1,0:T(8,128)(2,1)S(1)}, u32[]{:S(2)}, u32[]{:S(2)}) collective-permute-start(bf16[32,2048]{1,0:T(8,128)(2,1)S(1)} %slice.8), channel_id=1, source_target_pairs={{0,1},{1,2},{2,3},{3,0},{4,5},{5,6},{6,7},{7,4},{8,9},{9,10},{10,1... | collective-permute-start | bytes 393224 | tf_op jit(solution)/shard_map/ppermute | solution.py:354
  145.5 3.4 %copy-start.1 = (bf16[128,32,1024]{2,1,0:T(8,128)(2,1)S(1)}, bf16[128,32,1024]{2,1,0:T(8,128)(2,1)}, u32[]{:S(2)}) copy-start(bf16[128,32,1024]{2,1,0:T(8,128)(2,1)} %all-gather.3.cloned.1.call-done) | copy-start | bytes 25165828
  151.9 10.5 %collective-permute-start.24 = (bf16[64,2048]{1,0:T(8,128)(2,1)S(1)}, bf16[64,2048]{1,0:T(8,128)(2,1)S(1)}, u32[]{:S(2)}, u32[]{:S(2)}) collective-permute-start(bf16[64,2048]{1,0:T(8,128)(2,1)S(1)} %get-tuple-element.58), channel_id=1, source_target_pairs={{0,1},{1,2},{2,3},{3,0},{4,5},{5,6},{6,7},{7,4},{8,9},{9,10},{10,1... | collective-permute-start | bytes 786440 | tf_op jit(solution)/shard_map/ppermute | solution.py:354
  154.1 8.3 %collective-permute-start.23 = (bf16[64,2048]{1,0:T(8,128)(2,1)S(1)}, bf16[64,2048]{1,0:T(8,128)(2,1)S(1)}, u32[]{:S(2)}, u32[]{:S(2)}) collective-permute-start(bf16[64,2048]{1,0:T(8,128)(2,1)S(1)} %mixer.3), channel_id=1, source_target_pairs={{0,2},{1,3},{2,0},{3,1},{4,6},{5,7},{6,4},{7,5},{8,10},{9,11},{10,... | collective-permute-start | bytes 786440 | tf_op jit(solution)/shard_map/ppermute | solution.py:354
  154.2 11.3 %collective-permute-start.20 = (bf16[64,2048]{1,0:T(8,128)(2,1)S(1)}, bf16[64,2048]{1,0:T(8,128)(2,1)S(1)}, u32[]{:S(2)}, u32[]{:S(2)}) collective-permute-start(bf16[64,2048]{1,0:T(8,128)(2,1)S(1)} %get-tuple-element.57), channel_id=1, source_target_pairs={{0,3},{1,0},{2,1},{3,2},{4,7},{5,4},{6,5},{7,6},{8,11},{9,8},{10,9... | collective-permute-start | bytes 786440 | tf_op jit(solution)/shard_map/ppermute | solution.py:354
Sparse Core Ops, SparseCore 0:
  10.4 85.0 all-gather.2
